TPU v7x, 768 devices: a whole 4x8x12 slice. The times are simulated.
768 devices in a mesh: fs: 96 (over z, y), tp: 8 (over x, core).
Axes of the slice: x: 4, y: 8, z: 12, core: 2. Of those that a mesh axis runs over, the one named last changes fastest.
Arguments:
- saved_inputs: bfloat16 [49152, 3072], P('fs'), may hold values from -6 to 6
- query_cotangent: bfloat16 [49152, 3072], P('fs', 'tp'), may hold values from -0.21875 to 0.21875
- attn_outputs: bfloat16 [49152, 3072], P('fs', 'tp'), may hold values from -6 to 6
- out_cotangent: bfloat16 [49152, 3072], P('fs'), may hold values from -0.21875 to 0.21875
- left_factor: bfloat16 [3072, 384], P('fs', 'tp'), may hold values from -0.109375 to 0.109375
- right_factor: bfloat16 [3072, 384], P('fs', 'tp'), may hold values from -0.109375 to 0.109375
- query_master: float32 [3072, 3072], P('fs', 'tp'), may hold values from -0.109375 to 0.109375
- out_master: float32 [3072, 3072], P('tp', 'fs'), may hold values from -0.109375 to 0.109375
- first_moment: float32 [2, 384, 3072], P(None, 'fs', 'tp'), may hold values from -14 to 14
- second_moment: float32 [2, 384, 3072], P(None, 'fs', 'tp'), may hold values from 0.3 to 3
Outputs:
- query_new: float32 [3072, 3072], P('fs', 'tp')
- out_new: float32 [3072, 3072], P('tp', 'fs')
- query_copy: bfloat16 [3072, 3072], P(None, 'tp')
- out_copy: bfloat16 [3072, 3072], P('tp')
- first_new: float32 [2, 384, 3072], P(None, 'fs', 'tp')
- second_new: float32 [2, 384, 3072], P(None, 'fs', 'tp')
All inputs are finite; a program needn't handle non-finite values.
Results may differ from a plain program's by a relative error of at most 0.0025.
Values may be sent and summed in bfloat16 or wider, within the bound.
No kernel may reach another device: no remote copies, remote signals or barrier semaphores. Data moves between devices by JAX's collectives and lax.ppermute only.
A program may use at most 64 MiB of HBM per device.

v0:
```python
import jax
import jax.numpy as jnp
from jax import lax
from jax.sharding import Mesh
from jax.sharding import PartitionSpec as P

FS = ("fs_0", "fs_1")
TP = ("tp_0", "tp_1")
FS_TP = ("fs_0", "fs_1", "tp_0", "tp_1")


def side_by_side(arrays, axis, dim, along):
    ends, at = ([], 0)
    for a in arrays[:-1]:
        at += a.shape[along]
        ends.append(at)
    both = jnp.concatenate(arrays, axis=along)
    return tuple(jnp.split(lax.all_gather(both, axis, axis=dim, tiled=True), ends, axis=along))


def turned_gather(arrays, axis, dims):
    turned = [jnp.moveaxis(a, dim, 0) for a, dim in zip(arrays, dims)]
    widths = [t[0].size for t in turned]
    both = jnp.concatenate([t.reshape(-1, w) for t, w in zip(turned, widths)], axis=1)
    filled = lax.all_gather(both, axis, axis=0, tiled=True)
    blocks = jnp.split(filled, [sum(widths[:k]) for k in range(1, len(widths))], axis=1)
    return tuple(
        (
            jnp.moveaxis(b.reshape(-1, *t.shape[1:]), 0, dim)
            for b, t, dim in zip(blocks, turned, dims)
        )
    )


def sum_in_order(blocks, axes, sequence):
    inside = blocks.shape[1:]
    blocks = blocks.reshape(*(lax.axis_size(a) for a in axes), *inside)
    blocks = jnp.moveaxis(blocks, sequence, range(len(axes))).reshape(-1, *inside)
    for k in sequence:
        blocks = lax.psum_scatter(blocks, axes[k], scatter_dimension=0, tiled=True)
    return blocks[0]


def cut_along(value, dim, size):
    before, after = (value.shape[:dim], value.shape[dim + 1 :])
    return jnp.moveaxis(value.reshape(*before, size, -1, *after), dim, 0)


def sum_by_axis_2(value, axes, sequence, dim):
    size = lax.axis_size(axes)
    return sum_in_order(cut_along(value, dim, size), axes, sequence)


def joined_along(blocks, dim):
    dims = list(blocks.shape[1:])
    dims[dim] *= blocks.shape[0]
    return jnp.moveaxis(blocks, 0, dim).reshape(dims)


def gather_in_order(value, axes, sequence):
    blocks = value
    for k in sequence:
        blocks = lax.all_gather(blocks, axes[k])
    done = sequence[::-1]
    back = [done.index(k) for k in range(len(axes))]
    blocks = blocks.transpose(*back, *range(len(axes), blocks.ndim))
    return blocks.reshape(-1, *value.shape)


def gathered_by_axis(value, axes, sequence, dim):
    return joined_along(gather_in_order(value, axes, sequence), dim)


def over_axes(value, axes):
    for axis in axes:
        value = lax.psum(value, axis)
    return value


def moment_step(first, second, grads):
    first_next = 0.9 * first + 0.1 * grads
    second_next = 0.99 * second + 0.01 * grads * grads
    return (first_next, second_next, first_next / (jnp.sqrt(second_next) + 1e-08))


def body(
    saved_inputs,
    query_cotangent,
    attn_outputs,
    out_cotangent,
    left_factor,
    right_factor,
    query_master,
    out_master,
    first_moment,
    second_moment,
):
    pieces = side_by_side((left_factor, right_factor), FS, 0, 1)
    left_part = jnp.dot(saved_inputs, pieces[0], preferred_element_type=jnp.float32)
    right_part = jnp.dot(out_cotangent, pieces[1], preferred_element_type=jnp.float32)
    left_proj, right_proj, left_rows, right_rows = turned_gather(
        (
            left_part.astype(jnp.bfloat16),
            right_part.astype(jnp.bfloat16),
            left_factor,
            right_factor,
        ),
        TP,
        (1, 1, 1, 1),
    )
    rows = first_moment.shape[1]
    dims = (((0,), (0,)), ((), ()))
    grad_query = lax.dot_general(
        left_proj, query_cotangent, dims, preferred_element_type=jnp.float32
    )
    grad_output = lax.dot_general(
        right_proj, attn_outputs, dims, preferred_element_type=jnp.float32
    )
    summed = sum_by_axis_2(jnp.stack([grad_query, grad_output], axis=1), FS, (1, 0), 0)
    grads = jnp.transpose(summed, (1, 0, 2))
    first_new, second_new, own_direction = moment_step(first_moment, second_moment, grads)
    direction_all = gathered_by_axis(own_direction.astype(jnp.bfloat16), FS, (0, 1), 1)
    squares = jnp.sum(own_direction * own_direction, axis=(1, 2))
    total = over_axes(squares, FS_TP)
    entries = rows * lax.axis_size(FS) * own_direction.shape[2] * lax.axis_size(TP)
    scale = lax.rsqrt(total / entries + 1e-06)
    step_query = scale[0] * jnp.dot(left_rows, direction_all[0], preferred_element_type=jnp.float32)
    step_output = scale[1] * lax.dot_general(
        direction_all[1], right_rows, (((0,), (1,)), ((), ())), preferred_element_type=jnp.float32
    )
    query_new = query_master - 0.01 * step_query
    out_new = out_master - 0.01 * step_output
    query_copy, out_copy = turned_gather(
        (query_new.astype(jnp.bfloat16), out_new.astype(jnp.bfloat16)), FS, (0, 1)
    )
    return (query_new, out_new, query_copy, out_copy, first_new, second_new)


def solution(mesh):
    finer = Mesh(mesh.devices.reshape(12, 8, 4, 2), ("fs_0", "fs_1", "tp_0", "tp_1"))
    placed = (
        P(FS, None),
        P(FS, TP),
        P(FS, TP),
        P(FS, None),
        P(FS, TP),
        P(FS, TP),
        P(FS, TP),
        P(TP, FS),
        P(None, FS, TP),
        P(None, FS, TP),
    )
    return jax.shard_map(
        body,
        mesh=finer,
        in_specs=placed,
        out_specs=(
            P(FS, TP),
            P(TP, FS),
            P(None, TP),
            P(TP, None),
            P(None, FS, TP),
            P(None, FS, TP),
        ),
        check_vma=False,
    )
```

profile of v0, /device:TPU:2, one launch (start us, length us, event | category | flops | bytes accessed | tf_op | source)
XLA Modules:
  0.0 566.2 jit_solution(2769727349995203447)
XLA Ops:
  7.2 0.0 copy-start
  7.2 0.0 all-reduce.5.cloned.1.call-start
  7.2 0.9 copy.31
  8.2 0.8 pad_maximum_fusion.1
  9.0 0.8 copy.32
  9.7 0.0 copy-start.2
  9.7 86.5 %all_gather.21 = bf16[3072,96]{1,0:T(8,128)(2,1)S(1)} all-gather(bf16[32,96]{1,0:T(8,128)(2,1)S(1)} %pad_maximum_fusion.1), channel_id=1, replica_groups=mesh['fs_0'=12,'fs_1'=8,'tp_0'=4,'tp_1'=2] {'fs_0','fs_1'}, dimensions={0}, use_global_device_ids=true | all-gather | bytes 595968 | tf_op jit(solution)/shard_map/all_gather | solution.py:18
  96.2 0.0 copy-done
  96.2 1.5 convolution_convert_fusion
  97.7 0.0 copy-done.2
  97.7 1.1 convolution_convert_fusion.1
  98.8 0.1 concatenate.11
  98.9 13.6 %all_gather.22 = bf16[384,1088]{1,0:T(8,128)(2,1)S(1)} all-gather(bf16[48,1088]{1,0:T(8,128)(2,1)S(1)} %concatenate.11), channel_id=1, replica_groups=mesh['fs_0'=12,'fs_1'=8,'tp_0'=4,'tp_1'=2] {'tp_0','tp_1'}, dimensions={0}, use_global_device_ids=true | all-gather | bytes 940032 | tf_op jit(solution)/shard_map/all_gather | solution.py:25
  112.5 0.0 copy-start.1
  112.5 0.9 copy-done.1
  113.4 0.0 copy-start.3
  113.4 2.2 fusion.6
  115.7 2.0 stack.10
  117.7 0.0 copy-done.3
  117.7 2.2 fusion.8
  119.9 2.0 stack.9
  121.9 1.5 maximum_bitcast_fusion
  123.5 0.0 copy-start.6
  123.5 0.0 copy-start.7
  123.5 1.2 copy.33
  124.7 0.0 all-reduce.5.cloned.1.call-update
  124.7 0.0 all-reduce.7.cloned.1.call-start
  124.8 1.3 dynamic-slice
  126.7 0.0 copy-start.5
  126.7 79.1 %all-reduce.5.cloned.1.call-done = f32[96,4,2,384]{3,1,2,0:T(4,128)} async-done(((f32[96,4,2,384]{3,1,2,0:T(4,128)}), f32[96,4,2,384]{3,1,2,0:T(4,128)}) %all-reduce.5.cloned.1.call-update) | async-done | bytes 1179664
  205.8 1.6 constant_dynamic-slice_fusion
  207.4 0.0 all-reduce.7.cloned.1.call-update
  207.4 0.0 all-gather.4.cloned.1.call-start
  207.5 1.3 dynamic-slice.2
  208.7 111.3 %all-reduce.7.cloned.1.call-done = f32[12,4,2,384]{3,1,2,0:T(4,128)} async-done(((f32[12,4,2,384]{3,1,2,0:T(4,128)}), f32[12,4,2,384]{3,1,2,0:T(4,128)}) %all-reduce.7.cloned.1.call-update) | async-done | bytes 147472
  320.1 0.0 copy-done.6
  320.1 0.0 copy-done.7
  320.1 2.0 multiply_reduce_fusion
  322.1 21.3 %psum.28 = f32[2]{0:T(128)S(1)} all-reduce(f32[2]{0:T(128)S(1)} %get-tuple-element.30), channel_id=1, replica_groups=mesh['fs_0'=12,'fs_1'=8,'tp_0'=4,'tp_1'=2] {'fs_0'}, use_global_device_ids=true, to_apply=%region_3.0 | all-reduce | flops 2 | bytes 16 | tf_op jit(solution)/shard_map/psum | solution.py:76
  343.3 17.0 %psum.29 = f32[2]{0:T(128)S(1)} all-reduce(f32[2]{0:T(128)S(1)} %psum.28), channel_id=1, replica_groups=mesh['fs_0'=12,'fs_1'=8,'tp_0'=4,'tp_1'=2] {'fs_1'}, use_global_device_ids=true, to_apply=%region_4.0 | all-reduce | flops 2 | bytes 16 | tf_op jit(solution)/shard_map/psum | solution.py:76
  360.3 8.6 %psum.30 = f32[2]{0:T(128)S(1)} all-reduce(f32[2]{0:T(128)S(1)} %psum.29), channel_id=1, replica_groups=mesh['fs_0'=12,'fs_1'=8,'tp_0'=4,'tp_1'=2] {'tp_0'}, use_global_device_ids=true, to_apply=%region_5.0 | all-reduce | flops 2 | bytes 16 | tf_op jit(solution)/shard_map/psum | solution.py:76
  368.9 2.5 psum.31
  371.4 0.6 fusion.15
  372.0 21.3 %all-gather = bf16[24,4,384]{2,1,0:T(4,128)(2,1)S(1)} all-gather(bf16[2,4,384]{2,1,0:T(4,128)(2,1)S(1)} %get-tuple-element.31), channel_id=2, replica_groups=mesh['fs_0'=12,'fs_1'=8,'tp_0'=4,'tp_1'=2] {'fs_0'}, dimensions={0}, use_global_device_ids=true | all-gather | bytes 79872 | tf_op jit(solution)/shard_map/all_gather | solution.py:63
  393.3 25.5 %all-gather.1 = bf16[96,2,4,384]{3,2,1,0:T(4,128)(2,1)S(1)} all-gather(bf16[12,2,4,384]{3,2,1,0:T(4,128)(2,1)S(1)} %bitcast.41), channel_id=3, replica_groups=mesh['fs_0'=12,'fs_1'=8,'tp_0'=4,'tp_1'=2] {'fs_1'}, dimensions={0}, use_global_device_ids=true | all-gather | bytes 663552 | tf_op jit(solution)/shard_map/all_gather | solution.py:63
  418.8 0.2 copy.39
  419.0 0.8 fusion.14
  419.8 0.9 copy.36
  420.6 1.0 squeeze.19
  421.7 0.0 copy-done.5
  421.7 1.8 fusion.1
  423.5 0.0 copy-start.4
  423.5 1.8 copy.35
  425.4 1.0 squeeze.17
  426.4 2.4 fusion.16
  428.8 0.6 pad_maximum_fusion
  429.4 0.0 all-gather.4.cloned.1.call-update
  429.5 120.9 %all-gather.4.cloned.1.call-done = bf16[3072,768]{1,0:T(8,128)(2,1)} async-done(((bf16[32,768]{1,0:T(8,128)(2,1)}), bf16[3072,768]{1,0:T(8,128)(2,1)}) %all-gather.4.cloned.1.call-update) | async-done | bytes 4718608 | tf_op jit(solution)/shard_map/all_gather | solution.py:25
  550.4 5.0 slice_bitcast_fusion
  555.4 0.0 copy-done.4
  555.4 4.3 copy.37
  (2 shorter events, 0.0 us)
Async XLA Ops:
  7.2 89.1 %copy-start = (bf16[512,3072]{1,0:T(8,128)(2,1)S(1)}, bf16[512,3072]{1,0:T(8,128)(2,1)}, u32[]{:S(2)}) copy-start(bf16[512,3072]{1,0:T(8,128)(2,1)} %param.13) | copy-start | bytes 9437188
  7.2 198.6 %all-reduce.5.cloned.1.call-start = ((), (), s32[]{:S(2)}) async-start(), calls=%async_computation.1 | async-start | bytes 2359296
  9.7 88.0 %copy-start.2 = (bf16[512,3072]{1,0:T(8,128)(2,1)S(1)}, bf16[512,3072]{1,0:T(8,128)(2,1)}, u32[]{:S(2)}) copy-start(bf16[512,3072]{1,0:T(8,128)(2,1)} %param.10) | copy-start | bytes 9437188
  112.5 0.9 copy-start.1
  113.4 4.3 copy-start.3
  123.5 196.6 %copy-start.6 = (f32[2,4,384]{2,1,0:T(4,128)S(1)}, f32[2,4,384]{2,1,0:T(4,128)}, u32[]{:S(2)}) copy-start(f32[2,4,384]{2,1,0:T(4,128)} %param.19) | copy-start | bytes 36868
  123.5 196.6 %copy-start.7 = (f32[2,4,384]{2,1,0:T(4,128)S(1)}, f32[2,4,384]{2,1,0:T(4,128)}, u32[]{:S(2)}) copy-start(f32[2,4,384]{2,1,0:T(4,128)} %param.18) | copy-start | bytes 36868
  124.7 195.4 %all-reduce.7.cloned.1.call-start = ((), (), s32[]{:S(2)}) async-start(), calls=%async_computation.2 | async-start | bytes 294912
  126.7 294.9 %copy-start.5 = (f32[384,32]{0,1:T(8,128)S(1)}, f32[384,32]{0,1:T(8,128)}, u32[]{:S(2)}) copy-start(f32[384,32]{0,1:T(8,128)} %param.17) | copy-start | bytes 147460
  207.4 343.0 %all-gather.4.cloned.1.call-start = ((), (), s32[]{:S(2)}) async-start(), calls=%async_computation | async-start | bytes 4767744 | tf_op jit(solution)/shard_map/all_gather | solution.py:25
  423.5 131.9 %copy-start.4 = (f32[384,32]{0,1:T(8,128)}, f32[384,32]{0,1:T(8,128)S(1)}, u32[]{:S(2)}) copy-start(f32[384,32]{0,1:T(8,128)S(1)} %fusion.1) | copy-start | bytes 147460
Sparse Core Ops, SparseCore 0:
  124.9 80.9 all-reduce.4
  208.7 111.3 all-reduce.6
  429.6 120.7 all-gather.3
where the time goes:
time: 567 us; the launch traced here: 566 us
  waiting for transfers between devices  311 us (55%)
  blocking collectives  196 us (35%)
  local copies, waits for them, and re-layouts  27.8 us (5%)
  between operations  14.5 us (3%)
  matrix products  11.2 us (2%)
    unnamed x5, waiting for transfers between devices  190 us
    all_gather x1, waiting for transfers between devices, turned_gather(): filled = lax.all_gather(both, axis, axis=0, tiled=True)  121 us
    all_gather x1, blocking collectives, side_by_side(): lax.all_gather(both, axis, axis=dim, tiled=True)  86.5 us
    psum x4, blocking collectives, over_axes(): value = lax.psum(value, axis)  49.3 us
    all_gather x2, blocking collectives, gather_in_order(): blocks = lax.all_gather(blocks, axes[k])  46.8 us
    all_gather x1, blocking collectives, turned_gather(): filled = lax.all_gather(both, axis, axis=0, tiled=True)  13.6 us
  transfers between devices with their start and end apart: 3, of which 3 were waited for; matrix products, arithmetic and copies ran while one was open for 0% of the time, Pallas kernels for 0%

commit v1 on v0

v1 whole, which is shorter than its diff:
```python
import functools

import jax
import jax.numpy as jnp
from jax import lax
from jax.experimental import pallas as pl
from jax.experimental.pallas import tpu as pltpu
from jax.sharding import PartitionSpec as P


bf16 = jnp.bfloat16
f32 = jnp.float32
VMEM = pl.BlockSpec(memory_space=pltpu.VMEM)
SMEM = pl.BlockSpec(memory_space=pltpu.SMEM)


def cost(flops, nbytes):
    return pl.CostEstimate(flops=flops, bytes_accessed=nbytes, transcendentals=0)


def to_all(value, axis):
    n = lax.axis_size(axis)
    return lax.all_to_all(jnp.broadcast_to(value[None], (n, *value.shape)), axis, 0, 0)


def grad_kernel(proj, query_cotangent, attn_outputs, out):
    tokens = query_cotangent.shape[0]
    cols = query_cotangent.shape[1]
    first = jnp.dot(proj[:, :tokens], query_cotangent[...], preferred_element_type=f32)
    second = jnp.dot(proj[:, tokens:], attn_outputs[...], preferred_element_type=f32)
    first = first.reshape(-1, 8, cols)
    second = second.reshape(-1, 8, cols)
    both = jnp.concatenate([first[:, :4], second[:, :4], first[:, 4:], second[:, 4:]], axis=1)
    out[...] = both.astype(bf16)


def moment_kernel(pieces, first, second, first_new, second_new, low):
    rows = first.shape[1]
    grads = jnp.sum(pieces[...].astype(f32), axis=0)
    new_first = 0.9 * jnp.concatenate([first[0], first[1]], axis=0) + 0.1 * grads
    new_second = 0.99 * jnp.concatenate([second[0], second[1]], axis=0) + 0.01 * grads * grads
    direction = new_first / (jnp.sqrt(new_second) + 1e-08)
    first_new[0] = new_first[:rows]
    first_new[1] = new_first[rows:]
    second_new[0] = new_second[:rows]
    second_new[1] = new_second[rows:]
    squares = direction * direction
    lane = lax.broadcasted_iota(jnp.int32, (rows, 128), 1)
    sums = jnp.zeros((rows, 128), f32)
    for k in range(2):
        rest = jnp.sum(squares[k * rows : (k + 1) * rows], axis=(0, 1), keepdims=True)
        for part in range(3):
            rounded = rest.astype(bf16).astype(f32)
            sums = jnp.where(lane == 3 * k + part, rounded, sums)
            rest = rest - rounded
    sent = jnp.concatenate([direction[:rows], direction[rows:], sums], axis=1).astype(bf16)
    low[...] = jnp.broadcast_to(sent[None], low.shape)


def squares_kernel(low, out):
    sums = jnp.sum(low[:, :, -128:].astype(f32), axis=0)[:1]
    out[...] = jnp.broadcast_to(sums[None], out.shape)


def final_kernel(
    entries,
    place,
    low,
    squares,
    masters,
    held,
    other,
    query_copy,
    out_copy,
    query_new,
    out_new,
    direction,
    factors,
    tile,
):
    step = pl.program_id(0)
    tp, rank_cols, cols = direction.shape[1:]
    rows = low.shape[1]
    per_block = rank_cols // rows
    own = query_new.shape[0]
    span = query_copy.shape[0]

    @pl.when(step == 0)
    def _():
        for b in range(tp):
            chip, core = b % (tp // 2), b // (tp // 2)
            at = (place[1] + 2 * chip) % tp
            at = at + core * (1 - 2 * (at % 2))
            block = low[pl.ds(at * per_block, per_block)].astype(f32)
            for k in range(2):
                part = block[:, :, k * cols : (k + 1) * cols]
                part = jnp.concatenate([part[j] for j in range(per_block)], axis=0)
                direction[k, b] = part.astype(bf16)

    sums = jnp.sum(squares[...], axis=0)[:1]
    lane = lax.broadcasted_iota(jnp.int32, sums.shape, 1)
    for k, copy, new in ((0, query_copy, query_new), (1, out_copy, out_new)):
        total = jnp.sum(jnp.where(lane // 3 == k, sums, 0.0), axis=1, keepdims=True)
        scale = 0.01 * lax.rsqrt(total / entries + 1e-06)
        for c, half in enumerate((held, other)):
            for s in range(tp // 2):
                at = (c * (tp // 2) + s) * rank_cols
                factors[k, :, at : at + rank_cols] = half[s, :, k * rank_cols : (k + 1) * rank_cols]
        moved = jnp.dot(
            factors[k], direction[k].reshape(tp * rank_cols, cols), preferred_element_type=f32
        )
        kept = masters[:, k * own : (k + 1) * own].reshape(span, cols)
        fresh = kept - scale * moved
        if k == 0:
            copy[...] = fresh.astype(bf16)
        else:
            copy[...] = fresh.T.astype(bf16)

        @pl.when(step == place[0] // (span // own))
        def _():
            tile[...] = fresh
            new[...] = tile[pl.ds(pl.multiple_of(place[0] % (span // own) * own, own), own)]


def body(
    saved_inputs,
    query_cotangent,
    attn_outputs,
    out_cotangent,
    left_factor,
    right_factor,
    query_master,
    out_master,
    first_moment,
    second_moment,
):
    fs = lax.axis_size("fs")
    tp = lax.axis_size("tp")
    own, rank_cols = left_factor.shape
    rows = first_moment.shape[1]
    cols = first_moment.shape[2]
    width = fs * own
    ranks = tp * rank_cols

    masters = lax.all_gather(jnp.concatenate([query_master, out_master.T], axis=0), "fs")

    lanes = jnp.zeros((own, 128 - 2 * rank_cols), bf16)
    factors = to_all(jnp.concatenate([left_factor, right_factor, lanes], axis=1), "fs")
    factors = factors.reshape(width, 128)
    turned = (((0,), (1,)), ((), ()))
    left_part = lax.dot_general(
        factors[:, :rank_cols], saved_inputs, turned, preferred_element_type=f32
    )
    right_part = lax.dot_general(
        factors[:, rank_cols : 2 * rank_cols], out_cotangent, turned, preferred_element_type=f32
    )
    proj = jnp.concatenate([left_part.astype(bf16), right_part.astype(bf16)], axis=1)
    proj = lax.all_gather(proj, "tp", axis=0, tiled=True)

    proj, mine = lax.optimization_barrier((proj, factors))
    held = [mine]
    for step in range(1, tp // 2):
        held.append(lax.ppermute(mine, "tp", [((t + 2 * step) % tp, t) for t in range(tp)]))
    held = jnp.stack(held)

    partial = pl.pallas_call(
        grad_kernel,
        out_shape=jax.ShapeDtypeStruct((fs // 2, 4 * rows, cols), bf16),
        in_specs=[VMEM] * 3,
        out_specs=VMEM,
        cost_estimate=cost(4 * ranks * saved_inputs.shape[0] * cols, 2 << 20),
    )(proj, query_cotangent, attn_outputs)
    pieces = lax.all_to_all(partial.reshape(fs, 2 * rows, cols), "fs", 0, 0)
    other = lax.ppermute(held, "tp", [(t ^ 1, t) for t in range(tp)])
    first_new, second_new, low = pl.pallas_call(
        moment_kernel,
        out_shape=(
            jax.ShapeDtypeStruct(first_moment.shape, f32),
            jax.ShapeDtypeStruct(second_moment.shape, f32),
            jax.ShapeDtypeStruct((fs, rows, 2 * cols + 128), bf16),
        ),
        in_specs=[VMEM] * 3,
        out_specs=(VMEM, VMEM, VMEM),
        cost_estimate=cost(1 << 20, 2 << 20),
    )(pieces, first_moment, second_moment)
    low = lax.all_to_all(low, "fs", 0, 0)
    squares = pl.pallas_call(
        squares_kernel,
        out_shape=jax.ShapeDtypeStruct((tp, 8, 128), f32),
        in_specs=[VMEM],
        out_specs=VMEM,
        cost_estimate=cost(1 << 16, 1 << 16),
    )(low)
    squares = lax.all_to_all(squares, "tp", 0, 0)

    span = 256
    per = span // own
    place = jnp.stack([lax.axis_index("fs"), lax.axis_index("tp")]).astype(jnp.int32)
    query_copy, out_copy, query_new, out_new = pl.pallas_call(
        functools.partial(final_kernel, float(rows * fs * cols * tp)),
        grid=(width // span,),
        out_shape=(
            jax.ShapeDtypeStruct((width, cols), bf16),
            jax.ShapeDtypeStruct((cols, width), bf16),
            jax.ShapeDtypeStruct((own, cols), f32),
            jax.ShapeDtypeStruct((own, cols), f32),
        ),
        in_specs=[
            SMEM,
            VMEM,
            VMEM,
            pl.BlockSpec((per, 2 * own, cols), lambda i: (i, 0, 0)),
            pl.BlockSpec((tp // 2, span, 128), lambda i: (0, i, 0)),
            pl.BlockSpec((tp // 2, span, 128), lambda i: (0, i, 0)),
        ],
        out_specs=(
            pl.BlockSpec((span, cols), lambda i: (i, 0)),
            pl.BlockSpec((cols, span), lambda i: (0, i)),
            pl.BlockSpec((own, cols), lambda i: (0, 0)),
            pl.BlockSpec((own, cols), lambda i: (0, 0)),
        ),
        scratch_shapes=[
            pltpu.VMEM((2, tp, rank_cols, cols), bf16),
            pltpu.VMEM((2, span, ranks), bf16),
            pltpu.VMEM((span, cols), f32),
        ],
        cost_estimate=cost(4 * width * ranks * cols, 20 << 20),
    )(place, low, squares, masters, held, other)
    return (query_new, out_new.T, query_copy, out_copy, first_new, second_new)


def solution(mesh):
    both = P("fs", "tp")
    moment = P(None, "fs", "tp")

    return jax.shard_map(
        body,
        mesh=mesh,
        in_specs=(P("fs", None), both, both, P("fs", None), both, both, both, P("tp", "fs"), moment, moment),
        out_specs=(both, P("tp", "fs"), P(None, "tp"), P("tp", None), moment, moment),
        check_vma=False,
    )
```

time: 567 us -> 230 us (0.41)
  the two profiles are of different devices: /device:TPU:2 before, /device:TPU:8 now
where the time goes in v1:
time: 230 us; the launch traced here: 229 us
  waiting for transfers between devices  74.5 us (32%)
  blocking collectives  74.5 us (32%)
  starting transfers between devices  29.7 us (13%)
  Pallas kernels  24.4 us (11%)
  between operations  14.2 us (6%)
  other arithmetic  6.22 us (3%)
  matrix products  4.85 us (2%)
    all_to_all x1, blocking collectives, to_all(): lax.all_to_all(jnp.broadcast_to(value[None], (n, *value.shape)), axis, 0, 0)  59.8 us
    all_to_all x1, waiting for transfers between devices, body(): low = lax.all_to_all(low, 'fs', 0, 0)  39.3 us
    ppermute x3, waiting for transfers between devices, body(): lax.ppermute(mine, 'tp', [((t + 2 * step) % tp, t) for t in range(tp)])  22.3 us
    pallas_call x1, Pallas kernels, body(): pl.pallas_call(functools.partial(final_kernel, float(rows * fs * cols * t...  17.6 us
    all_gather x1, blocking collectives, body(): proj = lax.all_gather(proj, 'tp', axis=0, tiled=True)  14.8 us
    ppermute x3, starting transfers between devices, body(): lax.ppermute(mine, 'tp', [((t + 2 * step) % tp, t) for t in range(tp)])  9.81 us
    all_to_all x1, waiting for transfers between devices, body(): pieces = lax.all_to_all(partial.reshape(fs, 2 * rows, cols), 'fs', 0, 0)  7.97 us
    all_to_all x1, starting transfers between devices, body(): pieces = lax.all_to_all(partial.reshape(fs, 2 * rows, cols), 'fs', 0, 0)  7.66 us
  transfers between devices with their start and end apart: 8, of which 6 were waited for; matrix products, arithmetic and copies ran while one was open for 4% of the time, Pallas kernels for 3%

profile of v1, /device:TPU:8, one launch (start us, length us, event | category | flops | bytes accessed | tf_op | source)
XLA Modules:
  0.0 229.2 jit_solution(8923452008508831688)
XLA Ops:
  7.2 0.0 copy-start
  7.2 0.0 all-gather.3.cloned.1.call-start
  7.2 1.6 pad_maximum_fusion.2
  8.8 0.0 all-gather.3.cloned.1.call-update
  8.9 0.1 pad.10.clone
  9.0 0.8 maximum_maximum_fusion
  9.8 0.0 copy-start.1
  9.8 0.1 broadcast_in_dim.10
  9.9 59.8 %all_to_all.20 = bf16[96,32,128]{2,1,0:T(8,128)(2,1)} all-to-all(bf16[96,32,128]{2,1,0:T(8,128)(2,1)S(1)} %broadcast_in_dim.10), channel_id=1, replica_groups=mesh['fs'=96,'tp'=8] {'fs'}, dimensions={0} | all-to-all | bytes 1572864 | tf_op jit(solution)/shard_map/all_to_all | solution.py:23
  69.6 0.0 copy-done
  69.6 2.6 %convolution_convert_fusion = bf16[48,512]{1,0:T(8,128)(2,1)S(1)} fusion(bf16[512,3072]{1,0:T(8,128)(2,1)S(1)} %copy-done, bf16[3072,128]{1,0:T(8,128)(2,1)} %bitcast.2), kind=kOutput, calls=%fused_computation.1 | convolution fusion | flops 151019520 | bytes 3981312 | tf_op jit(solution)/shard_map/dot_general | solution.py:154
  72.3 0.0 copy-done.1
  72.3 2.2 convolution_convert_fusion.1
  74.5 14.8 %all_gather.9.proj = bf16[384,1024]{1,0:T(8,128)(2,1)} all-gather(bf16[48,1024]{1,0:T(8,128)(2,1)S(1)} %pad_maximum_fusion.1), channel_id=1, replica_groups=mesh['fs'=96,'tp'=8] {'tp'}, dimensions={0}, use_global_device_ids=true | all-gather | bytes 884736 | tf_op jit(solution)/shard_map/all_gather | solution.py:158
  89.3 3.2 %collective-permute-start.2 = (bf16[3072,128]{1,0:T(8,128)(2,1)}, bf16[3072,128]{1,0:T(8,128)(2,1)}, u32[]{:S(2)}, u32[]{:S(2)}) collective-permute-start(bf16[3072,128]{1,0:T(8,128)(2,1)} %bitcast.2), channel_id=1, source_target_pairs={{6,0},{7,1},{0,2},{1,3},{2,4},{3,5},{4,6},{5,7},{14,8},{15,9},{8,1... | collective-permute-start | bytes 2359304 | tf_op jit(solution)/shard_map/ppermute | solution.py:163
  92.5 4.6 %collective-permute-start.1 = (bf16[3072,128]{1,0:T(8,128)(2,1)}, bf16[3072,128]{1,0:T(8,128)(2,1)}, u32[]{:S(2)}, u32[]{:S(2)}) collective-permute-start(bf16[3072,128]{1,0:T(8,128)(2,1)} %bitcast.2), channel_id=1, source_target_pairs={{4,0},{5,1},{6,2},{7,3},{0,4},{1,5},{2,6},{3,7},{12,8},{13,9},{14,... | collective-permute-start | bytes 2359304 | tf_op jit(solution)/shard_map/ppermute | solution.py:163
  97.1 2.1 collective-permute-start
  99.1 2.7 %shard_map.145 = bf16[48,16,384]{2,1,0:T(8,128)(2,1)} custom-call(bf16[384,1024]{1,0:T(8,128)(2,1)} %all_gather.9.proj, bf16[512,384]{1,0:T(8,128)(2,1)} %query_cotangent.1, bf16[512,384]{1,0:T(8,128)(2,1)} %attn_outputs.1), custom_call_target="tpu_custom_call" | custom-call | flops 301989888 | bytes 2097152 | tf_op jit(solution)/shard_map/pallas_call | solution.py:166
  101.9 7.7 %all-to-all-start.1 = ((bf16[96,8,384]{2,1,0:T(8,128)(2,1)}), bf16[96,8,384]{2,1,0:T(8,128)(2,1)}, u32[]{:S(2)}, u32[]{:S(2)}) async-start(bf16[96,8,384]{2,1,0:T(8,128)(2,1)} %bitcast.14), calls=%async_computation.1 | async-start | bytes 1179648 | tf_op jit(solution)/shard_map/all_to_all | solution.py:173
  109.5 3.0 %collective-permute-done.2 = bf16[3072,128]{1,0:T(8,128)(2,1)} collective-permute-done((bf16[3072,128]{1,0:T(8,128)(2,1)}, bf16[3072,128]{1,0:T(8,128)(2,1)}, u32[]{:S(2)}, u32[]{:S(2)}) %collective-permute-start.2) | collective-permute-done | bytes 786464 | tf_op jit(solution)/shard_map/ppermute | solution.py:163
  112.5 17.6 %collective-permute-done.1 = bf16[3072,128]{1,0:T(8,128)(2,1)} collective-permute-done((bf16[3072,128]{1,0:T(8,128)(2,1)}, bf16[3072,128]{1,0:T(8,128)(2,1)}, u32[]{:S(2)}, u32[]{:S(2)}) %collective-permute-start.1) | collective-permute-done | bytes 786464 | tf_op jit(solution)/shard_map/ppermute | solution.py:163
  130.1 1.8 collective-permute-done
  131.9 3.2 %pad_maximum_fusion.held = bf16[4,3072,128]{2,1,0:T(8,128)(2,1)} fusion(bf16[1,3072,128]{2,1,0:T(8,128)(2,1)} %bitcast.9, bf16[1,3072,128]{2,1,0:T(8,128)(2,1)} %bitcast.8, bf16[1,3072,128]{2,1,0:T(8,128)(2,1)} %bitcast.7, bf16[1,3072,128]{2,1,0:T(8,128)(2,1)} %bitcast.6), kind=kLoop, calls=%fused_computation | loop fusion | flops 4718592 | bytes 6291456 | tf_op jit(solution)/shard_map/stack | solution.py:164
  135.1 1.9 collective-permute-start.3
  137.0 8.0 %all-to-all-done.1.pieces = bf16[96,8,384]{2,1,0:T(8,128)(2,1)} async-done(((bf16[96,8,384]{2,1,0:T(8,128)(2,1)}), bf16[96,8,384]{2,1,0:T(8,128)(2,1)}, u32[]{:S(2)}, u32[]{:S(2)}) %all-to-all-start.1) | async-done | bytes 589856 | tf_op jit(solution)/shard_map/all_to_all | solution.py:173
  145.0 2.2 shard_map.146
  147.2 6.9 %all-to-all-start.2 = ((bf16[96,4,896]{2,1,0:T(4,128)(2,1)}), bf16[96,4,896]{2,1,0:T(4,128)(2,1)}, u32[]{:S(2)}, u32[]{:S(2)}) async-start(bf16[96,4,896]{2,1,0:T(4,128)(2,1)} %get-tuple-element.16), calls=%async_computation.2 | async-start | bytes 1376256 | tf_op jit(solution)/shard_map/all_to_all | solution.py:186
  154.1 39.3 %all-to-all-done.2.low = bf16[96,4,896]{2,1,0:T(4,128)(2,1)} async-done(((bf16[96,4,896]{2,1,0:T(4,128)(2,1)}), bf16[96,4,896]{2,1,0:T(4,128)(2,1)}, u32[]{:S(2)}, u32[]{:S(2)}) %all-to-all-start.2) | async-done | bytes 688160 | tf_op jit(solution)/shard_map/all_to_all | solution.py:186
  193.5 1.8 shard_map.147
  195.3 3.4 %all-to-all-start.3 = ((f32[8,8,128]{2,1,0:T(8,128)}), f32[8,8,128]{2,1,0:T(8,128)S(1)}, u32[]{:S(2)}, u32[]{:S(2)}) async-start(f32[8,8,128]{2,1,0:T(8,128)} %shard_map.147), calls=%async_computation.3 | async-start | bytes 65536 | tf_op jit(solution)/shard_map/all_to_all | solution.py:194
  198.7 0.6 pad_add_fusion.place
  199.3 4.8 %all-to-all-done.3.squares = f32[8,8,128]{2,1,0:T(8,128)S(1)} async-done(((f32[8,8,128]{2,1,0:T(8,128)}), f32[8,8,128]{2,1,0:T(8,128)S(1)}, u32[]{:S(2)}, u32[]{:S(2)}) %all-to-all-start.3) | async-done | bytes 32800 | tf_op jit(solution)/shard_map/all_to_all | solution.py:194
  204.1 0.0 copy-start.2
  204.1 0.0 collective-permute-done.3.other
  204.1 0.0 all-gather.3.cloned.1.call-done
  204.1 0.6 copy-done.2
  204.7 17.6 %shard_map.148 = (bf16[3072,384]{1,0:T(8,128)(2,1)}, bf16[384,3072]{1,0:T(8,128)(2,1)}, f32[32,384]{1,0:T(8,128)}, f32[32,384]{1,0:T(8,128)}) custom-call(s32[2]{0:T(128)} %pad_add_fusion.place, bf16[96,4,896]{2,1,0:T(4,128)(2,1)} %all-to-all-done.2.low, f32[8,8,128]{2,1,0:T(8,128)} %copy-done.2, f32[96,64,384]{2,1,0:T(8,128)} %bitcast.13, ...), custom_call_target="tpu_custom_call" | custom-call | flops 1811939328 | bytes 20971520 | tf_op jit(solution)/shard_map/pallas_call | solution.py:199
  (2 shorter events, 0.0 us)
Async XLA Ops:
  7.2 62.5 %copy-start = (bf16[512,3072]{1,0:T(8,128)(2,1)S(1)}, bf16[512,3072]{1,0:T(8,128)(2,1)}, u32[]{:S(2)}) copy-start(bf16[512,3072]{1,0:T(8,128)(2,1)} %param.13) | copy-start | bytes 9437188
  7.2 196.9 %all-gather.3.cloned.1.call-start = ((), (), s32[]{:S(2)}) async-start(), calls=%async_computation.4 | async-start | bytes 9535488 | tf_op jit(solution)/shard_map/all_gather | solution.py:145
  9.8 62.5 %copy-start.1 = (bf16[512,3072]{1,0:T(8,128)(2,1)S(1)}, bf16[512,3072]{1,0:T(8,128)(2,1)}, u32[]{:S(2)}) copy-start(bf16[512,3072]{1,0:T(8,128)(2,1)} %param.10) | copy-start | bytes 9437188
  89.3 23.2 %collective-permute-start.2 = (bf16[3072,128]{1,0:T(8,128)(2,1)}, bf16[3072,128]{1,0:T(8,128)(2,1)}, u32[]{:S(2)}, u32[]{:S(2)}) collective-permute-start(bf16[3072,128]{1,0:T(8,128)(2,1)} %bitcast.2), channel_id=1, source_target_pairs={{6,0},{7,1},{0,2},{1,3},{2,4},{3,5},{4,6},{5,7},{14,8},{15,9},{8,1... | collective-permute-start | bytes 2359304 | tf_op jit(solution)/shard_map/ppermute | solution.py:163
  92.5 37.6 %collective-permute-start.1 = (bf16[3072,128]{1,0:T(8,128)(2,1)}, bf16[3072,128]{1,0:T(8,128)(2,1)}, u32[]{:S(2)}, u32[]{:S(2)}) collective-permute-start(bf16[3072,128]{1,0:T(8,128)(2,1)} %bitcast.2), channel_id=1, source_target_pairs={{4,0},{5,1},{6,2},{7,3},{0,4},{1,5},{2,6},{3,7},{12,8},{13,9},{14,... | collective-permute-start | bytes 2359304 | tf_op jit(solution)/shard_map/ppermute | solution.py:163
  97.1 34.8 %collective-permute-start = (bf16[3072,128]{1,0:T(8,128)(2,1)}, bf16[3072,128]{1,0:T(8,128)(2,1)}, u32[]{:S(2)}, u32[]{:S(2)}) collective-permute-start(bf16[3072,128]{1,0:T(8,128)(2,1)} %bitcast.2), channel_id=1, source_target_pairs={{2,0},{3,1},{4,2},{5,3},{6,4},{7,5},{0,6},{1,7},{10,8},{11,9},{12,... | collective-permute-start | bytes 2359304 | tf_op jit(solution)/shard_map/ppermute | solution.py:163
  101.9 43.1 %all-to-all-start.1 = ((bf16[96,8,384]{2,1,0:T(8,128)(2,1)}), bf16[96,8,384]{2,1,0:T(8,128)(2,1)}, u32[]{:S(2)}, u32[]{:S(2)}) async-start(bf16[96,8,384]{2,1,0:T(8,128)(2,1)} %bitcast.14), calls=%async_computation.1 | async-start | bytes 1179648 | tf_op jit(solution)/shard_map/all_to_all | solution.py:173
  135.1 69.0 %collective-permute-start.3 = (bf16[4,3072,128]{2,1,0:T(8,128)(2,1)}, bf16[4,3072,128]{2,1,0:T(8,128)(2,1)}, u32[]{:S(2)}, u32[]{:S(2)}) collective-permute-start(bf16[4,3072,128]{2,1,0:T(8,128)(2,1)} %pad_maximum_fusion.held), channel_id=1, source_target_pairs={{1,0},{0,1},{3,2},{2,3},{5,4},{4,5},{7,6},{6,7},{9,8},{8,9},{11,10... | collective-permute-start | bytes 9437192 | tf_op jit(solution)/shard_map/ppermute | solution.py:174
  147.2 46.3 %all-to-all-start.2 = ((bf16[96,4,896]{2,1,0:T(4,128)(2,1)}), bf16[96,4,896]{2,1,0:T(4,128)(2,1)}, u32[]{:S(2)}, u32[]{:S(2)}) async-start(bf16[96,4,896]{2,1,0:T(4,128)(2,1)} %get-tuple-element.16), calls=%async_computation.2 | async-start | bytes 1376256 | tf_op jit(solution)/shard_map/all_to_all | solution.py:186
  195.3 8.8 %all-to-all-start.3 = ((f32[8,8,128]{2,1,0:T(8,128)}), f32[8,8,128]{2,1,0:T(8,128)S(1)}, u32[]{:S(2)}, u32[]{:S(2)}) async-start(f32[8,8,128]{2,1,0:T(8,128)} %shard_map.147), calls=%async_computation.3 | async-start | bytes 65536 | tf_op jit(solution)/shard_map/all_to_all | solution.py:194
  204.1 0.6 copy-start.2
Sparse Core Ops, SparseCore 0:
  12.3 185.0 all-gather.2

commit v2 on v1

v2 whole, which is shorter than its diff:
```python
import functools

import jax
import jax.numpy as jnp
from jax import lax
from jax.experimental import pallas as pl
from jax.experimental.pallas import tpu as pltpu
from jax.sharding import Mesh
from jax.sharding import PartitionSpec as P


bf16 = jnp.bfloat16
f32 = jnp.float32
FS = ("z", "y")
VMEM = pl.BlockSpec(memory_space=pltpu.VMEM)
SMEM = pl.BlockSpec(memory_space=pltpu.SMEM)
REACH = 2.0**19
SMALL = pltpu.CompilerParams(vmem_limit_bytes=16 << 20)


def cost(flops, nbytes):
    return pl.CostEstimate(flops=flops, bytes_accessed=nbytes, transcendentals=0)


def send_kernel(left, right, query_master, out_master, out, masters):
    own = query_master.shape[0]
    masters[:own] = query_master[...]
    masters[own : 2 * own] = out_master[...]
    masters[2 * own :] = jnp.zeros((masters.shape[0] - 2 * own, masters.shape[1]), f32)
    both = jnp.concatenate([left[...].astype(f32), right[...].astype(f32)], axis=1)
    used = both.shape[1]
    free = 128 - used
    kept = out.shape[1]
    rest = both[kept:]
    tail = jnp.concatenate([rest[:, j : j + free] for j in range(0, used, free)], axis=0)
    packed = jnp.concatenate([both[:kept], tail], axis=1).astype(bf16)
    out[...] = jnp.broadcast_to(packed[None], out.shape)


def unpacked(packed, used):
    free = 128 - used
    parts = used // free
    height = packed.shape[1] // parts
    wide = packed.astype(f32)
    tail = [wide[:, j * height : (j + 1) * height, used:] for j in range(parts)]
    tail = jnp.concatenate(tail + [jnp.zeros_like(tail[0])], axis=2)
    return jnp.concatenate([wide, tail], axis=1)


def proj_kernel(used, packed, saved_inputs, out_cotangent, out, left, right):
    step = pl.program_id(0)
    rows = saved_inputs.shape[1]

    @pl.when(step == 0)
    def _():
        left[...] = jnp.zeros_like(left)
        right[...] = jnp.zeros_like(right)

    factors = unpacked(packed[...], used).reshape(rows, 128).astype(bf16)
    left[...] += jnp.dot(saved_inputs[...], factors, preferred_element_type=f32)
    right[...] += jnp.dot(out_cotangent[...], factors, preferred_element_type=f32)

    @pl.when(step == pl.num_programs(0) - 1)
    def _():
        lane = lax.broadcasted_iota(jnp.int32, left.shape, 1)
        both = jnp.where(lane < used // 2, left[...], right[...])
        out[...] = both.T[:used].astype(bf16)


def grad_kernel(rank_cols, proj, query_cotangent, attn_outputs, out):
    cols = query_cotangent.shape[1]
    parts = []
    for k, other in enumerate((query_cotangent, attn_outputs)):
        starts = range(k * rank_cols, proj.shape[0], 2 * rank_cols)
        ranks = jnp.concatenate([proj[at : at + rank_cols] for at in starts], axis=0)
        parts.append(jnp.dot(ranks, other[...], preferred_element_type=f32).reshape(-1, 8, cols))
    first, second = parts
    both = jnp.concatenate([first[:, :4], second[:, :4], first[:, 4:], second[:, 4:]], axis=1)
    out[...] = both.astype(bf16)


def moment_kernel(pieces, first, second, first_new, second_new, low):
    rows = first.shape[1]
    grads = jnp.sum(pieces[...].astype(f32), axis=0)
    new_first = 0.9 * jnp.concatenate([first[0], first[1]], axis=0) + 0.1 * grads
    new_second = 0.99 * jnp.concatenate([second[0], second[1]], axis=0) + 0.01 * grads * grads
    direction = new_first / (jnp.sqrt(new_second) + 1e-08)
    first_new[0] = new_first[:rows]
    first_new[1] = new_first[rows:]
    second_new[0] = new_second[:rows]
    second_new[1] = new_second[rows:]
    squares = direction * direction
    lane = lax.broadcasted_iota(jnp.int32, (rows, 128), 1)
    sums = jnp.zeros((rows, 128), f32)
    for k in range(2):
        rest = jnp.sum(squares[k * rows : (k + 1) * rows], axis=(0, 1), keepdims=True)
        for part in range(3):
            rounded = rest.astype(bf16).astype(f32)
            sums = jnp.where(lane == 3 * k + part, rounded, sums)
            rest = rest - rounded
    sent = jnp.concatenate([direction[:rows], direction[rows:], sums], axis=1).astype(bf16)
    low[...] = jnp.broadcast_to(sent[None], low.shape)


def coded(value):
    size = jnp.abs(value) * REACH
    size = size * size
    size = size * size
    size = size * size
    return jnp.where(value < 0.0, -size, size).astype(bf16)


def decoded(code):
    wide = code.astype(f32)
    size = jnp.sqrt(jnp.sqrt(jnp.sqrt(jnp.abs(wide)))) * (1.0 / REACH)
    return jnp.where(wide < 0.0, -size, size)


def prep_kernel(rank_cols, place, masters, held, other, left, right, query_master, out_master, own_left, own_right, tile):
    own = masters.shape[1] // 2
    span = left.shape[0]
    cols = masters.shape[2]
    query_master[...] = decoded(masters[:, :own].reshape(span, cols))
    out_master[...] = decoded(masters[:, own:].reshape(span, cols)).T
    sides = [[], []]
    for half in (held, other):
        for s in range(half.shape[0]):
            block = unpacked(half[s], 2 * rank_cols).reshape(span, 128)
            for k in range(2):
                sides[k].append(block[:, k * rank_cols : (k + 1) * rank_cols])
    both = [jnp.concatenate(side, axis=1) for side in sides]
    left[...] = both[0].astype(bf16)
    right[...] = both[1].T.astype(bf16)

    @pl.when(pl.program_id(0) == place[0] // (span // own))
    def _():
        rows = pl.ds(pl.multiple_of(place[0] % (span // own) * own, own), own)
        for side, out in zip(both, (own_left, own_right)):
            tile[...] = side
            out[...] = tile[rows].astype(bf16)


def sums_kernel(rank_cols, place, low, squares, first, second):
    tp = squares.shape[0]
    cols = first.shape[1]
    per_block = rank_cols // low.shape[1]
    sums = jnp.sum(low[:, :, -128:].astype(f32), axis=0)[:1]
    squares[...] = jnp.broadcast_to(sums[None], squares.shape)
    for b in range(tp):
        chip, core = b % (tp // 2), b // (tp // 2)
        at = (place[1] + 2 * chip) % tp
        at = at + core * (1 - 2 * (at % 2))
        block = low[pl.ds(at * per_block, per_block)].astype(f32)
        for k, out in enumerate((first, second)):
            part = block[:, :, k * cols : (k + 1) * cols]
            part = jnp.concatenate([part[j] for j in range(per_block)], axis=0)
            out[b * rank_cols : (b + 1) * rank_cols] = part.astype(bf16)


def final_kernel(
    entries,
    squares,
    first,
    second,
    left,
    right,
    query_all,
    out_all,
    own_left,
    own_right,
    query_master,
    out_master,
    query_copy,
    out_copy,
    query_new,
    out_new,
):
    step = pl.program_id(0)
    sums = jnp.sum(squares[...], axis=0)[:1]
    lane = lax.broadcasted_iota(jnp.int32, sums.shape, 1)
    scales = []
    for k in range(2):
        total = jnp.sum(jnp.where(lane // 3 == k, sums, 0.0), axis=1, keepdims=True)
        scales.append(0.01 * lax.rsqrt(total / entries + 1e-06))
    moved = jnp.dot(left[...], first[...], preferred_element_type=f32)
    query_copy[...] = (query_all[...] - scales[0] * moved).astype(bf16)
    across = (((0,), (0,)), ((), ()))
    moved = lax.dot_general(second[...], right[...], across, preferred_element_type=f32)
    out_copy[...] = (out_all[...] - scales[1] * moved).astype(bf16)

    @pl.when(step == 0)
    def _():
        moved = jnp.dot(own_left[...], first[...], preferred_element_type=f32)
        query_new[...] = query_master[...] - scales[0] * moved
        moved = jnp.dot(own_right[...], second[...], preferred_element_type=f32)
        out_new[...] = out_master[...] - scales[1] * moved


def far(value):
    return pltpu.with_memory_space_constraint(value, pltpu.HBM)


def body(
    saved_inputs,
    query_cotangent,
    attn_outputs,
    out_cotangent,
    left_factor,
    right_factor,
    query_master,
    out_master,
    first_moment,
    second_moment,
):
    depth = lax.axis_size("z")
    fs = lax.axis_size(FS)
    tp = lax.axis_size("tp")
    own, rank_cols = left_factor.shape
    rows = first_moment.shape[1]
    cols = first_moment.shape[2]
    tokens = saved_inputs.shape[0]
    width = fs * own
    ranks = tp * rank_cols
    used = 2 * rank_cols
    kept = own * used // 128

    place = jnp.stack([lax.axis_index(FS), lax.axis_index("tp")]).astype(jnp.int32)
    packed, masters = pl.pallas_call(
        send_kernel,
        out_shape=(
            jax.ShapeDtypeStruct((fs, kept, 128), bf16),
            pltpu.HBM((88, cols), f32),
        ),
        in_specs=[pl.BlockSpec()] * 4,
        out_specs=(VMEM, VMEM),
        compiler_params=SMALL,
        cost_estimate=cost(1 << 16, 1 << 20),
    )(far(left_factor), far(right_factor), far(query_master), far(out_master.T))
    masters = lax.all_gather(masters, "y")
    packed = lax.all_to_all(packed, FS, 0, 0)
    packed, masters = lax.optimization_barrier((packed, masters))
    masters = masters[:, : 2 * own]
    masters = lax.all_gather(coded(masters), "z").reshape(fs, 2 * own, cols)
    parts = 6
    proj = pl.pallas_call(
        functools.partial(proj_kernel, used),
        grid=(parts,),
        out_shape=jax.ShapeDtypeStruct((used, tokens), bf16),
        in_specs=[
            pl.BlockSpec((fs // parts, kept, 128), lambda i: (i, 0, 0)),
            pl.BlockSpec((tokens, width // parts), lambda i: (0, i)),
            pl.BlockSpec((tokens, width // parts), lambda i: (0, i)),
        ],
        out_specs=pl.BlockSpec((used, tokens), lambda i: (0, 0)),
        scratch_shapes=[pltpu.VMEM((tokens, 128), f32)] * 2,
        compiler_params=SMALL,
        cost_estimate=cost(4 * tokens * width * 128, 8 << 20),
    )(packed, far(saved_inputs), far(out_cotangent))
    proj = lax.all_gather(proj, "tp", axis=0, tiled=True)

    partial = pl.pallas_call(
        functools.partial(grad_kernel, rank_cols),
        out_shape=pltpu.HBM((fs // 2, 4 * rows, cols), bf16),
        in_specs=[VMEM] * 3,
        out_specs=VMEM,
        compiler_params=SMALL,
        cost_estimate=cost(4 * ranks * tokens * cols, 2 << 20),
    )(proj, query_cotangent, attn_outputs)
    pieces = lax.all_to_all(partial.reshape(fs, 2 * rows, cols), FS, 0, 0)

    held = [packed]
    for step in range(1, tp // 2):
        held.append(lax.ppermute(packed, "tp", [((t + 2 * step) % tp, t) for t in range(tp)]))
    held = jnp.stack(held)
    other = lax.ppermute(held, "tp", [(t ^ 1, t) for t in range(tp)])

    first_new, second_new, low = pl.pallas_call(
        moment_kernel,
        out_shape=(
            jax.ShapeDtypeStruct(first_moment.shape, f32),
            jax.ShapeDtypeStruct(second_moment.shape, f32),
            pltpu.HBM((fs, rows, 2 * cols + 128), bf16),
        ),
        in_specs=[VMEM] * 3,
        out_specs=(VMEM, VMEM, VMEM),
        compiler_params=SMALL,
        cost_estimate=cost(1 << 20, 2 << 20),
    )(pieces, first_moment, second_moment)
    low = lax.all_to_all(low, FS, 0, 0)

    span = width // depth
    per = fs // depth
    left, right, query_all, out_all, own_left, own_right = pl.pallas_call(
        functools.partial(prep_kernel, rank_cols),
        grid=(depth,),
        out_shape=(
            pltpu.HBM((width, ranks), bf16),
            pltpu.HBM((ranks, width), bf16),
            pltpu.HBM((width, cols), f32),
            pltpu.HBM((cols, width), f32),
            pltpu.HBM((own, ranks), bf16),
            pltpu.HBM((own, ranks), bf16),
        ),
        in_specs=[
            SMEM,
            pl.BlockSpec((per, 2 * own, cols), lambda i: (i, 0, 0)),
            pl.BlockSpec((tp // 2, per, kept, 128), lambda i: (0, i, 0, 0)),
            pl.BlockSpec((tp // 2, per, kept, 128), lambda i: (0, i, 0, 0)),
        ],
        out_specs=(
            pl.BlockSpec((span, ranks), lambda i: (i, 0)),
            pl.BlockSpec((ranks, span), lambda i: (0, i)),
            pl.BlockSpec((span, cols), lambda i: (i, 0)),
            pl.BlockSpec((cols, span), lambda i: (0, i)),
            pl.BlockSpec((own, ranks), lambda i: (0, 0)),
            pl.BlockSpec((own, ranks), lambda i: (0, 0)),
        ),
        scratch_shapes=[pltpu.VMEM((span, ranks), f32)],
        compiler_params=SMALL,
        cost_estimate=cost(1 << 30, 30 << 20),
    )(place, far(masters), far(held), far(other))

    squares, first, second = pl.pallas_call(
        functools.partial(sums_kernel, rank_cols),
        out_shape=(
            jax.ShapeDtypeStruct((tp, 8, 128), f32),
            jax.ShapeDtypeStruct((ranks, cols), bf16),
            jax.ShapeDtypeStruct((ranks, cols), bf16),
        ),
        in_specs=[SMEM, VMEM],
        out_specs=(VMEM, VMEM, VMEM),
        compiler_params=SMALL,
        cost_estimate=cost(1 << 16, 1 << 16),
    )(place, low)
    squares = lax.all_to_all(squares, "tp", 0, 0)

    query_copy, out_copy, query_new, out_new = pl.pallas_call(
        functools.partial(final_kernel, float(rows * fs * cols * tp)),
        grid=(depth,),
        out_shape=(
            jax.ShapeDtypeStruct((width, cols), bf16),
            jax.ShapeDtypeStruct((cols, width), bf16),
            jax.ShapeDtypeStruct((own, cols), f32),
            jax.ShapeDtypeStruct((own, cols), f32),
        ),
        in_specs=[
            VMEM,
            VMEM,
            VMEM,
            pl.BlockSpec((span, ranks), lambda i: (i, 0)),
            pl.BlockSpec((ranks, span), lambda i: (0, i)),
            pl.BlockSpec((span, cols), lambda i: (i, 0)),
            pl.BlockSpec((cols, span), lambda i: (0, i)),
            VMEM,
            VMEM,
            VMEM,
            VMEM,
        ],
        out_specs=(
            pl.BlockSpec((span, cols), lambda i: (i, 0)),
            pl.BlockSpec((cols, span), lambda i: (0, i)),
            pl.BlockSpec((own, cols), lambda i: (0, 0)),
            pl.BlockSpec((own, cols), lambda i: (0, 0)),
        ),
        compiler_params=SMALL,
        cost_estimate=cost(4 * width * ranks * cols, 20 << 20),
    )(
        squares,
        first,
        second,
        left,
        right,
        query_all,
        out_all,
        own_left,
        own_right,
        query_master,
        out_master.T,
    )
    return (query_new, out_new.T, query_copy, out_copy, first_new, second_new)


def solution(mesh):
    finer = Mesh(mesh.devices.reshape(12, 8, 8), ("z", "y", "tp"))
    both = P(FS, "tp")
    moment = P(None, FS, "tp")

    return jax.shard_map(
        body,
        mesh=finer,
        in_specs=(P(FS, None), both, both, P(FS, None), both, both, both, P("tp", FS), moment, moment),
        out_specs=(both, P("tp", FS), P(None, "tp"), P("tp", None), moment, moment),
        check_vma=False,
    )
```

time: 230 us -> 243 us (1.057)
  the two profiles are of different devices: /device:TPU:8 before, /device:TPU:1 now
where the time goes in v2:
time: 243 us; the launch traced here: 241 us
  blocking collectives  67.4 us (28%)
  waiting for transfers between devices  62.1 us (26%)
  starting transfers between devices  46.1 us (19%)
  Pallas kernels  38.1 us (16%)
  between operations  14.2 us (6%)
  local copies, waits for them, and re-layouts  9.5 us (4%)
  other arithmetic  3.9 us (2%)
    all_to_all x1, blocking collectives, body(): packed = lax.all_to_all(packed, FS, 0, 0)  49.6 us
    all_to_all x1, waiting for transfers between devices, body(): low = lax.all_to_all(low, FS, 0, 0)  30.2 us
    ppermute x3, waiting for transfers between devices, body(): lax.ppermute(packed, 'tp', [((t + 2 * step) % tp, t) for t in range(tp)])  27 us
    pallas_call x1, Pallas kernels, body(): pl.pallas_call(functools.partial(prep_kernel, rank_cols), grid=(depth,),...  18.9 us
    all_gather x1, blocking collectives, body(): proj = lax.all_gather(proj, 'tp', axis=0, tiled=True)  17.8 us
    all_to_all x1, starting transfers between devices, body(): low = lax.all_to_all(low, FS, 0, 0)  15 us
    all_to_all x1, starting transfers between devices, body(): pieces = lax.all_to_all(partial.reshape(fs, 2 * rows, cols), FS, 0, 0)  13.3 us
    unnamed x24, local copies, waits for them, and re-layouts  9.5 us
  transfers between devices with their start and end apart: 9, of which 5 were waited for; matrix products, arithmetic and copies ran while one was open for 1% of the time, Pallas kernels for 12%

profile of v2, /device:TPU:1, one launch (start us, length us, event | category | flops | bytes accessed | tf_op | source)
XLA Modules:
  0.0 241.3 jit_solution(6651515587384871708)
XLA Ops:
  7.2 0.0 all-gather.5.cloned.1.call-start
  7.2 1.5 shard_map.145
  8.7 0.0 all-gather.5.cloned.1.call-update
  8.8 0.0 all-gather.7.cloned.1.call-start
  8.8 49.6 %all_to_all.20.packed = bf16[96,24,128]{2,1,0:T(8,128)(2,1)S(1)} all-to-all(bf16[96,24,128]{2,1,0:T(8,128)(2,1)S(1)} %get-tuple-element.26), channel_id=1, replica_groups=mesh['z'=12,'y'=8,'tp'=8] {'z','y'}, dimensions={0} | all-to-all | bytes 1179648 | tf_op jit(solution)/shard_map/all_to_all | solution.py:240
  58.4 4.9 %all-gather.5.cloned.1.call-done = f32[704,384]{1,0:T(8,128)} async-done(((f32[88,384]{1,0:T(8,128)}), f32[704,384]{1,0:T(8,128)}) %all-gather.5.cloned.1.call-update) | async-done | bytes 1081360 | tf_op jit(solution)/shard_map/all_gather | solution.py:239
  63.3 2.1 fusion
  65.4 0.0 all-gather.7.cloned.1.call-update
  65.5 0.0 copy-start.4
  65.5 0.0 copy-start.5
  65.5 6.1 %shard_map.146 = bf16[96,512]{1,0:T(8,128)(2,1)S(1)} custom-call(bf16[96,24,128]{2,1,0:T(8,128)(2,1)S(1)} %all_to_all.20.packed, bf16[512,3072]{1,0:T(8,128)(2,1)} %saved_inputs.1, bf16[512,3072]{1,0:T(8,128)(2,1)} %out_cotangent.1), custom_call_target="tpu_custom_call" | custom-call | flops 805306368 | bytes 8388608 | tf_op jit(solution)/shard_map/pallas_call | solution.py:245
  71.5 17.8 %all_gather.17.proj = bf16[768,512]{1,0:T(8,128)(2,1)S(1)} all-gather(bf16[96,512]{1,0:T(8,128)(2,1)S(1)} %shard_map.146), channel_id=1, replica_groups=mesh['z'=12,'y'=8,'tp'=8] {'tp'}, dimensions={0}, use_global_device_ids=true | all-gather | bytes 884736 | tf_op jit(solution)/shard_map/all_gather | solution.py:259
  89.4 0.0 copy-done.4
  89.4 0.0 copy-done.5
  89.4 1.4 shard_map.147
  90.8 13.3 %all-to-all-start.1 = ((bf16[96,8,384]{2,1,0:T(8,128)(2,1)}), bf16[96,8,384]{2,1,0:T(8,128)(2,1)S(1)}, u32[]{:S(2)}, u32[]{:S(2)}) async-start(bf16[96,8,384]{2,1,0:T(8,128)(2,1)} %bitcast.13), calls=%async_computation.1 | async-start | bytes 1179648 | tf_op jit(solution)/shard_map/all_to_all | solution.py:269
  104.1 4.0 %collective-permute-start = (bf16[96,24,128]{2,1,0:T(8,128)(2,1)S(1)}, bf16[96,24,128]{2,1,0:T(8,128)(2,1)S(1)}, u32[]{:S(2)}, u32[]{:S(2)}) collective-permute-start(bf16[96,24,128]{2,1,0:T(8,128)(2,1)S(1)} %all_to_all.20.packed), channel_id=1, source_target_pairs={{2,0},{3,1},{4,2},{5,3},{6,4},{7,5},{0,6},{1,7},{10,8},{11,9},{12,... | collective-permute-start | bytes 1769480 | tf_op jit(solution)/shard_map/ppermute | solution.py:273
  108.1 2.5 %collective-permute-start.1 = (bf16[96,24,128]{2,1,0:T(8,128)(2,1)S(1)}, bf16[96,24,128]{2,1,0:T(8,128)(2,1)S(1)}, u32[]{:S(2)}, u32[]{:S(2)}) collective-permute-start(bf16[96,24,128]{2,1,0:T(8,128)(2,1)S(1)} %all_to_all.20.packed), channel_id=1, source_target_pairs={{4,0},{5,1},{6,2},{7,3},{0,4},{1,5},{2,6},{3,7},{12,8},{13,9},{14,... | collective-permute-start | bytes 1769480 | tf_op jit(solution)/shard_map/ppermute | solution.py:273
  110.6 1.9 collective-permute-start.2
  112.6 8.2 %collective-permute-done = bf16[96,24,128]{2,1,0:T(8,128)(2,1)S(1)} collective-permute-done((bf16[96,24,128]{2,1,0:T(8,128)(2,1)S(1)}, bf16[96,24,128]{2,1,0:T(8,128)(2,1)S(1)}, u32[]{:S(2)}, u32[]{:S(2)}) %collective-permute-start) | collective-permute-done | bytes 589856 | tf_op jit(solution)/shard_map/ppermute | solution.py:273
  120.8 4.9 %collective-permute-done.1 = bf16[96,24,128]{2,1,0:T(8,128)(2,1)S(1)} collective-permute-done((bf16[96,24,128]{2,1,0:T(8,128)(2,1)S(1)}, bf16[96,24,128]{2,1,0:T(8,128)(2,1)S(1)}, u32[]{:S(2)}, u32[]{:S(2)}) %collective-permute-start.1) | collective-permute-done | bytes 589856 | tf_op jit(solution)/shard_map/ppermute | solution.py:273
  125.8 13.8 %collective-permute-done.2 = bf16[96,24,128]{2,1,0:T(8,128)(2,1)S(1)} collective-permute-done((bf16[96,24,128]{2,1,0:T(8,128)(2,1)S(1)}, bf16[96,24,128]{2,1,0:T(8,128)(2,1)S(1)}, u32[]{:S(2)}, u32[]{:S(2)}) %collective-permute-start.2) | collective-permute-done | bytes 589856 | tf_op jit(solution)/shard_map/ppermute | solution.py:273
  139.5 0.0 copy-start.10
  139.5 0.0 copy-start.11
  139.5 1.7 pad_maximum_fusion.held
  141.2 2.3 collective-permute-start.3
  143.5 0.0 all-to-all-done.1.pieces
  143.5 0.0 copy-done.10
  143.6 0.0 copy-done.11
  143.6 1.1 shard_map.148
  144.7 15.0 %all-to-all-start.2 = ((bf16[96,4,896]{2,1,0:T(4,128)(2,1)}), bf16[96,4,896]{2,1,0:T(4,128)(2,1)S(1)}, u32[]{:S(2)}, u32[]{:S(2)}) async-start(bf16[96,4,896]{2,1,0:T(4,128)(2,1)} %get-tuple-element.29), calls=%async_computation.2 | async-start | bytes 1376256 | tf_op jit(solution)/shard_map/all_to_all | solution.py:289
  159.8 0.1 pad_add_fusion.place
  159.8 30.2 %all-to-all-done.2.low = bf16[96,4,896]{2,1,0:T(4,128)(2,1)S(1)} async-done(((bf16[96,4,896]{2,1,0:T(4,128)(2,1)}), bf16[96,4,896]{2,1,0:T(4,128)(2,1)S(1)}, u32[]{:S(2)}, u32[]{:S(2)}) %all-to-all-start.2) | async-done | bytes 688160 | tf_op jit(solution)/shard_map/all_to_all | solution.py:289
  190.0 1.3 shard_map.149
  191.3 6.9 %all-to-all-start.3 = ((f32[8,8,128]{2,1,0:T(8,128)}), f32[8,8,128]{2,1,0:T(8,128)S(1)}, u32[]{:S(2)}, u32[]{:S(2)}) async-start(f32[8,8,128]{2,1,0:T(8,128)} %get-tuple-element.30), calls=%async_computation.3 | async-start | bytes 65536 | tf_op jit(solution)/shard_map/all_to_all | solution.py:335
  198.2 0.0 copy-start.6
  198.2 0.0 copy-start.7
  198.2 0.0 collective-permute-done.3.other
  198.2 0.0 all-gather.7.cloned.1.call-done.masters
  198.3 18.9 %shard_map.150 = (bf16[3072,384]{1,0:T(8,128)(2,1)}, bf16[384,3072]{1,0:T(8,128)(2,1)}, f32[3072,384]{1,0:T(8,128)}, f32[384,3072]{1,0:T(8,128)}, bf16[32,384]{1,0:T(8,128)(2,1)}, /*index=5*/bf16[32,384]{1,0:T(8,128)(2,1)}) custom-call(s32[2]{0:T(128)S(1)} %pad_add_fusion.place, bf16[96,64,384]{2,1,0:T(8,128)(2,1)} %all-gather.7.cloned.1.call-done.masters, ...), custom_call_target="tpu_custom_call" | custom-call | flops 1073741824 | bytes 31457280 | tf_op jit(solution)/shard_map/pallas_call | solution.py:293
  217.2 0.0 all-to-all-done.3.squares
  217.2 0.0 copy-done.6
  217.2 0.0 copy-done.7
  217.2 0.0 copy-start
  217.2 2.3 copy-done
  219.6 0.0 copy-start.1
  219.6 2.3 copy-done.1
  221.9 0.0 copy-start.2
  221.9 1.7 copy-done.2
  223.6 0.0 copy-start.3
  223.6 1.7 copy-done.3
  225.2 0.0 copy-start.8
  225.2 0.7 copy-done.8
  226.0 0.0 copy-start.9
  226.0 0.7 copy-done.9
  226.7 7.8 %shard_map.151 = (bf16[3072,384]{1,0:T(8,128)(2,1)}, bf16[384,3072]{1,0:T(8,128)(2,1)}, f32[32,384]{1,0:T(8,128)}, f32[32,384]{1,0:T(8,128)}) custom-call(f32[8,8,128]{2,1,0:T(8,128)S(1)} %all-to-all-done.3.squares, bf16[384,384]{1,0:T(8,128)(2,1)S(1)} %get-tuple-element.31.first, bf16[384,384]{1,0:T(8,128)(2,1)S(1)} %get-tuple-element.32.second, ...), custom_call_target="tpu_custom_call" | custom-call | flops 1811939328 | bytes 20971520 | tf_op jit(solution)/shard_map/pallas_call | solution.py:337
Async XLA Ops:
  7.2 56.1 %all-gather.5.cloned.1.call-start = ((), (), s32[]{:S(2)}) async-start(), calls=%async_computation.4 | async-start | bytes 1216512 | tf_op jit(solution)/shard_map/all_gather | solution.py:239
  8.8 189.5 %all-gather.7.cloned.1.call-start = ((), (), s32[]{:S(2)}) async-start(), calls=%async_computation.5 | async-start | bytes 5111808 | tf_op jit(solution)/shard_map/all_gather | solution.py:243
  65.5 23.9 %copy-start.4 = (bf16[512,384]{1,0:T(8,128)(2,1)S(1)}, bf16[512,384]{1,0:T(8,128)(2,1)}, u32[]{:S(2)}) copy-start(bf16[512,384]{1,0:T(8,128)(2,1)} %query_cotangent.1) | copy-start | bytes 1179652
  65.5 23.9 %copy-start.5 = (bf16[512,384]{1,0:T(8,128)(2,1)S(1)}, bf16[512,384]{1,0:T(8,128)(2,1)}, u32[]{:S(2)}) copy-start(bf16[512,384]{1,0:T(8,128)(2,1)} %attn_outputs.1) | copy-start | bytes 1179652
  90.8 52.8 %all-to-all-start.1 = ((bf16[96,8,384]{2,1,0:T(8,128)(2,1)}), bf16[96,8,384]{2,1,0:T(8,128)(2,1)S(1)}, u32[]{:S(2)}, u32[]{:S(2)}) async-start(bf16[96,8,384]{2,1,0:T(8,128)(2,1)} %bitcast.13), calls=%async_computation.1 | async-start | bytes 1179648 | tf_op jit(solution)/shard_map/all_to_all | solution.py:269
  104.1 16.7 %collective-permute-start = (bf16[96,24,128]{2,1,0:T(8,128)(2,1)S(1)}, bf16[96,24,128]{2,1,0:T(8,128)(2,1)S(1)}, u32[]{:S(2)}, u32[]{:S(2)}) collective-permute-start(bf16[96,24,128]{2,1,0:T(8,128)(2,1)S(1)} %all_to_all.20.packed), channel_id=1, source_target_pairs={{2,0},{3,1},{4,2},{5,3},{6,4},{7,5},{0,6},{1,7},{10,8},{11,9},{12,... | collective-permute-start | bytes 1769480 | tf_op jit(solution)/shard_map/ppermute | solution.py:273
  108.1 17.6 %collective-permute-start.1 = (bf16[96,24,128]{2,1,0:T(8,128)(2,1)S(1)}, bf16[96,24,128]{2,1,0:T(8,128)(2,1)S(1)}, u32[]{:S(2)}, u32[]{:S(2)}) collective-permute-start(bf16[96,24,128]{2,1,0:T(8,128)(2,1)S(1)} %all_to_all.20.packed), channel_id=1, source_target_pairs={{4,0},{5,1},{6,2},{7,3},{0,4},{1,5},{2,6},{3,7},{12,8},{13,9},{14,... | collective-permute-start | bytes 1769480 | tf_op jit(solution)/shard_map/ppermute | solution.py:273
  110.6 28.9 %collective-permute-start.2 = (bf16[96,24,128]{2,1,0:T(8,128)(2,1)S(1)}, bf16[96,24,128]{2,1,0:T(8,128)(2,1)S(1)}, u32[]{:S(2)}, u32[]{:S(2)}) collective-permute-start(bf16[96,24,128]{2,1,0:T(8,128)(2,1)S(1)} %all_to_all.20.packed), channel_id=1, source_target_pairs={{6,0},{7,1},{0,2},{1,3},{2,4},{3,5},{4,6},{5,7},{14,8},{15,9},{8,1... | collective-permute-start | bytes 1769480 | tf_op jit(solution)/shard_map/ppermute | solution.py:273
  139.5 4.0 %copy-start.10 = (f32[2,4,384]{2,1,0:T(4,128)S(1)}, f32[2,4,384]{2,1,0:T(4,128)}, u32[]{:S(2)}) copy-start(f32[2,4,384]{2,1,0:T(4,128)} %first.1) | copy-start | bytes 36868
  139.5 4.0 %copy-start.11 = (f32[2,4,384]{2,1,0:T(4,128)S(1)}, f32[2,4,384]{2,1,0:T(4,128)}, u32[]{:S(2)}) copy-start(f32[2,4,384]{2,1,0:T(4,128)} %second.1) | copy-start | bytes 36868
  141.2 57.0 %collective-permute-start.3 = (bf16[4,96,24,128]{3,2,1,0:T(8,128)(2,1)}, bf16[4,96,24,128]{3,2,1,0:T(8,128)(2,1)}, u32[]{:S(2)}, u32[]{:S(2)}) collective-permute-start(bf16[4,96,24,128]{3,2,1,0:T(8,128)(2,1)} %pad_maximum_fusion.held), channel_id=1, source_target_pairs={{1,0},{0,1},{3,2},{2,3},{5,4},{4,5},{7,6},{6,7},{9,8},{8,9},{11,10... | collective-permute-start | bytes 7077896 | tf_op jit(solution)/shard_map/ppermute | solution.py:275
  144.7 45.3 %all-to-all-start.2 = ((bf16[96,4,896]{2,1,0:T(4,128)(2,1)}), bf16[96,4,896]{2,1,0:T(4,128)(2,1)S(1)}, u32[]{:S(2)}, u32[]{:S(2)}) async-start(bf16[96,4,896]{2,1,0:T(4,128)(2,1)} %get-tuple-element.29), calls=%async_computation.2 | async-start | bytes 1376256 | tf_op jit(solution)/shard_map/all_to_all | solution.py:289
  191.3 25.9 %all-to-all-start.3 = ((f32[8,8,128]{2,1,0:T(8,128)}), f32[8,8,128]{2,1,0:T(8,128)S(1)}, u32[]{:S(2)}, u32[]{:S(2)}) async-start(f32[8,8,128]{2,1,0:T(8,128)} %get-tuple-element.30), calls=%async_computation.3 | async-start | bytes 65536 | tf_op jit(solution)/shard_map/all_to_all | solution.py:335
  198.2 19.0 %copy-start.6 = (f32[32,384]{1,0:T(8,128)S(1)}, f32[32,384]{1,0:T(8,128)}, u32[]{:S(2)}) copy-start(f32[32,384]{1,0:T(8,128)} %query_master.3) | copy-start | bytes 147460
  198.2 19.0 %copy-start.7 = (f32[384,32]{0,1:T(8,128)S(1)}, f32[384,32]{0,1:T(8,128)}, u32[]{:S(2)}) copy-start(f32[384,32]{0,1:T(8,128)} %param.17) | copy-start | bytes 147460
  217.2 2.3 copy-start
  219.6 2.3 copy-start.1
  221.9 1.7 copy-start.2
  223.6 1.7 copy-start.3
  225.2 0.7 copy-start.8
  226.0 0.7 copy-start.9
Sparse Core Ops, SparseCore 0:
  10.9 52.3 all-gather.4
  65.7 88.8 all-gather.6

commit v3 on v2

--- a/solution.py
+++ b/solution.py
@@ -22,11 +22,32 @@
     return pl.CostEstimate(flops=flops, bytes_accessed=nbytes, transcendentals=0)
 
 
+def coded(value):
+    size = jnp.abs(value) * REACH
+    size = size * size
+    size = size * size
+    size = size * size
+    return jnp.where(value < 0.0, -size, size).astype(bf16)
+
+
+def decoded(code):
+    size = jnp.abs(code)
+    fourth = lax.rsqrt(lax.rsqrt(size))
+    eighth = fourth * lax.rsqrt(lax.rsqrt(lax.rsqrt(size))) * (1.0 / REACH)
+    return jnp.where(code == 0.0, 0.0, jnp.where(code < 0.0, -eighth, eighth))
+
+
+def turned(value):
+    n = value.shape[1]
+    row = lax.broadcasted_iota(jnp.int32, (n, n), 0)
+    eye = (row == lax.broadcasted_iota(jnp.int32, (n, n), 1)).astype(f32).astype(bf16)
+    return lax.dot_general(eye, value, (((1,), (1,)), ((), ())), preferred_element_type=f32)
+
+
 def send_kernel(left, right, query_master, out_master, out, masters):
     own = query_master.shape[0]
-    masters[:own] = query_master[...]
-    masters[own : 2 * own] = out_master[...]
-    masters[2 * own :] = jnp.zeros((masters.shape[0] - 2 * own, masters.shape[1]), f32)
+    masters[:own] = coded(query_master[...])
+    masters[own:] = coded(out_master[...])
     both = jnp.concatenate([left[...].astype(f32), right[...].astype(f32)], axis=1)
     used = both.shape[1]
     free = 128 - used
@@ -102,45 +123,31 @@
     low[...] = jnp.broadcast_to(sent[None], low.shape)
 
 
-def coded(value):
-    size = jnp.abs(value) * REACH
-    size = size * size
-    size = size * size
-    size = size * size
-    return jnp.where(value < 0.0, -size, size).astype(bf16)
-
-
-def decoded(code):
-    wide = code.astype(f32)
-    size = jnp.sqrt(jnp.sqrt(jnp.sqrt(jnp.abs(wide)))) * (1.0 / REACH)
-    return jnp.where(wide < 0.0, -size, size)
-
-
 def prep_kernel(rank_cols, place, masters, held, other, left, right, query_master, out_master, own_left, own_right, tile):
     own = masters.shape[1] // 2
     span = left.shape[0]
     cols = masters.shape[2]
-    query_master[...] = decoded(masters[:, :own].reshape(span, cols))
-    out_master[...] = decoded(masters[:, own:].reshape(span, cols)).T
+    query_master[...] = decoded(masters[:, :own].reshape(span, cols).astype(f32))
+    out_master[...] = decoded(turned(masters[:, own:].reshape(span, cols)))
     sides = [[], []]
     for half in (held, other):
         for s in range(half.shape[0]):
             block = unpacked(half[s], 2 * rank_cols).reshape(span, 128)
             for k in range(2):
                 sides[k].append(block[:, k * rank_cols : (k + 1) * rank_cols])
-    both = [jnp.concatenate(side, axis=1) for side in sides]
-    left[...] = both[0].astype(bf16)
-    right[...] = both[1].T.astype(bf16)
+    both = [jnp.concatenate(side, axis=1).astype(bf16) for side in sides]
+    left[...] = both[0]
+    right[...] = turned(both[1]).astype(bf16)
 
     @pl.when(pl.program_id(0) == place[0] // (span // own))
     def _():
         rows = pl.ds(pl.multiple_of(place[0] % (span // own) * own, own), own)
         for side, out in zip(both, (own_left, own_right)):
             tile[...] = side
-            out[...] = tile[rows].astype(bf16)
-
-
-def sums_kernel(rank_cols, place, low, squares, first, second):
+            out[...] = tile[rows]
+
+
+def sums_kernel(rank_cols, place, low, squares, first, second, second_turned):
     tp = squares.shape[0]
     cols = first.shape[1]
     per_block = rank_cols // low.shape[1]
@@ -155,6 +162,7 @@
             part = block[:, :, k * cols : (k + 1) * cols]
             part = jnp.concatenate([part[j] for j in range(per_block)], axis=0)
             out[b * rank_cols : (b + 1) * rank_cols] = part.astype(bf16)
+    second_turned[...] = turned(second[...]).astype(bf16)
 
 
 def final_kernel(
@@ -162,6 +170,7 @@
     squares,
     first,
     second,
+    second_turned,
     left,
     right,
     query_all,
@@ -184,8 +193,7 @@
         scales.append(0.01 * lax.rsqrt(total / entries + 1e-06))
     moved = jnp.dot(left[...], first[...], preferred_element_type=f32)
     query_copy[...] = (query_all[...] - scales[0] * moved).astype(bf16)
-    across = (((0,), (0,)), ((), ()))
-    moved = lax.dot_general(second[...], right[...], across, preferred_element_type=f32)
+    moved = jnp.dot(second_turned[...], right[...], preferred_element_type=f32)
     out_copy[...] = (out_all[...] - scales[1] * moved).astype(bf16)
 
     @pl.when(step == 0)
@@ -227,20 +235,14 @@
     place = jnp.stack([lax.axis_index(FS), lax.axis_index("tp")]).astype(jnp.int32)
     packed, masters = pl.pallas_call(
         send_kernel,
-        out_shape=(
-            jax.ShapeDtypeStruct((fs, kept, 128), bf16),
-            pltpu.HBM((88, cols), f32),
-        ),
+        out_shape=(jax.ShapeDtypeStruct((fs, kept, 128), bf16), pltpu.HBM((2 * own, cols), bf16)),
         in_specs=[pl.BlockSpec()] * 4,
         out_specs=(VMEM, VMEM),
         compiler_params=SMALL,
         cost_estimate=cost(1 << 16, 1 << 20),
     )(far(left_factor), far(right_factor), far(query_master), far(out_master.T))
-    masters = lax.all_gather(masters, "y")
+    masters = lax.all_gather(masters, FS)
     packed = lax.all_to_all(packed, FS, 0, 0)
-    packed, masters = lax.optimization_barrier((packed, masters))
-    masters = masters[:, : 2 * own]
-    masters = lax.all_gather(coded(masters), "z").reshape(fs, 2 * own, cols)
     parts = 6
     proj = pl.pallas_call(
         functools.partial(proj_kernel, used),
@@ -315,20 +317,21 @@
             pl.BlockSpec((own, ranks), lambda i: (0, 0)),
             pl.BlockSpec((own, ranks), lambda i: (0, 0)),
         ),
-        scratch_shapes=[pltpu.VMEM((span, ranks), f32)],
+        scratch_shapes=[pltpu.VMEM((span, ranks), bf16)],
         compiler_params=SMALL,
         cost_estimate=cost(1 << 30, 30 << 20),
     )(place, far(masters), far(held), far(other))
 
-    squares, first, second = pl.pallas_call(
+    squares, first, second, second_turned = pl.pallas_call(
         functools.partial(sums_kernel, rank_cols),
         out_shape=(
             jax.ShapeDtypeStruct((tp, 8, 128), f32),
             jax.ShapeDtypeStruct((ranks, cols), bf16),
             jax.ShapeDtypeStruct((ranks, cols), bf16),
+            jax.ShapeDtypeStruct((cols, ranks), bf16),
         ),
         in_specs=[SMEM, VMEM],
-        out_specs=(VMEM, VMEM, VMEM),
+        out_specs=(VMEM, VMEM, VMEM, VMEM),
         compiler_params=SMALL,
         cost_estimate=cost(1 << 16, 1 << 16),
     )(place, low)
@@ -347,14 +350,15 @@
             VMEM,
             VMEM,
             VMEM,
+            VMEM,
             pl.BlockSpec((span, ranks), lambda i: (i, 0)),
             pl.BlockSpec((ranks, span), lambda i: (0, i)),
             pl.BlockSpec((span, cols), lambda i: (i, 0)),
             pl.BlockSpec((cols, span), lambda i: (0, i)),
-            VMEM,
-            VMEM,
-            VMEM,
-            VMEM,
+            pl.BlockSpec((own, ranks), lambda i: (0, 0)),
+            pl.BlockSpec((own, ranks), lambda i: (0, 0)),
+            pl.BlockSpec((own, cols), lambda i: (0, 0)),
+            pl.BlockSpec((own, cols), lambda i: (0, 0)),
         ],
         out_specs=(
             pl.BlockSpec((span, cols), lambda i: (i, 0)),
@@ -368,14 +372,15 @@
         squares,
         first,
         second,
-        left,
-        right,
-        query_all,
-        out_all,
-        own_left,
-        own_right,
-        query_master,
-        out_master.T,
+        second_turned,
+        far(left),
+        far(right),
+        far(query_all),
+        far(out_all),
+        far(own_left),
+        far(own_right),
+        far(query_master),
+        far(out_master.T),
     )
     return (query_new, out_new.T, query_copy, out_copy, first_new, second_new)
 

time: 243 us -> 223 us (0.918)
  local copies, waits for them, and re-layouts: 9.5 us -> 0.01 us
  starting transfers between devices: 46.1 us -> 39.5 us
  waiting for transfers between devices: 62.1 us -> 57 us
  Pallas kernels: 38.1 us -> 41.2 us
    unnamed x24 -> x8, local copies, waits for them, and re-layouts: 9.5 us -> 0.01 us
    all_to_all x1, starting transfers between devices: 13.3 us -> 5.95 us  [body(): pieces = lax.all_to_all(partial.reshape(fs, 2 * rows, cols), FS, 0, 0)]
    pallas_call x1, Pallas kernels: 7.78 us -> 13 us  [body(): pl.pallas_call(functools.partial(final_kernel, float(rows * fs * cols * t...]
    all_gather x2 -> x1, waiting for transfers between devices: 4.92 us -> 0.01 us  [body(): masters = lax.all_gather(masters, FS)]
    pallas_call x1, Pallas kernels: 18.9 us -> 16.4 us  [body(): pl.pallas_call(functools.partial(prep_kernel, rank_cols), grid=(depth,),...]
  transfers between devices with their start and end apart: 9 -> 8, of which waited for: 5 -> 4; matrix products, arithmetic and copies ran while one was open for 1% -> 1% of each run, Pallas kernels for 12% -> 12%
where the time goes in v3:
time: 223 us; the launch traced here: 221 us
  blocking collectives  67.9 us (30%)
  waiting for transfers between devices  57 us (26%)
  Pallas kernels  41.2 us (18%)
  starting transfers between devices  39.5 us (18%)
  between operations  14.2 us (6%)
    all_to_all x1, blocking collectives, body(): packed = lax.all_to_all(packed, FS, 0, 0)  49.9 us
    all_to_all x1, waiting for transfers between devices, body(): low = lax.all_to_all(low, FS, 0, 0)  30.1 us
    ppermute x3, waiting for transfers between devices, body(): lax.ppermute(packed, 'tp', [((t + 2 * step) % tp, t) for t in range(tp)])  26.9 us
    all_gather x1, blocking collectives, body(): proj = lax.all_gather(proj, 'tp', axis=0, tiled=True)  18 us
    pallas_call x1, Pallas kernels, body(): pl.pallas_call(functools.partial(prep_kernel, rank_cols), grid=(depth,),...  16.4 us
    all_to_all x1, starting transfers between devices, body(): low = lax.all_to_all(low, FS, 0, 0)  15 us
    pallas_call x1, Pallas kernels, body(): pl.pallas_call(functools.partial(final_kernel, float(rows * fs * cols * t...  13 us
    ppermute x3, starting transfers between devices, body(): lax.ppermute(packed, 'tp', [((t + 2 * step) % tp, t) for t in range(tp)])  8.53 us
  transfers between devices with their start and end apart: 8, of which 4 were waited for; matrix products, arithmetic and copies ran while one was open for 1% of the time, Pallas kernels for 12%

profile of v3, /device:TPU:1, one launch (start us, length us, event | category | flops | bytes accessed | tf_op | source)
XLA Modules:
  0.0 221.5 jit_solution(4063714749453516663)
XLA Ops:
  7.2 0.0 all-gather.3.cloned.1.call-start
  7.2 1.6 shard_map.145
  8.8 0.0 all-gather.3.cloned.1.call-update
  8.9 49.9 %all_to_all.20.packed = bf16[96,24,128]{2,1,0:T(8,128)(2,1)S(1)} all-to-all(bf16[96,24,128]{2,1,0:T(8,128)(2,1)S(1)} %get-tuple-element.25), channel_id=1, replica_groups=mesh['z'=12,'y'=8,'tp'=8] {'z','y'}, dimensions={0} | all-to-all | bytes 1179648 | tf_op jit(solution)/shard_map/all_to_all | solution.py:245
  58.8 0.0 copy-start
  58.8 0.0 copy-start.1
  58.8 6.1 %shard_map.146 = bf16[96,512]{1,0:T(8,128)(2,1)S(1)} custom-call(bf16[96,24,128]{2,1,0:T(8,128)(2,1)S(1)} %all_to_all.20.packed, bf16[512,3072]{1,0:T(8,128)(2,1)} %saved_inputs.1, bf16[512,3072]{1,0:T(8,128)(2,1)} %out_cotangent.1), custom_call_target="tpu_custom_call" | custom-call | flops 805306368 | bytes 8388608 | tf_op jit(solution)/shard_map/pallas_call | solution.py:247
  64.9 18.0 %all_gather.9.proj = bf16[768,512]{1,0:T(8,128)(2,1)S(1)} all-gather(bf16[96,512]{1,0:T(8,128)(2,1)S(1)} %shard_map.146), channel_id=1, replica_groups=mesh['z'=12,'y'=8,'tp'=8] {'tp'}, dimensions={0}, use_global_device_ids=true | all-gather | bytes 884736 | tf_op jit(solution)/shard_map/all_gather | solution.py:261
  82.8 0.0 copy-done
  82.8 0.0 copy-done.1
  82.8 1.4 shard_map.147
  84.2 6.0 %all-to-all-start.1 = ((bf16[96,8,384]{2,1,0:T(8,128)(2,1)}), bf16[96,8,384]{2,1,0:T(8,128)(2,1)S(1)}, u32[]{:S(2)}, u32[]{:S(2)}) async-start(bf16[96,8,384]{2,1,0:T(8,128)(2,1)} %bitcast.12), calls=%async_computation.1 | async-start | bytes 1179648 | tf_op jit(solution)/shard_map/all_to_all | solution.py:271
  90.2 4.1 %collective-permute-start = (bf16[96,24,128]{2,1,0:T(8,128)(2,1)S(1)}, bf16[96,24,128]{2,1,0:T(8,128)(2,1)S(1)}, u32[]{:S(2)}, u32[]{:S(2)}) collective-permute-start(bf16[96,24,128]{2,1,0:T(8,128)(2,1)S(1)} %all_to_all.20.packed), channel_id=1, source_target_pairs={{2,0},{3,1},{4,2},{5,3},{6,4},{7,5},{0,6},{1,7},{10,8},{11,9},{12,... | collective-permute-start | bytes 1769480 | tf_op jit(solution)/shard_map/ppermute | solution.py:275
  94.3 2.5 %collective-permute-start.1 = (bf16[96,24,128]{2,1,0:T(8,128)(2,1)S(1)}, bf16[96,24,128]{2,1,0:T(8,128)(2,1)S(1)}, u32[]{:S(2)}, u32[]{:S(2)}) collective-permute-start(bf16[96,24,128]{2,1,0:T(8,128)(2,1)S(1)} %all_to_all.20.packed), channel_id=1, source_target_pairs={{4,0},{5,1},{6,2},{7,3},{0,4},{1,5},{2,6},{3,7},{12,8},{13,9},{14,... | collective-permute-start | bytes 1769480 | tf_op jit(solution)/shard_map/ppermute | solution.py:275
  96.8 1.9 collective-permute-start.2
  98.7 8.6 %collective-permute-done = bf16[96,24,128]{2,1,0:T(8,128)(2,1)S(1)} collective-permute-done((bf16[96,24,128]{2,1,0:T(8,128)(2,1)S(1)}, bf16[96,24,128]{2,1,0:T(8,128)(2,1)S(1)}, u32[]{:S(2)}, u32[]{:S(2)}) %collective-permute-start) | collective-permute-done | bytes 589856 | tf_op jit(solution)/shard_map/ppermute | solution.py:275
  107.3 4.9 %collective-permute-done.1 = bf16[96,24,128]{2,1,0:T(8,128)(2,1)S(1)} collective-permute-done((bf16[96,24,128]{2,1,0:T(8,128)(2,1)S(1)}, bf16[96,24,128]{2,1,0:T(8,128)(2,1)S(1)}, u32[]{:S(2)}, u32[]{:S(2)}) %collective-permute-start.1) | collective-permute-done | bytes 589856 | tf_op jit(solution)/shard_map/ppermute | solution.py:275
  112.2 13.4 %collective-permute-done.2 = bf16[96,24,128]{2,1,0:T(8,128)(2,1)S(1)} collective-permute-done((bf16[96,24,128]{2,1,0:T(8,128)(2,1)S(1)}, bf16[96,24,128]{2,1,0:T(8,128)(2,1)S(1)}, u32[]{:S(2)}, u32[]{:S(2)}) %collective-permute-start.2) | collective-permute-done | bytes 589856 | tf_op jit(solution)/shard_map/ppermute | solution.py:275
  125.6 0.0 copy-start.2
  125.6 0.0 copy-start.3
  125.6 1.7 pad_maximum_fusion.held
  127.3 2.4 %collective-permute-start.3 = (bf16[4,96,24,128]{3,2,1,0:T(8,128)(2,1)}, bf16[4,96,24,128]{3,2,1,0:T(8,128)(2,1)}, u32[]{:S(2)}, u32[]{:S(2)}) collective-permute-start(bf16[4,96,24,128]{3,2,1,0:T(8,128)(2,1)} %pad_maximum_fusion.held), channel_id=1, source_target_pairs={{1,0},{0,1},{3,2},{2,3},{5,4},{4,5},{7,6},{6,7},{9,8},{8,9},{11,10... | collective-permute-start | bytes 7077896 | tf_op jit(solution)/shard_map/ppermute | solution.py:277
  129.7 0.0 all-to-all-done.1.pieces
  129.7 0.0 copy-done.2
  129.7 0.0 copy-done.3
  129.7 1.1 shard_map.148
  130.9 15.0 %all-to-all-start.2 = ((bf16[96,4,896]{2,1,0:T(4,128)(2,1)}), bf16[96,4,896]{2,1,0:T(4,128)(2,1)S(1)}, u32[]{:S(2)}, u32[]{:S(2)}) async-start(bf16[96,4,896]{2,1,0:T(4,128)(2,1)} %get-tuple-element.26), calls=%async_computation.2 | async-start | bytes 1376256 | tf_op jit(solution)/shard_map/all_to_all | solution.py:291
  145.9 0.1 pad_add_fusion.place
  146.0 30.1 %all-to-all-done.2.low = bf16[96,4,896]{2,1,0:T(4,128)(2,1)S(1)} async-done(((bf16[96,4,896]{2,1,0:T(4,128)(2,1)}), bf16[96,4,896]{2,1,0:T(4,128)(2,1)S(1)}, u32[]{:S(2)}, u32[]{:S(2)}) %all-to-all-start.2) | async-done | bytes 688160 | tf_op jit(solution)/shard_map/all_to_all | solution.py:291
  176.1 1.6 shard_map.149
  177.7 7.5 %all-to-all-start.3 = ((f32[8,8,128]{2,1,0:T(8,128)}), f32[8,8,128]{2,1,0:T(8,128)S(1)}, u32[]{:S(2)}, u32[]{:S(2)}) async-start(f32[8,8,128]{2,1,0:T(8,128)} %get-tuple-element.27), calls=%async_computation.3 | async-start | bytes 65536 | tf_op jit(solution)/shard_map/all_to_all | solution.py:338
  185.2 0.0 collective-permute-done.3.other
  185.2 0.0 all-gather.3.cloned.1.call-done
  185.2 16.4 %shard_map.150 = (bf16[3072,384]{1,0:T(8,128)(2,1)}, bf16[384,3072]{1,0:T(8,128)(2,1)}, f32[3072,384]{1,0:T(8,128)}, f32[384,3072]{1,0:T(8,128)}, bf16[32,384]{1,0:T(8,128)(2,1)}, /*index=5*/bf16[32,384]{1,0:T(8,128)(2,1)}) custom-call(s32[2]{0:T(128)S(1)} %pad_add_fusion.place, bf16[96,64,384]{2,1,0:T(8,128)(2,1)} %bitcast.11, ...), custom_call_target="tpu_custom_call" | custom-call | flops 1073741824 | bytes 31457280 | tf_op jit(solution)/shard_map/pallas_call | solution.py:295
  201.6 0.0 all-to-all-done.3.squares
  201.6 13.0 %shard_map.151 = (bf16[3072,384]{1,0:T(8,128)(2,1)}, bf16[384,3072]{1,0:T(8,128)(2,1)}, f32[32,384]{1,0:T(8,128)}, f32[32,384]{1,0:T(8,128)}) custom-call(f32[8,8,128]{2,1,0:T(8,128)S(1)} %all-to-all-done.3.squares, bf16[384,384]{1,0:T(8,128)(2,1)S(1)} %get-tuple-element.28.first, bf16[384,384]{1,0:T(8,128)(2,1)S(1)} %get-tuple-element.29.second, ...), custom_call_target="tpu_custom_call" | custom-call | flops 1811939328 | bytes 20971520 | tf_op jit(solution)/shard_map/pallas_call | solution.py:340
Async XLA Ops:
  7.2 178.0 %all-gather.3.cloned.1.call-start = ((), (), s32[]{:S(2)}) async-start(), calls=%async_computation.4 | async-start | bytes 4767744 | tf_op jit(solution)/shard_map/all_gather | solution.py:244
  58.8 24.0 %copy-start = (bf16[512,384]{1,0:T(8,128)(2,1)S(1)}, bf16[512,384]{1,0:T(8,128)(2,1)}, u32[]{:S(2)}) copy-start(bf16[512,384]{1,0:T(8,128)(2,1)} %query_cotangent.1) | copy-start | bytes 1179652
  58.8 24.0 %copy-start.1 = (bf16[512,384]{1,0:T(8,128)(2,1)S(1)}, bf16[512,384]{1,0:T(8,128)(2,1)}, u32[]{:S(2)}) copy-start(bf16[512,384]{1,0:T(8,128)(2,1)} %attn_outputs.1) | copy-start | bytes 1179652
  84.2 45.5 %all-to-all-start.1 = ((bf16[96,8,384]{2,1,0:T(8,128)(2,1)}), bf16[96,8,384]{2,1,0:T(8,128)(2,1)S(1)}, u32[]{:S(2)}, u32[]{:S(2)}) async-start(bf16[96,8,384]{2,1,0:T(8,128)(2,1)} %bitcast.12), calls=%async_computation.1 | async-start | bytes 1179648 | tf_op jit(solution)/shard_map/all_to_all | solution.py:271
  90.2 17.1 %collective-permute-start = (bf16[96,24,128]{2,1,0:T(8,128)(2,1)S(1)}, bf16[96,24,128]{2,1,0:T(8,128)(2,1)S(1)}, u32[]{:S(2)}, u32[]{:S(2)}) collective-permute-start(bf16[96,24,128]{2,1,0:T(8,128)(2,1)S(1)} %all_to_all.20.packed), channel_id=1, source_target_pairs={{2,0},{3,1},{4,2},{5,3},{6,4},{7,5},{0,6},{1,7},{10,8},{11,9},{12,... | collective-permute-start | bytes 1769480 | tf_op jit(solution)/shard_map/ppermute | solution.py:275
  94.3 17.9 %collective-permute-start.1 = (bf16[96,24,128]{2,1,0:T(8,128)(2,1)S(1)}, bf16[96,24,128]{2,1,0:T(8,128)(2,1)S(1)}, u32[]{:S(2)}, u32[]{:S(2)}) collective-permute-start(bf16[96,24,128]{2,1,0:T(8,128)(2,1)S(1)} %all_to_all.20.packed), channel_id=1, source_target_pairs={{4,0},{5,1},{6,2},{7,3},{0,4},{1,5},{2,6},{3,7},{12,8},{13,9},{14,... | collective-permute-start | bytes 1769480 | tf_op jit(solution)/shard_map/ppermute | solution.py:275
  96.8 28.8 %collective-permute-start.2 = (bf16[96,24,128]{2,1,0:T(8,128)(2,1)S(1)}, bf16[96,24,128]{2,1,0:T(8,128)(2,1)S(1)}, u32[]{:S(2)}, u32[]{:S(2)}) collective-permute-start(bf16[96,24,128]{2,1,0:T(8,128)(2,1)S(1)} %all_to_all.20.packed), channel_id=1, source_target_pairs={{6,0},{7,1},{0,2},{1,3},{2,4},{3,5},{4,6},{5,7},{14,8},{15,9},{8,1... | collective-permute-start | bytes 1769480 | tf_op jit(solution)/shard_map/ppermute | solution.py:275
  125.6 4.1 %copy-start.2 = (f32[2,4,384]{2,1,0:T(4,128)S(1)}, f32[2,4,384]{2,1,0:T(4,128)}, u32[]{:S(2)}) copy-start(f32[2,4,384]{2,1,0:T(4,128)} %first.1) | copy-start | bytes 36868
  125.6 4.1 %copy-start.3 = (f32[2,4,384]{2,1,0:T(4,128)S(1)}, f32[2,4,384]{2,1,0:T(4,128)}, u32[]{:S(2)}) copy-start(f32[2,4,384]{2,1,0:T(4,128)} %second.1) | copy-start | bytes 36868
  127.3 57.9 %collective-permute-start.3 = (bf16[4,96,24,128]{3,2,1,0:T(8,128)(2,1)}, bf16[4,96,24,128]{3,2,1,0:T(8,128)(2,1)}, u32[]{:S(2)}, u32[]{:S(2)}) collective-permute-start(bf16[4,96,24,128]{3,2,1,0:T(8,128)(2,1)} %pad_maximum_fusion.held), channel_id=1, source_target_pairs={{1,0},{0,1},{3,2},{2,3},{5,4},{4,5},{7,6},{6,7},{9,8},{8,9},{11,10... | collective-permute-start | bytes 7077896 | tf_op jit(solution)/shard_map/ppermute | solution.py:277
  130.9 45.2 %all-to-all-start.2 = ((bf16[96,4,896]{2,1,0:T(4,128)(2,1)}), bf16[96,4,896]{2,1,0:T(4,128)(2,1)S(1)}, u32[]{:S(2)}, u32[]{:S(2)}) async-start(bf16[96,4,896]{2,1,0:T(4,128)(2,1)} %get-tuple-element.26), calls=%async_computation.2 | async-start | bytes 1376256 | tf_op jit(solution)/shard_map/all_to_all | solution.py:291
  177.7 23.9 %all-to-all-start.3 = ((f32[8,8,128]{2,1,0:T(8,128)}), f32[8,8,128]{2,1,0:T(8,128)S(1)}, u32[]{:S(2)}, u32[]{:S(2)}) async-start(f32[8,8,128]{2,1,0:T(8,128)} %get-tuple-element.27), calls=%async_computation.3 | async-start | bytes 65536 | tf_op jit(solution)/shard_map/all_to_all | solution.py:338
Sparse Core Ops, SparseCore 0:
  12.3 136.2 all-gather.2

commit v4 on v3

--- a/solution.py
+++ b/solution.py
@@ -13,6 +13,7 @@
 f32 = jnp.float32
 FS = ("z", "y")
 VMEM = pl.BlockSpec(memory_space=pltpu.VMEM)
+ANY = pl.BlockSpec(memory_space=pl.ANY)
 SMEM = pl.BlockSpec(memory_space=pltpu.SMEM)
 REACH = 2.0**19
 SMALL = pltpu.CompilerParams(vmem_limit_bytes=16 << 20)
@@ -68,24 +69,26 @@
     return jnp.concatenate([wide, tail], axis=1)
 
 
-def proj_kernel(used, packed, saved_inputs, out_cotangent, out, left, right):
-    step = pl.program_id(0)
-    rows = saved_inputs.shape[1]
-
-    @pl.when(step == 0)
-    def _():
-        left[...] = jnp.zeros_like(left)
-        right[...] = jnp.zeros_like(right)
-
-    factors = unpacked(packed[...], used).reshape(rows, 128).astype(bf16)
-    left[...] += jnp.dot(saved_inputs[...], factors, preferred_element_type=f32)
-    right[...] += jnp.dot(out_cotangent[...], factors, preferred_element_type=f32)
-
-    @pl.when(step == pl.num_programs(0) - 1)
-    def _():
-        lane = lax.broadcasted_iota(jnp.int32, left.shape, 1)
-        both = jnp.where(lane < used // 2, left[...], right[...])
-        out[...] = both.T[:used].astype(bf16)
+def proj_kernel(used, parts, packed, saved_inputs, out_cotangent, out, near_inputs, near_cotangent, arrived):
+    width = saved_inputs.shape[1] // parts
+    count = packed.shape[0] // parts
+    pairs = ((saved_inputs, near_inputs), (out_cotangent, near_cotangent))
+    spans = [pl.ds(i * width, width) for i in range(parts)]
+    copies = [
+        [pltpu.make_async_copy(x.at[:, at], y.at[:, at], arrived.at[i, k]) for k, (x, y) in enumerate(pairs)]
+        for i, at in enumerate(spans)
+    ]
+    for pair in copies:
+        for copy in pair:
+            copy.start()
+    sums = [0.0, 0.0]
+    for i, at in enumerate(spans):
+        factors = unpacked(packed[i * count : (i + 1) * count], used).reshape(width, 128).astype(bf16)
+        for k, (_, near) in enumerate(pairs):
+            copies[i][k].wait()
+            sums[k] = sums[k] + jnp.dot(near[:, at], factors, preferred_element_type=f32)
+    lane = lax.broadcasted_iota(jnp.int32, sums[0].shape, 1)
+    out[...] = jnp.where(lane < used // 2, sums[0], sums[1]).T[:used].astype(bf16)
 
 
 def grad_kernel(rank_cols, proj, query_cotangent, attn_outputs, out):
@@ -123,12 +126,9 @@
     low[...] = jnp.broadcast_to(sent[None], low.shape)
 
 
-def prep_kernel(rank_cols, place, masters, held, other, left, right, query_master, out_master, own_left, own_right, tile):
-    own = masters.shape[1] // 2
+def prep_kernel(rank_cols, place, held, other, left, right, own_left, own_right, tile):
+    own = own_left.shape[0]
     span = left.shape[0]
-    cols = masters.shape[2]
-    query_master[...] = decoded(masters[:, :own].reshape(span, cols).astype(f32))
-    out_master[...] = decoded(turned(masters[:, own:].reshape(span, cols)))
     sides = [[], []]
     for half in (held, other):
         for s in range(half.shape[0]):
@@ -167,14 +167,14 @@
 
 def final_kernel(
     entries,
+    span,
     squares,
     first,
     second,
     second_turned,
     left,
     right,
-    query_all,
-    out_all,
+    masters,
     own_left,
     own_right,
     query_master,
@@ -183,25 +183,75 @@
     out_copy,
     query_new,
     out_new,
+    near_left,
+    near_right,
+    near_masters,
+    near_query,
+    near_out,
+    near_own,
+    near_master,
+    near_new,
+    arrived,
+    own_arrived,
+    left_for,
+    own_left_for,
 ):
-    step = pl.program_id(0)
+    width = left.shape[0]
+    cols = first.shape[1]
+    own = query_master.shape[0]
+    per = span // own
+    parts = width // span
+    spans = [pl.ds(i * span, span) for i in range(parts)]
+    copies = []
+    for i, at in enumerate(spans):
+        held = pl.ds(i * per, per)
+        ways = (
+            (left.at[at], near_left.at[at]),
+            (masters.at[held], near_masters.at[held]),
+            (right.at[:, at], near_right.at[:, at]),
+        )
+        copies.append([pltpu.make_async_copy(x, y, arrived.at[i, k]) for k, (x, y) in enumerate(ways)])
+    ways = (
+        (own_left, near_own.at[0]),
+        (own_right, near_own.at[1]),
+        (query_master, near_master.at[0]),
+        (out_master, near_master.at[1]),
+    )
+    own_copies = [pltpu.make_async_copy(x, y, own_arrived.at[k]) for k, (x, y) in enumerate(ways)]
+    for copy in [c for part in copies for c in part] + own_copies:
+        copy.start()
+
     sums = jnp.sum(squares[...], axis=0)[:1]
     lane = lax.broadcasted_iota(jnp.int32, sums.shape, 1)
     scales = []
     for k in range(2):
         total = jnp.sum(jnp.where(lane // 3 == k, sums, 0.0), axis=1, keepdims=True)
         scales.append(0.01 * lax.rsqrt(total / entries + 1e-06))
-    moved = jnp.dot(left[...], first[...], preferred_element_type=f32)
-    query_copy[...] = (query_all[...] - scales[0] * moved).astype(bf16)
-    moved = jnp.dot(second_turned[...], right[...], preferred_element_type=f32)
-    out_copy[...] = (out_all[...] - scales[1] * moved).astype(bf16)
-
-    @pl.when(step == 0)
-    def _():
-        moved = jnp.dot(own_left[...], first[...], preferred_element_type=f32)
-        query_new[...] = query_master[...] - scales[0] * moved
-        moved = jnp.dot(own_right[...], second[...], preferred_element_type=f32)
-        out_new[...] = out_master[...] - scales[1] * moved
+
+    sent = []
+    for i, at in enumerate(spans):
+        for copy in copies[i]:
+            copy.wait()
+        codes = near_masters[i * per : (i + 1) * per]
+        moved = jnp.dot(near_left[at], first[...], preferred_element_type=f32)
+        kept = decoded(codes[:, :own].reshape(span, cols).astype(f32))
+        near_query[at] = (kept - scales[0] * moved).astype(bf16)
+        sent.append(pltpu.make_async_copy(near_query.at[at], query_copy.at[at], left_for.at[i, 0]))
+        sent[-1].start()
+        moved = jnp.dot(second_turned[...], near_right[:, at], preferred_element_type=f32)
+        kept = decoded(turned(codes[:, own:].reshape(span, cols)))
+        near_out[:, at] = (kept - scales[1] * moved).astype(bf16)
+        sent.append(pltpu.make_async_copy(near_out.at[:, at], out_copy.at[:, at], left_for.at[i, 1]))
+        sent[-1].start()
+    for copy in own_copies:
+        copy.wait()
+    for k, (step, new) in enumerate(((first, query_new), (second, out_new))):
+        moved = jnp.dot(near_own[k], step[...], preferred_element_type=f32)
+        near_new[k] = near_master[k] - scales[k] * moved
+        sent.append(pltpu.make_async_copy(near_new.at[k], new, own_left_for.at[k]))
+        sent[-1].start()
+    for copy in sent:
+        copy.wait()
 
 
 def far(value):
@@ -220,7 +270,6 @@
     first_moment,
     second_moment,
 ):
-    depth = lax.axis_size("z")
     fs = lax.axis_size(FS)
     tp = lax.axis_size("tp")
     own, rank_cols = left_factor.shape
@@ -235,7 +284,10 @@
     place = jnp.stack([lax.axis_index(FS), lax.axis_index("tp")]).astype(jnp.int32)
     packed, masters = pl.pallas_call(
         send_kernel,
-        out_shape=(jax.ShapeDtypeStruct((fs, kept, 128), bf16), pltpu.HBM((2 * own, cols), bf16)),
+        out_shape=(
+            jax.ShapeDtypeStruct((fs, kept, 128), bf16),
+            pltpu.HBM((2 * own, cols), bf16),
+        ),
         in_specs=[pl.BlockSpec()] * 4,
         out_specs=(VMEM, VMEM),
         compiler_params=SMALL,
@@ -245,16 +297,11 @@
     packed = lax.all_to_all(packed, FS, 0, 0)
     parts = 6
     proj = pl.pallas_call(
-        functools.partial(proj_kernel, used),
-        grid=(parts,),
+        functools.partial(proj_kernel, used, parts),
         out_shape=jax.ShapeDtypeStruct((used, tokens), bf16),
-        in_specs=[
-            pl.BlockSpec((fs // parts, kept, 128), lambda i: (i, 0, 0)),
-            pl.BlockSpec((tokens, width // parts), lambda i: (0, i)),
-            pl.BlockSpec((tokens, width // parts), lambda i: (0, i)),
-        ],
-        out_specs=pl.BlockSpec((used, tokens), lambda i: (0, 0)),
-        scratch_shapes=[pltpu.VMEM((tokens, 128), f32)] * 2,
+        in_specs=[VMEM, ANY, ANY],
+        out_specs=VMEM,
+        scratch_shapes=[pltpu.VMEM((tokens, width), bf16)] * 2 + [pltpu.SemaphoreType.DMA((parts, 2))],
         compiler_params=SMALL,
         cost_estimate=cost(4 * tokens * width * 128, 8 << 20),
     )(packed, far(saved_inputs), far(out_cotangent))
@@ -290,37 +337,32 @@
     )(pieces, first_moment, second_moment)
     low = lax.all_to_all(low, FS, 0, 0)
 
-    span = width // depth
-    per = fs // depth
-    left, right, query_all, out_all, own_left, own_right = pl.pallas_call(
+    span = width // 6
+    per = span // own
+    left, right, own_left, own_right = pl.pallas_call(
         functools.partial(prep_kernel, rank_cols),
-        grid=(depth,),
+        grid=(width // span,),
         out_shape=(
             pltpu.HBM((width, ranks), bf16),
             pltpu.HBM((ranks, width), bf16),
-            pltpu.HBM((width, cols), f32),
-            pltpu.HBM((cols, width), f32),
             pltpu.HBM((own, ranks), bf16),
             pltpu.HBM((own, ranks), bf16),
         ),
         in_specs=[
             SMEM,
-            pl.BlockSpec((per, 2 * own, cols), lambda i: (i, 0, 0)),
             pl.BlockSpec((tp // 2, per, kept, 128), lambda i: (0, i, 0, 0)),
             pl.BlockSpec((tp // 2, per, kept, 128), lambda i: (0, i, 0, 0)),
         ],
         out_specs=(
             pl.BlockSpec((span, ranks), lambda i: (i, 0)),
             pl.BlockSpec((ranks, span), lambda i: (0, i)),
-            pl.BlockSpec((span, cols), lambda i: (i, 0)),
-            pl.BlockSpec((cols, span), lambda i: (0, i)),
             pl.BlockSpec((own, ranks), lambda i: (0, 0)),
             pl.BlockSpec((own, ranks), lambda i: (0, 0)),
         ),
         scratch_shapes=[pltpu.VMEM((span, ranks), bf16)],
         compiler_params=SMALL,
         cost_estimate=cost(1 << 30, 30 << 20),
-    )(place, far(masters), far(held), far(other))
+    )(place, far(held), far(other))
 
     squares, first, second, second_turned = pl.pallas_call(
         functools.partial(sums_kernel, rank_cols),
@@ -337,36 +379,32 @@
     )(place, low)
     squares = lax.all_to_all(squares, "tp", 0, 0)
 
+    parts = width // span
     query_copy, out_copy, query_new, out_new = pl.pallas_call(
-        functools.partial(final_kernel, float(rows * fs * cols * tp)),
-        grid=(depth,),
+        functools.partial(final_kernel, float(rows * fs * cols * tp), span),
         out_shape=(
-            jax.ShapeDtypeStruct((width, cols), bf16),
-            jax.ShapeDtypeStruct((cols, width), bf16),
-            jax.ShapeDtypeStruct((own, cols), f32),
-            jax.ShapeDtypeStruct((own, cols), f32),
-        ),
-        in_specs=[
-            VMEM,
-            VMEM,
-            VMEM,
-            VMEM,
-            pl.BlockSpec((span, ranks), lambda i: (i, 0)),
-            pl.BlockSpec((ranks, span), lambda i: (0, i)),
-            pl.BlockSpec((span, cols), lambda i: (i, 0)),
-            pl.BlockSpec((cols, span), lambda i: (0, i)),
-            pl.BlockSpec((own, ranks), lambda i: (0, 0)),
-            pl.BlockSpec((own, ranks), lambda i: (0, 0)),
-            pl.BlockSpec((own, cols), lambda i: (0, 0)),
-            pl.BlockSpec((own, cols), lambda i: (0, 0)),
+            pltpu.HBM((width, cols), bf16),
+            pltpu.HBM((cols, width), bf16),
+            pltpu.HBM((own, cols), f32),
+            pltpu.HBM((own, cols), f32),
+        ),
+        in_specs=[VMEM] * 4 + [ANY] * 7,
+        out_specs=(ANY,) * 4,
+        scratch_shapes=[
+            pltpu.VMEM((width, ranks), bf16),
+            pltpu.VMEM((ranks, width), bf16),
+            pltpu.VMEM(masters.shape, bf16),
+            pltpu.VMEM((width, cols), bf16),
+            pltpu.VMEM((cols, width), bf16),
+            pltpu.VMEM((2, own, ranks), bf16),
+            pltpu.VMEM((2, own, cols), f32),
+            pltpu.VMEM((2, own, cols), f32),
+            pltpu.SemaphoreType.DMA((parts, 3)),
+            pltpu.SemaphoreType.DMA((4,)),
+            pltpu.SemaphoreType.DMA((parts, 2)),
+            pltpu.SemaphoreType.DMA((2,)),
         ],
-        out_specs=(
-            pl.BlockSpec((span, cols), lambda i: (i, 0)),
-            pl.BlockSpec((cols, span), lambda i: (0, i)),
-            pl.BlockSpec((own, cols), lambda i: (0, 0)),
-            pl.BlockSpec((own, cols), lambda i: (0, 0)),
-        ),
-        compiler_params=SMALL,
+        compiler_params=pltpu.CompilerParams(vmem_limit_bytes=32 << 20),
         cost_estimate=cost(4 * width * ranks * cols, 20 << 20),
     )(
         squares,
@@ -375,8 +413,7 @@
         second_turned,
         far(left),
         far(right),
-        far(query_all),
-        far(out_all),
+        far(masters),
         far(own_left),
         far(own_right),
         far(query_master),

time: 223 us -> 209 us (0.937)
  Pallas kernels: 41.2 us -> 30.2 us
    pallas_call x2, Pallas kernels: 22.5 us -> 14.8 us  [the longest x1 9.4 us: body(): pl.pallas_call(functools.partial(prep_kernel, rank_cols), grid=(width //...]
    pallas_call x1, Pallas kernels: 13 us -> 9.7 us  [body(): pl.pallas_call(functools.partial(final_kernel, float(rows * fs * cols * t...]
    ppermute x3, waiting for transfers between devices: 26.9 us -> 23.7 us  [body(): lax.ppermute(packed, 'tp', [((t + 2 * step) % tp, t) for t in range(tp)])]
  transfers between devices with their start and end apart: 8 -> 8, of which waited for: 4 -> 4; matrix products, arithmetic and copies ran while one was open for 1% -> 1% of each run, Pallas kernels for 12% -> 9%
where the time goes in v4:
time: 209 us
  blocking collectives  67.9 us (32%)
  waiting for transfers between devices  55 us (26%)
  starting transfers between devices  39.4 us (19%)
  Pallas kernels  30.2 us (14%)
  between operations  14.2 us (7%)
    all_to_all x1, blocking collectives, body(): packed = lax.all_to_all(packed, FS, 0, 0)  49.9 us
    all_to_all x1, waiting for transfers between devices, body(): low = lax.all_to_all(low, FS, 0, 0)  31.4 us
    ppermute x3, waiting for transfers between devices, body(): lax.ppermute(packed, 'tp', [((t + 2 * step) % tp, t) for t in range(tp)])  23.7 us
    all_gather x1, blocking collectives, body(): proj = lax.all_gather(proj, 'tp', axis=0, tiled=True)  17.9 us
    all_to_all x1, starting transfers between devices, body(): low = lax.all_to_all(low, FS, 0, 0)  15 us
    pallas_call x1, Pallas kernels, body(): pl.pallas_call(functools.partial(final_kernel, float(rows * fs * cols * t...  9.7 us
    pallas_call x1, Pallas kernels, body(): pl.pallas_call(functools.partial(prep_kernel, rank_cols), grid=(width //...  9.4 us
    ppermute x3, starting transfers between devices, body(): lax.ppermute(packed, 'tp', [((t + 2 * step) % tp, t) for t in range(tp)])  9.15 us
  transfers between devices with their start and end apart: 8, of which 4 were waited for; matrix products, arithmetic and copies ran while one was open for 1% of the time, Pallas kernels for 9%

profile of v4, /device:TPU:1, one launch (start us, length us, event | category | flops | bytes accessed | tf_op | source)
XLA Modules:
  0.0 208.5 jit_solution(10877775103987303929)
XLA Ops:
  7.2 0.0 all-gather.3.cloned.1.call-start
  7.2 1.6 shard_map.145
  8.8 0.0 all-gather.3.cloned.1.call-update
  8.9 49.9 %all_to_all.20.packed = bf16[96,24,128]{2,1,0:T(8,128)(2,1)S(1)} all-to-all(bf16[96,24,128]{2,1,0:T(8,128)(2,1)S(1)} %get-tuple-element.23), channel_id=1, replica_groups=mesh['z'=12,'y'=8,'tp'=8] {'z','y'}, dimensions={0} | all-to-all | bytes 1179648 | tf_op jit(solution)/shard_map/all_to_all | solution.py:297
  58.8 0.0 copy-start
  58.8 0.0 copy-start.1
  58.8 5.4 %shard_map.146 = bf16[96,512]{1,0:T(8,128)(2,1)S(1)} custom-call(bf16[96,24,128]{2,1,0:T(8,128)(2,1)S(1)} %all_to_all.20.packed, bf16[512,3072]{1,0:T(8,128)(2,1)} %saved_inputs.1, bf16[512,3072]{1,0:T(8,128)(2,1)} %out_cotangent.1), custom_call_target="tpu_custom_call" | custom-call | flops 805306368 | bytes 8388608 | tf_op jit(solution)/shard_map/pallas_call | solution.py:299
  64.2 17.9 %all_gather.9.proj = bf16[768,512]{1,0:T(8,128)(2,1)S(1)} all-gather(bf16[96,512]{1,0:T(8,128)(2,1)S(1)} %shard_map.146), channel_id=1, replica_groups=mesh['z'=12,'y'=8,'tp'=8] {'tp'}, dimensions={0}, use_global_device_ids=true | all-gather | bytes 884736 | tf_op jit(solution)/shard_map/all_gather | solution.py:308
  82.2 0.0 copy-done
  82.2 0.0 copy-done.1
  82.2 1.4 shard_map.147
  83.6 6.0 %all-to-all-start.1 = ((bf16[96,8,384]{2,1,0:T(8,128)(2,1)}), bf16[96,8,384]{2,1,0:T(8,128)(2,1)S(1)}, u32[]{:S(2)}, u32[]{:S(2)}) async-start(bf16[96,8,384]{2,1,0:T(8,128)(2,1)} %bitcast.12), calls=%async_computation.1 | async-start | bytes 1179648 | tf_op jit(solution)/shard_map/all_to_all | solution.py:318
  89.5 2.9 %collective-permute-start.2 = (bf16[96,24,128]{2,1,0:T(8,128)(2,1)S(1)}, bf16[96,24,128]{2,1,0:T(8,128)(2,1)S(1)}, u32[]{:S(2)}, u32[]{:S(2)}) collective-permute-start(bf16[96,24,128]{2,1,0:T(8,128)(2,1)S(1)} %all_to_all.20.packed), channel_id=1, source_target_pairs={{6,0},{7,1},{0,2},{1,3},{2,4},{3,5},{4,6},{5,7},{14,8},{15,9},{8,1... | collective-permute-start | bytes 1769480 | tf_op jit(solution)/shard_map/ppermute | solution.py:322
  92.5 4.3 %collective-permute-start.1 = (bf16[96,24,128]{2,1,0:T(8,128)(2,1)S(1)}, bf16[96,24,128]{2,1,0:T(8,128)(2,1)S(1)}, u32[]{:S(2)}, u32[]{:S(2)}) collective-permute-start(bf16[96,24,128]{2,1,0:T(8,128)(2,1)S(1)} %all_to_all.20.packed), channel_id=1, source_target_pairs={{4,0},{5,1},{6,2},{7,3},{0,4},{1,5},{2,6},{3,7},{12,8},{13,9},{14,... | collective-permute-start | bytes 1769480 | tf_op jit(solution)/shard_map/ppermute | solution.py:322
  96.8 1.9 collective-permute-start
  98.7 8.8 %collective-permute-done.2 = bf16[96,24,128]{2,1,0:T(8,128)(2,1)S(1)} collective-permute-done((bf16[96,24,128]{2,1,0:T(8,128)(2,1)S(1)}, bf16[96,24,128]{2,1,0:T(8,128)(2,1)S(1)}, u32[]{:S(2)}, u32[]{:S(2)}) %collective-permute-start.2) | collective-permute-done | bytes 589856 | tf_op jit(solution)/shard_map/ppermute | solution.py:322
  107.5 13.3 %collective-permute-done.1 = bf16[96,24,128]{2,1,0:T(8,128)(2,1)S(1)} collective-permute-done((bf16[96,24,128]{2,1,0:T(8,128)(2,1)S(1)}, bf16[96,24,128]{2,1,0:T(8,128)(2,1)S(1)}, u32[]{:S(2)}, u32[]{:S(2)}) %collective-permute-start.1) | collective-permute-done | bytes 589856 | tf_op jit(solution)/shard_map/ppermute | solution.py:322
  120.7 1.6 collective-permute-done
  122.4 0.0 copy-start.2
  122.4 0.0 copy-start.3
  122.4 1.7 pad_maximum_fusion.held
  124.1 3.1 %collective-permute-start.3 = (bf16[4,96,24,128]{3,2,1,0:T(8,128)(2,1)}, bf16[4,96,24,128]{3,2,1,0:T(8,128)(2,1)}, u32[]{:S(2)}, u32[]{:S(2)}) collective-permute-start(bf16[4,96,24,128]{3,2,1,0:T(8,128)(2,1)} %pad_maximum_fusion.held), channel_id=1, source_target_pairs={{1,0},{0,1},{3,2},{2,3},{5,4},{4,5},{7,6},{6,7},{9,8},{8,9},{11,10... | collective-permute-start | bytes 7077896 | tf_op jit(solution)/shard_map/ppermute | solution.py:324
  127.2 0.0 all-to-all-done.1.pieces
  127.2 0.0 copy-done.2
  127.2 0.0 copy-done.3
  127.2 1.1 shard_map.148
  128.3 15.0 %all-to-all-start.2 = ((bf16[96,4,896]{2,1,0:T(4,128)(2,1)}), bf16[96,4,896]{2,1,0:T(4,128)(2,1)S(1)}, u32[]{:S(2)}, u32[]{:S(2)}) async-start(bf16[96,4,896]{2,1,0:T(4,128)(2,1)} %get-tuple-element.24), calls=%async_computation.2 | async-start | bytes 1376256 | tf_op jit(solution)/shard_map/all_to_all | solution.py:338
  143.4 0.1 pad_add_fusion.place
  143.5 31.4 %all-to-all-done.2.low = bf16[96,4,896]{2,1,0:T(4,128)(2,1)S(1)} async-done(((bf16[96,4,896]{2,1,0:T(4,128)(2,1)}), bf16[96,4,896]{2,1,0:T(4,128)(2,1)S(1)}, u32[]{:S(2)}, u32[]{:S(2)}) %all-to-all-start.2) | async-done | bytes 688160 | tf_op jit(solution)/shard_map/all_to_all | solution.py:338
  174.8 1.6 shard_map.149
  176.4 6.1 %all-to-all-start.3 = ((f32[8,8,128]{2,1,0:T(8,128)}), f32[8,8,128]{2,1,0:T(8,128)S(1)}, u32[]{:S(2)}, u32[]{:S(2)}) async-start(f32[8,8,128]{2,1,0:T(8,128)} %get-tuple-element.25), calls=%async_computation.3 | async-start | bytes 65536 | tf_op jit(solution)/shard_map/all_to_all | solution.py:380
  182.5 0.0 collective-permute-done.3.other
  182.5 9.4 %shard_map.150 = (bf16[3072,384]{1,0:T(8,128)(2,1)}, bf16[384,3072]{1,0:T(8,128)(2,1)}, bf16[32,384]{1,0:T(8,128)(2,1)}, bf16[32,384]{1,0:T(8,128)(2,1)}) custom-call(s32[2]{0:T(128)S(1)} %pad_add_fusion.place, bf16[4,96,24,128]{3,2,1,0:T(8,128)(2,1)} %pad_maximum_fusion.held, bf16[4,96,24,128]{3,2,1,0:T(8,128)(2,1)} %collective-permute-done.3.other), custom_call_target="tpu_custom_call" | custom-call | flops 1073741824 | bytes 31457280 | tf_op jit(solution)/shard_map/pallas_call | solution.py:342
  191.9 0.0 all-to-all-done.3.squares
  191.9 0.0 all-gather.3.cloned.1.call-done
  192.0 9.7 %shard_map.151 = (bf16[3072,384]{1,0:T(8,128)(2,1)}, bf16[384,3072]{1,0:T(8,128)(2,1)}, f32[32,384]{1,0:T(8,128)}, f32[32,384]{1,0:T(8,128)}) custom-call(f32[8,8,128]{2,1,0:T(8,128)S(1)} %all-to-all-done.3.squares, bf16[384,384]{1,0:T(8,128)(2,1)S(1)} %get-tuple-element.26.first, bf16[384,384]{1,0:T(8,128)(2,1)S(1)} %get-tuple-element.27.second, ...), custom_call_target="tpu_custom_call" | custom-call | flops 1811939328 | bytes 20971520 | tf_op jit(solution)/shard_map/pallas_call | solution.py:383
Async XLA Ops:
  7.2 184.8 %all-gather.3.cloned.1.call-start = ((), (), s32[]{:S(2)}) async-start(), calls=%async_computation.4 | async-start | bytes 4767744 | tf_op jit(solution)/shard_map/all_gather | solution.py:296
  58.8 23.4 %copy-start = (bf16[512,384]{1,0:T(8,128)(2,1)S(1)}, bf16[512,384]{1,0:T(8,128)(2,1)}, u32[]{:S(2)}) copy-start(bf16[512,384]{1,0:T(8,128)(2,1)} %query_cotangent.1) | copy-start | bytes 1179652
  58.8 23.4 %copy-start.1 = (bf16[512,384]{1,0:T(8,128)(2,1)S(1)}, bf16[512,384]{1,0:T(8,128)(2,1)}, u32[]{:S(2)}) copy-start(bf16[512,384]{1,0:T(8,128)(2,1)} %attn_outputs.1) | copy-start | bytes 1179652
  83.6 43.6 %all-to-all-start.1 = ((bf16[96,8,384]{2,1,0:T(8,128)(2,1)}), bf16[96,8,384]{2,1,0:T(8,128)(2,1)S(1)}, u32[]{:S(2)}, u32[]{:S(2)}) async-start(bf16[96,8,384]{2,1,0:T(8,128)(2,1)} %bitcast.12), calls=%async_computation.1 | async-start | bytes 1179648 | tf_op jit(solution)/shard_map/all_to_all | solution.py:318
  89.5 17.9 %collective-permute-start.2 = (bf16[96,24,128]{2,1,0:T(8,128)(2,1)S(1)}, bf16[96,24,128]{2,1,0:T(8,128)(2,1)S(1)}, u32[]{:S(2)}, u32[]{:S(2)}) collective-permute-start(bf16[96,24,128]{2,1,0:T(8,128)(2,1)S(1)} %all_to_all.20.packed), channel_id=1, source_target_pairs={{6,0},{7,1},{0,2},{1,3},{2,4},{3,5},{4,6},{5,7},{14,8},{15,9},{8,1... | collective-permute-start | bytes 1769480 | tf_op jit(solution)/shard_map/ppermute | solution.py:322
  92.5 28.3 %collective-permute-start.1 = (bf16[96,24,128]{2,1,0:T(8,128)(2,1)S(1)}, bf16[96,24,128]{2,1,0:T(8,128)(2,1)S(1)}, u32[]{:S(2)}, u32[]{:S(2)}) collective-permute-start(bf16[96,24,128]{2,1,0:T(8,128)(2,1)S(1)} %all_to_all.20.packed), channel_id=1, source_target_pairs={{4,0},{5,1},{6,2},{7,3},{0,4},{1,5},{2,6},{3,7},{12,8},{13,9},{14,... | collective-permute-start | bytes 1769480 | tf_op jit(solution)/shard_map/ppermute | solution.py:322
  96.8 25.6 %collective-permute-start = (bf16[96,24,128]{2,1,0:T(8,128)(2,1)S(1)}, bf16[96,24,128]{2,1,0:T(8,128)(2,1)S(1)}, u32[]{:S(2)}, u32[]{:S(2)}) collective-permute-start(bf16[96,24,128]{2,1,0:T(8,128)(2,1)S(1)} %all_to_all.20.packed), channel_id=1, source_target_pairs={{2,0},{3,1},{4,2},{5,3},{6,4},{7,5},{0,6},{1,7},{10,8},{11,9},{12,... | collective-permute-start | bytes 1769480 | tf_op jit(solution)/shard_map/ppermute | solution.py:322
  122.4 4.8 %copy-start.2 = (f32[2,4,384]{2,1,0:T(4,128)S(1)}, f32[2,4,384]{2,1,0:T(4,128)}, u32[]{:S(2)}) copy-start(f32[2,4,384]{2,1,0:T(4,128)} %first.1) | copy-start | bytes 36868
  122.4 4.8 %copy-start.3 = (f32[2,4,384]{2,1,0:T(4,128)S(1)}, f32[2,4,384]{2,1,0:T(4,128)}, u32[]{:S(2)}) copy-start(f32[2,4,384]{2,1,0:T(4,128)} %second.1) | copy-start | bytes 36868
  124.1 58.5 %collective-permute-start.3 = (bf16[4,96,24,128]{3,2,1,0:T(8,128)(2,1)}, bf16[4,96,24,128]{3,2,1,0:T(8,128)(2,1)}, u32[]{:S(2)}, u32[]{:S(2)}) collective-permute-start(bf16[4,96,24,128]{3,2,1,0:T(8,128)(2,1)} %pad_maximum_fusion.held), channel_id=1, source_target_pairs={{1,0},{0,1},{3,2},{2,3},{5,4},{4,5},{7,6},{6,7},{9,8},{8,9},{11,10... | collective-permute-start | bytes 7077896 | tf_op jit(solution)/shard_map/ppermute | solution.py:324
  128.3 46.5 %all-to-all-start.2 = ((bf16[96,4,896]{2,1,0:T(4,128)(2,1)}), bf16[96,4,896]{2,1,0:T(4,128)(2,1)S(1)}, u32[]{:S(2)}, u32[]{:S(2)}) async-start(bf16[96,4,896]{2,1,0:T(4,128)(2,1)} %get-tuple-element.24), calls=%async_computation.2 | async-start | bytes 1376256 | tf_op jit(solution)/shard_map/all_to_all | solution.py:338
  176.4 15.5 %all-to-all-start.3 = ((f32[8,8,128]{2,1,0:T(8,128)}), f32[8,8,128]{2,1,0:T(8,128)S(1)}, u32[]{:S(2)}, u32[]{:S(2)}) async-start(f32[8,8,128]{2,1,0:T(8,128)} %get-tuple-element.25), calls=%async_computation.3 | async-start | bytes 65536 | tf_op jit(solution)/shard_map/all_to_all | solution.py:380
Sparse Core Ops, SparseCore 0:
  12.3 135.8 all-gather.2

commit v5 on v4

--- a/solution.py
+++ b/solution.py
@@ -46,9 +46,8 @@
 
 
 def send_kernel(left, right, query_master, out_master, out, masters):
-    own = query_master.shape[0]
-    masters[:own] = coded(query_master[...])
-    masters[own:] = coded(out_master[...])
+    codes = jnp.concatenate([coded(query_master[...]), coded(out_master[...])], axis=0)
+    masters[...] = jnp.broadcast_to(codes[None], masters.shape)
     both = jnp.concatenate([left[...].astype(f32), right[...].astype(f32)], axis=1)
     used = both.shape[1]
     free = 128 - used
@@ -147,6 +146,31 @@
             out[...] = tile[rows]
 
 
+def decode_kernel(span, masters, query_master, out_master, near, near_query, near_out, arrived, left_for):
+    own = masters.shape[1] // 2
+    cols = masters.shape[2]
+    per = span // own
+    parts = masters.shape[0] // per
+    spans = [pl.ds(i * span, span) for i in range(parts)]
+    copies = []
+    for i in range(parts):
+        held = pl.ds(i * per, per)
+        copies.append(pltpu.make_async_copy(masters.at[held], near.at[held], arrived.at[i]))
+        copies[-1].start()
+    sent = []
+    for i, at in enumerate(spans):
+        copies[i].wait()
+        codes = near[i * per : (i + 1) * per]
+        near_query[at] = decoded(codes[:, :own].reshape(span, cols).astype(f32))
+        near_out[:, at] = decoded(turned(codes[:, own:].reshape(span, cols)))
+        sent.append(pltpu.make_async_copy(near_query.at[at], query_master.at[at], left_for.at[i, 0]))
+        sent.append(pltpu.make_async_copy(near_out.at[:, at], out_master.at[:, at], left_for.at[i, 1]))
+        sent[-2].start()
+        sent[-1].start()
+    for copy in sent:
+        copy.wait()
+
+
 def sums_kernel(rank_cols, place, low, squares, first, second, second_turned):
     tp = squares.shape[0]
     cols = first.shape[1]
@@ -174,7 +198,8 @@
     second_turned,
     left,
     right,
-    masters,
+    query_all,
+    out_all,
     own_left,
     own_right,
     query_master,
@@ -185,7 +210,8 @@
     out_new,
     near_left,
     near_right,
-    near_masters,
+    near_query_all,
+    near_out_all,
     near_query,
     near_out,
     near_own,
@@ -197,18 +223,15 @@
     own_left_for,
 ):
     width = left.shape[0]
-    cols = first.shape[1]
-    own = query_master.shape[0]
-    per = span // own
     parts = width // span
     spans = [pl.ds(i * span, span) for i in range(parts)]
     copies = []
     for i, at in enumerate(spans):
-        held = pl.ds(i * per, per)
         ways = (
             (left.at[at], near_left.at[at]),
-            (masters.at[held], near_masters.at[held]),
+            (query_all.at[at], near_query_all.at[at]),
             (right.at[:, at], near_right.at[:, at]),
+            (out_all.at[:, at], near_out_all.at[:, at]),
         )
         copies.append([pltpu.make_async_copy(x, y, arrived.at[i, k]) for k, (x, y) in enumerate(ways)])
     ways = (
@@ -232,15 +255,12 @@
     for i, at in enumerate(spans):
         for copy in copies[i]:
             copy.wait()
-        codes = near_masters[i * per : (i + 1) * per]
         moved = jnp.dot(near_left[at], first[...], preferred_element_type=f32)
-        kept = decoded(codes[:, :own].reshape(span, cols).astype(f32))
-        near_query[at] = (kept - scales[0] * moved).astype(bf16)
+        near_query[at] = (near_query_all[at] - scales[0] * moved).astype(bf16)
         sent.append(pltpu.make_async_copy(near_query.at[at], query_copy.at[at], left_for.at[i, 0]))
         sent[-1].start()
         moved = jnp.dot(second_turned[...], near_right[:, at], preferred_element_type=f32)
-        kept = decoded(turned(codes[:, own:].reshape(span, cols)))
-        near_out[:, at] = (kept - scales[1] * moved).astype(bf16)
+        near_out[:, at] = (near_out_all[:, at] - scales[1] * moved).astype(bf16)
         sent.append(pltpu.make_async_copy(near_out.at[:, at], out_copy.at[:, at], left_for.at[i, 1]))
         sent[-1].start()
     for copy in own_copies:
@@ -270,6 +290,7 @@
     first_moment,
     second_moment,
 ):
+    height = lax.axis_size("y")
     fs = lax.axis_size(FS)
     tp = lax.axis_size("tp")
     own, rank_cols = left_factor.shape
@@ -286,15 +307,16 @@
         send_kernel,
         out_shape=(
             jax.ShapeDtypeStruct((fs, kept, 128), bf16),
-            pltpu.HBM((2 * own, cols), bf16),
+            pltpu.HBM((height, 2 * own, cols), bf16),
         ),
         in_specs=[pl.BlockSpec()] * 4,
         out_specs=(VMEM, VMEM),
         compiler_params=SMALL,
         cost_estimate=cost(1 << 16, 1 << 20),
     )(far(left_factor), far(right_factor), far(query_master), far(out_master.T))
-    masters = lax.all_gather(masters, FS)
     packed = lax.all_to_all(packed, FS, 0, 0)
+    masters = lax.all_to_all(masters, "y", 0, 0)
+    masters = lax.all_gather(masters, "z").reshape(fs, 2 * own, cols)
     parts = 6
     proj = pl.pallas_call(
         functools.partial(proj_kernel, used, parts),
@@ -364,6 +386,23 @@
         cost_estimate=cost(1 << 30, 30 << 20),
     )(place, far(held), far(other))
 
+    parts = width // span
+    query_all, out_all = pl.pallas_call(
+        functools.partial(decode_kernel, span),
+        out_shape=(pltpu.HBM((width, cols), f32), pltpu.HBM((cols, width), f32)),
+        in_specs=[ANY],
+        out_specs=(ANY, ANY),
+        scratch_shapes=[
+            pltpu.VMEM(masters.shape, bf16),
+            pltpu.VMEM((width, cols), f32),
+            pltpu.VMEM((cols, width), f32),
+            pltpu.SemaphoreType.DMA((parts,)),
+            pltpu.SemaphoreType.DMA((parts, 2)),
+        ],
+        compiler_params=pltpu.CompilerParams(vmem_limit_bytes=24 << 20),
+        cost_estimate=cost(1 << 30, 15 << 20),
+    )(far(masters))
+
     squares, first, second, second_turned = pl.pallas_call(
         functools.partial(sums_kernel, rank_cols),
         out_shape=(
@@ -388,18 +427,19 @@
             pltpu.HBM((own, cols), f32),
             pltpu.HBM((own, cols), f32),
         ),
-        in_specs=[VMEM] * 4 + [ANY] * 7,
+        in_specs=[VMEM] * 4 + [ANY] * 8,
         out_specs=(ANY,) * 4,
         scratch_shapes=[
             pltpu.VMEM((width, ranks), bf16),
             pltpu.VMEM((ranks, width), bf16),
-            pltpu.VMEM(masters.shape, bf16),
+            pltpu.VMEM((width, cols), f32),
+            pltpu.VMEM((cols, width), f32),
             pltpu.VMEM((width, cols), bf16),
             pltpu.VMEM((cols, width), bf16),
             pltpu.VMEM((2, own, ranks), bf16),
             pltpu.VMEM((2, own, cols), f32),
             pltpu.VMEM((2, own, cols), f32),
-            pltpu.SemaphoreType.DMA((parts, 3)),
+            pltpu.SemaphoreType.DMA((parts, 4)),
             pltpu.SemaphoreType.DMA((4,)),
             pltpu.SemaphoreType.DMA((parts, 2)),
             pltpu.SemaphoreType.DMA((2,)),
@@ -413,7 +453,8 @@
         second_turned,
         far(left),
         far(right),
-        far(masters),
+        far(query_all),
+        far(out_all),
         far(own_left),
         far(own_right),
         far(query_master),

time: 209 us -> 228 us (1.091)
  blocking collectives: 67.9 us -> 86.6 us
  waiting for transfers between devices: 55 us -> 44.2 us
  Pallas kernels: 30.2 us -> 38.7 us
  starting transfers between devices: 39.4 us -> 42 us
    all_to_all x0 -> x1, blocking collectives: none -> 18.5 us  [body(): masters = lax.all_to_all(masters, 'y', 0, 0)]
    all_to_all x1, waiting for transfers between devices: 31.4 us -> 20.8 us  [body(): low = lax.all_to_all(low, FS, 0, 0)]
    pallas_call x0 -> x1, Pallas kernels: none -> 9.92 us  [body(): pl.pallas_call(functools.partial(decode_kernel, span), out_shape=(pltpu.H...]
  transfers between devices with their start and end apart: 8 -> 8, of which waited for: 4 -> 4; matrix products, arithmetic and copies ran while one was open for 1% -> 1% of each run, Pallas kernels for 9% -> 13%
where the time goes in v5:
time: 228 us; the launch traced here: 227 us
  blocking collectives  86.6 us (38%)
  waiting for transfers between devices  44.2 us (19%)
  starting transfers between devices  42 us (18%)
  Pallas kernels  38.7 us (17%)
  between operations  14.2 us (6%)
    all_to_all x1, blocking collectives, body(): packed = lax.all_to_all(packed, FS, 0, 0)  49.3 us
    ppermute x3, waiting for transfers between devices, body(): lax.ppermute(packed, 'tp', [((t + 2 * step) % tp, t) for t in range(tp)])  23.4 us
    all_to_all x1, waiting for transfers between devices, body(): low = lax.all_to_all(low, FS, 0, 0)  20.8 us
    all_gather x1, blocking collectives, body(): proj = lax.all_gather(proj, 'tp', axis=0, tiled=True)  18.8 us
    all_to_all x1, blocking collectives, body(): masters = lax.all_to_all(masters, 'y', 0, 0)  18.5 us
    all_to_all x1, starting transfers between devices, body(): low = lax.all_to_all(low, FS, 0, 0)  15 us
    pallas_call x1, Pallas kernels, body(): pl.pallas_call(functools.partial(decode_kernel, span), out_shape=(pltpu.H...  9.92 us
    pallas_call x1, Pallas kernels, body(): pl.pallas_call(functools.partial(prep_kernel, rank_cols), grid=(width //...  9.41 us
  transfers between devices with their start and end apart: 8, of which 4 were waited for; matrix products, arithmetic and copies ran while one was open for 1% of the time, Pallas kernels for 13%

profile of v5, /device:TPU:1, one launch (start us, length us, event | category | flops | bytes accessed | tf_op | source)
XLA Modules:
  0.0 227.4 jit_solution(4807662744117298941)
XLA Ops:
  7.2 0.0 all-gather.3.cloned.1.call-start
  7.2 1.8 shard_map.145
  9.0 18.5 %all_to_all.25 = bf16[8,64,384]{2,1,0:T(8,128)(2,1)} all-to-all(bf16[8,64,384]{2,1,0:T(8,128)(2,1)} %get-tuple-element.33), channel_id=1, replica_groups=mesh['z'=12,'y'=8,'tp'=8] {'y'}, dimensions={0} | all-to-all | bytes 786432 | tf_op jit(solution)/shard_map/all_to_all | solution.py:318
  27.5 0.0 all-gather.3.cloned.1.call-update
  27.5 49.3 %all_to_all.26.packed = bf16[96,24,128]{2,1,0:T(8,128)(2,1)S(1)} all-to-all(bf16[96,24,128]{2,1,0:T(8,128)(2,1)S(1)} %get-tuple-element.25), channel_id=1, replica_groups=mesh['z'=12,'y'=8,'tp'=8] {'z','y'}, dimensions={0} | all-to-all | bytes 1179648 | tf_op jit(solution)/shard_map/all_to_all | solution.py:317
  76.8 0.0 copy-start
  76.8 0.0 copy-start.1
  76.8 5.4 %shard_map.146 = bf16[96,512]{1,0:T(8,128)(2,1)S(1)} custom-call(bf16[96,24,128]{2,1,0:T(8,128)(2,1)S(1)} %all_to_all.26.packed, bf16[512,3072]{1,0:T(8,128)(2,1)} %saved_inputs.1, bf16[512,3072]{1,0:T(8,128)(2,1)} %out_cotangent.1), custom_call_target="tpu_custom_call" | custom-call | flops 805306368 | bytes 8388608 | tf_op jit(solution)/shard_map/pallas_call | solution.py:321
  82.2 18.8 %all_gather.9.proj = bf16[768,512]{1,0:T(8,128)(2,1)S(1)} all-gather(bf16[96,512]{1,0:T(8,128)(2,1)S(1)} %shard_map.146), channel_id=1, replica_groups=mesh['z'=12,'y'=8,'tp'=8] {'tp'}, dimensions={0}, use_global_device_ids=true | all-gather | bytes 884736 | tf_op jit(solution)/shard_map/all_gather | solution.py:330
  101.0 0.0 copy-done
  101.0 0.0 copy-done.1
  101.0 1.4 shard_map.147
  102.4 6.9 %all-to-all-start.1 = ((bf16[96,8,384]{2,1,0:T(8,128)(2,1)}), bf16[96,8,384]{2,1,0:T(8,128)(2,1)S(1)}, u32[]{:S(2)}, u32[]{:S(2)}) async-start(bf16[96,8,384]{2,1,0:T(8,128)(2,1)} %bitcast.10), calls=%async_computation.1 | async-start | bytes 1179648 | tf_op jit(solution)/shard_map/all_to_all | solution.py:340
  109.2 2.8 %collective-permute-start.2 = (bf16[96,24,128]{2,1,0:T(8,128)(2,1)S(1)}, bf16[96,24,128]{2,1,0:T(8,128)(2,1)S(1)}, u32[]{:S(2)}, u32[]{:S(2)}) collective-permute-start(bf16[96,24,128]{2,1,0:T(8,128)(2,1)S(1)} %all_to_all.26.packed), channel_id=1, source_target_pairs={{6,0},{7,1},{0,2},{1,3},{2,4},{3,5},{4,6},{5,7},{14,8},{15,9},{8,1... | collective-permute-start | bytes 1769480 | tf_op jit(solution)/shard_map/ppermute | solution.py:344
  112.1 4.3 %collective-permute-start.1 = (bf16[96,24,128]{2,1,0:T(8,128)(2,1)S(1)}, bf16[96,24,128]{2,1,0:T(8,128)(2,1)S(1)}, u32[]{:S(2)}, u32[]{:S(2)}) collective-permute-start(bf16[96,24,128]{2,1,0:T(8,128)(2,1)S(1)} %all_to_all.26.packed), channel_id=1, source_target_pairs={{4,0},{5,1},{6,2},{7,3},{0,4},{1,5},{2,6},{3,7},{12,8},{13,9},{14,... | collective-permute-start | bytes 1769480 | tf_op jit(solution)/shard_map/ppermute | solution.py:344
  116.4 1.9 collective-permute-start
  118.3 8.6 %collective-permute-done.2 = bf16[96,24,128]{2,1,0:T(8,128)(2,1)S(1)} collective-permute-done((bf16[96,24,128]{2,1,0:T(8,128)(2,1)S(1)}, bf16[96,24,128]{2,1,0:T(8,128)(2,1)S(1)}, u32[]{:S(2)}, u32[]{:S(2)}) %collective-permute-start.2) | collective-permute-done | bytes 589856 | tf_op jit(solution)/shard_map/ppermute | solution.py:344
  126.9 13.2 %collective-permute-done.1 = bf16[96,24,128]{2,1,0:T(8,128)(2,1)S(1)} collective-permute-done((bf16[96,24,128]{2,1,0:T(8,128)(2,1)S(1)}, bf16[96,24,128]{2,1,0:T(8,128)(2,1)S(1)}, u32[]{:S(2)}, u32[]{:S(2)}) %collective-permute-start.1) | collective-permute-done | bytes 589856 | tf_op jit(solution)/shard_map/ppermute | solution.py:344
  140.1 1.7 collective-permute-done
  141.7 0.0 copy-start.2
  141.7 0.0 copy-start.3
  141.7 1.7 pad_maximum_fusion.held
  143.4 3.5 %collective-permute-start.3 = (bf16[4,96,24,128]{3,2,1,0:T(8,128)(2,1)}, bf16[4,96,24,128]{3,2,1,0:T(8,128)(2,1)}, u32[]{:S(2)}, u32[]{:S(2)}) collective-permute-start(bf16[4,96,24,128]{3,2,1,0:T(8,128)(2,1)} %pad_maximum_fusion.held), channel_id=1, source_target_pairs={{1,0},{0,1},{3,2},{2,3},{5,4},{4,5},{7,6},{6,7},{9,8},{8,9},{11,10... | collective-permute-start | bytes 7077896 | tf_op jit(solution)/shard_map/ppermute | solution.py:346
  146.9 0.0 all-to-all-done.1.pieces
  146.9 0.0 copy-done.2
  146.9 0.0 copy-done.3
  146.9 1.1 shard_map.148
  148.0 15.0 %all-to-all-start.2 = ((bf16[96,4,896]{2,1,0:T(4,128)(2,1)}), bf16[96,4,896]{2,1,0:T(4,128)(2,1)S(1)}, u32[]{:S(2)}, u32[]{:S(2)}) async-start(bf16[96,4,896]{2,1,0:T(4,128)(2,1)} %get-tuple-element.26), calls=%async_computation.2 | async-start | bytes 1376256 | tf_op jit(solution)/shard_map/all_to_all | solution.py:360
  163.1 0.1 pad_add_fusion.place
  163.2 0.0 collective-permute-done.3.other
  163.2 9.4 %shard_map.150 = (bf16[3072,384]{1,0:T(8,128)(2,1)}, bf16[384,3072]{1,0:T(8,128)(2,1)}, bf16[32,384]{1,0:T(8,128)(2,1)}, bf16[32,384]{1,0:T(8,128)(2,1)}) custom-call(s32[2]{0:T(128)S(1)} %pad_add_fusion.place, bf16[4,96,24,128]{3,2,1,0:T(8,128)(2,1)} %pad_maximum_fusion.held, bf16[4,96,24,128]{3,2,1,0:T(8,128)(2,1)} %collective-permute-done.3.other), custom_call_target="tpu_custom_call" | custom-call | flops 1073741824 | bytes 31457280 | tf_op jit(solution)/shard_map/pallas_call | solution.py:364
  172.6 20.8 %all-to-all-done.2.low = bf16[96,4,896]{2,1,0:T(4,128)(2,1)S(1)} async-done(((bf16[96,4,896]{2,1,0:T(4,128)(2,1)}), bf16[96,4,896]{2,1,0:T(4,128)(2,1)S(1)}, u32[]{:S(2)}, u32[]{:S(2)}) %all-to-all-start.2) | async-done | bytes 688160 | tf_op jit(solution)/shard_map/all_to_all | solution.py:360
  193.4 1.6 shard_map.149
  194.9 7.6 %all-to-all-start.3 = ((f32[8,8,128]{2,1,0:T(8,128)}), f32[8,8,128]{2,1,0:T(8,128)S(1)}, u32[]{:S(2)}, u32[]{:S(2)}) async-start(f32[8,8,128]{2,1,0:T(8,128)} %get-tuple-element.27), calls=%async_computation.3 | async-start | bytes 65536 | tf_op jit(solution)/shard_map/all_to_all | solution.py:419
  202.5 0.0 all-gather.3.cloned.1.call-done.masters
  202.5 9.9 %shard_map.151 = (f32[3072,384]{1,0:T(8,128)}, f32[384,3072]{1,0:T(8,128)}) custom-call(bf16[96,64,384]{2,1,0:T(8,128)(2,1)} %all-gather.3.cloned.1.call-done.masters), custom_call_target="tpu_custom_call" | custom-call | flops 1073741824 | bytes 15728640 | tf_op jit(solution)/shard_map/pallas_call | solution.py:390
  212.5 0.0 all-to-all-done.3.squares
  212.5 8.1 %shard_map.152 = (bf16[3072,384]{1,0:T(8,128)(2,1)}, bf16[384,3072]{1,0:T(8,128)(2,1)}, f32[32,384]{1,0:T(8,128)}, f32[32,384]{1,0:T(8,128)}) custom-call(f32[8,8,128]{2,1,0:T(8,128)S(1)} %all-to-all-done.3.squares, bf16[384,384]{1,0:T(8,128)(2,1)S(1)} %get-tuple-element.28.first, bf16[384,384]{1,0:T(8,128)(2,1)S(1)} %get-tuple-element.29.second, ...), custom_call_target="tpu_custom_call" | custom-call | flops 1811939328 | bytes 20971520 | tf_op jit(solution)/shard_map/pallas_call | solution.py:422
Async XLA Ops:
  7.2 195.4 %all-gather.3.cloned.1.call-start = ((), (), s32[]{:S(2)}) async-start(), calls=%async_computation.5 | async-start | bytes 5111808 | tf_op jit(solution)/shard_map/all_gather | solution.py:319
  76.8 24.2 %copy-start = (bf16[512,384]{1,0:T(8,128)(2,1)S(1)}, bf16[512,384]{1,0:T(8,128)(2,1)}, u32[]{:S(2)}) copy-start(bf16[512,384]{1,0:T(8,128)(2,1)} %query_cotangent.1) | copy-start | bytes 1179652
  76.8 24.2 %copy-start.1 = (bf16[512,384]{1,0:T(8,128)(2,1)S(1)}, bf16[512,384]{1,0:T(8,128)(2,1)}, u32[]{:S(2)}) copy-start(bf16[512,384]{1,0:T(8,128)(2,1)} %attn_outputs.1) | copy-start | bytes 1179652
  102.4 44.5 %all-to-all-start.1 = ((bf16[96,8,384]{2,1,0:T(8,128)(2,1)}), bf16[96,8,384]{2,1,0:T(8,128)(2,1)S(1)}, u32[]{:S(2)}, u32[]{:S(2)}) async-start(bf16[96,8,384]{2,1,0:T(8,128)(2,1)} %bitcast.10), calls=%async_computation.1 | async-start | bytes 1179648 | tf_op jit(solution)/shard_map/all_to_all | solution.py:340
  109.2 17.7 %collective-permute-start.2 = (bf16[96,24,128]{2,1,0:T(8,128)(2,1)S(1)}, bf16[96,24,128]{2,1,0:T(8,128)(2,1)S(1)}, u32[]{:S(2)}, u32[]{:S(2)}) collective-permute-start(bf16[96,24,128]{2,1,0:T(8,128)(2,1)S(1)} %all_to_all.26.packed), channel_id=1, source_target_pairs={{6,0},{7,1},{0,2},{1,3},{2,4},{3,5},{4,6},{5,7},{14,8},{15,9},{8,1... | collective-permute-start | bytes 1769480 | tf_op jit(solution)/shard_map/ppermute | solution.py:344
  112.1 28.0 %collective-permute-start.1 = (bf16[96,24,128]{2,1,0:T(8,128)(2,1)S(1)}, bf16[96,24,128]{2,1,0:T(8,128)(2,1)S(1)}, u32[]{:S(2)}, u32[]{:S(2)}) collective-permute-start(bf16[96,24,128]{2,1,0:T(8,128)(2,1)S(1)} %all_to_all.26.packed), channel_id=1, source_target_pairs={{4,0},{5,1},{6,2},{7,3},{0,4},{1,5},{2,6},{3,7},{12,8},{13,9},{14,... | collective-permute-start | bytes 1769480 | tf_op jit(solution)/shard_map/ppermute | solution.py:344
  116.4 25.3 %collective-permute-start = (bf16[96,24,128]{2,1,0:T(8,128)(2,1)S(1)}, bf16[96,24,128]{2,1,0:T(8,128)(2,1)S(1)}, u32[]{:S(2)}, u32[]{:S(2)}) collective-permute-start(bf16[96,24,128]{2,1,0:T(8,128)(2,1)S(1)} %all_to_all.26.packed), channel_id=1, source_target_pairs={{2,0},{3,1},{4,2},{5,3},{6,4},{7,5},{0,6},{1,7},{10,8},{11,9},{12,... | collective-permute-start | bytes 1769480 | tf_op jit(solution)/shard_map/ppermute | solution.py:344
  141.7 5.2 %copy-start.2 = (f32[2,4,384]{2,1,0:T(4,128)S(1)}, f32[2,4,384]{2,1,0:T(4,128)}, u32[]{:S(2)}) copy-start(f32[2,4,384]{2,1,0:T(4,128)} %first.1) | copy-start | bytes 36868
  141.7 5.2 %copy-start.3 = (f32[2,4,384]{2,1,0:T(4,128)S(1)}, f32[2,4,384]{2,1,0:T(4,128)}, u32[]{:S(2)}) copy-start(f32[2,4,384]{2,1,0:T(4,128)} %second.1) | copy-start | bytes 36868
  143.4 19.8 %collective-permute-start.3 = (bf16[4,96,24,128]{3,2,1,0:T(8,128)(2,1)}, bf16[4,96,24,128]{3,2,1,0:T(8,128)(2,1)}, u32[]{:S(2)}, u32[]{:S(2)}) collective-permute-start(bf16[4,96,24,128]{3,2,1,0:T(8,128)(2,1)} %pad_maximum_fusion.held), channel_id=1, source_target_pairs={{1,0},{0,1},{3,2},{2,3},{5,4},{4,5},{7,6},{6,7},{9,8},{8,9},{11,10... | collective-permute-start | bytes 7077896 | tf_op jit(solution)/shard_map/ppermute | solution.py:346
  148.0 45.3 %all-to-all-start.2 = ((bf16[96,4,896]{2,1,0:T(4,128)(2,1)}), bf16[96,4,896]{2,1,0:T(4,128)(2,1)S(1)}, u32[]{:S(2)}, u32[]{:S(2)}) async-start(bf16[96,4,896]{2,1,0:T(4,128)(2,1)} %get-tuple-element.26), calls=%async_computation.2 | async-start | bytes 1376256 | tf_op jit(solution)/shard_map/all_to_all | solution.py:360
  194.9 17.5 %all-to-all-start.3 = ((f32[8,8,128]{2,1,0:T(8,128)}), f32[8,8,128]{2,1,0:T(8,128)S(1)}, u32[]{:S(2)}, u32[]{:S(2)}) async-start(f32[8,8,128]{2,1,0:T(8,128)} %get-tuple-element.27), calls=%async_computation.3 | async-start | bytes 65536 | tf_op jit(solution)/shard_map/all_to_all | solution.py:419
Sparse Core Ops, SparseCore 0:
  27.6 95.1 all-gather.2

commit v6 on v4

--- a/solution.py
+++ b/solution.py
@@ -21,6 +21,9 @@
 
 def cost(flops, nbytes):
     return pl.CostEstimate(flops=flops, bytes_accessed=nbytes, transcendentals=0)
+
+
+LONG = cost(1 << 35, 1 << 26)
 
 
 def coded(value):
@@ -59,6 +62,10 @@
     out[...] = jnp.broadcast_to(packed[None], out.shape)
 
 
+def hold_kernel(masters, packed, out):
+    pass
+
+
 def unpacked(packed, used):
     free = 128 - used
     parts = used // free
@@ -69,26 +76,16 @@
     return jnp.concatenate([wide, tail], axis=1)
 
 
-def proj_kernel(used, parts, packed, saved_inputs, out_cotangent, out, near_inputs, near_cotangent, arrived):
-    width = saved_inputs.shape[1] // parts
-    count = packed.shape[0] // parts
-    pairs = ((saved_inputs, near_inputs), (out_cotangent, near_cotangent))
-    spans = [pl.ds(i * width, width) for i in range(parts)]
-    copies = [
-        [pltpu.make_async_copy(x.at[:, at], y.at[:, at], arrived.at[i, k]) for k, (x, y) in enumerate(pairs)]
-        for i, at in enumerate(spans)
-    ]
-    for pair in copies:
-        for copy in pair:
-            copy.start()
-    sums = [0.0, 0.0]
-    for i, at in enumerate(spans):
-        factors = unpacked(packed[i * count : (i + 1) * count], used).reshape(width, 128).astype(bf16)
-        for k, (_, near) in enumerate(pairs):
-            copies[i][k].wait()
-            sums[k] = sums[k] + jnp.dot(near[:, at], factors, preferred_element_type=f32)
-    lane = lax.broadcasted_iota(jnp.int32, sums[0].shape, 1)
-    out[...] = jnp.where(lane < used // 2, sums[0], sums[1]).T[:used].astype(bf16)
+def proj_kernel(used, packed, saved_inputs, out_cotangent, out, factors):
+    own = factors.shape[0] // packed.shape[0]
+    step = 8
+    for i in range(0, packed.shape[0], step):
+        block = unpacked(packed[i : i + step], used).reshape(step * own, 128)
+        factors[i * own : (i + step) * own] = block.astype(bf16)
+    left = jnp.dot(saved_inputs[...], factors[...], preferred_element_type=f32)
+    right = jnp.dot(out_cotangent[...], factors[...], preferred_element_type=f32)
+    lane = lax.broadcasted_iota(jnp.int32, left.shape, 1)
+    out[...] = jnp.where(lane < used // 2, left, right).T[:used].astype(bf16)
 
 
 def grad_kernel(rank_cols, proj, query_cotangent, attn_outputs, out):
@@ -183,15 +180,11 @@
     out_copy,
     query_new,
     out_new,
-    near_left,
-    near_right,
-    near_masters,
     near_query,
     near_out,
     near_own,
     near_master,
     near_new,
-    arrived,
     own_arrived,
     left_for,
     own_left_for,
@@ -202,15 +195,6 @@
     per = span // own
     parts = width // span
     spans = [pl.ds(i * span, span) for i in range(parts)]
-    copies = []
-    for i, at in enumerate(spans):
-        held = pl.ds(i * per, per)
-        ways = (
-            (left.at[at], near_left.at[at]),
-            (masters.at[held], near_masters.at[held]),
-            (right.at[:, at], near_right.at[:, at]),
-        )
-        copies.append([pltpu.make_async_copy(x, y, arrived.at[i, k]) for k, (x, y) in enumerate(ways)])
     ways = (
         (own_left, near_own.at[0]),
         (own_right, near_own.at[1]),
@@ -218,7 +202,7 @@
         (out_master, near_master.at[1]),
     )
     own_copies = [pltpu.make_async_copy(x, y, own_arrived.at[k]) for k, (x, y) in enumerate(ways)]
-    for copy in [c for part in copies for c in part] + own_copies:
+    for copy in own_copies:
         copy.start()
 
     sums = jnp.sum(squares[...], axis=0)[:1]
@@ -230,15 +214,13 @@
 
     sent = []
     for i, at in enumerate(spans):
-        for copy in copies[i]:
-            copy.wait()
-        codes = near_masters[i * per : (i + 1) * per]
-        moved = jnp.dot(near_left[at], first[...], preferred_element_type=f32)
+        codes = masters[i * per : (i + 1) * per]
+        moved = jnp.dot(left[at], first[...], preferred_element_type=f32)
         kept = decoded(codes[:, :own].reshape(span, cols).astype(f32))
         near_query[at] = (kept - scales[0] * moved).astype(bf16)
         sent.append(pltpu.make_async_copy(near_query.at[at], query_copy.at[at], left_for.at[i, 0]))
         sent[-1].start()
-        moved = jnp.dot(second_turned[...], near_right[:, at], preferred_element_type=f32)
+        moved = jnp.dot(second_turned[...], right[:, at], preferred_element_type=f32)
         kept = decoded(turned(codes[:, own:].reshape(span, cols)))
         near_out[:, at] = (kept - scales[1] * moved).astype(bf16)
         sent.append(pltpu.make_async_copy(near_out.at[:, at], out_copy.at[:, at], left_for.at[i, 1]))
@@ -284,27 +266,32 @@
     place = jnp.stack([lax.axis_index(FS), lax.axis_index("tp")]).astype(jnp.int32)
     packed, masters = pl.pallas_call(
         send_kernel,
-        out_shape=(
-            jax.ShapeDtypeStruct((fs, kept, 128), bf16),
-            pltpu.HBM((2 * own, cols), bf16),
-        ),
+        out_shape=(jax.ShapeDtypeStruct((fs, kept, 128), bf16), pltpu.HBM((2 * own, cols), bf16)),
         in_specs=[pl.BlockSpec()] * 4,
         out_specs=(VMEM, VMEM),
         compiler_params=SMALL,
         cost_estimate=cost(1 << 16, 1 << 20),
     )(far(left_factor), far(right_factor), far(query_master), far(out_master.T))
+    packed = pl.pallas_call(
+        hold_kernel,
+        out_shape=jax.ShapeDtypeStruct(packed.shape, bf16),
+        in_specs=[ANY, ANY],
+        out_specs=ANY,
+        input_output_aliases={1: 0},
+        compiler_params=SMALL,
+        cost_estimate=LONG,
+    )(far(masters), packed)
     masters = lax.all_gather(masters, FS)
     packed = lax.all_to_all(packed, FS, 0, 0)
-    parts = 6
     proj = pl.pallas_call(
-        functools.partial(proj_kernel, used, parts),
+        functools.partial(proj_kernel, used),
         out_shape=jax.ShapeDtypeStruct((used, tokens), bf16),
-        in_specs=[VMEM, ANY, ANY],
+        in_specs=[VMEM] * 3,
         out_specs=VMEM,
-        scratch_shapes=[pltpu.VMEM((tokens, width), bf16)] * 2 + [pltpu.SemaphoreType.DMA((parts, 2))],
+        scratch_shapes=[pltpu.VMEM((width, 128), bf16)],
         compiler_params=SMALL,
         cost_estimate=cost(4 * tokens * width * 128, 8 << 20),
-    )(packed, far(saved_inputs), far(out_cotangent))
+    )(packed, saved_inputs, out_cotangent)
     proj = lax.all_gather(proj, "tp", axis=0, tiled=True)
 
     partial = pl.pallas_call(
@@ -364,6 +351,7 @@
         cost_estimate=cost(1 << 30, 30 << 20),
     )(place, far(held), far(other))
 
+    low, masters = lax.optimization_barrier((low, masters))
     squares, first, second, second_turned = pl.pallas_call(
         functools.partial(sums_kernel, rank_cols),
         out_shape=(
@@ -373,9 +361,9 @@
             jax.ShapeDtypeStruct((cols, ranks), bf16),
         ),
         in_specs=[SMEM, VMEM],
-        out_specs=(VMEM, VMEM, VMEM, VMEM),
-        compiler_params=SMALL,
-        cost_estimate=cost(1 << 16, 1 << 16),
+        out_specs=(VMEM,) * 4,
+        compiler_params=SMALL,
+        cost_estimate=LONG,
     )(place, low)
     squares = lax.all_to_all(squares, "tp", 0, 0)
 
@@ -388,18 +376,14 @@
             pltpu.HBM((own, cols), f32),
             pltpu.HBM((own, cols), f32),
         ),
-        in_specs=[VMEM] * 4 + [ANY] * 7,
+        in_specs=[VMEM] * 7 + [ANY] * 4,
         out_specs=(ANY,) * 4,
         scratch_shapes=[
-            pltpu.VMEM((width, ranks), bf16),
-            pltpu.VMEM((ranks, width), bf16),
-            pltpu.VMEM(masters.shape, bf16),
             pltpu.VMEM((width, cols), bf16),
             pltpu.VMEM((cols, width), bf16),
             pltpu.VMEM((2, own, ranks), bf16),
             pltpu.VMEM((2, own, cols), f32),
             pltpu.VMEM((2, own, cols), f32),
-            pltpu.SemaphoreType.DMA((parts, 3)),
             pltpu.SemaphoreType.DMA((4,)),
             pltpu.SemaphoreType.DMA((parts, 2)),
             pltpu.SemaphoreType.DMA((2,)),
@@ -411,9 +395,9 @@
         first,
         second,
         second_turned,
-        far(left),
-        far(right),
-        far(masters),
+        left,
+        right,
+        masters,
         far(own_left),
         far(own_right),
         far(query_master),

time: 209 us -> 203 us (0.971)
  blocking collectives: 67.9 us -> 103 us
  waiting for transfers between devices: 55 us -> 24.9 us
  starting transfers between devices: 39.4 us -> 28.1 us
  Pallas kernels: 30.2 us -> 24.4 us
  local copies, waits for them, and re-layouts: 0.01 us -> 5.69 us
    all_to_all x0 -> x1, blocking collectives: none -> 34.4 us  [body(): pieces = lax.all_to_all(partial.reshape(fs, 2 * rows, cols), FS, 0, 0)]
    all_to_all x1, waiting for transfers between devices: 31.4 us -> 0.01 us  [body(): low = lax.all_to_all(low, FS, 0, 0)]
    all_to_all x1, starting transfers between devices: 15 us -> 8.04 us  [body(): low = lax.all_to_all(low, FS, 0, 0)]
    all_to_all x1 -> x0, starting transfers between devices: 5.95 us -> none  [body(): pieces = lax.all_to_all(partial.reshape(fs, 2 * rows, cols), FS, 0, 0)]
    unnamed x8 -> x18, local copies, waits for them, and re-layouts: 0.01 us -> 5.69 us
    pallas_call x1 -> x2, Pallas kernels: 5.42 us -> 1.96 us  [the longest x1 1.96 us: body(): pl.pallas_call(functools.partial(proj_kernel, used), out_shape=jax.ShapeD...]
    pallas_call x1, Pallas kernels: 9.7 us -> 7.38 us  [body(): pl.pallas_call(functools.partial(final_kernel, float(rows * fs * cols * t...]
  transfers between devices with their start and end apart: 8 -> 7, of which waited for: 4 -> 4; matrix products, arithmetic and copies ran while one was open for 1% -> 1% of each run, Pallas kernels for 9% -> 8%
where the time goes in v6:
time: 203 us; the launch traced here: 202 us
  blocking collectives  103 us (51%)
  starting transfers between devices  28.1 us (14%)
  waiting for transfers between devices  24.9 us (12%)
  Pallas kernels  24.4 us (12%)
  between operations  14.2 us (7%)
  local copies, waits for them, and re-layouts  5.69 us (3%)
    all_to_all x1, blocking collectives, body(): packed = lax.all_to_all(packed, FS, 0, 0)  50.2 us
    all_to_all x1, blocking collectives, body(): pieces = lax.all_to_all(partial.reshape(fs, 2 * rows, cols), FS, 0, 0)  34.4 us
    ppermute x3, waiting for transfers between devices, body(): lax.ppermute(packed, 'tp', [((t + 2 * step) % tp, t) for t in range(tp)])  23.4 us
    all_gather x1, blocking collectives, body(): proj = lax.all_gather(proj, 'tp', axis=0, tiled=True)  18.1 us
    pallas_call x1, Pallas kernels, body(): pl.pallas_call(functools.partial(prep_kernel, rank_cols), grid=(width //...  9.32 us
    ppermute x3, starting transfers between devices, body(): lax.ppermute(packed, 'tp', [((t + 2 * step) % tp, t) for t in range(tp)])  8.98 us
    all_to_all x1, starting transfers between devices, body(): low = lax.all_to_all(low, FS, 0, 0)  8.04 us
    all_to_all x1, starting transfers between devices, body(): squares = lax.all_to_all(squares, 'tp', 0, 0)  7.57 us
  transfers between devices with their start and end apart: 7, of which 4 were waited for; matrix products, arithmetic and copies ran while one was open for 1% of the time, Pallas kernels for 8%

profile of v6, /device:TPU:1, one launch (start us, length us, event | category | flops | bytes accessed | tf_op | source)
XLA Modules:
  0.0 201.7 jit_solution(9208887698746375169)
XLA Ops:
  7.2 0.0 all-gather.3.cloned.1.call-start
  7.2 1.6 shard_map.145
  8.8 0.0 all-gather.3.cloned.1.call-update
  8.9 0.0 copy-start.1
  8.9 0.0 copy-start.2
  8.9 50.2 %all_to_all.20.packed = bf16[96,24,128]{2,1,0:T(8,128)(2,1)S(1)} all-to-all(bf16[96,24,128]{2,1,0:T(8,128)(2,1)S(1)} %shard_map.146), channel_id=1, replica_groups=mesh['z'=12,'y'=8,'tp'=8] {'z','y'}, dimensions={0} | all-to-all | bytes 1179648 | tf_op jit(solution)/shard_map/all_to_all | solution.py:285
  59.1 0.0 copy-done.1
  59.1 0.0 copy-done.2
  59.1 0.0 copy-start.5
  59.1 0.0 copy-start.6
  59.1 2.0 shard_map.147
  61.1 0.0 copy-start.7
  61.1 0.0 copy-start.8
  61.1 18.1 %all_gather.9.proj = bf16[768,512]{1,0:T(8,128)(2,1)S(1)} all-gather(bf16[96,512]{1,0:T(8,128)(2,1)S(1)} %shard_map.147), channel_id=1, replica_groups=mesh['z'=12,'y'=8,'tp'=8] {'tp'}, dimensions={0}, use_global_device_ids=true | all-gather | bytes 884736 | tf_op jit(solution)/shard_map/all_gather | solution.py:295
  79.2 0.0 copy-done.5
  79.2 0.0 copy-done.6
  79.2 1.4 shard_map.148
  80.6 34.4 %all_to_all.21.pieces = bf16[96,8,384]{2,1,0:T(8,128)(2,1)S(1)} all-to-all(bf16[96,8,384]{2,1,0:T(8,128)(2,1)} %bitcast.12), channel_id=1, replica_groups=mesh['z'=12,'y'=8,'tp'=8] {'z','y'}, dimensions={0} | all-to-all | bytes 1179648 | tf_op jit(solution)/shard_map/all_to_all | solution.py:305
  115.0 0.0 copy-done.7
  115.0 0.0 copy-done.8
  115.0 1.1 shard_map.149
  116.1 8.0 %all-to-all-start.2 = ((bf16[96,4,896]{2,1,0:T(4,128)(2,1)}), bf16[96,4,896]{2,1,0:T(4,128)(2,1)S(1)}, u32[]{:S(2)}, u32[]{:S(2)}) async-start(bf16[96,4,896]{2,1,0:T(4,128)(2,1)} %get-tuple-element.27), calls=%async_computation.2 | async-start | bytes 1376256 | tf_op jit(solution)/shard_map/all_to_all | solution.py:325
  124.1 2.8 %collective-permute-start.2 = (bf16[96,24,128]{2,1,0:T(8,128)(2,1)S(1)}, bf16[96,24,128]{2,1,0:T(8,128)(2,1)S(1)}, u32[]{:S(2)}, u32[]{:S(2)}) collective-permute-start(bf16[96,24,128]{2,1,0:T(8,128)(2,1)S(1)} %all_to_all.20.packed), channel_id=1, source_target_pairs={{6,0},{7,1},{0,2},{1,3},{2,4},{3,5},{4,6},{5,7},{14,8},{15,9},{8,1... | collective-permute-start | bytes 1769480 | tf_op jit(solution)/shard_map/ppermute | solution.py:309
  126.9 4.3 %collective-permute-start.1 = (bf16[96,24,128]{2,1,0:T(8,128)(2,1)S(1)}, bf16[96,24,128]{2,1,0:T(8,128)(2,1)S(1)}, u32[]{:S(2)}, u32[]{:S(2)}) collective-permute-start(bf16[96,24,128]{2,1,0:T(8,128)(2,1)S(1)} %all_to_all.20.packed), channel_id=1, source_target_pairs={{4,0},{5,1},{6,2},{7,3},{0,4},{1,5},{2,6},{3,7},{12,8},{13,9},{14,... | collective-permute-start | bytes 1769480 | tf_op jit(solution)/shard_map/ppermute | solution.py:309
  131.2 1.9 collective-permute-start
  133.1 0.1 pad_add_fusion.place
  133.2 7.3 %collective-permute-done.2 = bf16[96,24,128]{2,1,0:T(8,128)(2,1)S(1)} collective-permute-done((bf16[96,24,128]{2,1,0:T(8,128)(2,1)S(1)}, bf16[96,24,128]{2,1,0:T(8,128)(2,1)S(1)}, u32[]{:S(2)}, u32[]{:S(2)}) %collective-permute-start.2) | collective-permute-done | bytes 589856 | tf_op jit(solution)/shard_map/ppermute | solution.py:309
  140.6 13.0 %collective-permute-done.1 = bf16[96,24,128]{2,1,0:T(8,128)(2,1)S(1)} collective-permute-done((bf16[96,24,128]{2,1,0:T(8,128)(2,1)S(1)}, bf16[96,24,128]{2,1,0:T(8,128)(2,1)S(1)}, u32[]{:S(2)}, u32[]{:S(2)}) %collective-permute-start.1) | collective-permute-done | bytes 589856 | tf_op jit(solution)/shard_map/ppermute | solution.py:309
  153.6 3.0 %collective-permute-done = bf16[96,24,128]{2,1,0:T(8,128)(2,1)S(1)} collective-permute-done((bf16[96,24,128]{2,1,0:T(8,128)(2,1)S(1)}, bf16[96,24,128]{2,1,0:T(8,128)(2,1)S(1)}, u32[]{:S(2)}, u32[]{:S(2)}) %collective-permute-start) | collective-permute-done | bytes 589856 | tf_op jit(solution)/shard_map/ppermute | solution.py:309
  156.6 1.7 pad_maximum_fusion.held
  158.3 3.5 %collective-permute-start.3 = (bf16[4,96,24,128]{3,2,1,0:T(8,128)(2,1)}, bf16[4,96,24,128]{3,2,1,0:T(8,128)(2,1)}, u32[]{:S(2)}, u32[]{:S(2)}) collective-permute-start(bf16[4,96,24,128]{3,2,1,0:T(8,128)(2,1)} %pad_maximum_fusion.held), channel_id=1, source_target_pairs={{1,0},{0,1},{3,2},{2,3},{5,4},{4,5},{7,6},{6,7},{9,8},{8,9},{11,10... | collective-permute-start | bytes 7077896 | tf_op jit(solution)/shard_map/ppermute | solution.py:311
  161.8 0.0 all-to-all-done.2.low
  161.8 1.5 all-gather.3.cloned.1.call-done
  163.3 1.6 shard_map.150
  164.9 7.6 %all-to-all-start.3 = ((f32[8,8,128]{2,1,0:T(8,128)}), f32[8,8,128]{2,1,0:T(8,128)S(1)}, u32[]{:S(2)}, u32[]{:S(2)}) async-start(f32[8,8,128]{2,1,0:T(8,128)} %get-tuple-element.29), calls=%async_computation.3 | async-start | bytes 65536 | tf_op jit(solution)/shard_map/all_to_all | solution.py:368
  172.5 0.0 collective-permute-done.3.other
  172.5 9.3 %shard_map.151 = (bf16[3072,384]{1,0:T(8,128)(2,1)}, bf16[384,3072]{1,0:T(8,128)(2,1)}, bf16[32,384]{1,0:T(8,128)(2,1)}, bf16[32,384]{1,0:T(8,128)(2,1)}) custom-call(s32[2]{0:T(128)S(1)} %pad_add_fusion.place, bf16[4,96,24,128]{3,2,1,0:T(8,128)(2,1)} %pad_maximum_fusion.held, bf16[4,96,24,128]{3,2,1,0:T(8,128)(2,1)} %collective-permute-done.3.other), custom_call_target="tpu_custom_call" | custom-call | flops 1073741824 | bytes 31457280 | tf_op jit(solution)/shard_map/pallas_call | solution.py:329
  181.8 0.0 all-to-all-done.3.squares
  181.8 0.0 copy-start
  181.8 2.3 %copy-done = bf16[6144,384]{1,0:T(8,128)(2,1)S(1)} copy-done((bf16[6144,384]{1,0:T(8,128)(2,1)S(1)}, bf16[6144,384]{1,0:T(8,128)(2,1)}, u32[]{:S(2)}) %copy-start) | copy-done | bytes 4718616
  184.1 0.0 copy-start.3
  184.1 1.7 copy-done.3
  185.8 0.0 copy-start.4
  185.8 1.7 copy-done.4
  187.5 7.4 %shard_map.152 = (bf16[3072,384]{1,0:T(8,128)(2,1)}, bf16[384,3072]{1,0:T(8,128)(2,1)}, f32[32,384]{1,0:T(8,128)}, f32[32,384]{1,0:T(8,128)}) custom-call(f32[8,8,128]{2,1,0:T(8,128)S(1)} %all-to-all-done.3.squares, bf16[384,384]{1,0:T(8,128)(2,1)S(1)} %get-tuple-element.30.first, bf16[384,384]{1,0:T(8,128)(2,1)S(1)} %get-tuple-element.31.second, ...), custom_call_target="tpu_custom_call" | custom-call | flops 1811939328 | bytes 20971520 | tf_op jit(solution)/shard_map/pallas_call | solution.py:371
  (1 shorter events, 0.0 us)
Async XLA Ops:
  7.2 156.1 %all-gather.3.cloned.1.call-start = ((), (), s32[]{:S(2)}) async-start(), calls=%async_computation.4 | async-start | bytes 4767744 | tf_op jit(solution)/shard_map/all_gather | solution.py:284
  8.9 50.2 %copy-start.1 = (bf16[512,3072]{1,0:T(8,128)(2,1)S(1)}, bf16[512,3072]{1,0:T(8,128)(2,1)}, u32[]{:S(2)}) copy-start(bf16[512,3072]{1,0:T(8,128)(2,1)} %saved_inputs.1) | copy-start | bytes 9437188
  8.9 50.2 %copy-start.2 = (bf16[512,3072]{1,0:T(8,128)(2,1)S(1)}, bf16[512,3072]{1,0:T(8,128)(2,1)}, u32[]{:S(2)}) copy-start(bf16[512,3072]{1,0:T(8,128)(2,1)} %out_cotangent.1) | copy-start | bytes 9437188
  59.1 20.1 %copy-start.5 = (bf16[512,384]{1,0:T(8,128)(2,1)S(1)}, bf16[512,384]{1,0:T(8,128)(2,1)}, u32[]{:S(2)}) copy-start(bf16[512,384]{1,0:T(8,128)(2,1)} %query_cotangent.1) | copy-start | bytes 1179652
  59.1 20.1 %copy-start.6 = (bf16[512,384]{1,0:T(8,128)(2,1)S(1)}, bf16[512,384]{1,0:T(8,128)(2,1)}, u32[]{:S(2)}) copy-start(bf16[512,384]{1,0:T(8,128)(2,1)} %attn_outputs.1) | copy-start | bytes 1179652
  61.1 53.9 %copy-start.7 = (f32[2,4,384]{2,1,0:T(4,128)S(1)}, f32[2,4,384]{2,1,0:T(4,128)}, u32[]{:S(2)}) copy-start(f32[2,4,384]{2,1,0:T(4,128)} %first.1) | copy-start | bytes 36868
  61.1 53.9 %copy-start.8 = (f32[2,4,384]{2,1,0:T(4,128)S(1)}, f32[2,4,384]{2,1,0:T(4,128)}, u32[]{:S(2)}) copy-start(f32[2,4,384]{2,1,0:T(4,128)} %second.1) | copy-start | bytes 36868
  116.1 45.7 %all-to-all-start.2 = ((bf16[96,4,896]{2,1,0:T(4,128)(2,1)}), bf16[96,4,896]{2,1,0:T(4,128)(2,1)S(1)}, u32[]{:S(2)}, u32[]{:S(2)}) async-start(bf16[96,4,896]{2,1,0:T(4,128)(2,1)} %get-tuple-element.27), calls=%async_computation.2 | async-start | bytes 1376256 | tf_op jit(solution)/shard_map/all_to_all | solution.py:325
  124.1 16.4 %collective-permute-start.2 = (bf16[96,24,128]{2,1,0:T(8,128)(2,1)S(1)}, bf16[96,24,128]{2,1,0:T(8,128)(2,1)S(1)}, u32[]{:S(2)}, u32[]{:S(2)}) collective-permute-start(bf16[96,24,128]{2,1,0:T(8,128)(2,1)S(1)} %all_to_all.20.packed), channel_id=1, source_target_pairs={{6,0},{7,1},{0,2},{1,3},{2,4},{3,5},{4,6},{5,7},{14,8},{15,9},{8,1... | collective-permute-start | bytes 1769480 | tf_op jit(solution)/shard_map/ppermute | solution.py:309
  126.9 26.7 %collective-permute-start.1 = (bf16[96,24,128]{2,1,0:T(8,128)(2,1)S(1)}, bf16[96,24,128]{2,1,0:T(8,128)(2,1)S(1)}, u32[]{:S(2)}, u32[]{:S(2)}) collective-permute-start(bf16[96,24,128]{2,1,0:T(8,128)(2,1)S(1)} %all_to_all.20.packed), channel_id=1, source_target_pairs={{4,0},{5,1},{6,2},{7,3},{0,4},{1,5},{2,6},{3,7},{12,8},{13,9},{14,... | collective-permute-start | bytes 1769480 | tf_op jit(solution)/shard_map/ppermute | solution.py:309
  131.2 25.4 %collective-permute-start = (bf16[96,24,128]{2,1,0:T(8,128)(2,1)S(1)}, bf16[96,24,128]{2,1,0:T(8,128)(2,1)S(1)}, u32[]{:S(2)}, u32[]{:S(2)}) collective-permute-start(bf16[96,24,128]{2,1,0:T(8,128)(2,1)S(1)} %all_to_all.20.packed), channel_id=1, source_target_pairs={{2,0},{3,1},{4,2},{5,3},{6,4},{7,5},{0,6},{1,7},{10,8},{11,9},{12,... | collective-permute-start | bytes 1769480 | tf_op jit(solution)/shard_map/ppermute | solution.py:309
  158.3 14.2 %collective-permute-start.3 = (bf16[4,96,24,128]{3,2,1,0:T(8,128)(2,1)}, bf16[4,96,24,128]{3,2,1,0:T(8,128)(2,1)}, u32[]{:S(2)}, u32[]{:S(2)}) collective-permute-start(bf16[4,96,24,128]{3,2,1,0:T(8,128)(2,1)} %pad_maximum_fusion.held), channel_id=1, source_target_pairs={{1,0},{0,1},{3,2},{2,3},{5,4},{4,5},{7,6},{6,7},{9,8},{8,9},{11,10... | collective-permute-start | bytes 7077896 | tf_op jit(solution)/shard_map/ppermute | solution.py:311
  164.9 16.9 %all-to-all-start.3 = ((f32[8,8,128]{2,1,0:T(8,128)}), f32[8,8,128]{2,1,0:T(8,128)S(1)}, u32[]{:S(2)}, u32[]{:S(2)}) async-start(f32[8,8,128]{2,1,0:T(8,128)} %get-tuple-element.29), calls=%async_computation.3 | async-start | bytes 65536 | tf_op jit(solution)/shard_map/all_to_all | solution.py:368
  181.8 2.3 %copy-start = (bf16[6144,384]{1,0:T(8,128)(2,1)S(1)}, bf16[6144,384]{1,0:T(8,128)(2,1)}, u32[]{:S(2)}) copy-start(bf16[6144,384]{1,0:T(8,128)(2,1)} %all-gather.3.cloned.1.call-done) | copy-start | bytes 14155780
  184.1 1.7 copy-start.3
  185.8 1.7 copy-start.4
Sparse Core Ops, SparseCore 0:
  12.3 150.9 all-gather.2

commit v7 on v6

--- a/solution.py
+++ b/solution.py
@@ -15,7 +15,7 @@
 VMEM = pl.BlockSpec(memory_space=pltpu.VMEM)
 ANY = pl.BlockSpec(memory_space=pl.ANY)
 SMEM = pl.BlockSpec(memory_space=pltpu.SMEM)
-REACH = 2.0**19
+REACH = 2.0**34
 SMALL = pltpu.CompilerParams(vmem_limit_bytes=16 << 20)
 
 
@@ -27,25 +27,16 @@
 
 
 def coded(value):
-    size = jnp.abs(value) * REACH
-    size = size * size
+    size = value * REACH
     size = size * size
     size = size * size
     return jnp.where(value < 0.0, -size, size).astype(bf16)
 
 
 def decoded(code):
-    size = jnp.abs(code)
-    fourth = lax.rsqrt(lax.rsqrt(size))
-    eighth = fourth * lax.rsqrt(lax.rsqrt(lax.rsqrt(size))) * (1.0 / REACH)
-    return jnp.where(code == 0.0, 0.0, jnp.where(code < 0.0, -eighth, eighth))
-
-
-def turned(value):
-    n = value.shape[1]
-    row = lax.broadcasted_iota(jnp.int32, (n, n), 0)
-    eye = (row == lax.broadcasted_iota(jnp.int32, (n, n), 1)).astype(f32).astype(bf16)
-    return lax.dot_general(eye, value, (((1,), (1,)), ((), ())), preferred_element_type=f32)
+    wide = code.astype(f32)
+    size = lax.rsqrt(lax.rsqrt(jnp.abs(wide))) * (1.0 / REACH)
+    return jnp.where(wide < 0.0, -size, size)
 
 
 def send_kernel(left, right, query_master, out_master, out, masters):
@@ -134,7 +125,7 @@
                 sides[k].append(block[:, k * rank_cols : (k + 1) * rank_cols])
     both = [jnp.concatenate(side, axis=1).astype(bf16) for side in sides]
     left[...] = both[0]
-    right[...] = turned(both[1]).astype(bf16)
+    right[...] = both[1].T
 
     @pl.when(pl.program_id(0) == place[0] // (span // own))
     def _():
@@ -144,31 +135,18 @@
             out[...] = tile[rows]
 
 
-def sums_kernel(rank_cols, place, low, squares, first, second, second_turned):
-    tp = squares.shape[0]
-    cols = first.shape[1]
-    per_block = rank_cols // low.shape[1]
+def sums_kernel(low, squares):
     sums = jnp.sum(low[:, :, -128:].astype(f32), axis=0)[:1]
     squares[...] = jnp.broadcast_to(sums[None], squares.shape)
-    for b in range(tp):
-        chip, core = b % (tp // 2), b // (tp // 2)
-        at = (place[1] + 2 * chip) % tp
-        at = at + core * (1 - 2 * (at % 2))
-        block = low[pl.ds(at * per_block, per_block)].astype(f32)
-        for k, out in enumerate((first, second)):
-            part = block[:, :, k * cols : (k + 1) * cols]
-            part = jnp.concatenate([part[j] for j in range(per_block)], axis=0)
-            out[b * rank_cols : (b + 1) * rank_cols] = part.astype(bf16)
-    second_turned[...] = turned(second[...]).astype(bf16)
 
 
 def final_kernel(
     entries,
     span,
+    rank_cols,
+    place,
     squares,
-    first,
-    second,
-    second_turned,
+    low,
     left,
     right,
     masters,
@@ -180,11 +158,17 @@
     out_copy,
     query_new,
     out_new,
+    near_left,
+    near_right,
+    near_masters,
     near_query,
     near_out,
     near_own,
     near_master,
     near_new,
+    first,
+    second,
+    arrived,
     own_arrived,
     left_for,
     own_left_for,
@@ -195,6 +179,15 @@
     per = span // own
     parts = width // span
     spans = [pl.ds(i * span, span) for i in range(parts)]
+    copies = []
+    for i, at in enumerate(spans):
+        held = pl.ds(i * per, per)
+        ways = (
+            (left.at[at], near_left.at[at]),
+            (masters.at[held], near_masters.at[held]),
+            (right.at[:, at], near_right.at[:, at]),
+        )
+        copies.append([pltpu.make_async_copy(x, y, arrived.at[i, k]) for k, (x, y) in enumerate(ways)])
     ways = (
         (own_left, near_own.at[0]),
         (own_right, near_own.at[1]),
@@ -202,10 +195,23 @@
         (out_master, near_master.at[1]),
     )
     own_copies = [pltpu.make_async_copy(x, y, own_arrived.at[k]) for k, (x, y) in enumerate(ways)]
-    for copy in own_copies:
+    for copy in [c for part in copies for c in part] + own_copies:
         copy.start()
 
-    sums = jnp.sum(squares[...], axis=0)[:1]
+    tp = squares.shape[0]
+    per_block = rank_cols // low.shape[1]
+    for b in range(tp):
+        chip, core = b % (tp // 2), b // (tp // 2)
+        at = (place[1] + 2 * chip) % tp
+        at = at + core * (1 - 2 * (at % 2))
+        block = low[pl.ds(at * per_block, per_block)].astype(f32)
+        for k, step in enumerate((first, second)):
+            part = block[:, :, k * cols : (k + 1) * cols]
+            part = jnp.concatenate([part[j] for j in range(per_block)], axis=0)
+            step[b * rank_cols : (b + 1) * rank_cols] = part.astype(bf16)
+    second_turned = second[...].T
+
+    sums = jnp.sum(squares[...], axis=0)
     lane = lax.broadcasted_iota(jnp.int32, sums.shape, 1)
     scales = []
     for k in range(2):
@@ -214,14 +220,16 @@
 
     sent = []
     for i, at in enumerate(spans):
-        codes = masters[i * per : (i + 1) * per]
-        moved = jnp.dot(left[at], first[...], preferred_element_type=f32)
-        kept = decoded(codes[:, :own].reshape(span, cols).astype(f32))
+        for copy in copies[i]:
+            copy.wait()
+        codes = near_masters[i * per : (i + 1) * per]
+        moved = jnp.dot(near_left[at], first[...], preferred_element_type=f32)
+        kept = decoded(codes[:, :own].reshape(span, cols))
         near_query[at] = (kept - scales[0] * moved).astype(bf16)
         sent.append(pltpu.make_async_copy(near_query.at[at], query_copy.at[at], left_for.at[i, 0]))
         sent[-1].start()
-        moved = jnp.dot(second_turned[...], right[:, at], preferred_element_type=f32)
-        kept = decoded(turned(codes[:, own:].reshape(span, cols)))
+        moved = jnp.dot(second_turned, near_right[:, at], preferred_element_type=f32)
+        kept = decoded(codes[:, own:].reshape(span, cols).T)
         near_out[:, at] = (kept - scales[1] * moved).astype(bf16)
         sent.append(pltpu.make_async_copy(near_out.at[:, at], out_copy.at[:, at], left_for.at[i, 1]))
         sent[-1].start()
@@ -351,39 +359,39 @@
         cost_estimate=cost(1 << 30, 30 << 20),
     )(place, far(held), far(other))
 
-    low, masters = lax.optimization_barrier((low, masters))
-    squares, first, second, second_turned = pl.pallas_call(
-        functools.partial(sums_kernel, rank_cols),
-        out_shape=(
-            jax.ShapeDtypeStruct((tp, 8, 128), f32),
-            jax.ShapeDtypeStruct((ranks, cols), bf16),
-            jax.ShapeDtypeStruct((ranks, cols), bf16),
-            jax.ShapeDtypeStruct((cols, ranks), bf16),
-        ),
-        in_specs=[SMEM, VMEM],
-        out_specs=(VMEM,) * 4,
+    squares = pl.pallas_call(
+        sums_kernel,
+        out_shape=jax.ShapeDtypeStruct((tp, 1, 128), f32),
+        in_specs=[VMEM],
+        out_specs=VMEM,
         compiler_params=SMALL,
         cost_estimate=LONG,
-    )(place, low)
+    )(low)
     squares = lax.all_to_all(squares, "tp", 0, 0)
 
     parts = width // span
     query_copy, out_copy, query_new, out_new = pl.pallas_call(
-        functools.partial(final_kernel, float(rows * fs * cols * tp), span),
+        functools.partial(final_kernel, float(rows * fs * cols * tp), span, rank_cols),
         out_shape=(
             pltpu.HBM((width, cols), bf16),
             pltpu.HBM((cols, width), bf16),
             pltpu.HBM((own, cols), f32),
             pltpu.HBM((own, cols), f32),
         ),
-        in_specs=[VMEM] * 7 + [ANY] * 4,
+        in_specs=[SMEM] + [VMEM] * 2 + [ANY] * 7,
         out_specs=(ANY,) * 4,
         scratch_shapes=[
+            pltpu.VMEM((width, ranks), bf16),
+            pltpu.VMEM((ranks, width), bf16),
+            pltpu.VMEM(masters.shape, bf16),
             pltpu.VMEM((width, cols), bf16),
             pltpu.VMEM((cols, width), bf16),
             pltpu.VMEM((2, own, ranks), bf16),
             pltpu.VMEM((2, own, cols), f32),
             pltpu.VMEM((2, own, cols), f32),
+            pltpu.VMEM((ranks, cols), bf16),
+            pltpu.VMEM((ranks, cols), bf16),
+            pltpu.SemaphoreType.DMA((parts, 3)),
             pltpu.SemaphoreType.DMA((4,)),
             pltpu.SemaphoreType.DMA((parts, 2)),
             pltpu.SemaphoreType.DMA((2,)),
@@ -391,13 +399,12 @@
         compiler_params=pltpu.CompilerParams(vmem_limit_bytes=32 << 20),
         cost_estimate=cost(4 * width * ranks * cols, 20 << 20),
     )(
+        place,
         squares,
-        first,
-        second,
-        second_turned,
-        left,
-        right,
-        masters,
+        low,
+        far(left),
+        far(right),
+        far(masters),
         far(own_left),
         far(own_right),
         far(query_master),

time: 203 us -> 193 us (0.951)
  local copies, waits for them, and re-layouts: 5.69 us -> 0.03 us
    unnamed x18 -> x12, local copies, waits for them, and re-layouts: 5.69 us -> 0.03 us
  transfers between devices with their start and end apart: 7 -> 7, of which waited for: 4 -> 3; matrix products, arithmetic and copies ran while one was open for 1% -> 1% of each run, Pallas kernels for 8% -> 7%
where the time goes in v7:
time: 193 us; the launch traced here: 192 us
  blocking collectives  103 us (53%)
  starting transfers between devices  26.3 us (14%)
  Pallas kernels  23.7 us (12%)
  waiting for transfers between devices  23.5 us (12%)
  between operations  14.2 us (7%)
    all_to_all x1, blocking collectives, body(): packed = lax.all_to_all(packed, FS, 0, 0)  50.2 us
    all_to_all x1, blocking collectives, body(): pieces = lax.all_to_all(partial.reshape(fs, 2 * rows, cols), FS, 0, 0)  34.4 us
    ppermute x3, waiting for transfers between devices, body(): lax.ppermute(packed, 'tp', [((t + 2 * step) % tp, t) for t in range(tp)])  23.4 us
    all_gather x1, blocking collectives, body(): proj = lax.all_gather(proj, 'tp', axis=0, tiled=True)  18.1 us
    ppermute x3, starting transfers between devices, body(): lax.ppermute(packed, 'tp', [((t + 2 * step) % tp, t) for t in range(tp)])  8.93 us
    pallas_call x1, Pallas kernels, body(): pl.pallas_call(functools.partial(prep_kernel, rank_cols), grid=(width //...  8.77 us
    pallas_call x1, Pallas kernels, body(): pl.pallas_call(functools.partial(final_kernel, float(rows * fs * cols * t...  8.11 us
    all_to_all x1, starting transfers between devices, body(): low = lax.all_to_all(low, FS, 0, 0)  8.04 us
  transfers between devices with their start and end apart: 7, of which 3 were waited for; matrix products, arithmetic and copies ran while one was open for 1% of the time, Pallas kernels for 7%

profile of v7, /device:TPU:1, one launch (start us, length us, event | category | flops | bytes accessed | tf_op | source)
XLA Modules:
  0.0 192.1 jit_solution(17693621456971867551)
XLA Ops:
  7.2 0.0 all-gather.3.cloned.1.call-start
  7.2 1.6 shard_map.145
  8.8 0.0 all-gather.3.cloned.1.call-update
  8.9 0.0 copy-start
  8.9 0.0 copy-start.1
  8.9 50.2 %all_to_all.20.packed = bf16[96,24,128]{2,1,0:T(8,128)(2,1)S(1)} all-to-all(bf16[96,24,128]{2,1,0:T(8,128)(2,1)S(1)} %shard_map.146), channel_id=1, replica_groups=mesh['z'=12,'y'=8,'tp'=8] {'z','y'}, dimensions={0} | all-to-all | bytes 1179648 | tf_op jit(solution)/shard_map/all_to_all | solution.py:293
  59.1 0.0 copy-done
  59.1 0.0 copy-done.1
  59.1 0.0 copy-start.2
  59.1 0.0 copy-start.3
  59.1 2.0 %shard_map.147 = bf16[96,512]{1,0:T(8,128)(2,1)S(1)} custom-call(bf16[96,24,128]{2,1,0:T(8,128)(2,1)S(1)} %all_to_all.20.packed, bf16[512,3072]{1,0:T(8,128)(2,1)S(1)} %copy-done, bf16[512,3072]{1,0:T(8,128)(2,1)S(1)} %copy-done.1), custom_call_target="tpu_custom_call" | custom-call | flops 805306368 | bytes 8388608 | tf_op jit(solution)/shard_map/pallas_call | solution.py:294
  61.0 0.0 copy-start.4
  61.1 0.0 copy-start.5
  61.1 18.1 %all_gather.9.proj = bf16[768,512]{1,0:T(8,128)(2,1)S(1)} all-gather(bf16[96,512]{1,0:T(8,128)(2,1)S(1)} %shard_map.147), channel_id=1, replica_groups=mesh['z'=12,'y'=8,'tp'=8] {'tp'}, dimensions={0}, use_global_device_ids=true | all-gather | bytes 884736 | tf_op jit(solution)/shard_map/all_gather | solution.py:303
  79.2 0.0 copy-done.2
  79.2 0.0 copy-done.3
  79.2 1.4 shard_map.148
  80.6 34.4 %all_to_all.21.pieces = bf16[96,8,384]{2,1,0:T(8,128)(2,1)S(1)} all-to-all(bf16[96,8,384]{2,1,0:T(8,128)(2,1)} %bitcast.12), channel_id=1, replica_groups=mesh['z'=12,'y'=8,'tp'=8] {'z','y'}, dimensions={0} | all-to-all | bytes 1179648 | tf_op jit(solution)/shard_map/all_to_all | solution.py:313
  115.0 0.0 copy-done.4
  115.0 0.0 copy-done.5
  115.0 1.1 shard_map.149
  116.1 8.0 %all-to-all-start.2 = ((bf16[96,4,896]{2,1,0:T(4,128)(2,1)}), bf16[96,4,896]{2,1,0:T(4,128)(2,1)S(1)}, u32[]{:S(2)}, u32[]{:S(2)}) async-start(bf16[96,4,896]{2,1,0:T(4,128)(2,1)} %get-tuple-element.21), calls=%async_computation.2 | async-start | bytes 1376256 | tf_op jit(solution)/shard_map/all_to_all | solution.py:333
  124.1 2.7 %collective-permute-start.2 = (bf16[96,24,128]{2,1,0:T(8,128)(2,1)S(1)}, bf16[96,24,128]{2,1,0:T(8,128)(2,1)S(1)}, u32[]{:S(2)}, u32[]{:S(2)}) collective-permute-start(bf16[96,24,128]{2,1,0:T(8,128)(2,1)S(1)} %all_to_all.20.packed), channel_id=1, source_target_pairs={{6,0},{7,1},{0,2},{1,3},{2,4},{3,5},{4,6},{5,7},{14,8},{15,9},{8,1... | collective-permute-start | bytes 1769480 | tf_op jit(solution)/shard_map/ppermute | solution.py:317
  126.9 4.3 %collective-permute-start.1 = (bf16[96,24,128]{2,1,0:T(8,128)(2,1)S(1)}, bf16[96,24,128]{2,1,0:T(8,128)(2,1)S(1)}, u32[]{:S(2)}, u32[]{:S(2)}) collective-permute-start(bf16[96,24,128]{2,1,0:T(8,128)(2,1)S(1)} %all_to_all.20.packed), channel_id=1, source_target_pairs={{4,0},{5,1},{6,2},{7,3},{0,4},{1,5},{2,6},{3,7},{12,8},{13,9},{14,... | collective-permute-start | bytes 1769480 | tf_op jit(solution)/shard_map/ppermute | solution.py:317
  131.1 1.9 %collective-permute-start = (bf16[96,24,128]{2,1,0:T(8,128)(2,1)S(1)}, bf16[96,24,128]{2,1,0:T(8,128)(2,1)S(1)}, u32[]{:S(2)}, u32[]{:S(2)}) collective-permute-start(bf16[96,24,128]{2,1,0:T(8,128)(2,1)S(1)} %all_to_all.20.packed), channel_id=1, source_target_pairs={{2,0},{3,1},{4,2},{5,3},{6,4},{7,5},{0,6},{1,7},{10,8},{11,9},{12,... | collective-permute-start | bytes 1769480 | tf_op jit(solution)/shard_map/ppermute | solution.py:317
  133.1 0.1 pad_add_fusion.place
  133.2 7.4 %collective-permute-done.2 = bf16[96,24,128]{2,1,0:T(8,128)(2,1)S(1)} collective-permute-done((bf16[96,24,128]{2,1,0:T(8,128)(2,1)S(1)}, bf16[96,24,128]{2,1,0:T(8,128)(2,1)S(1)}, u32[]{:S(2)}, u32[]{:S(2)}) %collective-permute-start.2) | collective-permute-done | bytes 589856 | tf_op jit(solution)/shard_map/ppermute | solution.py:317
  140.6 12.9 %collective-permute-done.1 = bf16[96,24,128]{2,1,0:T(8,128)(2,1)S(1)} collective-permute-done((bf16[96,24,128]{2,1,0:T(8,128)(2,1)S(1)}, bf16[96,24,128]{2,1,0:T(8,128)(2,1)S(1)}, u32[]{:S(2)}, u32[]{:S(2)}) %collective-permute-start.1) | collective-permute-done | bytes 589856 | tf_op jit(solution)/shard_map/ppermute | solution.py:317
  153.5 3.1 %collective-permute-done = bf16[96,24,128]{2,1,0:T(8,128)(2,1)S(1)} collective-permute-done((bf16[96,24,128]{2,1,0:T(8,128)(2,1)S(1)}, bf16[96,24,128]{2,1,0:T(8,128)(2,1)S(1)}, u32[]{:S(2)}, u32[]{:S(2)}) %collective-permute-start) | collective-permute-done | bytes 589856 | tf_op jit(solution)/shard_map/ppermute | solution.py:317
  156.6 1.7 pad_maximum_fusion.held
  158.3 3.5 %collective-permute-start.3 = (bf16[4,96,24,128]{3,2,1,0:T(8,128)(2,1)}, bf16[4,96,24,128]{3,2,1,0:T(8,128)(2,1)}, u32[]{:S(2)}, u32[]{:S(2)}) collective-permute-start(bf16[4,96,24,128]{3,2,1,0:T(8,128)(2,1)} %pad_maximum_fusion.held), channel_id=1, source_target_pairs={{1,0},{0,1},{3,2},{2,3},{5,4},{4,5},{7,6},{6,7},{9,8},{8,9},{11,10... | collective-permute-start | bytes 7077896 | tf_op jit(solution)/shard_map/ppermute | solution.py:319
  161.8 0.0 all-to-all-done.2.low
  161.8 0.7 shard_map.150
  162.5 5.8 %all-to-all-start.3 = ((f32[8,1,128]{2,1,0:T(1,128)}), f32[8,1,128]{2,1,0:T(1,128)S(1)}, u32[]{:S(2)}, u32[]{:S(2)}) async-start(f32[8,1,128]{2,1,0:T(1,128)} %shard_map.150), calls=%async_computation.3 | async-start | bytes 8192 | tf_op jit(solution)/shard_map/all_to_all | solution.py:370
  168.3 0.0 collective-permute-done.3.other
  168.3 8.8 %shard_map.151 = (bf16[3072,384]{1,0:T(8,128)(2,1)}, bf16[384,3072]{1,0:T(8,128)(2,1)}, bf16[32,384]{1,0:T(8,128)(2,1)}, bf16[32,384]{1,0:T(8,128)(2,1)}) custom-call(s32[2]{0:T(128)S(1)} %pad_add_fusion.place, bf16[4,96,24,128]{3,2,1,0:T(8,128)(2,1)} %pad_maximum_fusion.held, bf16[4,96,24,128]{3,2,1,0:T(8,128)(2,1)} %collective-permute-done.3.other), custom_call_target="tpu_custom_call" | custom-call | flops 1073741824 | bytes 31457280 | tf_op jit(solution)/shard_map/pallas_call | solution.py:337
  177.1 0.0 all-to-all-done.3.squares
  177.1 0.0 all-gather.3.cloned.1.call-done
  177.1 8.1 %shard_map.152 = (bf16[3072,384]{1,0:T(8,128)(2,1)}, bf16[384,3072]{1,0:T(8,128)(2,1)}, f32[32,384]{1,0:T(8,128)}, f32[32,384]{1,0:T(8,128)}) custom-call(s32[2]{0:T(128)S(1)} %pad_add_fusion.place, f32[8,1,128]{2,1,0:T(1,128)S(1)} %all-to-all-done.3.squares, bf16[96,4,896]{2,1,0:T(4,128)(2,1)S(1)} %all-to-all-done.2.low, ...), custom_call_target="tpu_custom_call" | custom-call | flops 1811939328 | bytes 20971520 | tf_op jit(solution)/shard_map/pallas_call | solution.py:373
  (1 shorter events, 0.0 us)
Async XLA Ops:
  7.2 170.0 %all-gather.3.cloned.1.call-start = ((), (), s32[]{:S(2)}) async-start(), calls=%async_computation.4 | async-start | bytes 4767744 | tf_op jit(solution)/shard_map/all_gather | solution.py:292
  8.9 50.2 %copy-start = (bf16[512,3072]{1,0:T(8,128)(2,1)S(1)}, bf16[512,3072]{1,0:T(8,128)(2,1)}, u32[]{:S(2)}) copy-start(bf16[512,3072]{1,0:T(8,128)(2,1)} %saved_inputs.1) | copy-start | bytes 9437188
  8.9 50.2 %copy-start.1 = (bf16[512,3072]{1,0:T(8,128)(2,1)S(1)}, bf16[512,3072]{1,0:T(8,128)(2,1)}, u32[]{:S(2)}) copy-start(bf16[512,3072]{1,0:T(8,128)(2,1)} %out_cotangent.1) | copy-start | bytes 9437188
  59.1 20.1 %copy-start.2 = (bf16[512,384]{1,0:T(8,128)(2,1)S(1)}, bf16[512,384]{1,0:T(8,128)(2,1)}, u32[]{:S(2)}) copy-start(bf16[512,384]{1,0:T(8,128)(2,1)} %query_cotangent.1) | copy-start | bytes 1179652
  59.1 20.1 %copy-start.3 = (bf16[512,384]{1,0:T(8,128)(2,1)S(1)}, bf16[512,384]{1,0:T(8,128)(2,1)}, u32[]{:S(2)}) copy-start(bf16[512,384]{1,0:T(8,128)(2,1)} %attn_outputs.1) | copy-start | bytes 1179652
  61.0 53.9 %copy-start.4 = (f32[2,4,384]{2,1,0:T(4,128)S(1)}, f32[2,4,384]{2,1,0:T(4,128)}, u32[]{:S(2)}) copy-start(f32[2,4,384]{2,1,0:T(4,128)} %first.1) | copy-start | bytes 36868
  61.1 53.9 %copy-start.5 = (f32[2,4,384]{2,1,0:T(4,128)S(1)}, f32[2,4,384]{2,1,0:T(4,128)}, u32[]{:S(2)}) copy-start(f32[2,4,384]{2,1,0:T(4,128)} %second.1) | copy-start | bytes 36868
  116.1 45.7 %all-to-all-start.2 = ((bf16[96,4,896]{2,1,0:T(4,128)(2,1)}), bf16[96,4,896]{2,1,0:T(4,128)(2,1)S(1)}, u32[]{:S(2)}, u32[]{:S(2)}) async-start(bf16[96,4,896]{2,1,0:T(4,128)(2,1)} %get-tuple-element.21), calls=%async_computation.2 | async-start | bytes 1376256 | tf_op jit(solution)/shard_map/all_to_all | solution.py:333
  124.1 16.4 %collective-permute-start.2 = (bf16[96,24,128]{2,1,0:T(8,128)(2,1)S(1)}, bf16[96,24,128]{2,1,0:T(8,128)(2,1)S(1)}, u32[]{:S(2)}, u32[]{:S(2)}) collective-permute-start(bf16[96,24,128]{2,1,0:T(8,128)(2,1)S(1)} %all_to_all.20.packed), channel_id=1, source_target_pairs={{6,0},{7,1},{0,2},{1,3},{2,4},{3,5},{4,6},{5,7},{14,8},{15,9},{8,1... | collective-permute-start | bytes 1769480 | tf_op jit(solution)/shard_map/ppermute | solution.py:317
  126.9 26.7 %collective-permute-start.1 = (bf16[96,24,128]{2,1,0:T(8,128)(2,1)S(1)}, bf16[96,24,128]{2,1,0:T(8,128)(2,1)S(1)}, u32[]{:S(2)}, u32[]{:S(2)}) collective-permute-start(bf16[96,24,128]{2,1,0:T(8,128)(2,1)S(1)} %all_to_all.20.packed), channel_id=1, source_target_pairs={{4,0},{5,1},{6,2},{7,3},{0,4},{1,5},{2,6},{3,7},{12,8},{13,9},{14,... | collective-permute-start | bytes 1769480 | tf_op jit(solution)/shard_map/ppermute | solution.py:317
  131.1 25.5 %collective-permute-start = (bf16[96,24,128]{2,1,0:T(8,128)(2,1)S(1)}, bf16[96,24,128]{2,1,0:T(8,128)(2,1)S(1)}, u32[]{:S(2)}, u32[]{:S(2)}) collective-permute-start(bf16[96,24,128]{2,1,0:T(8,128)(2,1)S(1)} %all_to_all.20.packed), channel_id=1, source_target_pairs={{2,0},{3,1},{4,2},{5,3},{6,4},{7,5},{0,6},{1,7},{10,8},{11,9},{12,... | collective-permute-start | bytes 1769480 | tf_op jit(solution)/shard_map/ppermute | solution.py:317
  158.3 10.0 %collective-permute-start.3 = (bf16[4,96,24,128]{3,2,1,0:T(8,128)(2,1)}, bf16[4,96,24,128]{3,2,1,0:T(8,128)(2,1)}, u32[]{:S(2)}, u32[]{:S(2)}) collective-permute-start(bf16[4,96,24,128]{3,2,1,0:T(8,128)(2,1)} %pad_maximum_fusion.held), channel_id=1, source_target_pairs={{1,0},{0,1},{3,2},{2,3},{5,4},{4,5},{7,6},{6,7},{9,8},{8,9},{11,10... | collective-permute-start | bytes 7077896 | tf_op jit(solution)/shard_map/ppermute | solution.py:319
  162.5 14.6 %all-to-all-start.3 = ((f32[8,1,128]{2,1,0:T(1,128)}), f32[8,1,128]{2,1,0:T(1,128)S(1)}, u32[]{:S(2)}, u32[]{:S(2)}) async-start(f32[8,1,128]{2,1,0:T(1,128)} %shard_map.150), calls=%async_computation.3 | async-start | bytes 8192 | tf_op jit(solution)/shard_map/all_to_all | solution.py:370
Sparse Core Ops, SparseCore 0:
  12.3 150.9 all-gather.2

commit v8 on v7

--- a/solution.py
+++ b/solution.py
@@ -135,8 +135,12 @@
             out[...] = tile[rows]
 
 
+def spread_kernel(low, out):
+    out[...] = jnp.broadcast_to(low[...][None], out.shape)
+
+
 def sums_kernel(low, squares):
-    sums = jnp.sum(low[:, :, -128:].astype(f32), axis=0)[:1]
+    sums = jnp.sum(low[:, :, :, -128:].astype(f32), axis=(0, 1))[:1]
     squares[...] = jnp.broadcast_to(sums[None], squares.shape)
 
 
@@ -199,15 +203,16 @@
         copy.start()
 
     tp = squares.shape[0]
-    per_block = rank_cols // low.shape[1]
+    height = low.shape[0]
+    per_block = rank_cols // low.shape[2]
     for b in range(tp):
         chip, core = b % (tp // 2), b // (tp // 2)
         at = (place[1] + 2 * chip) % tp
         at = at + core * (1 - 2 * (at % 2))
-        block = low[pl.ds(at * per_block, per_block)].astype(f32)
+        held = [at * per_block + j for j in range(per_block)]
+        block = [low[j % height, j // height].astype(f32) for j in held]
         for k, step in enumerate((first, second)):
-            part = block[:, :, k * cols : (k + 1) * cols]
-            part = jnp.concatenate([part[j] for j in range(per_block)], axis=0)
+            part = jnp.concatenate([piece[:, k * cols : (k + 1) * cols] for piece in block], axis=0)
             step[b * rank_cols : (b + 1) * rank_cols] = part.astype(bf16)
     second_turned = second[...].T
 
@@ -260,7 +265,9 @@
     first_moment,
     second_moment,
 ):
-    fs = lax.axis_size(FS)
+    depth = lax.axis_size("z")
+    height = lax.axis_size("y")
+    fs = depth * height
     tp = lax.axis_size("tp")
     own, rank_cols = left_factor.shape
     rows = first_moment.shape[1]
@@ -323,14 +330,23 @@
         out_shape=(
             jax.ShapeDtypeStruct(first_moment.shape, f32),
             jax.ShapeDtypeStruct(second_moment.shape, f32),
-            pltpu.HBM((fs, rows, 2 * cols + 128), bf16),
+            pltpu.HBM((depth, rows, 2 * cols + 128), bf16),
         ),
         in_specs=[VMEM] * 3,
         out_specs=(VMEM, VMEM, VMEM),
         compiler_params=SMALL,
         cost_estimate=cost(1 << 20, 2 << 20),
     )(pieces, first_moment, second_moment)
-    low = lax.all_to_all(low, FS, 0, 0)
+    low = lax.all_to_all(low, "z", 0, 0)
+    low = pl.pallas_call(
+        spread_kernel,
+        out_shape=pltpu.HBM((height, *low.shape), bf16),
+        in_specs=[VMEM],
+        out_specs=VMEM,
+        compiler_params=SMALL,
+        cost_estimate=cost(1 << 16, 1 << 20),
+    )(low)
+    low = lax.all_to_all(low, "y", 0, 0)
 
     span = width // 6
     per = span // own

time: 193 us -> 203 us (1.052)
  blocking collectives: 103 us -> 118 us
  starting transfers between devices: 26.3 us -> 20.4 us
    all_to_all x0 -> x1, blocking collectives: none -> 15.2 us  [body(): low = lax.all_to_all(low, 'z', 0, 0)]
    all_to_all x1, starting transfers between devices: 8.04 us -> 3.77 us  [body(): low = lax.all_to_all(low, 'y', 0, 0)]
where the time goes in v8:
time: 203 us; the launch traced here: 202 us
  blocking collectives  118 us (58%)
  Pallas kernels  24.9 us (12%)
  waiting for transfers between devices  23.2 us (11%)
  starting transfers between devices  20.4 us (10%)
  between operations  14.2 us (7%)
    all_to_all x1, blocking collectives, body(): packed = lax.all_to_all(packed, FS, 0, 0)  50.2 us
    all_to_all x1, blocking collectives, body(): pieces = lax.all_to_all(partial.reshape(fs, 2 * rows, cols), FS, 0, 0)  34.4 us
    ppermute x3, waiting for transfers between devices, body(): lax.ppermute(packed, 'tp', [((t + 2 * step) % tp, t) for t in range(tp)])  23.2 us
    all_gather x1, blocking collectives, body(): proj = lax.all_gather(proj, 'tp', axis=0, tiled=True)  18.1 us
    all_to_all x1, blocking collectives, body(): low = lax.all_to_all(low, 'z', 0, 0)  15.2 us
    ppermute x3, starting transfers between devices, body(): lax.ppermute(packed, 'tp', [((t + 2 * step) % tp, t) for t in range(tp)])  9.16 us
    pallas_call x1, Pallas kernels, body(): pl.pallas_call(functools.partial(prep_kernel, rank_cols), grid=(width //...  8.77 us
    pallas_call x1, Pallas kernels, body(): pl.pallas_call(functools.partial(final_kernel, float(rows * fs * cols * t...  8.68 us
  transfers between devices with their start and end apart: 7, of which 3 were waited for; matrix products, arithmetic and copies ran while one was open for 1% of the time, Pallas kernels for 7%

profile of v8, /device:TPU:1, one launch (start us, length us, event | category | flops | bytes accessed | tf_op | source)
XLA Modules:
  0.0 202.4 jit_solution(7358585014041092997)
XLA Ops:
  7.2 0.0 all-gather.3.cloned.1.call-start
  7.2 1.6 shard_map.145
  8.8 0.0 all-gather.3.cloned.1.call-update
  8.9 0.0 copy-start
  8.9 0.0 copy-start.1
  8.9 50.2 %all_to_all.25.packed = bf16[96,24,128]{2,1,0:T(8,128)(2,1)S(1)} all-to-all(bf16[96,24,128]{2,1,0:T(8,128)(2,1)S(1)} %shard_map.146), channel_id=1, replica_groups=mesh['z'=12,'y'=8,'tp'=8] {'z','y'}, dimensions={0} | all-to-all | bytes 1179648 | tf_op jit(solution)/shard_map/all_to_all | solution.py:300
  59.1 0.0 copy-done
  59.1 0.0 copy-done.1
  59.1 0.0 copy-start.2
  59.1 0.0 copy-start.3
  59.1 2.0 shard_map.147
  61.0 0.0 copy-start.4
  61.1 0.0 copy-start.5
  61.1 18.1 %all_gather.9.proj = bf16[768,512]{1,0:T(8,128)(2,1)S(1)} all-gather(bf16[96,512]{1,0:T(8,128)(2,1)S(1)} %shard_map.147), channel_id=1, replica_groups=mesh['z'=12,'y'=8,'tp'=8] {'tp'}, dimensions={0}, use_global_device_ids=true | all-gather | bytes 884736 | tf_op jit(solution)/shard_map/all_gather | solution.py:310
  79.2 0.0 copy-done.2
  79.2 0.0 copy-done.3
  79.2 1.4 shard_map.148
  80.6 34.4 %all_to_all.26.pieces = bf16[96,8,384]{2,1,0:T(8,128)(2,1)S(1)} all-to-all(bf16[96,8,384]{2,1,0:T(8,128)(2,1)} %bitcast.12), channel_id=1, replica_groups=mesh['z'=12,'y'=8,'tp'=8] {'z','y'}, dimensions={0} | all-to-all | bytes 1179648 | tf_op jit(solution)/shard_map/all_to_all | solution.py:320
  115.0 0.0 copy-done.4
  115.0 0.0 copy-done.5
  115.0 0.9 shard_map.149
  115.9 15.2 %all_to_all.27.low = bf16[12,4,896]{2,1,0:T(4,128)(2,1)S(1)} all-to-all(bf16[12,4,896]{2,1,0:T(4,128)(2,1)} %get-tuple-element.21), channel_id=1, replica_groups=mesh['z'=12,'y'=8,'tp'=8] {'z'}, dimensions={0} | all-to-all | bytes 172032 | tf_op jit(solution)/shard_map/all_to_all | solution.py:340
  131.1 0.9 shard_map.150
  132.0 3.8 %all-to-all-start.3 = ((bf16[8,12,4,896]{3,2,1,0:T(4,128)(2,1)}), bf16[8,12,4,896]{3,2,1,0:T(4,128)(2,1)S(1)}, u32[]{:S(2)}, u32[]{:S(2)}) async-start(bf16[8,12,4,896]{3,2,1,0:T(4,128)(2,1)} %shard_map.150), calls=%async_computation.3 | async-start | bytes 1376256 | tf_op jit(solution)/shard_map/all_to_all | solution.py:349
  135.7 2.9 %collective-permute-start.2 = (bf16[96,24,128]{2,1,0:T(8,128)(2,1)S(1)}, bf16[96,24,128]{2,1,0:T(8,128)(2,1)S(1)}, u32[]{:S(2)}, u32[]{:S(2)}) collective-permute-start(bf16[96,24,128]{2,1,0:T(8,128)(2,1)S(1)} %all_to_all.25.packed), channel_id=1, source_target_pairs={{6,0},{7,1},{0,2},{1,3},{2,4},{3,5},{4,6},{5,7},{14,8},{15,9},{8,1... | collective-permute-start | bytes 1769480 | tf_op jit(solution)/shard_map/ppermute | solution.py:324
  138.6 4.4 %collective-permute-start.1 = (bf16[96,24,128]{2,1,0:T(8,128)(2,1)S(1)}, bf16[96,24,128]{2,1,0:T(8,128)(2,1)S(1)}, u32[]{:S(2)}, u32[]{:S(2)}) collective-permute-start(bf16[96,24,128]{2,1,0:T(8,128)(2,1)S(1)} %all_to_all.25.packed), channel_id=1, source_target_pairs={{4,0},{5,1},{6,2},{7,3},{0,4},{1,5},{2,6},{3,7},{12,8},{13,9},{14,... | collective-permute-start | bytes 1769480 | tf_op jit(solution)/shard_map/ppermute | solution.py:324
  143.0 1.9 collective-permute-start
  144.9 0.1 pad_add_fusion.place
  145.0 4.9 %collective-permute-done.2 = bf16[96,24,128]{2,1,0:T(8,128)(2,1)S(1)} collective-permute-done((bf16[96,24,128]{2,1,0:T(8,128)(2,1)S(1)}, bf16[96,24,128]{2,1,0:T(8,128)(2,1)S(1)}, u32[]{:S(2)}, u32[]{:S(2)}) %collective-permute-start.2) | collective-permute-done | bytes 589856 | tf_op jit(solution)/shard_map/ppermute | solution.py:324
  149.9 13.6 %collective-permute-done.1 = bf16[96,24,128]{2,1,0:T(8,128)(2,1)S(1)} collective-permute-done((bf16[96,24,128]{2,1,0:T(8,128)(2,1)S(1)}, bf16[96,24,128]{2,1,0:T(8,128)(2,1)S(1)}, u32[]{:S(2)}, u32[]{:S(2)}) %collective-permute-start.1) | collective-permute-done | bytes 589856 | tf_op jit(solution)/shard_map/ppermute | solution.py:324
  163.5 4.7 %collective-permute-done = bf16[96,24,128]{2,1,0:T(8,128)(2,1)S(1)} collective-permute-done((bf16[96,24,128]{2,1,0:T(8,128)(2,1)S(1)}, bf16[96,24,128]{2,1,0:T(8,128)(2,1)S(1)}, u32[]{:S(2)}, u32[]{:S(2)}) %collective-permute-start) | collective-permute-done | bytes 589856 | tf_op jit(solution)/shard_map/ppermute | solution.py:324
  168.2 1.7 pad_maximum_fusion.held
  169.9 3.5 %collective-permute-start.3 = (bf16[4,96,24,128]{3,2,1,0:T(8,128)(2,1)}, bf16[4,96,24,128]{3,2,1,0:T(8,128)(2,1)}, u32[]{:S(2)}, u32[]{:S(2)}) collective-permute-start(bf16[4,96,24,128]{3,2,1,0:T(8,128)(2,1)} %pad_maximum_fusion.held), channel_id=1, source_target_pairs={{1,0},{0,1},{3,2},{2,3},{5,4},{4,5},{7,6},{6,7},{9,8},{8,9},{11,10... | collective-permute-start | bytes 7077896 | tf_op jit(solution)/shard_map/ppermute | solution.py:326
  173.4 0.0 all-to-all-done.3.low
  173.4 0.7 shard_map.151
  174.1 4.0 %all-to-all-start.4 = ((f32[8,1,128]{2,1,0:T(1,128)}), f32[8,1,128]{2,1,0:T(1,128)S(1)}, u32[]{:S(2)}, u32[]{:S(2)}) async-start(f32[8,1,128]{2,1,0:T(1,128)} %shard_map.151), calls=%async_computation.4 | async-start | bytes 8192 | tf_op jit(solution)/shard_map/all_to_all | solution.py:386
  178.1 0.0 collective-permute-done.3.other
  178.1 8.8 %shard_map.152 = (bf16[3072,384]{1,0:T(8,128)(2,1)}, bf16[384,3072]{1,0:T(8,128)(2,1)}, bf16[32,384]{1,0:T(8,128)(2,1)}, bf16[32,384]{1,0:T(8,128)(2,1)}) custom-call(s32[2]{0:T(128)S(1)} %pad_add_fusion.place, bf16[4,96,24,128]{3,2,1,0:T(8,128)(2,1)} %pad_maximum_fusion.held, bf16[4,96,24,128]{3,2,1,0:T(8,128)(2,1)} %collective-permute-done.3.other), custom_call_target="tpu_custom_call" | custom-call | flops 1073741824 | bytes 31457280 | tf_op jit(solution)/shard_map/pallas_call | solution.py:353
  186.9 0.0 all-to-all-done.4.squares
  186.9 0.0 all-gather.3.cloned.1.call-done
  186.9 8.7 %shard_map.153 = (bf16[3072,384]{1,0:T(8,128)(2,1)}, bf16[384,3072]{1,0:T(8,128)(2,1)}, f32[32,384]{1,0:T(8,128)}, f32[32,384]{1,0:T(8,128)}) custom-call(s32[2]{0:T(128)S(1)} %pad_add_fusion.place, f32[8,1,128]{2,1,0:T(1,128)S(1)} %all-to-all-done.4.squares, bf16[8,12,4,896]{3,2,1,0:T(4,128)(2,1)S(1)} %all-to-all-done.3.low, ...), custom_call_target="tpu_custom_call" | custom-call | flops 1811939328 | bytes 20971520 | tf_op jit(solution)/shard_map/pallas_call | solution.py:389
  (1 shorter events, 0.0 us)
Async XLA Ops:
  7.2 179.7 %all-gather.3.cloned.1.call-start = ((), (), s32[]{:S(2)}) async-start(), calls=%async_computation.5 | async-start | bytes 4767744 | tf_op jit(solution)/shard_map/all_gather | solution.py:299
  8.9 50.2 %copy-start = (bf16[512,3072]{1,0:T(8,128)(2,1)S(1)}, bf16[512,3072]{1,0:T(8,128)(2,1)}, u32[]{:S(2)}) copy-start(bf16[512,3072]{1,0:T(8,128)(2,1)} %saved_inputs.1) | copy-start | bytes 9437188
  8.9 50.2 %copy-start.1 = (bf16[512,3072]{1,0:T(8,128)(2,1)S(1)}, bf16[512,3072]{1,0:T(8,128)(2,1)}, u32[]{:S(2)}) copy-start(bf16[512,3072]{1,0:T(8,128)(2,1)} %out_cotangent.1) | copy-start | bytes 9437188
  59.1 20.1 %copy-start.2 = (bf16[512,384]{1,0:T(8,128)(2,1)S(1)}, bf16[512,384]{1,0:T(8,128)(2,1)}, u32[]{:S(2)}) copy-start(bf16[512,384]{1,0:T(8,128)(2,1)} %query_cotangent.1) | copy-start | bytes 1179652
  59.1 20.1 %copy-start.3 = (bf16[512,384]{1,0:T(8,128)(2,1)S(1)}, bf16[512,384]{1,0:T(8,128)(2,1)}, u32[]{:S(2)}) copy-start(bf16[512,384]{1,0:T(8,128)(2,1)} %attn_outputs.1) | copy-start | bytes 1179652
  61.0 53.9 %copy-start.4 = (f32[2,4,384]{2,1,0:T(4,128)S(1)}, f32[2,4,384]{2,1,0:T(4,128)}, u32[]{:S(2)}) copy-start(f32[2,4,384]{2,1,0:T(4,128)} %first.1) | copy-start | bytes 36868
  61.1 53.9 %copy-start.5 = (f32[2,4,384]{2,1,0:T(4,128)S(1)}, f32[2,4,384]{2,1,0:T(4,128)}, u32[]{:S(2)}) copy-start(f32[2,4,384]{2,1,0:T(4,128)} %second.1) | copy-start | bytes 36868
  132.0 41.4 %all-to-all-start.3 = ((bf16[8,12,4,896]{3,2,1,0:T(4,128)(2,1)}), bf16[8,12,4,896]{3,2,1,0:T(4,128)(2,1)S(1)}, u32[]{:S(2)}, u32[]{:S(2)}) async-start(bf16[8,12,4,896]{3,2,1,0:T(4,128)(2,1)} %shard_map.150), calls=%async_computation.3 | async-start | bytes 1376256 | tf_op jit(solution)/shard_map/all_to_all | solution.py:349
  135.7 14.2 %collective-permute-start.2 = (bf16[96,24,128]{2,1,0:T(8,128)(2,1)S(1)}, bf16[96,24,128]{2,1,0:T(8,128)(2,1)S(1)}, u32[]{:S(2)}, u32[]{:S(2)}) collective-permute-start(bf16[96,24,128]{2,1,0:T(8,128)(2,1)S(1)} %all_to_all.25.packed), channel_id=1, source_target_pairs={{6,0},{7,1},{0,2},{1,3},{2,4},{3,5},{4,6},{5,7},{14,8},{15,9},{8,1... | collective-permute-start | bytes 1769480 | tf_op jit(solution)/shard_map/ppermute | solution.py:324
  138.6 24.9 %collective-permute-start.1 = (bf16[96,24,128]{2,1,0:T(8,128)(2,1)S(1)}, bf16[96,24,128]{2,1,0:T(8,128)(2,1)S(1)}, u32[]{:S(2)}, u32[]{:S(2)}) collective-permute-start(bf16[96,24,128]{2,1,0:T(8,128)(2,1)S(1)} %all_to_all.25.packed), channel_id=1, source_target_pairs={{4,0},{5,1},{6,2},{7,3},{0,4},{1,5},{2,6},{3,7},{12,8},{13,9},{14,... | collective-permute-start | bytes 1769480 | tf_op jit(solution)/shard_map/ppermute | solution.py:324
  143.0 25.2 %collective-permute-start = (bf16[96,24,128]{2,1,0:T(8,128)(2,1)S(1)}, bf16[96,24,128]{2,1,0:T(8,128)(2,1)S(1)}, u32[]{:S(2)}, u32[]{:S(2)}) collective-permute-start(bf16[96,24,128]{2,1,0:T(8,128)(2,1)S(1)} %all_to_all.25.packed), channel_id=1, source_target_pairs={{2,0},{3,1},{4,2},{5,3},{6,4},{7,5},{0,6},{1,7},{10,8},{11,9},{12,... | collective-permute-start | bytes 1769480 | tf_op jit(solution)/shard_map/ppermute | solution.py:324
  169.9 8.2 %collective-permute-start.3 = (bf16[4,96,24,128]{3,2,1,0:T(8,128)(2,1)}, bf16[4,96,24,128]{3,2,1,0:T(8,128)(2,1)}, u32[]{:S(2)}, u32[]{:S(2)}) collective-permute-start(bf16[4,96,24,128]{3,2,1,0:T(8,128)(2,1)} %pad_maximum_fusion.held), channel_id=1, source_target_pairs={{1,0},{0,1},{3,2},{2,3},{5,4},{4,5},{7,6},{6,7},{9,8},{8,9},{11,10... | collective-permute-start | bytes 7077896 | tf_op jit(solution)/shard_map/ppermute | solution.py:326
  174.1 12.8 %all-to-all-start.4 = ((f32[8,1,128]{2,1,0:T(1,128)}), f32[8,1,128]{2,1,0:T(1,128)S(1)}, u32[]{:S(2)}, u32[]{:S(2)}) async-start(f32[8,1,128]{2,1,0:T(1,128)} %shard_map.151), calls=%async_computation.4 | async-start | bytes 8192 | tf_op jit(solution)/shard_map/all_to_all | solution.py:386
Sparse Core Ops, SparseCore 0:
  12.3 134.7 all-gather.2

commit v9 on v8

--- a/solution.py
+++ b/solution.py
@@ -135,6 +135,31 @@
             out[...] = tile[rows]
 
 
+def decode_kernel(span, masters, query_all, out_all, near, near_query, near_out, arrived, left_for):
+    own = masters.shape[1] // 2
+    cols = masters.shape[2]
+    per = span // own
+    parts = masters.shape[0] // per
+    copies = []
+    for i in range(parts):
+        held = pl.ds(i * per, per)
+        copies.append(pltpu.make_async_copy(masters.at[held], near.at[held], arrived.at[i]))
+        copies[-1].start()
+    sent = []
+    for i in range(parts):
+        at = pl.ds(i * span, span)
+        copies[i].wait()
+        codes = near[i * per : (i + 1) * per]
+        near_query[at] = decoded(codes[:, :own].reshape(span, cols))
+        sent.append(pltpu.make_async_copy(near_query.at[at], query_all.at[at], left_for.at[i, 0]))
+        sent[-1].start()
+        near_out[:, at] = decoded(codes[:, own:].reshape(span, cols).T)
+        sent.append(pltpu.make_async_copy(near_out.at[:, at], out_all.at[:, at], left_for.at[i, 1]))
+        sent[-1].start()
+    for copy in sent:
+        copy.wait()
+
+
 def spread_kernel(low, out):
     out[...] = jnp.broadcast_to(low[...][None], out.shape)
 
@@ -153,7 +178,8 @@
     low,
     left,
     right,
-    masters,
+    query_all,
+    out_all,
     own_left,
     own_right,
     query_master,
@@ -162,9 +188,6 @@
     out_copy,
     query_new,
     out_new,
-    near_left,
-    near_right,
-    near_masters,
     near_query,
     near_out,
     near_own,
@@ -172,26 +195,13 @@
     near_new,
     first,
     second,
-    arrived,
     own_arrived,
     left_for,
     own_left_for,
 ):
     width = left.shape[0]
     cols = first.shape[1]
-    own = query_master.shape[0]
-    per = span // own
     parts = width // span
-    spans = [pl.ds(i * span, span) for i in range(parts)]
-    copies = []
-    for i, at in enumerate(spans):
-        held = pl.ds(i * per, per)
-        ways = (
-            (left.at[at], near_left.at[at]),
-            (masters.at[held], near_masters.at[held]),
-            (right.at[:, at], near_right.at[:, at]),
-        )
-        copies.append([pltpu.make_async_copy(x, y, arrived.at[i, k]) for k, (x, y) in enumerate(ways)])
     ways = (
         (own_left, near_own.at[0]),
         (own_right, near_own.at[1]),
@@ -199,7 +209,7 @@
         (out_master, near_master.at[1]),
     )
     own_copies = [pltpu.make_async_copy(x, y, own_arrived.at[k]) for k, (x, y) in enumerate(ways)]
-    for copy in [c for part in copies for c in part] + own_copies:
+    for copy in own_copies:
         copy.start()
 
     tp = squares.shape[0]
@@ -224,18 +234,14 @@
         scales.append(0.01 * lax.rsqrt(total / entries + 1e-06))
 
     sent = []
-    for i, at in enumerate(spans):
-        for copy in copies[i]:
-            copy.wait()
-        codes = near_masters[i * per : (i + 1) * per]
-        moved = jnp.dot(near_left[at], first[...], preferred_element_type=f32)
-        kept = decoded(codes[:, :own].reshape(span, cols))
-        near_query[at] = (kept - scales[0] * moved).astype(bf16)
+    for i in range(parts):
+        at = pl.ds(i * span, span)
+        moved = jnp.dot(left[at], first[...], preferred_element_type=f32)
+        near_query[at] = (query_all[at] - scales[0] * moved).astype(bf16)
         sent.append(pltpu.make_async_copy(near_query.at[at], query_copy.at[at], left_for.at[i, 0]))
         sent[-1].start()
-        moved = jnp.dot(second_turned, near_right[:, at], preferred_element_type=f32)
-        kept = decoded(codes[:, own:].reshape(span, cols).T)
-        near_out[:, at] = (kept - scales[1] * moved).astype(bf16)
+        moved = jnp.dot(second_turned, right[:, at], preferred_element_type=f32)
+        near_out[:, at] = (out_all[:, at] - scales[1] * moved).astype(bf16)
         sent.append(pltpu.make_async_copy(near_out.at[:, at], out_copy.at[:, at], left_for.at[i, 1]))
         sent[-1].start()
     for copy in own_copies:
@@ -375,6 +381,23 @@
         cost_estimate=cost(1 << 30, 30 << 20),
     )(place, far(held), far(other))
 
+    parts = width // span
+    query_all, out_all = pl.pallas_call(
+        functools.partial(decode_kernel, span),
+        out_shape=(pltpu.HBM((width, cols), f32), pltpu.HBM((cols, width), f32)),
+        in_specs=[ANY],
+        out_specs=(ANY, ANY),
+        scratch_shapes=[
+            pltpu.VMEM(masters.shape, bf16),
+            pltpu.VMEM((width, cols), f32),
+            pltpu.VMEM((cols, width), f32),
+            pltpu.SemaphoreType.DMA((parts,)),
+            pltpu.SemaphoreType.DMA((parts, 2)),
+        ],
+        compiler_params=pltpu.CompilerParams(vmem_limit_bytes=24 << 20),
+        cost_estimate=cost(1 << 30, 15 << 20),
+    )(far(masters))
+
     squares = pl.pallas_call(
         sums_kernel,
         out_shape=jax.ShapeDtypeStruct((tp, 1, 128), f32),
@@ -385,7 +408,6 @@
     )(low)
     squares = lax.all_to_all(squares, "tp", 0, 0)
 
-    parts = width // span
     query_copy, out_copy, query_new, out_new = pl.pallas_call(
         functools.partial(final_kernel, float(rows * fs * cols * tp), span, rank_cols),
         out_shape=(
@@ -394,12 +416,9 @@
             pltpu.HBM((own, cols), f32),
             pltpu.HBM((own, cols), f32),
         ),
-        in_specs=[SMEM] + [VMEM] * 2 + [ANY] * 7,
+        in_specs=[SMEM] + [VMEM] * 6 + [ANY] * 4,
         out_specs=(ANY,) * 4,
         scratch_shapes=[
-            pltpu.VMEM((width, ranks), bf16),
-            pltpu.VMEM((ranks, width), bf16),
-            pltpu.VMEM(masters.shape, bf16),
             pltpu.VMEM((width, cols), bf16),
             pltpu.VMEM((cols, width), bf16),
             pltpu.VMEM((2, own, ranks), bf16),
@@ -407,20 +426,20 @@
             pltpu.VMEM((2, own, cols), f32),
             pltpu.VMEM((ranks, cols), bf16),
             pltpu.VMEM((ranks, cols), bf16),
-            pltpu.SemaphoreType.DMA((parts, 3)),
             pltpu.SemaphoreType.DMA((4,)),
             pltpu.SemaphoreType.DMA((parts, 2)),
             pltpu.SemaphoreType.DMA((2,)),
         ],
-        compiler_params=pltpu.CompilerParams(vmem_limit_bytes=32 << 20),
+        compiler_params=SMALL,
         cost_estimate=cost(4 * width * ranks * cols, 20 << 20),
     )(
         place,
         squares,
         low,
-        far(left),
-        far(right),
-        far(masters),
+        left,
+        right,
+        query_all,
+        out_all,
         far(own_left),
         far(own_right),
         far(query_master),

time: 203 us -> 219 us (1.079)
  blocking collectives: 118 us -> 95.8 us
  waiting for transfers between devices: 23.2 us -> 39 us
  starting transfers between devices: 20.4 us -> 32.2 us
  local copies, waits for them, and re-layouts: 0.03 us -> 6.37 us
  Pallas kernels: 24.9 us -> 28.3 us
    all_to_all x1 -> x0, blocking collectives: 34.4 us -> none  [body(): pieces = lax.all_to_all(partial.reshape(fs, 2 * rows, cols), FS, 0, 0)]
    all_to_all x0 -> x1, waiting for transfers between devices: none -> 29 us  [body(): pieces = lax.all_to_all(partial.reshape(fs, 2 * rows, cols), FS, 0, 0)]
    ppermute x3, waiting for transfers between devices: 23.2 us -> 0.01 us  [body(): lax.ppermute(packed, 'tp', [((t + 2 * step) % tp, t) for t in range(tp)])]
    all_gather x1, blocking collectives: 18.1 us -> 30.1 us  [body(): proj = lax.all_gather(proj, 'tp', axis=0, tiled=True)]
    all_to_all x1, waiting for transfers between devices: 0.01 us -> 9.89 us  [body(): low = lax.all_to_all(low, 'y', 0, 0)]
    all_to_all x0 -> x1, starting transfers between devices: none -> 8.06 us  [body(): pieces = lax.all_to_all(partial.reshape(fs, 2 * rows, cols), FS, 0, 0)]
    pallas_call x0 -> x1, Pallas kernels: none -> 6.58 us  [body(): pl.pallas_call(functools.partial(decode_kernel, span), out_shape=(pltpu.H...]
    unnamed x12 -> x20, local copies, waits for them, and re-layouts: 0.03 us -> 6.37 us
  transfers between devices with their start and end apart: 7 -> 8, of which waited for: 3 -> 2; matrix products, arithmetic and copies ran while one was open for 1% -> 1% of each run, Pallas kernels for 7% -> 10%
where the time goes in v9:
time: 219 us; the launch traced here: 218 us
  blocking collectives  95.8 us (44%)
  waiting for transfers between devices  39 us (18%)
  starting transfers between devices  32.2 us (15%)
  Pallas kernels  28.3 us (13%)
  between operations  14.2 us (6%)
  local copies, waits for them, and re-layouts  6.37 us (3%)
    all_to_all x1, blocking collectives, body(): packed = lax.all_to_all(packed, FS, 0, 0)  50.2 us
    all_gather x1, blocking collectives, body(): proj = lax.all_gather(proj, 'tp', axis=0, tiled=True)  30.1 us
    all_to_all x1, waiting for transfers between devices, body(): pieces = lax.all_to_all(partial.reshape(fs, 2 * rows, cols), FS, 0, 0)  29 us
    all_to_all x1, blocking collectives, body(): low = lax.all_to_all(low, 'z', 0, 0)  15.4 us
    ppermute x3, starting transfers between devices, body(): lax.ppermute(packed, 'tp', [((t + 2 * step) % tp, t) for t in range(tp)])  10.7 us
    all_to_all x1, waiting for transfers between devices, body(): low = lax.all_to_all(low, 'y', 0, 0)  9.89 us
    pallas_call x1, Pallas kernels, body(): pl.pallas_call(functools.partial(prep_kernel, rank_cols), grid=(width //...  8.71 us
    all_to_all x1, starting transfers between devices, body(): pieces = lax.all_to_all(partial.reshape(fs, 2 * rows, cols), FS, 0, 0)  8.06 us
  transfers between devices with their start and end apart: 8, of which 2 were waited for; matrix products, arithmetic and copies ran while one was open for 1% of the time, Pallas kernels for 10%

profile of v9, /device:TPU:1, one launch (start us, length us, event | category | flops | bytes accessed | tf_op | source)
XLA Modules:
  0.0 217.6 jit_solution(3611636726497536418)
XLA Ops:
  7.2 0.0 all-gather.3.cloned.1.call-start
  7.2 1.6 shard_map.145
  8.8 0.0 all-gather.3.cloned.1.call-update
  8.9 0.0 copy-start.2
  8.9 0.0 copy-start.3
  8.9 50.2 %all_to_all.25.packed = bf16[96,24,128]{2,1,0:T(8,128)(2,1)S(1)} all-to-all(bf16[96,24,128]{2,1,0:T(8,128)(2,1)S(1)} %shard_map.146), channel_id=1, replica_groups=mesh['z'=12,'y'=8,'tp'=8] {'z','y'}, dimensions={0} | all-to-all | bytes 1179648 | tf_op jit(solution)/shard_map/all_to_all | solution.py:306
  59.1 0.0 copy-start.6
  59.1 0.0 copy-start.7
  59.1 3.2 %collective-permute-start.2 = (bf16[96,24,128]{2,1,0:T(8,128)(2,1)S(1)}, bf16[96,24,128]{2,1,0:T(8,128)(2,1)S(1)}, u32[]{:S(2)}, u32[]{:S(2)}) collective-permute-start(bf16[96,24,128]{2,1,0:T(8,128)(2,1)S(1)} %all_to_all.25.packed), channel_id=1, source_target_pairs={{6,0},{7,1},{0,2},{1,3},{2,4},{3,5},{4,6},{5,7},{14,8},{15,9},{8,1... | collective-permute-start | bytes 1769480 | tf_op jit(solution)/shard_map/ppermute | solution.py:330
  62.3 4.4 %collective-permute-start.1 = (bf16[96,24,128]{2,1,0:T(8,128)(2,1)S(1)}, bf16[96,24,128]{2,1,0:T(8,128)(2,1)S(1)}, u32[]{:S(2)}, u32[]{:S(2)}) collective-permute-start(bf16[96,24,128]{2,1,0:T(8,128)(2,1)S(1)} %all_to_all.25.packed), channel_id=1, source_target_pairs={{4,0},{5,1},{6,2},{7,3},{0,4},{1,5},{2,6},{3,7},{12,8},{13,9},{14,... | collective-permute-start | bytes 1769480 | tf_op jit(solution)/shard_map/ppermute | solution.py:330
  66.7 3.1 %collective-permute-start = (bf16[96,24,128]{2,1,0:T(8,128)(2,1)S(1)}, bf16[96,24,128]{2,1,0:T(8,128)(2,1)S(1)}, u32[]{:S(2)}, u32[]{:S(2)}) collective-permute-start(bf16[96,24,128]{2,1,0:T(8,128)(2,1)S(1)} %all_to_all.25.packed), channel_id=1, source_target_pairs={{2,0},{3,1},{4,2},{5,3},{6,4},{7,5},{0,6},{1,7},{10,8},{11,9},{12,... | collective-permute-start | bytes 1769480 | tf_op jit(solution)/shard_map/ppermute | solution.py:330
  69.8 0.0 copy-done.2
  69.8 0.0 copy-done.3
  69.8 2.0 shard_map.147
  71.8 30.1 %all_gather.9.proj = bf16[768,512]{1,0:T(8,128)(2,1)S(1)} all-gather(bf16[96,512]{1,0:T(8,128)(2,1)S(1)} %shard_map.147), channel_id=1, replica_groups=mesh['z'=12,'y'=8,'tp'=8] {'tp'}, dimensions={0}, use_global_device_ids=true | all-gather | bytes 884736 | tf_op jit(solution)/shard_map/all_gather | solution.py:316
  101.9 0.0 copy-done.6
  101.9 0.0 copy-done.7
  101.9 1.4 shard_map.148
  103.3 8.1 %all-to-all-start.1 = ((bf16[96,8,384]{2,1,0:T(8,128)(2,1)}), bf16[96,8,384]{2,1,0:T(8,128)(2,1)S(1)}, u32[]{:S(2)}, u32[]{:S(2)}) async-start(bf16[96,8,384]{2,1,0:T(8,128)(2,1)} %bitcast.12), calls=%async_computation.1 | async-start | bytes 1179648 | tf_op jit(solution)/shard_map/all_to_all | solution.py:326
  111.4 0.0 collective-permute-done.2
  111.4 0.0 collective-permute-done.1
  111.4 0.0 collective-permute-done
  111.4 0.0 copy-start.8
  111.4 0.0 copy-start.9
  111.4 1.7 pad_maximum_fusion.held
  113.1 2.3 %collective-permute-start.3 = (bf16[4,96,24,128]{3,2,1,0:T(8,128)(2,1)}, bf16[4,96,24,128]{3,2,1,0:T(8,128)(2,1)}, u32[]{:S(2)}, u32[]{:S(2)}) collective-permute-start(bf16[4,96,24,128]{3,2,1,0:T(8,128)(2,1)} %pad_maximum_fusion.held), channel_id=1, source_target_pairs={{1,0},{0,1},{3,2},{2,3},{5,4},{4,5},{7,6},{6,7},{9,8},{8,9},{11,10... | collective-permute-start | bytes 7077896 | tf_op jit(solution)/shard_map/ppermute | solution.py:332
  115.5 29.0 %all-to-all-done.1.pieces = bf16[96,8,384]{2,1,0:T(8,128)(2,1)S(1)} async-done(((bf16[96,8,384]{2,1,0:T(8,128)(2,1)}), bf16[96,8,384]{2,1,0:T(8,128)(2,1)S(1)}, u32[]{:S(2)}, u32[]{:S(2)}) %all-to-all-start.1) | async-done | bytes 589856 | tf_op jit(solution)/shard_map/all_to_all | solution.py:326
  144.5 0.0 copy-done.8
  144.5 0.0 copy-done.9
  144.5 0.9 shard_map.149
  145.4 15.4 %all_to_all.26.low = bf16[12,4,896]{2,1,0:T(4,128)(2,1)S(1)} all-to-all(bf16[12,4,896]{2,1,0:T(4,128)(2,1)} %get-tuple-element.23), channel_id=1, replica_groups=mesh['z'=12,'y'=8,'tp'=8] {'z'}, dimensions={0} | all-to-all | bytes 172032 | tf_op jit(solution)/shard_map/all_to_all | solution.py:346
  160.9 0.9 shard_map.150
  161.8 3.5 %all-to-all-start.3 = ((bf16[8,12,4,896]{3,2,1,0:T(4,128)(2,1)}), bf16[8,12,4,896]{3,2,1,0:T(4,128)(2,1)S(1)}, u32[]{:S(2)}, u32[]{:S(2)}) async-start(bf16[8,12,4,896]{3,2,1,0:T(4,128)(2,1)} %shard_map.150), calls=%async_computation.3 | async-start | bytes 1376256 | tf_op jit(solution)/shard_map/all_to_all | solution.py:355
  165.3 0.1 pad_add_fusion.place
  165.4 0.0 collective-permute-done.3.other
  165.4 8.7 %shard_map.152 = (bf16[3072,384]{1,0:T(8,128)(2,1)}, bf16[384,3072]{1,0:T(8,128)(2,1)}, bf16[32,384]{1,0:T(8,128)(2,1)}, bf16[32,384]{1,0:T(8,128)(2,1)}) custom-call(s32[2]{0:T(128)S(1)} %pad_add_fusion.place, bf16[4,96,24,128]{3,2,1,0:T(8,128)(2,1)} %pad_maximum_fusion.held, bf16[4,96,24,128]{3,2,1,0:T(8,128)(2,1)} %collective-permute-done.3.other), custom_call_target="tpu_custom_call" | custom-call | flops 1073741824 | bytes 31457280 | tf_op jit(solution)/shard_map/pallas_call | solution.py:359
  174.1 9.9 %all-to-all-done.3.low = bf16[8,12,4,896]{3,2,1,0:T(4,128)(2,1)S(1)} async-done(((bf16[8,12,4,896]{3,2,1,0:T(4,128)(2,1)}), bf16[8,12,4,896]{3,2,1,0:T(4,128)(2,1)S(1)}, u32[]{:S(2)}, u32[]{:S(2)}) %all-to-all-start.3) | async-done | bytes 688160 | tf_op jit(solution)/shard_map/all_to_all | solution.py:355
  184.0 0.7 shard_map.151
  184.7 7.5 %all-to-all-start.4 = ((f32[8,1,128]{2,1,0:T(1,128)}), f32[8,1,128]{2,1,0:T(1,128)S(1)}, u32[]{:S(2)}, u32[]{:S(2)}) async-start(f32[8,1,128]{2,1,0:T(1,128)} %shard_map.151), calls=%async_computation.4 | async-start | bytes 8192 | tf_op jit(solution)/shard_map/all_to_all | solution.py:409
  192.2 0.0 all-gather.3.cloned.1.call-done
  192.2 0.0 copy-start.4
  192.2 6.6 %shard_map.153 = (f32[3072,384]{1,0:T(8,128)}, f32[384,3072]{1,0:T(8,128)}) custom-call(bf16[96,64,384]{2,1,0:T(8,128)(2,1)} %bitcast.11), custom_call_target="tpu_custom_call" | custom-call | flops 1073741824 | bytes 15728640 | tf_op jit(solution)/shard_map/pallas_call | solution.py:385
  198.8 0.0 all-to-all-done.4.squares
  198.8 0.0 copy-done.4
  198.8 0.0 copy-start
  198.9 2.3 %copy-done = f32[3072,384]{1,0:T(8,128)S(1)} copy-done((f32[3072,384]{1,0:T(8,128)S(1)}, f32[3072,384]{1,0:T(8,128)}, u32[]{:S(2)}) %copy-start) | copy-done | bytes 4718616
  201.2 0.0 copy-start.1
  201.2 2.3 %copy-done.1 = f32[384,3072]{1,0:T(8,128)S(1)} copy-done((f32[384,3072]{1,0:T(8,128)S(1)}, f32[384,3072]{1,0:T(8,128)}, u32[]{:S(2)}) %copy-start.1) | copy-done | bytes 4718616
  203.5 0.0 copy-start.5
  203.5 1.7 copy-done.5
  205.2 5.6 %shard_map.154 = (bf16[3072,384]{1,0:T(8,128)(2,1)}, bf16[384,3072]{1,0:T(8,128)(2,1)}, f32[32,384]{1,0:T(8,128)}, f32[32,384]{1,0:T(8,128)}) custom-call(s32[2]{0:T(128)S(1)} %pad_add_fusion.place, f32[8,1,128]{2,1,0:T(1,128)S(1)} %all-to-all-done.4.squares, bf16[8,12,4,896]{3,2,1,0:T(4,128)(2,1)S(1)} %all-to-all-done.3.low, ...), custom_call_target="tpu_custom_call" | custom-call | flops 1811939328 | bytes 20971520 | tf_op jit(solution)/shard_map/pallas_call | solution.py:411
  (1 shorter events, 0.0 us)
Async XLA Ops:
  7.2 185.1 %all-gather.3.cloned.1.call-start = ((), (), s32[]{:S(2)}) async-start(), calls=%async_computation.5 | async-start | bytes 4767744 | tf_op jit(solution)/shard_map/all_gather | solution.py:305
  8.9 60.9 %copy-start.2 = (bf16[512,3072]{1,0:T(8,128)(2,1)S(1)}, bf16[512,3072]{1,0:T(8,128)(2,1)}, u32[]{:S(2)}) copy-start(bf16[512,3072]{1,0:T(8,128)(2,1)} %saved_inputs.1) | copy-start | bytes 9437188
  8.9 60.9 %copy-start.3 = (bf16[512,3072]{1,0:T(8,128)(2,1)S(1)}, bf16[512,3072]{1,0:T(8,128)(2,1)}, u32[]{:S(2)}) copy-start(bf16[512,3072]{1,0:T(8,128)(2,1)} %out_cotangent.1) | copy-start | bytes 9437188
  59.1 42.8 %copy-start.6 = (bf16[512,384]{1,0:T(8,128)(2,1)S(1)}, bf16[512,384]{1,0:T(8,128)(2,1)}, u32[]{:S(2)}) copy-start(bf16[512,384]{1,0:T(8,128)(2,1)} %query_cotangent.1) | copy-start | bytes 1179652
  59.1 42.8 %copy-start.7 = (bf16[512,384]{1,0:T(8,128)(2,1)S(1)}, bf16[512,384]{1,0:T(8,128)(2,1)}, u32[]{:S(2)}) copy-start(bf16[512,384]{1,0:T(8,128)(2,1)} %attn_outputs.1) | copy-start | bytes 1179652
  59.1 52.3 %collective-permute-start.2 = (bf16[96,24,128]{2,1,0:T(8,128)(2,1)S(1)}, bf16[96,24,128]{2,1,0:T(8,128)(2,1)S(1)}, u32[]{:S(2)}, u32[]{:S(2)}) collective-permute-start(bf16[96,24,128]{2,1,0:T(8,128)(2,1)S(1)} %all_to_all.25.packed), channel_id=1, source_target_pairs={{6,0},{7,1},{0,2},{1,3},{2,4},{3,5},{4,6},{5,7},{14,8},{15,9},{8,1... | collective-permute-start | bytes 1769480 | tf_op jit(solution)/shard_map/ppermute | solution.py:330
  62.3 49.1 %collective-permute-start.1 = (bf16[96,24,128]{2,1,0:T(8,128)(2,1)S(1)}, bf16[96,24,128]{2,1,0:T(8,128)(2,1)S(1)}, u32[]{:S(2)}, u32[]{:S(2)}) collective-permute-start(bf16[96,24,128]{2,1,0:T(8,128)(2,1)S(1)} %all_to_all.25.packed), channel_id=1, source_target_pairs={{4,0},{5,1},{6,2},{7,3},{0,4},{1,5},{2,6},{3,7},{12,8},{13,9},{14,... | collective-permute-start | bytes 1769480 | tf_op jit(solution)/shard_map/ppermute | solution.py:330
  66.7 44.7 %collective-permute-start = (bf16[96,24,128]{2,1,0:T(8,128)(2,1)S(1)}, bf16[96,24,128]{2,1,0:T(8,128)(2,1)S(1)}, u32[]{:S(2)}, u32[]{:S(2)}) collective-permute-start(bf16[96,24,128]{2,1,0:T(8,128)(2,1)S(1)} %all_to_all.25.packed), channel_id=1, source_target_pairs={{2,0},{3,1},{4,2},{5,3},{6,4},{7,5},{0,6},{1,7},{10,8},{11,9},{12,... | collective-permute-start | bytes 1769480 | tf_op jit(solution)/shard_map/ppermute | solution.py:330
  103.3 41.2 %all-to-all-start.1 = ((bf16[96,8,384]{2,1,0:T(8,128)(2,1)}), bf16[96,8,384]{2,1,0:T(8,128)(2,1)S(1)}, u32[]{:S(2)}, u32[]{:S(2)}) async-start(bf16[96,8,384]{2,1,0:T(8,128)(2,1)} %bitcast.12), calls=%async_computation.1 | async-start | bytes 1179648 | tf_op jit(solution)/shard_map/all_to_all | solution.py:326
  111.4 33.1 %copy-start.8 = (f32[2,4,384]{2,1,0:T(4,128)S(1)}, f32[2,4,384]{2,1,0:T(4,128)}, u32[]{:S(2)}) copy-start(f32[2,4,384]{2,1,0:T(4,128)} %first.1) | copy-start | bytes 36868
  111.4 33.1 %copy-start.9 = (f32[2,4,384]{2,1,0:T(4,128)S(1)}, f32[2,4,384]{2,1,0:T(4,128)}, u32[]{:S(2)}) copy-start(f32[2,4,384]{2,1,0:T(4,128)} %second.1) | copy-start | bytes 36868
  113.1 52.3 %collective-permute-start.3 = (bf16[4,96,24,128]{3,2,1,0:T(8,128)(2,1)}, bf16[4,96,24,128]{3,2,1,0:T(8,128)(2,1)}, u32[]{:S(2)}, u32[]{:S(2)}) collective-permute-start(bf16[4,96,24,128]{3,2,1,0:T(8,128)(2,1)} %pad_maximum_fusion.held), channel_id=1, source_target_pairs={{1,0},{0,1},{3,2},{2,3},{5,4},{4,5},{7,6},{6,7},{9,8},{8,9},{11,10... | collective-permute-start | bytes 7077896 | tf_op jit(solution)/shard_map/ppermute | solution.py:332
  161.8 22.2 %all-to-all-start.3 = ((bf16[8,12,4,896]{3,2,1,0:T(4,128)(2,1)}), bf16[8,12,4,896]{3,2,1,0:T(4,128)(2,1)S(1)}, u32[]{:S(2)}, u32[]{:S(2)}) async-start(bf16[8,12,4,896]{3,2,1,0:T(4,128)(2,1)} %shard_map.150), calls=%async_computation.3 | async-start | bytes 1376256 | tf_op jit(solution)/shard_map/all_to_all | solution.py:355
  184.7 14.1 %all-to-all-start.4 = ((f32[8,1,128]{2,1,0:T(1,128)}), f32[8,1,128]{2,1,0:T(1,128)S(1)}, u32[]{:S(2)}, u32[]{:S(2)}) async-start(f32[8,1,128]{2,1,0:T(1,128)} %shard_map.151), calls=%async_computation.4 | async-start | bytes 8192 | tf_op jit(solution)/shard_map/all_to_all | solution.py:409
  192.2 6.6 %copy-start.4 = (bf16[3072,384]{1,0:T(8,128)(2,1)S(1)}, bf16[3072,384]{1,0:T(8,128)(2,1)}, u32[]{:S(2)}) copy-start(bf16[3072,384]{1,0:T(8,128)(2,1)} %get-tuple-element.24.left) | copy-start | bytes 7077892
  198.8 2.3 %copy-start = (f32[3072,384]{1,0:T(8,128)S(1)}, f32[3072,384]{1,0:T(8,128)}, u32[]{:S(2)}) copy-start(f32[3072,384]{1,0:T(8,128)} %get-tuple-element.26.query_all) | copy-start | bytes 14155780
  201.2 2.3 %copy-start.1 = (f32[384,3072]{1,0:T(8,128)S(1)}, f32[384,3072]{1,0:T(8,128)}, u32[]{:S(2)}) copy-start(f32[384,3072]{1,0:T(8,128)} %get-tuple-element.27.out_all) | copy-start | bytes 14155780
  203.5 1.7 copy-start.5
Sparse Core Ops, SparseCore 0:
  12.3 145.9 all-gather.2

commit v10 on v8

--- a/solution.py
+++ b/solution.py
@@ -162,9 +162,6 @@
     out_copy,
     query_new,
     out_new,
-    near_left,
-    near_right,
-    near_masters,
     near_query,
     near_out,
     near_own,
@@ -172,7 +169,6 @@
     near_new,
     first,
     second,
-    arrived,
     own_arrived,
     left_for,
     own_left_for,
@@ -182,16 +178,6 @@
     own = query_master.shape[0]
     per = span // own
     parts = width // span
-    spans = [pl.ds(i * span, span) for i in range(parts)]
-    copies = []
-    for i, at in enumerate(spans):
-        held = pl.ds(i * per, per)
-        ways = (
-            (left.at[at], near_left.at[at]),
-            (masters.at[held], near_masters.at[held]),
-            (right.at[:, at], near_right.at[:, at]),
-        )
-        copies.append([pltpu.make_async_copy(x, y, arrived.at[i, k]) for k, (x, y) in enumerate(ways)])
     ways = (
         (own_left, near_own.at[0]),
         (own_right, near_own.at[1]),
@@ -199,7 +185,7 @@
         (out_master, near_master.at[1]),
     )
     own_copies = [pltpu.make_async_copy(x, y, own_arrived.at[k]) for k, (x, y) in enumerate(ways)]
-    for copy in [c for part in copies for c in part] + own_copies:
+    for copy in own_copies:
         copy.start()
 
     tp = squares.shape[0]
@@ -224,16 +210,15 @@
         scales.append(0.01 * lax.rsqrt(total / entries + 1e-06))
 
     sent = []
-    for i, at in enumerate(spans):
-        for copy in copies[i]:
-            copy.wait()
-        codes = near_masters[i * per : (i + 1) * per]
-        moved = jnp.dot(near_left[at], first[...], preferred_element_type=f32)
+    for i in range(parts):
+        at = pl.ds(i * span, span)
+        codes = masters[i * per : (i + 1) * per]
+        moved = jnp.dot(left[at], first[...], preferred_element_type=f32)
         kept = decoded(codes[:, :own].reshape(span, cols))
         near_query[at] = (kept - scales[0] * moved).astype(bf16)
         sent.append(pltpu.make_async_copy(near_query.at[at], query_copy.at[at], left_for.at[i, 0]))
         sent[-1].start()
-        moved = jnp.dot(second_turned, near_right[:, at], preferred_element_type=f32)
+        moved = jnp.dot(second_turned, right[:, at], preferred_element_type=f32)
         kept = decoded(codes[:, own:].reshape(span, cols).T)
         near_out[:, at] = (kept - scales[1] * moved).astype(bf16)
         sent.append(pltpu.make_async_copy(near_out.at[:, at], out_copy.at[:, at], left_for.at[i, 1]))
@@ -375,6 +360,8 @@
         cost_estimate=cost(1 << 30, 30 << 20),
     )(place, far(held), far(other))
 
+    low, masters = lax.optimization_barrier((low, masters))
+    parts = width // span
     squares = pl.pallas_call(
         sums_kernel,
         out_shape=jax.ShapeDtypeStruct((tp, 1, 128), f32),
@@ -385,7 +372,6 @@
     )(low)
     squares = lax.all_to_all(squares, "tp", 0, 0)
 
-    parts = width // span
     query_copy, out_copy, query_new, out_new = pl.pallas_call(
         functools.partial(final_kernel, float(rows * fs * cols * tp), span, rank_cols),
         out_shape=(
@@ -394,12 +380,9 @@
             pltpu.HBM((own, cols), f32),
             pltpu.HBM((own, cols), f32),
         ),
-        in_specs=[SMEM] + [VMEM] * 2 + [ANY] * 7,
+        in_specs=[SMEM] + [VMEM] * 5 + [ANY] * 4,
         out_specs=(ANY,) * 4,
         scratch_shapes=[
-            pltpu.VMEM((width, ranks), bf16),
-            pltpu.VMEM((ranks, width), bf16),
-            pltpu.VMEM(masters.shape, bf16),
             pltpu.VMEM((width, cols), bf16),
             pltpu.VMEM((cols, width), bf16),
             pltpu.VMEM((2, own, ranks), bf16),
@@ -407,20 +390,19 @@
             pltpu.VMEM((2, own, cols), f32),
             pltpu.VMEM((ranks, cols), bf16),
             pltpu.VMEM((ranks, cols), bf16),
-            pltpu.SemaphoreType.DMA((parts, 3)),
             pltpu.SemaphoreType.DMA((4,)),
             pltpu.SemaphoreType.DMA((parts, 2)),
             pltpu.SemaphoreType.DMA((2,)),
         ],
-        compiler_params=pltpu.CompilerParams(vmem_limit_bytes=32 << 20),
+        compiler_params=SMALL,
         cost_estimate=cost(4 * width * ranks * cols, 20 << 20),
     )(
         place,
         squares,
         low,
-        far(left),
-        far(right),
-        far(masters),
+        left,
+        right,
+        masters,
         far(own_left),
         far(own_right),
         far(query_master),

time: 203 us -> 207 us (1.020)
  local copies, waits for them, and re-layouts: 0.03 us -> 5.69 us
    unnamed x12 -> x18, local copies, waits for them, and re-layouts: 0.03 us -> 5.69 us
where the time goes in v10:
time: 207 us; the launch traced here: 206 us
  blocking collectives  118 us (57%)
  Pallas kernels  23.3 us (11%)
  waiting for transfers between devices  23.2 us (11%)
  starting transfers between devices  20.4 us (10%)
  between operations  14.2 us (7%)
  local copies, waits for them, and re-layouts  5.69 us (3%)
    all_to_all x1, blocking collectives, body(): packed = lax.all_to_all(packed, FS, 0, 0)  50.2 us
    all_to_all x1, blocking collectives, body(): pieces = lax.all_to_all(partial.reshape(fs, 2 * rows, cols), FS, 0, 0)  34.4 us
    ppermute x3, waiting for transfers between devices, body(): lax.ppermute(packed, 'tp', [((t + 2 * step) % tp, t) for t in range(tp)])  23.2 us
    all_gather x1, blocking collectives, body(): proj = lax.all_gather(proj, 'tp', axis=0, tiled=True)  18.1 us
    all_to_all x1, blocking collectives, body(): low = lax.all_to_all(low, 'z', 0, 0)  15.2 us
    ppermute x3, starting transfers between devices, body(): lax.ppermute(packed, 'tp', [((t + 2 * step) % tp, t) for t in range(tp)])  9.16 us
    pallas_call x1, Pallas kernels, body(): pl.pallas_call(functools.partial(prep_kernel, rank_cols), grid=(width //...  8.74 us
    pallas_call x1, Pallas kernels, body(): pl.pallas_call(functools.partial(final_kernel, float(rows * fs * cols * t...  7.09 us
  transfers between devices with their start and end apart: 7, of which 3 were waited for; matrix products, arithmetic and copies ran while one was open for 1% of the time, Pallas kernels for 7%

profile of v10, /device:TPU:1, one launch (start us, length us, event | category | flops | bytes accessed | tf_op | source)
XLA Modules:
  0.0 206.5 jit_solution(5886092516591871432)
XLA Ops:
  7.2 0.0 all-gather.3.cloned.1.call-start
  7.2 1.6 shard_map.145
  8.8 0.0 all-gather.3.cloned.1.call-update
  8.9 0.0 copy-start.1
  8.9 0.0 copy-start.2
  8.9 50.2 %all_to_all.25.packed = bf16[96,24,128]{2,1,0:T(8,128)(2,1)S(1)} all-to-all(bf16[96,24,128]{2,1,0:T(8,128)(2,1)S(1)} %shard_map.146), channel_id=1, replica_groups=mesh['z'=12,'y'=8,'tp'=8] {'z','y'}, dimensions={0} | all-to-all | bytes 1179648 | tf_op jit(solution)/shard_map/all_to_all | solution.py:285
  59.1 0.0 copy-done.1
  59.1 0.0 copy-done.2
  59.1 0.0 copy-start.5
  59.1 0.0 copy-start.6
  59.1 2.0 shard_map.147
  61.0 0.0 copy-start.7
  61.1 0.0 copy-start.8
  61.1 18.1 %all_gather.9.proj = bf16[768,512]{1,0:T(8,128)(2,1)S(1)} all-gather(bf16[96,512]{1,0:T(8,128)(2,1)S(1)} %shard_map.147), channel_id=1, replica_groups=mesh['z'=12,'y'=8,'tp'=8] {'tp'}, dimensions={0}, use_global_device_ids=true | all-gather | bytes 884736 | tf_op jit(solution)/shard_map/all_gather | solution.py:295
  79.2 0.0 copy-done.5
  79.2 0.0 copy-done.6
  79.2 1.4 shard_map.148
  80.6 34.4 %all_to_all.26.pieces = bf16[96,8,384]{2,1,0:T(8,128)(2,1)S(1)} all-to-all(bf16[96,8,384]{2,1,0:T(8,128)(2,1)} %bitcast.12), channel_id=1, replica_groups=mesh['z'=12,'y'=8,'tp'=8] {'z','y'}, dimensions={0} | all-to-all | bytes 1179648 | tf_op jit(solution)/shard_map/all_to_all | solution.py:305
  115.0 0.0 copy-done.7
  115.0 0.0 copy-done.8
  115.0 0.9 shard_map.149
  115.9 15.2 %all_to_all.27.low = bf16[12,4,896]{2,1,0:T(4,128)(2,1)S(1)} all-to-all(bf16[12,4,896]{2,1,0:T(4,128)(2,1)} %get-tuple-element.23), channel_id=1, replica_groups=mesh['z'=12,'y'=8,'tp'=8] {'z'}, dimensions={0} | all-to-all | bytes 172032 | tf_op jit(solution)/shard_map/all_to_all | solution.py:325
  131.1 0.9 shard_map.150
  132.0 3.8 %all-to-all-start.3 = ((bf16[8,12,4,896]{3,2,1,0:T(4,128)(2,1)}), bf16[8,12,4,896]{3,2,1,0:T(4,128)(2,1)S(1)}, u32[]{:S(2)}, u32[]{:S(2)}) async-start(bf16[8,12,4,896]{3,2,1,0:T(4,128)(2,1)} %shard_map.150), calls=%async_computation.3 | async-start | bytes 1376256 | tf_op jit(solution)/shard_map/all_to_all | solution.py:334
  135.7 2.9 %collective-permute-start.2 = (bf16[96,24,128]{2,1,0:T(8,128)(2,1)S(1)}, bf16[96,24,128]{2,1,0:T(8,128)(2,1)S(1)}, u32[]{:S(2)}, u32[]{:S(2)}) collective-permute-start(bf16[96,24,128]{2,1,0:T(8,128)(2,1)S(1)} %all_to_all.25.packed), channel_id=1, source_target_pairs={{6,0},{7,1},{0,2},{1,3},{2,4},{3,5},{4,6},{5,7},{14,8},{15,9},{8,1... | collective-permute-start | bytes 1769480 | tf_op jit(solution)/shard_map/ppermute | solution.py:309
  138.6 4.4 %collective-permute-start.1 = (bf16[96,24,128]{2,1,0:T(8,128)(2,1)S(1)}, bf16[96,24,128]{2,1,0:T(8,128)(2,1)S(1)}, u32[]{:S(2)}, u32[]{:S(2)}) collective-permute-start(bf16[96,24,128]{2,1,0:T(8,128)(2,1)S(1)} %all_to_all.25.packed), channel_id=1, source_target_pairs={{4,0},{5,1},{6,2},{7,3},{0,4},{1,5},{2,6},{3,7},{12,8},{13,9},{14,... | collective-permute-start | bytes 1769480 | tf_op jit(solution)/shard_map/ppermute | solution.py:309
  143.0 1.9 collective-permute-start
  144.9 0.1 pad_add_fusion.place
  145.0 4.9 %collective-permute-done.2 = bf16[96,24,128]{2,1,0:T(8,128)(2,1)S(1)} collective-permute-done((bf16[96,24,128]{2,1,0:T(8,128)(2,1)S(1)}, bf16[96,24,128]{2,1,0:T(8,128)(2,1)S(1)}, u32[]{:S(2)}, u32[]{:S(2)}) %collective-permute-start.2) | collective-permute-done | bytes 589856 | tf_op jit(solution)/shard_map/ppermute | solution.py:309
  149.9 13.6 %collective-permute-done.1 = bf16[96,24,128]{2,1,0:T(8,128)(2,1)S(1)} collective-permute-done((bf16[96,24,128]{2,1,0:T(8,128)(2,1)S(1)}, bf16[96,24,128]{2,1,0:T(8,128)(2,1)S(1)}, u32[]{:S(2)}, u32[]{:S(2)}) %collective-permute-start.1) | collective-permute-done | bytes 589856 | tf_op jit(solution)/shard_map/ppermute | solution.py:309
  163.5 4.7 %collective-permute-done = bf16[96,24,128]{2,1,0:T(8,128)(2,1)S(1)} collective-permute-done((bf16[96,24,128]{2,1,0:T(8,128)(2,1)S(1)}, bf16[96,24,128]{2,1,0:T(8,128)(2,1)S(1)}, u32[]{:S(2)}, u32[]{:S(2)}) %collective-permute-start) | collective-permute-done | bytes 589856 | tf_op jit(solution)/shard_map/ppermute | solution.py:309
  168.2 1.7 pad_maximum_fusion.held
  169.9 3.5 %collective-permute-start.3 = (bf16[4,96,24,128]{3,2,1,0:T(8,128)(2,1)}, bf16[4,96,24,128]{3,2,1,0:T(8,128)(2,1)}, u32[]{:S(2)}, u32[]{:S(2)}) collective-permute-start(bf16[4,96,24,128]{3,2,1,0:T(8,128)(2,1)} %pad_maximum_fusion.held), channel_id=1, source_target_pairs={{1,0},{0,1},{3,2},{2,3},{5,4},{4,5},{7,6},{6,7},{9,8},{8,9},{11,10... | collective-permute-start | bytes 7077896 | tf_op jit(solution)/shard_map/ppermute | solution.py:311
  173.4 0.0 all-to-all-done.3.low
  173.4 0.0 all-gather.3.cloned.1.call-done
  173.4 0.7 shard_map.151
  174.1 4.0 %all-to-all-start.4 = ((f32[8,1,128]{2,1,0:T(1,128)}), f32[8,1,128]{2,1,0:T(1,128)S(1)}, u32[]{:S(2)}, u32[]{:S(2)}) async-start(f32[8,1,128]{2,1,0:T(1,128)} %shard_map.151), calls=%async_computation.4 | async-start | bytes 8192 | tf_op jit(solution)/shard_map/all_to_all | solution.py:373
  178.1 0.0 collective-permute-done.3.other
  178.1 8.7 %shard_map.152 = (bf16[3072,384]{1,0:T(8,128)(2,1)}, bf16[384,3072]{1,0:T(8,128)(2,1)}, bf16[32,384]{1,0:T(8,128)(2,1)}, bf16[32,384]{1,0:T(8,128)(2,1)}) custom-call(s32[2]{0:T(128)S(1)} %pad_add_fusion.place, bf16[4,96,24,128]{3,2,1,0:T(8,128)(2,1)} %pad_maximum_fusion.held, bf16[4,96,24,128]{3,2,1,0:T(8,128)(2,1)} %collective-permute-done.3.other), custom_call_target="tpu_custom_call" | custom-call | flops 1073741824 | bytes 31457280 | tf_op jit(solution)/shard_map/pallas_call | solution.py:338
  186.9 0.0 all-to-all-done.4.squares
  186.9 0.0 copy-start
  186.9 2.3 %copy-done = bf16[6144,384]{1,0:T(8,128)(2,1)S(1)} copy-done((bf16[6144,384]{1,0:T(8,128)(2,1)S(1)}, bf16[6144,384]{1,0:T(8,128)(2,1)}, u32[]{:S(2)}) %copy-start) | copy-done | bytes 4718616
  189.2 0.0 copy-start.3
  189.2 1.7 copy-done.3
  190.9 0.0 copy-start.4
  190.9 1.7 copy-done.4
  192.5 7.1 %shard_map.153 = (bf16[3072,384]{1,0:T(8,128)(2,1)}, bf16[384,3072]{1,0:T(8,128)(2,1)}, f32[32,384]{1,0:T(8,128)}, f32[32,384]{1,0:T(8,128)}) custom-call(s32[2]{0:T(128)S(1)} %pad_add_fusion.place, f32[8,1,128]{2,1,0:T(1,128)S(1)} %all-to-all-done.4.squares, bf16[8,12,4,896]{3,2,1,0:T(4,128)(2,1)S(1)} %all-to-all-done.3.low, ...), custom_call_target="tpu_custom_call" | custom-call | flops 1811939328 | bytes 20971520 | tf_op jit(solution)/shard_map/pallas_call | solution.py:375
  (1 shorter events, 0.0 us)
Async XLA Ops:
  7.2 166.2 %all-gather.3.cloned.1.call-start = ((), (), s32[]{:S(2)}) async-start(), calls=%async_computation.5 | async-start | bytes 4767744 | tf_op jit(solution)/shard_map/all_gather | solution.py:284
  8.9 50.2 %copy-start.1 = (bf16[512,3072]{1,0:T(8,128)(2,1)S(1)}, bf16[512,3072]{1,0:T(8,128)(2,1)}, u32[]{:S(2)}) copy-start(bf16[512,3072]{1,0:T(8,128)(2,1)} %saved_inputs.1) | copy-start | bytes 9437188
  8.9 50.2 %copy-start.2 = (bf16[512,3072]{1,0:T(8,128)(2,1)S(1)}, bf16[512,3072]{1,0:T(8,128)(2,1)}, u32[]{:S(2)}) copy-start(bf16[512,3072]{1,0:T(8,128)(2,1)} %out_cotangent.1) | copy-start | bytes 9437188
  59.1 20.1 %copy-start.5 = (bf16[512,384]{1,0:T(8,128)(2,1)S(1)}, bf16[512,384]{1,0:T(8,128)(2,1)}, u32[]{:S(2)}) copy-start(bf16[512,384]{1,0:T(8,128)(2,1)} %query_cotangent.1) | copy-start | bytes 1179652
  59.1 20.1 %copy-start.6 = (bf16[512,384]{1,0:T(8,128)(2,1)S(1)}, bf16[512,384]{1,0:T(8,128)(2,1)}, u32[]{:S(2)}) copy-start(bf16[512,384]{1,0:T(8,128)(2,1)} %attn_outputs.1) | copy-start | bytes 1179652
  61.0 53.9 %copy-start.7 = (f32[2,4,384]{2,1,0:T(4,128)S(1)}, f32[2,4,384]{2,1,0:T(4,128)}, u32[]{:S(2)}) copy-start(f32[2,4,384]{2,1,0:T(4,128)} %first.1) | copy-start | bytes 36868
  61.1 53.9 %copy-start.8 = (f32[2,4,384]{2,1,0:T(4,128)S(1)}, f32[2,4,384]{2,1,0:T(4,128)}, u32[]{:S(2)}) copy-start(f32[2,4,384]{2,1,0:T(4,128)} %second.1) | copy-start | bytes 36868
  132.0 41.4 %all-to-all-start.3 = ((bf16[8,12,4,896]{3,2,1,0:T(4,128)(2,1)}), bf16[8,12,4,896]{3,2,1,0:T(4,128)(2,1)S(1)}, u32[]{:S(2)}, u32[]{:S(2)}) async-start(bf16[8,12,4,896]{3,2,1,0:T(4,128)(2,1)} %shard_map.150), calls=%async_computation.3 | async-start | bytes 1376256 | tf_op jit(solution)/shard_map/all_to_all | solution.py:334
  135.7 14.2 %collective-permute-start.2 = (bf16[96,24,128]{2,1,0:T(8,128)(2,1)S(1)}, bf16[96,24,128]{2,1,0:T(8,128)(2,1)S(1)}, u32[]{:S(2)}, u32[]{:S(2)}) collective-permute-start(bf16[96,24,128]{2,1,0:T(8,128)(2,1)S(1)} %all_to_all.25.packed), channel_id=1, source_target_pairs={{6,0},{7,1},{0,2},{1,3},{2,4},{3,5},{4,6},{5,7},{14,8},{15,9},{8,1... | collective-permute-start | bytes 1769480 | tf_op jit(solution)/shard_map/ppermute | solution.py:309
  138.6 24.9 %collective-permute-start.1 = (bf16[96,24,128]{2,1,0:T(8,128)(2,1)S(1)}, bf16[96,24,128]{2,1,0:T(8,128)(2,1)S(1)}, u32[]{:S(2)}, u32[]{:S(2)}) collective-permute-start(bf16[96,24,128]{2,1,0:T(8,128)(2,1)S(1)} %all_to_all.25.packed), channel_id=1, source_target_pairs={{4,0},{5,1},{6,2},{7,3},{0,4},{1,5},{2,6},{3,7},{12,8},{13,9},{14,... | collective-permute-start | bytes 1769480 | tf_op jit(solution)/shard_map/ppermute | solution.py:309
  143.0 25.2 %collective-permute-start = (bf16[96,24,128]{2,1,0:T(8,128)(2,1)S(1)}, bf16[96,24,128]{2,1,0:T(8,128)(2,1)S(1)}, u32[]{:S(2)}, u32[]{:S(2)}) collective-permute-start(bf16[96,24,128]{2,1,0:T(8,128)(2,1)S(1)} %all_to_all.25.packed), channel_id=1, source_target_pairs={{2,0},{3,1},{4,2},{5,3},{6,4},{7,5},{0,6},{1,7},{10,8},{11,9},{12,... | collective-permute-start | bytes 1769480 | tf_op jit(solution)/shard_map/ppermute | solution.py:309
  169.9 8.2 %collective-permute-start.3 = (bf16[4,96,24,128]{3,2,1,0:T(8,128)(2,1)}, bf16[4,96,24,128]{3,2,1,0:T(8,128)(2,1)}, u32[]{:S(2)}, u32[]{:S(2)}) collective-permute-start(bf16[4,96,24,128]{3,2,1,0:T(8,128)(2,1)} %pad_maximum_fusion.held), channel_id=1, source_target_pairs={{1,0},{0,1},{3,2},{2,3},{5,4},{4,5},{7,6},{6,7},{9,8},{8,9},{11,10... | collective-permute-start | bytes 7077896 | tf_op jit(solution)/shard_map/ppermute | solution.py:311
  174.1 12.8 %all-to-all-start.4 = ((f32[8,1,128]{2,1,0:T(1,128)}), f32[8,1,128]{2,1,0:T(1,128)S(1)}, u32[]{:S(2)}, u32[]{:S(2)}) async-start(f32[8,1,128]{2,1,0:T(1,128)} %shard_map.151), calls=%async_computation.4 | async-start | bytes 8192 | tf_op jit(solution)/shard_map/all_to_all | solution.py:373
  186.9 2.3 %copy-start = (bf16[6144,384]{1,0:T(8,128)(2,1)S(1)}, bf16[6144,384]{1,0:T(8,128)(2,1)}, u32[]{:S(2)}) copy-start(bf16[6144,384]{1,0:T(8,128)(2,1)} %all-gather.3.cloned.1.call-done) | copy-start | bytes 14155780
  189.2 1.7 copy-start.3
  190.9 1.7 copy-start.4
Sparse Core Ops, SparseCore 0:
  12.3 134.7 all-gather.2

commit v11 on v10

--- a/solution.py
+++ b/solution.py
@@ -89,6 +89,14 @@
     first, second = parts
     both = jnp.concatenate([first[:, :4], second[:, :4], first[:, 4:], second[:, 4:]], axis=1)
     out[...] = both.astype(bf16)
+
+
+def in_three(total):
+    parts = []
+    for _ in range(3):
+        parts.append(total.astype(bf16).astype(f32))
+        total = total - parts[-1]
+    return parts
 
 
 def moment_kernel(pieces, first, second, first_new, second_new, low):
@@ -105,11 +113,9 @@
     lane = lax.broadcasted_iota(jnp.int32, (rows, 128), 1)
     sums = jnp.zeros((rows, 128), f32)
     for k in range(2):
-        rest = jnp.sum(squares[k * rows : (k + 1) * rows], axis=(0, 1), keepdims=True)
-        for part in range(3):
-            rounded = rest.astype(bf16).astype(f32)
-            sums = jnp.where(lane == 3 * k + part, rounded, sums)
-            rest = rest - rounded
+        total = jnp.sum(squares[k * rows : (k + 1) * rows], axis=(0, 1), keepdims=True)
+        for part, value in enumerate(in_three(total)):
+            sums = jnp.where(lane == 3 * k + part, value, sums)
     sent = jnp.concatenate([direction[:rows], direction[rows:], sums], axis=1).astype(bf16)
     low[...] = jnp.broadcast_to(sent[None], low.shape)
 
@@ -117,38 +123,56 @@
 def prep_kernel(rank_cols, place, held, other, left, right, own_left, own_right, tile):
     own = own_left.shape[0]
     span = left.shape[0]
-    sides = [[], []]
-    for half in (held, other):
-        for s in range(half.shape[0]):
-            block = unpacked(half[s], 2 * rank_cols).reshape(span, 128)
+    chips = held.shape[0]
+    blocks = [[unpacked(half[s], 2 * rank_cols).reshape(span, 128) for s in range(chips)] for half in (held, other)]
+    here = place[1] % 2 == 0
+    by_core = [
+        [jnp.where(here, near, far) for near, far in zip(blocks[core], blocks[1 - core])] for core in range(2)
+    ]
+    for chip in range(chips):
+
+        @pl.when(place[1] // 2 == chip)
+        def _():
             for k in range(2):
-                sides[k].append(block[:, k * rank_cols : (k + 1) * rank_cols])
-    both = [jnp.concatenate(side, axis=1).astype(bf16) for side in sides]
-    left[...] = both[0]
-    right[...] = both[1].T
+                at = slice(k * rank_cols, (k + 1) * rank_cols)
+                side = [by_core[core][(s - chip) % chips][:, at] for s in range(chips) for core in range(2)]
+                side = jnp.concatenate(side, axis=1).astype(bf16)
+                tile[k] = side
+    left[...] = tile[0]
+    right[...] = tile[1].T
 
     @pl.when(pl.program_id(0) == place[0] // (span // own))
     def _():
         rows = pl.ds(pl.multiple_of(place[0] % (span // own) * own, own), own)
-        for side, out in zip(both, (own_left, own_right)):
-            tile[...] = side
-            out[...] = tile[rows]
+        own_left[...] = tile[0, rows]
+        own_right[...] = tile[1, rows]
 
 
 def spread_kernel(low, out):
-    out[...] = jnp.broadcast_to(low[...][None], out.shape)
+    depth, _, lanes = low.shape
+    lanes = lanes - 128
+    sums = jnp.sum(low[:, :, lanes:].astype(f32), axis=0)
+    lane = lax.broadcasted_iota(jnp.int32, sums.shape, 1)
+    squares = jnp.zeros(sums.shape, f32)
+    for k in range(2):
+        total = jnp.sum(jnp.where(lane // 3 == k, sums, 0.0)[:1], axis=1, keepdims=True)
+        for part, value in enumerate(in_three(total)):
+            squares = jnp.where(lane == 3 * k + part, value, squares)
+    squares = jnp.concatenate([squares] * (lanes // 128), axis=1).astype(bf16)
+    for y in range(out.shape[0]):
+        out[y, :depth] = low[:, :, :lanes]
+        out[y, depth] = squares
 
 
 def sums_kernel(low, squares):
-    sums = jnp.sum(low[:, :, :, -128:].astype(f32), axis=(0, 1))[:1]
+    depth = low.shape[1] - 1
+    sums = jnp.sum(low[:, depth, :, :128].astype(f32), axis=0)[:1]
     squares[...] = jnp.broadcast_to(sums[None], squares.shape)
 
 
 def final_kernel(
     entries,
     span,
-    rank_cols,
-    place,
     squares,
     low,
     left,
@@ -188,18 +212,14 @@
     for copy in own_copies:
         copy.start()
 
-    tp = squares.shape[0]
     height = low.shape[0]
-    per_block = rank_cols // low.shape[2]
-    for b in range(tp):
-        chip, core = b % (tp // 2), b // (tp // 2)
-        at = (place[1] + 2 * chip) % tp
-        at = at + core * (1 - 2 * (at % 2))
-        held = [at * per_block + j for j in range(per_block)]
-        block = [low[j % height, j // height].astype(f32) for j in held]
-        for k, step in enumerate((first, second)):
-            part = jnp.concatenate([piece[:, k * cols : (k + 1) * cols] for piece in block], axis=0)
-            step[b * rank_cols : (b + 1) * rank_cols] = part.astype(bf16)
+    rows = low.shape[2]
+    group = 16 // rows
+    for g in range(0, first.shape[0] // rows, group):
+        part = [low[f % height, f // height].astype(f32) for f in range(g, g + group)]
+        part = jnp.concatenate(part, axis=0).astype(bf16)
+        first[g * rows : (g + group) * rows] = part[:, :cols]
+        second[g * rows : (g + group) * rows] = part[:, cols:]
     second_turned = second[...].T
 
     sums = jnp.sum(squares[...], axis=0)
@@ -266,7 +286,10 @@
     place = jnp.stack([lax.axis_index(FS), lax.axis_index("tp")]).astype(jnp.int32)
     packed, masters = pl.pallas_call(
         send_kernel,
-        out_shape=(jax.ShapeDtypeStruct((fs, kept, 128), bf16), pltpu.HBM((2 * own, cols), bf16)),
+        out_shape=(
+            jax.ShapeDtypeStruct((fs, kept, 128), bf16),
+            pltpu.HBM((2 * own, cols), bf16),
+        ),
         in_specs=[pl.BlockSpec()] * 4,
         out_specs=(VMEM, VMEM),
         compiler_params=SMALL,
@@ -325,7 +348,7 @@
     low = lax.all_to_all(low, "z", 0, 0)
     low = pl.pallas_call(
         spread_kernel,
-        out_shape=pltpu.HBM((height, *low.shape), bf16),
+        out_shape=pltpu.HBM((height, depth + 1, rows, 2 * cols), bf16),
         in_specs=[VMEM],
         out_specs=VMEM,
         compiler_params=SMALL,
@@ -333,7 +356,7 @@
     )(low)
     low = lax.all_to_all(low, "y", 0, 0)
 
-    span = width // 6
+    span = width // 4
     per = span // own
     left, right, own_left, own_right = pl.pallas_call(
         functools.partial(prep_kernel, rank_cols),
@@ -355,7 +378,7 @@
             pl.BlockSpec((own, ranks), lambda i: (0, 0)),
             pl.BlockSpec((own, ranks), lambda i: (0, 0)),
         ),
-        scratch_shapes=[pltpu.VMEM((span, ranks), bf16)],
+        scratch_shapes=[pltpu.VMEM((2, span, ranks), bf16)],
         compiler_params=SMALL,
         cost_estimate=cost(1 << 30, 30 << 20),
     )(place, far(held), far(other))
@@ -373,14 +396,14 @@
     squares = lax.all_to_all(squares, "tp", 0, 0)
 
     query_copy, out_copy, query_new, out_new = pl.pallas_call(
-        functools.partial(final_kernel, float(rows * fs * cols * tp), span, rank_cols),
+        functools.partial(final_kernel, float(rows * fs * cols * tp), span),
         out_shape=(
             pltpu.HBM((width, cols), bf16),
             pltpu.HBM((cols, width), bf16),
             pltpu.HBM((own, cols), f32),
             pltpu.HBM((own, cols), f32),
         ),
-        in_specs=[SMEM] + [VMEM] * 5 + [ANY] * 4,
+        in_specs=[VMEM] * 5 + [ANY] * 4,
         out_specs=(ANY,) * 4,
         scratch_shapes=[
             pltpu.VMEM((width, cols), bf16),
@@ -397,7 +420,6 @@
         compiler_params=SMALL,
         cost_estimate=cost(4 * width * ranks * cols, 20 << 20),
     )(
-        place,
         squares,
         low,
         left,

time: 207 us -> 206 us (level)
  no operation moved by 1% of the time
where the time goes in v11:
time: 206 us; the launch traced here: 205 us
  blocking collectives  118 us (57%)
  waiting for transfers between devices  22.8 us (11%)
  Pallas kernels  21.7 us (11%)
  starting transfers between devices  20.9 us (10%)
  between operations  14.2 us (7%)
  local copies, waits for them, and re-layouts  5.69 us (3%)
    all_to_all x1, blocking collectives, body(): packed = lax.all_to_all(packed, FS, 0, 0)  50.2 us
    all_to_all x1, blocking collectives, body(): pieces = lax.all_to_all(partial.reshape(fs, 2 * rows, cols), FS, 0, 0)  34.4 us
    ppermute x3, waiting for transfers between devices, body(): lax.ppermute(packed, 'tp', [((t + 2 * step) % tp, t) for t in range(tp)])  22.8 us
    all_gather x1, blocking collectives, body(): proj = lax.all_gather(proj, 'tp', axis=0, tiled=True)  18.1 us
    all_to_all x1, blocking collectives, body(): low = lax.all_to_all(low, 'z', 0, 0)  15.2 us
    ppermute x3, starting transfers between devices, body(): lax.ppermute(packed, 'tp', [((t + 2 * step) % tp, t) for t in range(tp)])  9.57 us
    pallas_call x1, Pallas kernels, body(): pl.pallas_call(functools.partial(prep_kernel, rank_cols), grid=(width //...  8.9 us
    unnamed x18, local copies, waits for them, and re-layouts  5.69 us
  transfers between devices with their start and end apart: 7, of which 3 were waited for; matrix products, arithmetic and copies ran while one was open for 1% of the time, Pallas kernels for 7%

profile of v11, /device:TPU:1, one launch (start us, length us, event | category | flops | bytes accessed | tf_op | source)
XLA Modules:
  0.0 204.8 jit_solution(456801402628501647)
XLA Ops:
  7.2 0.0 all-gather.3.cloned.1.call-start
  7.2 1.6 shard_map.145
  8.8 0.0 all-gather.3.cloned.1.call-update
  8.9 0.0 copy-start.1
  8.9 0.0 copy-start.2
  8.9 50.2 %all_to_all.25.packed = bf16[96,24,128]{2,1,0:T(8,128)(2,1)S(1)} all-to-all(bf16[96,24,128]{2,1,0:T(8,128)(2,1)S(1)} %shard_map.146), channel_id=1, replica_groups=mesh['z'=12,'y'=8,'tp'=8] {'z','y'}, dimensions={0} | all-to-all | bytes 1179648 | tf_op jit(solution)/shard_map/all_to_all | solution.py:308
  59.1 0.0 copy-done.1
  59.1 0.0 copy-done.2
  59.1 0.0 copy-start.5
  59.1 0.0 copy-start.6
  59.1 2.0 shard_map.147
  61.0 0.0 copy-start.7
  61.1 0.0 copy-start.8
  61.1 18.1 %all_gather.9.proj = bf16[768,512]{1,0:T(8,128)(2,1)S(1)} all-gather(bf16[96,512]{1,0:T(8,128)(2,1)S(1)} %shard_map.147), channel_id=1, replica_groups=mesh['z'=12,'y'=8,'tp'=8] {'tp'}, dimensions={0}, use_global_device_ids=true | all-gather | bytes 884736 | tf_op jit(solution)/shard_map/all_gather | solution.py:318
  79.2 0.0 copy-done.5
  79.2 0.0 copy-done.6
  79.2 1.4 shard_map.148
  80.6 34.4 %all_to_all.26.pieces = bf16[96,8,384]{2,1,0:T(8,128)(2,1)S(1)} all-to-all(bf16[96,8,384]{2,1,0:T(8,128)(2,1)} %bitcast.12), channel_id=1, replica_groups=mesh['z'=12,'y'=8,'tp'=8] {'z','y'}, dimensions={0} | all-to-all | bytes 1179648 | tf_op jit(solution)/shard_map/all_to_all | solution.py:328
  115.0 0.0 copy-done.7
  115.0 0.0 copy-done.8
  115.0 0.9 shard_map.149
  115.9 15.2 %all_to_all.27.low = bf16[12,4,896]{2,1,0:T(4,128)(2,1)S(1)} all-to-all(bf16[12,4,896]{2,1,0:T(4,128)(2,1)} %get-tuple-element.23), channel_id=1, replica_groups=mesh['z'=12,'y'=8,'tp'=8] {'z'}, dimensions={0} | all-to-all | bytes 172032 | tf_op jit(solution)/shard_map/all_to_all | solution.py:348
  131.1 0.9 shard_map.150
  132.0 3.8 %all-to-all-start.3 = ((bf16[8,13,4,768]{3,2,1,0:T(4,128)(2,1)}), bf16[8,13,4,768]{3,2,1,0:T(4,128)(2,1)S(1)}, u32[]{:S(2)}, u32[]{:S(2)}) async-start(bf16[8,13,4,768]{3,2,1,0:T(4,128)(2,1)} %shard_map.150), calls=%async_computation.3 | async-start | bytes 1277952 | tf_op jit(solution)/shard_map/all_to_all | solution.py:357
  135.8 3.4 %collective-permute-start.2 = (bf16[96,24,128]{2,1,0:T(8,128)(2,1)S(1)}, bf16[96,24,128]{2,1,0:T(8,128)(2,1)S(1)}, u32[]{:S(2)}, u32[]{:S(2)}) collective-permute-start(bf16[96,24,128]{2,1,0:T(8,128)(2,1)S(1)} %all_to_all.25.packed), channel_id=1, source_target_pairs={{6,0},{7,1},{0,2},{1,3},{2,4},{3,5},{4,6},{5,7},{14,8},{15,9},{8,1... | collective-permute-start | bytes 1769480 | tf_op jit(solution)/shard_map/ppermute | solution.py:332
  139.1 3.8 %collective-permute-start.1 = (bf16[96,24,128]{2,1,0:T(8,128)(2,1)S(1)}, bf16[96,24,128]{2,1,0:T(8,128)(2,1)S(1)}, u32[]{:S(2)}, u32[]{:S(2)}) collective-permute-start(bf16[96,24,128]{2,1,0:T(8,128)(2,1)S(1)} %all_to_all.25.packed), channel_id=1, source_target_pairs={{4,0},{5,1},{6,2},{7,3},{0,4},{1,5},{2,6},{3,7},{12,8},{13,9},{14,... | collective-permute-start | bytes 1769480 | tf_op jit(solution)/shard_map/ppermute | solution.py:332
  143.0 2.4 %collective-permute-start = (bf16[96,24,128]{2,1,0:T(8,128)(2,1)S(1)}, bf16[96,24,128]{2,1,0:T(8,128)(2,1)S(1)}, u32[]{:S(2)}, u32[]{:S(2)}) collective-permute-start(bf16[96,24,128]{2,1,0:T(8,128)(2,1)S(1)} %all_to_all.25.packed), channel_id=1, source_target_pairs={{2,0},{3,1},{4,2},{5,3},{6,4},{7,5},{0,6},{1,7},{10,8},{11,9},{12,... | collective-permute-start | bytes 1769480 | tf_op jit(solution)/shard_map/ppermute | solution.py:332
  145.4 0.1 pad_add_fusion.place
  145.5 4.6 %collective-permute-done.2 = bf16[96,24,128]{2,1,0:T(8,128)(2,1)S(1)} collective-permute-done((bf16[96,24,128]{2,1,0:T(8,128)(2,1)S(1)}, bf16[96,24,128]{2,1,0:T(8,128)(2,1)S(1)}, u32[]{:S(2)}, u32[]{:S(2)}) %collective-permute-start.2) | collective-permute-done | bytes 589856 | tf_op jit(solution)/shard_map/ppermute | solution.py:332
  150.1 13.4 %collective-permute-done.1 = bf16[96,24,128]{2,1,0:T(8,128)(2,1)S(1)} collective-permute-done((bf16[96,24,128]{2,1,0:T(8,128)(2,1)S(1)}, bf16[96,24,128]{2,1,0:T(8,128)(2,1)S(1)}, u32[]{:S(2)}, u32[]{:S(2)}) %collective-permute-start.1) | collective-permute-done | bytes 589856 | tf_op jit(solution)/shard_map/ppermute | solution.py:332
  163.4 4.8 %collective-permute-done = bf16[96,24,128]{2,1,0:T(8,128)(2,1)S(1)} collective-permute-done((bf16[96,24,128]{2,1,0:T(8,128)(2,1)S(1)}, bf16[96,24,128]{2,1,0:T(8,128)(2,1)S(1)}, u32[]{:S(2)}, u32[]{:S(2)}) %collective-permute-start) | collective-permute-done | bytes 589856 | tf_op jit(solution)/shard_map/ppermute | solution.py:332
  168.2 1.7 pad_maximum_fusion.held
  169.9 3.5 %collective-permute-start.3 = (bf16[4,96,24,128]{3,2,1,0:T(8,128)(2,1)}, bf16[4,96,24,128]{3,2,1,0:T(8,128)(2,1)}, u32[]{:S(2)}, u32[]{:S(2)}) collective-permute-start(bf16[4,96,24,128]{3,2,1,0:T(8,128)(2,1)} %pad_maximum_fusion.held), channel_id=1, source_target_pairs={{1,0},{0,1},{3,2},{2,3},{5,4},{4,5},{7,6},{6,7},{9,8},{8,9},{11,10... | collective-permute-start | bytes 7077896 | tf_op jit(solution)/shard_map/ppermute | solution.py:334
  173.4 0.0 all-to-all-done.3.low
  173.4 0.0 all-gather.3.cloned.1.call-done
  173.4 0.6 shard_map.151
  174.0 4.0 %all-to-all-start.4 = ((f32[8,1,128]{2,1,0:T(1,128)}), f32[8,1,128]{2,1,0:T(1,128)S(1)}, u32[]{:S(2)}, u32[]{:S(2)}) async-start(f32[8,1,128]{2,1,0:T(1,128)} %shard_map.151), calls=%async_computation.4 | async-start | bytes 8192 | tf_op jit(solution)/shard_map/all_to_all | solution.py:396
  178.1 0.0 collective-permute-done.3.other
  178.1 8.9 %shard_map.152 = (bf16[3072,384]{1,0:T(8,128)(2,1)}, bf16[384,3072]{1,0:T(8,128)(2,1)}, bf16[32,384]{1,0:T(8,128)(2,1)}, bf16[32,384]{1,0:T(8,128)(2,1)}) custom-call(s32[2]{0:T(128)S(1)} %pad_add_fusion.place, bf16[4,96,24,128]{3,2,1,0:T(8,128)(2,1)} %pad_maximum_fusion.held, bf16[4,96,24,128]{3,2,1,0:T(8,128)(2,1)} %collective-permute-done.3.other), custom_call_target="tpu_custom_call" | custom-call | flops 1073741824 | bytes 31457280 | tf_op jit(solution)/shard_map/pallas_call | solution.py:361
  187.0 0.0 all-to-all-done.4.squares
  187.0 0.0 copy-start
  187.0 2.3 %copy-done = bf16[6144,384]{1,0:T(8,128)(2,1)S(1)} copy-done((bf16[6144,384]{1,0:T(8,128)(2,1)S(1)}, bf16[6144,384]{1,0:T(8,128)(2,1)}, u32[]{:S(2)}) %copy-start) | copy-done | bytes 4718616
  189.3 0.0 copy-start.3
  189.3 1.7 copy-done.3
  191.0 0.0 copy-start.4
  191.0 1.7 copy-done.4
  192.6 5.3 %shard_map.153 = (bf16[3072,384]{1,0:T(8,128)(2,1)}, bf16[384,3072]{1,0:T(8,128)(2,1)}, f32[32,384]{1,0:T(8,128)}, f32[32,384]{1,0:T(8,128)}) custom-call(f32[8,1,128]{2,1,0:T(1,128)S(1)} %all-to-all-done.4.squares, bf16[8,13,4,768]{3,2,1,0:T(4,128)(2,1)S(1)} %all-to-all-done.3.low, bf16[3072,384]{1,0:T(8,128)(2,1)S(1)} %copy-done.3, ...), custom_call_target="tpu_custom_call" | custom-call | flops 1811939328 | bytes 20971520 | tf_op jit(solution)/shard_map/pallas_call | solution.py:398
  (1 shorter events, 0.0 us)
Async XLA Ops:
  7.2 166.3 %all-gather.3.cloned.1.call-start = ((), (), s32[]{:S(2)}) async-start(), calls=%async_computation.5 | async-start | bytes 4767744 | tf_op jit(solution)/shard_map/all_gather | solution.py:307
  8.9 50.2 %copy-start.1 = (bf16[512,3072]{1,0:T(8,128)(2,1)S(1)}, bf16[512,3072]{1,0:T(8,128)(2,1)}, u32[]{:S(2)}) copy-start(bf16[512,3072]{1,0:T(8,128)(2,1)} %saved_inputs.1) | copy-start | bytes 9437188
  8.9 50.2 %copy-start.2 = (bf16[512,3072]{1,0:T(8,128)(2,1)S(1)}, bf16[512,3072]{1,0:T(8,128)(2,1)}, u32[]{:S(2)}) copy-start(bf16[512,3072]{1,0:T(8,128)(2,1)} %out_cotangent.1) | copy-start | bytes 9437188
  59.1 20.1 %copy-start.5 = (bf16[512,384]{1,0:T(8,128)(2,1)S(1)}, bf16[512,384]{1,0:T(8,128)(2,1)}, u32[]{:S(2)}) copy-start(bf16[512,384]{1,0:T(8,128)(2,1)} %query_cotangent.1) | copy-start | bytes 1179652
  59.1 20.1 %copy-start.6 = (bf16[512,384]{1,0:T(8,128)(2,1)S(1)}, bf16[512,384]{1,0:T(8,128)(2,1)}, u32[]{:S(2)}) copy-start(bf16[512,384]{1,0:T(8,128)(2,1)} %attn_outputs.1) | copy-start | bytes 1179652
  61.0 53.9 %copy-start.7 = (f32[2,4,384]{2,1,0:T(4,128)S(1)}, f32[2,4,384]{2,1,0:T(4,128)}, u32[]{:S(2)}) copy-start(f32[2,4,384]{2,1,0:T(4,128)} %first.1) | copy-start | bytes 36868
  61.1 53.9 %copy-start.8 = (f32[2,4,384]{2,1,0:T(4,128)S(1)}, f32[2,4,384]{2,1,0:T(4,128)}, u32[]{:S(2)}) copy-start(f32[2,4,384]{2,1,0:T(4,128)} %second.1) | copy-start | bytes 36868
  132.0 41.4 %all-to-all-start.3 = ((bf16[8,13,4,768]{3,2,1,0:T(4,128)(2,1)}), bf16[8,13,4,768]{3,2,1,0:T(4,128)(2,1)S(1)}, u32[]{:S(2)}, u32[]{:S(2)}) async-start(bf16[8,13,4,768]{3,2,1,0:T(4,128)(2,1)} %shard_map.150), calls=%async_computation.3 | async-start | bytes 1277952 | tf_op jit(solution)/shard_map/all_to_all | solution.py:357
  135.8 14.3 %collective-permute-start.2 = (bf16[96,24,128]{2,1,0:T(8,128)(2,1)S(1)}, bf16[96,24,128]{2,1,0:T(8,128)(2,1)S(1)}, u32[]{:S(2)}, u32[]{:S(2)}) collective-permute-start(bf16[96,24,128]{2,1,0:T(8,128)(2,1)S(1)} %all_to_all.25.packed), channel_id=1, source_target_pairs={{6,0},{7,1},{0,2},{1,3},{2,4},{3,5},{4,6},{5,7},{14,8},{15,9},{8,1... | collective-permute-start | bytes 1769480 | tf_op jit(solution)/shard_map/ppermute | solution.py:332
  139.1 24.3 %collective-permute-start.1 = (bf16[96,24,128]{2,1,0:T(8,128)(2,1)S(1)}, bf16[96,24,128]{2,1,0:T(8,128)(2,1)S(1)}, u32[]{:S(2)}, u32[]{:S(2)}) collective-permute-start(bf16[96,24,128]{2,1,0:T(8,128)(2,1)S(1)} %all_to_all.25.packed), channel_id=1, source_target_pairs={{4,0},{5,1},{6,2},{7,3},{0,4},{1,5},{2,6},{3,7},{12,8},{13,9},{14,... | collective-permute-start | bytes 1769480 | tf_op jit(solution)/shard_map/ppermute | solution.py:332
  143.0 25.3 %collective-permute-start = (bf16[96,24,128]{2,1,0:T(8,128)(2,1)S(1)}, bf16[96,24,128]{2,1,0:T(8,128)(2,1)S(1)}, u32[]{:S(2)}, u32[]{:S(2)}) collective-permute-start(bf16[96,24,128]{2,1,0:T(8,128)(2,1)S(1)} %all_to_all.25.packed), channel_id=1, source_target_pairs={{2,0},{3,1},{4,2},{5,3},{6,4},{7,5},{0,6},{1,7},{10,8},{11,9},{12,... | collective-permute-start | bytes 1769480 | tf_op jit(solution)/shard_map/ppermute | solution.py:332
  169.9 8.1 %collective-permute-start.3 = (bf16[4,96,24,128]{3,2,1,0:T(8,128)(2,1)}, bf16[4,96,24,128]{3,2,1,0:T(8,128)(2,1)}, u32[]{:S(2)}, u32[]{:S(2)}) collective-permute-start(bf16[4,96,24,128]{3,2,1,0:T(8,128)(2,1)} %pad_maximum_fusion.held), channel_id=1, source_target_pairs={{1,0},{0,1},{3,2},{2,3},{5,4},{4,5},{7,6},{6,7},{9,8},{8,9},{11,10... | collective-permute-start | bytes 7077896 | tf_op jit(solution)/shard_map/ppermute | solution.py:334
  174.0 12.9 %all-to-all-start.4 = ((f32[8,1,128]{2,1,0:T(1,128)}), f32[8,1,128]{2,1,0:T(1,128)S(1)}, u32[]{:S(2)}, u32[]{:S(2)}) async-start(f32[8,1,128]{2,1,0:T(1,128)} %shard_map.151), calls=%async_computation.4 | async-start | bytes 8192 | tf_op jit(solution)/shard_map/all_to_all | solution.py:396
  187.0 2.3 %copy-start = (bf16[6144,384]{1,0:T(8,128)(2,1)S(1)}, bf16[6144,384]{1,0:T(8,128)(2,1)}, u32[]{:S(2)}) copy-start(bf16[6144,384]{1,0:T(8,128)(2,1)} %all-gather.3.cloned.1.call-done) | copy-start | bytes 14155780
  189.3 1.7 copy-start.3
  191.0 1.7 copy-start.4
Sparse Core Ops, SparseCore 0:
  12.3 134.7 all-gather.2

commit v12 on v11

--- a/solution.py
+++ b/solution.py
@@ -88,7 +88,15 @@
         parts.append(jnp.dot(ranks, other[...], preferred_element_type=f32).reshape(-1, 8, cols))
     first, second = parts
     both = jnp.concatenate([first[:, :4], second[:, :4], first[:, 4:], second[:, 4:]], axis=1)
-    out[...] = both.astype(bf16)
+    height, depth = out.shape[:2]
+    both = both.astype(bf16).reshape(depth, height // 2, 16, cols)
+    for y in range(0, height, 2):
+        out[y] = both[:, y // 2, :8]
+        out[y + 1] = both[:, y // 2, 8:]
+
+
+def fold_kernel(pieces, out):
+    out[...] = jnp.sum(pieces[...].astype(f32), axis=0)
 
 
 def in_three(total):
@@ -101,7 +109,7 @@
 
 def moment_kernel(pieces, first, second, first_new, second_new, low):
     rows = first.shape[1]
-    grads = jnp.sum(pieces[...].astype(f32), axis=0)
+    grads = jnp.sum(pieces[...], axis=0)
     new_first = 0.9 * jnp.concatenate([first[0], first[1]], axis=0) + 0.1 * grads
     new_second = 0.99 * jnp.concatenate([second[0], second[1]], axis=0) + 0.01 * grads * grads
     direction = new_first / (jnp.sqrt(new_second) + 1e-08)
@@ -319,13 +327,22 @@
 
     partial = pl.pallas_call(
         functools.partial(grad_kernel, rank_cols),
-        out_shape=pltpu.HBM((fs // 2, 4 * rows, cols), bf16),
+        out_shape=pltpu.HBM((height, depth, 2 * rows, cols), bf16),
         in_specs=[VMEM] * 3,
         out_specs=VMEM,
         compiler_params=SMALL,
         cost_estimate=cost(4 * ranks * tokens * cols, 2 << 20),
     )(proj, query_cotangent, attn_outputs)
-    pieces = lax.all_to_all(partial.reshape(fs, 2 * rows, cols), FS, 0, 0)
+    pieces = lax.all_to_all(partial, "y", 0, 0)
+    pieces = pl.pallas_call(
+        fold_kernel,
+        out_shape=jax.ShapeDtypeStruct((depth, 2 * rows, cols), f32),
+        in_specs=[VMEM],
+        out_specs=VMEM,
+        compiler_params=SMALL,
+        cost_estimate=cost(1 << 20, 1 << 20),
+    )(pieces)
+    pieces = lax.all_to_all(pieces, "z", 0, 0)
 
     held = [packed]
     for step in range(1, tp // 2):

time: 206 us -> 210 us (1.019)
  blocking collectives: 118 us -> 122 us
    all_to_all x1 -> x2, blocking collectives: 34.4 us -> 39.6 us  [the longest x1 22.8 us: body(): pieces = lax.all_to_all(partial, 'y', 0, 0)]
where the time goes in v12:
time: 210 us; the launch traced here: 209 us
  blocking collectives  122 us (58%)
  waiting for transfers between devices  24 us (11%)
  Pallas kernels  21.6 us (10%)
  starting transfers between devices  19.5 us (9%)
  between operations  14.2 us (7%)
  local copies, waits for them, and re-layouts  5.69 us (3%)
    all_to_all x1, blocking collectives, body(): packed = lax.all_to_all(packed, FS, 0, 0)  50.2 us
    ppermute x3, waiting for transfers between devices, body(): lax.ppermute(packed, 'tp', [((t + 2 * step) % tp, t) for t in range(tp)])  23.9 us
    all_to_all x1, blocking collectives, body(): pieces = lax.all_to_all(partial, 'y', 0, 0)  22.8 us
    all_gather x1, blocking collectives, body(): proj = lax.all_gather(proj, 'tp', axis=0, tiled=True)  18.1 us
    all_to_all x1, blocking collectives, body(): pieces = lax.all_to_all(pieces, 'z', 0, 0)  16.8 us
    all_to_all x1, blocking collectives, body(): low = lax.all_to_all(low, 'z', 0, 0)  14.3 us
    pallas_call x1, Pallas kernels, body(): pl.pallas_call(functools.partial(prep_kernel, rank_cols), grid=(width //...  8.9 us
    ppermute x3, starting transfers between devices, body(): lax.ppermute(packed, 'tp', [((t + 2 * step) % tp, t) for t in range(tp)])  8.41 us
  transfers between devices with their start and end apart: 7, of which 3 were waited for; matrix products, arithmetic and copies ran while one was open for 1% of the time, Pallas kernels for 7%

profile of v12, /device:TPU:1, one launch (start us, length us, event | category | flops | bytes accessed | tf_op | source)
XLA Modules:
  0.0 208.9 jit_solution(14892830304577713807)
XLA Ops:
  7.2 0.0 all-gather.3.cloned.1.call-start
  7.2 1.6 shard_map.145
  8.8 0.0 all-gather.3.cloned.1.call-update
  8.9 0.0 copy-start.1
  8.9 0.0 copy-start.2
  8.9 50.2 %all_to_all.30.packed = bf16[96,24,128]{2,1,0:T(8,128)(2,1)S(1)} all-to-all(bf16[96,24,128]{2,1,0:T(8,128)(2,1)S(1)} %shard_map.146), channel_id=1, replica_groups=mesh['z'=12,'y'=8,'tp'=8] {'z','y'}, dimensions={0} | all-to-all | bytes 1179648 | tf_op jit(solution)/shard_map/all_to_all | solution.py:316
  59.1 0.0 copy-done.1
  59.1 0.0 copy-done.2
  59.1 0.0 copy-start.5
  59.1 0.0 copy-start.6
  59.1 2.0 shard_map.147
  61.0 18.1 %all_gather.9.proj = bf16[768,512]{1,0:T(8,128)(2,1)S(1)} all-gather(bf16[96,512]{1,0:T(8,128)(2,1)S(1)} %shard_map.147), channel_id=1, replica_groups=mesh['z'=12,'y'=8,'tp'=8] {'tp'}, dimensions={0}, use_global_device_ids=true | all-gather | bytes 884736 | tf_op jit(solution)/shard_map/all_gather | solution.py:326
  79.2 0.0 copy-done.5
  79.2 0.0 copy-done.6
  79.2 0.0 copy-start.7
  79.2 0.0 copy-start.8
  79.2 1.4 shard_map.148
  80.6 22.8 %all_to_all.31.pieces = bf16[8,12,8,384]{3,2,1,0:T(8,128)(2,1)S(1)} all-to-all(bf16[8,12,8,384]{3,2,1,0:T(8,128)(2,1)} %shard_map.148), channel_id=1, replica_groups=mesh['z'=12,'y'=8,'tp'=8] {'y'}, dimensions={0} | all-to-all | bytes 1179648 | tf_op jit(solution)/shard_map/all_to_all | solution.py:336
  103.4 0.1 shard_map.149
  103.5 16.8 %all_to_all.32.pieces = f32[12,8,384]{2,1,0:T(8,128)S(1)} all-to-all(f32[12,8,384]{2,1,0:T(8,128)S(1)} %shard_map.149), channel_id=1, replica_groups=mesh['z'=12,'y'=8,'tp'=8] {'z'}, dimensions={0} | all-to-all | bytes 294912 | tf_op jit(solution)/shard_map/all_to_all | solution.py:345
  120.2 0.0 copy-done.7
  120.2 0.0 copy-done.8
  120.3 0.8 shard_map.150
  121.1 14.3 %all_to_all.33.low = bf16[12,4,896]{2,1,0:T(4,128)(2,1)S(1)} all-to-all(bf16[12,4,896]{2,1,0:T(4,128)(2,1)} %get-tuple-element.23), channel_id=1, replica_groups=mesh['z'=12,'y'=8,'tp'=8] {'z'}, dimensions={0} | all-to-all | bytes 172032 | tf_op jit(solution)/shard_map/all_to_all | solution.py:365
  135.3 0.9 shard_map.151
  136.3 3.5 %all-to-all-start.4 = ((bf16[8,13,4,768]{3,2,1,0:T(4,128)(2,1)}), bf16[8,13,4,768]{3,2,1,0:T(4,128)(2,1)S(1)}, u32[]{:S(2)}, u32[]{:S(2)}) async-start(bf16[8,13,4,768]{3,2,1,0:T(4,128)(2,1)} %shard_map.151), calls=%async_computation.4 | async-start | bytes 1277952 | tf_op jit(solution)/shard_map/all_to_all | solution.py:374
  139.8 1.9 collective-permute-start.2
  141.8 4.1 %collective-permute-start.1 = (bf16[96,24,128]{2,1,0:T(8,128)(2,1)S(1)}, bf16[96,24,128]{2,1,0:T(8,128)(2,1)S(1)}, u32[]{:S(2)}, u32[]{:S(2)}) collective-permute-start(bf16[96,24,128]{2,1,0:T(8,128)(2,1)S(1)} %all_to_all.30.packed), channel_id=1, source_target_pairs={{4,0},{5,1},{6,2},{7,3},{0,4},{1,5},{2,6},{3,7},{12,8},{13,9},{14,... | collective-permute-start | bytes 1769480 | tf_op jit(solution)/shard_map/ppermute | solution.py:349
  145.9 2.4 %collective-permute-start = (bf16[96,24,128]{2,1,0:T(8,128)(2,1)S(1)}, bf16[96,24,128]{2,1,0:T(8,128)(2,1)S(1)}, u32[]{:S(2)}, u32[]{:S(2)}) collective-permute-start(bf16[96,24,128]{2,1,0:T(8,128)(2,1)S(1)} %all_to_all.30.packed), channel_id=1, source_target_pairs={{2,0},{3,1},{4,2},{5,3},{6,4},{7,5},{0,6},{1,7},{10,8},{11,9},{12,... | collective-permute-start | bytes 1769480 | tf_op jit(solution)/shard_map/ppermute | solution.py:349
  148.3 0.1 pad_add_fusion.place
  148.4 7.3 %collective-permute-done.2 = bf16[96,24,128]{2,1,0:T(8,128)(2,1)S(1)} collective-permute-done((bf16[96,24,128]{2,1,0:T(8,128)(2,1)S(1)}, bf16[96,24,128]{2,1,0:T(8,128)(2,1)S(1)}, u32[]{:S(2)}, u32[]{:S(2)}) %collective-permute-start.2) | collective-permute-done | bytes 589856 | tf_op jit(solution)/shard_map/ppermute | solution.py:349
  155.7 9.9 %collective-permute-done.1 = bf16[96,24,128]{2,1,0:T(8,128)(2,1)S(1)} collective-permute-done((bf16[96,24,128]{2,1,0:T(8,128)(2,1)S(1)}, bf16[96,24,128]{2,1,0:T(8,128)(2,1)S(1)}, u32[]{:S(2)}, u32[]{:S(2)}) %collective-permute-start.1) | collective-permute-done | bytes 589856 | tf_op jit(solution)/shard_map/ppermute | solution.py:349
  165.6 6.7 %collective-permute-done = bf16[96,24,128]{2,1,0:T(8,128)(2,1)S(1)} collective-permute-done((bf16[96,24,128]{2,1,0:T(8,128)(2,1)S(1)}, bf16[96,24,128]{2,1,0:T(8,128)(2,1)S(1)}, u32[]{:S(2)}, u32[]{:S(2)}) %collective-permute-start) | collective-permute-done | bytes 589856 | tf_op jit(solution)/shard_map/ppermute | solution.py:349
  172.3 1.7 pad_maximum_fusion.held
  174.0 3.5 %collective-permute-start.3 = (bf16[4,96,24,128]{3,2,1,0:T(8,128)(2,1)}, bf16[4,96,24,128]{3,2,1,0:T(8,128)(2,1)}, u32[]{:S(2)}, u32[]{:S(2)}) collective-permute-start(bf16[4,96,24,128]{3,2,1,0:T(8,128)(2,1)} %pad_maximum_fusion.held), channel_id=1, source_target_pairs={{1,0},{0,1},{3,2},{2,3},{5,4},{4,5},{7,6},{6,7},{9,8},{8,9},{11,10... | collective-permute-start | bytes 7077896 | tf_op jit(solution)/shard_map/ppermute | solution.py:351
  177.5 0.0 all-to-all-done.4.low
  177.5 0.0 all-gather.3.cloned.1.call-done
  177.5 0.6 shard_map.152
  178.1 4.0 %all-to-all-start.5 = ((f32[8,1,128]{2,1,0:T(1,128)}), f32[8,1,128]{2,1,0:T(1,128)S(1)}, u32[]{:S(2)}, u32[]{:S(2)}) async-start(f32[8,1,128]{2,1,0:T(1,128)} %shard_map.152), calls=%async_computation.5 | async-start | bytes 8192 | tf_op jit(solution)/shard_map/all_to_all | solution.py:413
  182.1 0.0 collective-permute-done.3.other
  182.1 8.9 %shard_map.153 = (bf16[3072,384]{1,0:T(8,128)(2,1)}, bf16[384,3072]{1,0:T(8,128)(2,1)}, bf16[32,384]{1,0:T(8,128)(2,1)}, bf16[32,384]{1,0:T(8,128)(2,1)}) custom-call(s32[2]{0:T(128)S(1)} %pad_add_fusion.place, bf16[4,96,24,128]{3,2,1,0:T(8,128)(2,1)} %pad_maximum_fusion.held, bf16[4,96,24,128]{3,2,1,0:T(8,128)(2,1)} %collective-permute-done.3.other), custom_call_target="tpu_custom_call" | custom-call | flops 1073741824 | bytes 31457280 | tf_op jit(solution)/shard_map/pallas_call | solution.py:378
  191.0 0.0 all-to-all-done.5.squares
  191.0 0.0 copy-start
  191.1 2.3 %copy-done = bf16[6144,384]{1,0:T(8,128)(2,1)S(1)} copy-done((bf16[6144,384]{1,0:T(8,128)(2,1)S(1)}, bf16[6144,384]{1,0:T(8,128)(2,1)}, u32[]{:S(2)}) %copy-start) | copy-done | bytes 4718616
  193.4 0.0 copy-start.3
  193.4 1.7 copy-done.3
  195.0 0.0 copy-start.4
  195.0 1.7 copy-done.4
  196.7 5.3 %shard_map.154 = (bf16[3072,384]{1,0:T(8,128)(2,1)}, bf16[384,3072]{1,0:T(8,128)(2,1)}, f32[32,384]{1,0:T(8,128)}, f32[32,384]{1,0:T(8,128)}) custom-call(f32[8,1,128]{2,1,0:T(1,128)S(1)} %all-to-all-done.5.squares, bf16[8,13,4,768]{3,2,1,0:T(4,128)(2,1)S(1)} %all-to-all-done.4.low, bf16[3072,384]{1,0:T(8,128)(2,1)S(1)} %copy-done.3, ...), custom_call_target="tpu_custom_call" | custom-call | flops 1811939328 | bytes 20971520 | tf_op jit(solution)/shard_map/pallas_call | solution.py:415
  (1 shorter events, 0.0 us)
Async XLA Ops:
  7.2 170.3 %all-gather.3.cloned.1.call-start = ((), (), s32[]{:S(2)}) async-start(), calls=%async_computation.6 | async-start | bytes 4767744 | tf_op jit(solution)/shard_map/all_gather | solution.py:315
  8.9 50.2 %copy-start.1 = (bf16[512,3072]{1,0:T(8,128)(2,1)S(1)}, bf16[512,3072]{1,0:T(8,128)(2,1)}, u32[]{:S(2)}) copy-start(bf16[512,3072]{1,0:T(8,128)(2,1)} %saved_inputs.1) | copy-start | bytes 9437188
  8.9 50.2 %copy-start.2 = (bf16[512,3072]{1,0:T(8,128)(2,1)S(1)}, bf16[512,3072]{1,0:T(8,128)(2,1)}, u32[]{:S(2)}) copy-start(bf16[512,3072]{1,0:T(8,128)(2,1)} %out_cotangent.1) | copy-start | bytes 9437188
  59.1 20.1 %copy-start.5 = (bf16[512,384]{1,0:T(8,128)(2,1)S(1)}, bf16[512,384]{1,0:T(8,128)(2,1)}, u32[]{:S(2)}) copy-start(bf16[512,384]{1,0:T(8,128)(2,1)} %query_cotangent.1) | copy-start | bytes 1179652
  59.1 20.1 %copy-start.6 = (bf16[512,384]{1,0:T(8,128)(2,1)S(1)}, bf16[512,384]{1,0:T(8,128)(2,1)}, u32[]{:S(2)}) copy-start(bf16[512,384]{1,0:T(8,128)(2,1)} %attn_outputs.1) | copy-start | bytes 1179652
  79.2 41.1 %copy-start.7 = (f32[2,4,384]{2,1,0:T(4,128)S(1)}, f32[2,4,384]{2,1,0:T(4,128)}, u32[]{:S(2)}) copy-start(f32[2,4,384]{2,1,0:T(4,128)} %first.1) | copy-start | bytes 36868
  79.2 41.1 %copy-start.8 = (f32[2,4,384]{2,1,0:T(4,128)S(1)}, f32[2,4,384]{2,1,0:T(4,128)}, u32[]{:S(2)}) copy-start(f32[2,4,384]{2,1,0:T(4,128)} %second.1) | copy-start | bytes 36868
  136.3 41.2 %all-to-all-start.4 = ((bf16[8,13,4,768]{3,2,1,0:T(4,128)(2,1)}), bf16[8,13,4,768]{3,2,1,0:T(4,128)(2,1)S(1)}, u32[]{:S(2)}, u32[]{:S(2)}) async-start(bf16[8,13,4,768]{3,2,1,0:T(4,128)(2,1)} %shard_map.151), calls=%async_computation.4 | async-start | bytes 1277952 | tf_op jit(solution)/shard_map/all_to_all | solution.py:374
  139.8 15.9 %collective-permute-start.2 = (bf16[96,24,128]{2,1,0:T(8,128)(2,1)S(1)}, bf16[96,24,128]{2,1,0:T(8,128)(2,1)S(1)}, u32[]{:S(2)}, u32[]{:S(2)}) collective-permute-start(bf16[96,24,128]{2,1,0:T(8,128)(2,1)S(1)} %all_to_all.30.packed), channel_id=1, source_target_pairs={{6,0},{7,1},{0,2},{1,3},{2,4},{3,5},{4,6},{5,7},{14,8},{15,9},{8,1... | collective-permute-start | bytes 1769480 | tf_op jit(solution)/shard_map/ppermute | solution.py:349
  141.8 23.8 %collective-permute-start.1 = (bf16[96,24,128]{2,1,0:T(8,128)(2,1)S(1)}, bf16[96,24,128]{2,1,0:T(8,128)(2,1)S(1)}, u32[]{:S(2)}, u32[]{:S(2)}) collective-permute-start(bf16[96,24,128]{2,1,0:T(8,128)(2,1)S(1)} %all_to_all.30.packed), channel_id=1, source_target_pairs={{4,0},{5,1},{6,2},{7,3},{0,4},{1,5},{2,6},{3,7},{12,8},{13,9},{14,... | collective-permute-start | bytes 1769480 | tf_op jit(solution)/shard_map/ppermute | solution.py:349
  145.9 26.4 %collective-permute-start = (bf16[96,24,128]{2,1,0:T(8,128)(2,1)S(1)}, bf16[96,24,128]{2,1,0:T(8,128)(2,1)S(1)}, u32[]{:S(2)}, u32[]{:S(2)}) collective-permute-start(bf16[96,24,128]{2,1,0:T(8,128)(2,1)S(1)} %all_to_all.30.packed), channel_id=1, source_target_pairs={{2,0},{3,1},{4,2},{5,3},{6,4},{7,5},{0,6},{1,7},{10,8},{11,9},{12,... | collective-permute-start | bytes 1769480 | tf_op jit(solution)/shard_map/ppermute | solution.py:349
  174.0 8.1 %collective-permute-start.3 = (bf16[4,96,24,128]{3,2,1,0:T(8,128)(2,1)}, bf16[4,96,24,128]{3,2,1,0:T(8,128)(2,1)}, u32[]{:S(2)}, u32[]{:S(2)}) collective-permute-start(bf16[4,96,24,128]{3,2,1,0:T(8,128)(2,1)} %pad_maximum_fusion.held), channel_id=1, source_target_pairs={{1,0},{0,1},{3,2},{2,3},{5,4},{4,5},{7,6},{6,7},{9,8},{8,9},{11,10... | collective-permute-start | bytes 7077896 | tf_op jit(solution)/shard_map/ppermute | solution.py:351
  178.1 12.9 %all-to-all-start.5 = ((f32[8,1,128]{2,1,0:T(1,128)}), f32[8,1,128]{2,1,0:T(1,128)S(1)}, u32[]{:S(2)}, u32[]{:S(2)}) async-start(f32[8,1,128]{2,1,0:T(1,128)} %shard_map.152), calls=%async_computation.5 | async-start | bytes 8192 | tf_op jit(solution)/shard_map/all_to_all | solution.py:413
  191.0 2.3 %copy-start = (bf16[6144,384]{1,0:T(8,128)(2,1)S(1)}, bf16[6144,384]{1,0:T(8,128)(2,1)}, u32[]{:S(2)}) copy-start(bf16[6144,384]{1,0:T(8,128)(2,1)} %all-gather.3.cloned.1.call-done) | copy-start | bytes 14155780
  193.4 1.7 copy-start.3
  195.0 1.7 copy-start.4
Sparse Core Ops, SparseCore 0:
  12.3 133.7 all-gather.2

commit v13 on v11

--- a/solution.py
+++ b/solution.py
@@ -53,6 +53,15 @@
     out[...] = jnp.broadcast_to(packed[None], out.shape)
 
 
+def copies_kernel(packed, out):
+    out[...] = jnp.broadcast_to(packed[...][None], out.shape)
+
+
+def by_place(packed):
+    height, depth = packed.shape[:2]
+    return jnp.concatenate([packed[y, z][None] for z in range(depth) for y in range(height)], axis=0)
+
+
 def hold_kernel(masters, packed, out):
     pass
 
@@ -68,11 +77,11 @@
 
 
 def proj_kernel(used, packed, saved_inputs, out_cotangent, out, factors):
-    own = factors.shape[0] // packed.shape[0]
-    step = 8
-    for i in range(0, packed.shape[0], step):
-        block = unpacked(packed[i : i + step], used).reshape(step * own, 128)
-        factors[i * own : (i + step) * own] = block.astype(bf16)
+    depth = packed.shape[1]
+    span = factors.shape[0] // depth
+    for z in range(depth):
+        block = unpacked(by_place(packed[:, z : z + 1]), used).reshape(span, 128)
+        factors[z * span : (z + 1) * span] = block.astype(bf16)
     left = jnp.dot(saved_inputs[...], factors[...], preferred_element_type=f32)
     right = jnp.dot(out_cotangent[...], factors[...], preferred_element_type=f32)
     lane = lax.broadcasted_iota(jnp.int32, left.shape, 1)
@@ -124,7 +133,7 @@
     own = own_left.shape[0]
     span = left.shape[0]
     chips = held.shape[0]
-    blocks = [[unpacked(half[s], 2 * rank_cols).reshape(span, 128) for s in range(chips)] for half in (held, other)]
+    blocks = [[unpacked(by_place(half[s]), 2 * rank_cols).reshape(span, 128) for s in range(chips)] for half in (held, other)]
     here = place[1] % 2 == 0
     by_core = [
         [jnp.where(here, near, far) for near, far in zip(blocks[core], blocks[1 - core])] for core in range(2)
@@ -287,7 +296,7 @@
     packed, masters = pl.pallas_call(
         send_kernel,
         out_shape=(
-            jax.ShapeDtypeStruct((fs, kept, 128), bf16),
+            jax.ShapeDtypeStruct((depth, kept, 128), bf16),
             pltpu.HBM((2 * own, cols), bf16),
         ),
         in_specs=[pl.BlockSpec()] * 4,
@@ -305,7 +314,16 @@
         cost_estimate=LONG,
     )(far(masters), packed)
     masters = lax.all_gather(masters, FS)
-    packed = lax.all_to_all(packed, FS, 0, 0)
+    packed = lax.all_to_all(packed, "z", 0, 0)
+    packed = pl.pallas_call(
+        copies_kernel,
+        out_shape=jax.ShapeDtypeStruct((height, depth, kept, 128), bf16),
+        in_specs=[VMEM],
+        out_specs=VMEM,
+        compiler_params=SMALL,
+        cost_estimate=cost(1 << 16, 1 << 20),
+    )(packed)
+    packed = lax.all_to_all(packed, "y", 0, 0)
     proj = pl.pallas_call(
         functools.partial(proj_kernel, used),
         out_shape=jax.ShapeDtypeStruct((used, tokens), bf16),
@@ -369,8 +387,8 @@
         ),
         in_specs=[
             SMEM,
-            pl.BlockSpec((tp // 2, per, kept, 128), lambda i: (0, i, 0, 0)),
-            pl.BlockSpec((tp // 2, per, kept, 128), lambda i: (0, i, 0, 0)),
+            pl.BlockSpec((tp // 2, height, per // height, kept, 128), lambda i: (0, 0, i, 0, 0)),
+            pl.BlockSpec((tp // 2, height, per // height, kept, 128), lambda i: (0, 0, i, 0, 0)),
         ],
         out_specs=(
             pl.BlockSpec((span, ranks), lambda i: (i, 0)),

time: 206 us -> 204 us (level)
    all_to_all x1 -> x2, blocking collectives: 50.2 us -> 48.5 us  [the longest x1 25.5 us: body(): packed = lax.all_to_all(packed, 'z', 0, 0)]
where the time goes in v13:
time: 204 us; the launch traced here: 203 us
  blocking collectives  116 us (57%)
  waiting for transfers between devices  23.1 us (11%)
  Pallas kernels  21.7 us (11%)
  starting transfers between devices  20.4 us (10%)
  between operations  14.2 us (7%)
  local copies, waits for them, and re-layouts  5.69 us (3%)
    all_to_all x1, blocking collectives, body(): pieces = lax.all_to_all(partial.reshape(fs, 2 * rows, cols), FS, 0, 0)  33.7 us
    all_to_all x1, blocking collectives, body(): packed = lax.all_to_all(packed, 'z', 0, 0)  25.5 us
    ppermute x3, waiting for transfers between devices, body(): lax.ppermute(packed, 'tp', [((t + 2 * step) % tp, t) for t in range(tp)])  23.1 us
    all_to_all x1, blocking collectives, body(): packed = lax.all_to_all(packed, 'y', 0, 0)  23 us
    all_gather x1, blocking collectives, body(): proj = lax.all_gather(proj, 'tp', axis=0, tiled=True)  17.8 us
    all_to_all x1, blocking collectives, body(): low = lax.all_to_all(low, 'z', 0, 0)  16.2 us
    ppermute x3, starting transfers between devices, body(): lax.ppermute(packed, 'tp', [((t + 2 * step) % tp, t) for t in range(tp)])  9.31 us
    pallas_call x1, Pallas kernels, body(): pl.pallas_call(functools.partial(prep_kernel, rank_cols), grid=(width //...  8.91 us
  transfers between devices with their start and end apart: 7, of which 3 were waited for; matrix products, arithmetic and copies ran while one was open for 1% of the time, Pallas kernels for 7%

profile of v13, /device:TPU:1, one launch (start us, length us, event | category | flops | bytes accessed | tf_op | source)
XLA Modules:
  0.0 203.0 jit_solution(1156770096620043480)
XLA Ops:
  7.2 0.0 all-gather.3.cloned.1.call-start
  7.2 1.6 shard_map.145
  8.8 0.0 all-gather.3.cloned.1.call-update
  8.9 0.0 copy-start.1
  8.9 0.0 copy-start.2
  8.9 25.5 %all_to_all.30.packed = bf16[12,24,128]{2,1,0:T(8,128)(2,1)S(1)} all-to-all(bf16[12,24,128]{2,1,0:T(8,128)(2,1)S(1)} %shard_map.146), channel_id=1, replica_groups=mesh['z'=12,'y'=8,'tp'=8] {'z'}, dimensions={0} | all-to-all | bytes 147456 | tf_op jit(solution)/shard_map/all_to_all | solution.py:317
  34.4 0.1 shard_map.147
  34.5 23.0 %all_to_all.31.packed = bf16[8,12,24,128]{3,2,1,0:T(8,128)(2,1)S(1)} all-to-all(bf16[8,12,24,128]{3,2,1,0:T(8,128)(2,1)S(1)} %shard_map.147), channel_id=1, replica_groups=mesh['z'=12,'y'=8,'tp'=8] {'y'}, dimensions={0} | all-to-all | bytes 1179648 | tf_op jit(solution)/shard_map/all_to_all | solution.py:326
  57.4 0.0 copy-done.1
  57.4 0.0 copy-done.2
  57.5 0.0 copy-start.5
  57.5 0.0 copy-start.6
  57.5 2.0 shard_map.148
  59.4 0.0 copy-start.7
  59.4 0.0 copy-start.8
  59.4 17.8 %all_gather.9.proj = bf16[768,512]{1,0:T(8,128)(2,1)S(1)} all-gather(bf16[96,512]{1,0:T(8,128)(2,1)S(1)} %shard_map.148), channel_id=1, replica_groups=mesh['z'=12,'y'=8,'tp'=8] {'tp'}, dimensions={0}, use_global_device_ids=true | all-gather | bytes 884736 | tf_op jit(solution)/shard_map/all_gather | solution.py:336
  77.3 0.0 copy-done.5
  77.3 0.0 copy-done.6
  77.3 1.4 shard_map.149
  78.7 33.7 %all_to_all.32.pieces = bf16[96,8,384]{2,1,0:T(8,128)(2,1)S(1)} all-to-all(bf16[96,8,384]{2,1,0:T(8,128)(2,1)} %bitcast.12), channel_id=1, replica_groups=mesh['z'=12,'y'=8,'tp'=8] {'z','y'}, dimensions={0} | all-to-all | bytes 1179648 | tf_op jit(solution)/shard_map/all_to_all | solution.py:346
  112.3 0.0 copy-done.7
  112.3 0.0 copy-done.8
  112.3 0.9 shard_map.150
  113.2 16.2 %all_to_all.33.low = bf16[12,4,896]{2,1,0:T(4,128)(2,1)S(1)} all-to-all(bf16[12,4,896]{2,1,0:T(4,128)(2,1)} %get-tuple-element.23), channel_id=1, replica_groups=mesh['z'=12,'y'=8,'tp'=8] {'z'}, dimensions={0} | all-to-all | bytes 172032 | tf_op jit(solution)/shard_map/all_to_all | solution.py:366
  129.4 0.9 shard_map.151
  130.4 3.5 %all-to-all-start.4 = ((bf16[8,13,4,768]{3,2,1,0:T(4,128)(2,1)}), bf16[8,13,4,768]{3,2,1,0:T(4,128)(2,1)S(1)}, u32[]{:S(2)}, u32[]{:S(2)}) async-start(bf16[8,13,4,768]{3,2,1,0:T(4,128)(2,1)} %shard_map.151), calls=%async_computation.4 | async-start | bytes 1277952 | tf_op jit(solution)/shard_map/all_to_all | solution.py:375
  133.9 3.1 %collective-permute-start.2 = (bf16[8,12,24,128]{3,2,1,0:T(8,128)(2,1)S(1)}, bf16[8,12,24,128]{3,2,1,0:T(8,128)(2,1)S(1)}, u32[]{:S(2)}, u32[]{:S(2)}) collective-permute-start(bf16[8,12,24,128]{3,2,1,0:T(8,128)(2,1)S(1)} %all_to_all.31.packed), channel_id=1, source_target_pairs={{6,0},{7,1},{0,2},{1,3},{2,4},{3,5},{4,6},{5,7},{14,8},{15,9},{8,1... | collective-permute-start | bytes 1769480 | tf_op jit(solution)/shard_map/ppermute | solution.py:350
  137.0 4.3 %collective-permute-start.1 = (bf16[8,12,24,128]{3,2,1,0:T(8,128)(2,1)S(1)}, bf16[8,12,24,128]{3,2,1,0:T(8,128)(2,1)S(1)}, u32[]{:S(2)}, u32[]{:S(2)}) collective-permute-start(bf16[8,12,24,128]{3,2,1,0:T(8,128)(2,1)S(1)} %all_to_all.31.packed), channel_id=1, source_target_pairs={{4,0},{5,1},{6,2},{7,3},{0,4},{1,5},{2,6},{3,7},{12,8},{13,9},{14,... | collective-permute-start | bytes 1769480 | tf_op jit(solution)/shard_map/ppermute | solution.py:350
  141.3 1.9 collective-permute-start
  143.3 0.1 pad_add_fusion.place
  143.4 5.2 %collective-permute-done.2 = bf16[8,12,24,128]{3,2,1,0:T(8,128)(2,1)S(1)} collective-permute-done((bf16[8,12,24,128]{3,2,1,0:T(8,128)(2,1)S(1)}, bf16[8,12,24,128]{3,2,1,0:T(8,128)(2,1)S(1)}, u32[]{:S(2)}, u32[]{:S(2)}) %collective-permute-start.2) | collective-permute-done | bytes 589856 | tf_op jit(solution)/shard_map/ppermute | solution.py:350
  148.6 13.9 %collective-permute-done.1 = bf16[8,12,24,128]{3,2,1,0:T(8,128)(2,1)S(1)} collective-permute-done((bf16[8,12,24,128]{3,2,1,0:T(8,128)(2,1)S(1)}, bf16[8,12,24,128]{3,2,1,0:T(8,128)(2,1)S(1)}, u32[]{:S(2)}, u32[]{:S(2)}) %collective-permute-start.1) | collective-permute-done | bytes 589856 | tf_op jit(solution)/shard_map/ppermute | solution.py:350
  162.4 4.0 %collective-permute-done = bf16[8,12,24,128]{3,2,1,0:T(8,128)(2,1)S(1)} collective-permute-done((bf16[8,12,24,128]{3,2,1,0:T(8,128)(2,1)S(1)}, bf16[8,12,24,128]{3,2,1,0:T(8,128)(2,1)S(1)}, u32[]{:S(2)}, u32[]{:S(2)}) %collective-permute-start) | collective-permute-done | bytes 589856 | tf_op jit(solution)/shard_map/ppermute | solution.py:350
  166.4 1.7 pad_maximum_fusion.held
  168.1 3.5 %collective-permute-start.3 = (bf16[4,8,12,24,128]{4,3,2,1,0:T(8,128)(2,1)}, bf16[4,8,12,24,128]{4,3,2,1,0:T(8,128)(2,1)}, u32[]{:S(2)}, u32[]{:S(2)}) collective-permute-start(bf16[4,8,12,24,128]{4,3,2,1,0:T(8,128)(2,1)} %pad_maximum_fusion.held), channel_id=1, source_target_pairs={{1,0},{0,1},{3,2},{2,3},{5,4},{4,5},{7,6},{6,7},{9,8},{8,9},{11,10... | collective-permute-start | bytes 7077896 | tf_op jit(solution)/shard_map/ppermute | solution.py:352
  171.6 0.0 all-to-all-done.4.low
  171.6 0.0 all-gather.3.cloned.1.call-done
  171.6 0.6 shard_map.152
  172.2 4.0 %all-to-all-start.5 = ((f32[8,1,128]{2,1,0:T(1,128)}), f32[8,1,128]{2,1,0:T(1,128)S(1)}, u32[]{:S(2)}, u32[]{:S(2)}) async-start(f32[8,1,128]{2,1,0:T(1,128)} %shard_map.152), calls=%async_computation.5 | async-start | bytes 8192 | tf_op jit(solution)/shard_map/all_to_all | solution.py:414
  176.2 0.0 collective-permute-done.3.other
  176.2 8.9 %shard_map.153 = (bf16[3072,384]{1,0:T(8,128)(2,1)}, bf16[384,3072]{1,0:T(8,128)(2,1)}, bf16[32,384]{1,0:T(8,128)(2,1)}, bf16[32,384]{1,0:T(8,128)(2,1)}) custom-call(s32[2]{0:T(128)S(1)} %pad_add_fusion.place, bf16[4,8,12,24,128]{4,3,2,1,0:T(8,128)(2,1)} %pad_maximum_fusion.held, bf16[4,8,12,24,128]{4,3,2,1,0:T(8,128)(2,1)} %collective-permute-done.3.other), custom_call_target="tpu_custom_call" | custom-call | flops 1073741824 | bytes 31457280 | tf_op jit(solution)/shard_map/pallas_call | solution.py:379
  185.1 0.0 all-to-all-done.5.squares
  185.1 0.0 copy-start
  185.2 2.3 %copy-done = bf16[6144,384]{1,0:T(8,128)(2,1)S(1)} copy-done((bf16[6144,384]{1,0:T(8,128)(2,1)S(1)}, bf16[6144,384]{1,0:T(8,128)(2,1)}, u32[]{:S(2)}) %copy-start) | copy-done | bytes 4718616
  187.5 0.0 copy-start.3
  187.5 1.7 copy-done.3
  189.2 0.0 copy-start.4
  189.2 1.7 copy-done.4
  190.8 5.3 %shard_map.154 = (bf16[3072,384]{1,0:T(8,128)(2,1)}, bf16[384,3072]{1,0:T(8,128)(2,1)}, f32[32,384]{1,0:T(8,128)}, f32[32,384]{1,0:T(8,128)}) custom-call(f32[8,1,128]{2,1,0:T(1,128)S(1)} %all-to-all-done.5.squares, bf16[8,13,4,768]{3,2,1,0:T(4,128)(2,1)S(1)} %all-to-all-done.4.low, bf16[3072,384]{1,0:T(8,128)(2,1)S(1)} %copy-done.3, ...), custom_call_target="tpu_custom_call" | custom-call | flops 1811939328 | bytes 20971520 | tf_op jit(solution)/shard_map/pallas_call | solution.py:416
  (1 shorter events, 0.0 us)
Async XLA Ops:
  7.2 164.4 %all-gather.3.cloned.1.call-start = ((), (), s32[]{:S(2)}) async-start(), calls=%async_computation.6 | async-start | bytes 4767744 | tf_op jit(solution)/shard_map/all_gather | solution.py:316
  8.9 48.6 %copy-start.1 = (bf16[512,3072]{1,0:T(8,128)(2,1)S(1)}, bf16[512,3072]{1,0:T(8,128)(2,1)}, u32[]{:S(2)}) copy-start(bf16[512,3072]{1,0:T(8,128)(2,1)} %saved_inputs.1) | copy-start | bytes 9437188
  8.9 48.6 %copy-start.2 = (bf16[512,3072]{1,0:T(8,128)(2,1)S(1)}, bf16[512,3072]{1,0:T(8,128)(2,1)}, u32[]{:S(2)}) copy-start(bf16[512,3072]{1,0:T(8,128)(2,1)} %out_cotangent.1) | copy-start | bytes 9437188
  57.5 19.8 %copy-start.5 = (bf16[512,384]{1,0:T(8,128)(2,1)S(1)}, bf16[512,384]{1,0:T(8,128)(2,1)}, u32[]{:S(2)}) copy-start(bf16[512,384]{1,0:T(8,128)(2,1)} %query_cotangent.1) | copy-start | bytes 1179652
  57.5 19.8 %copy-start.6 = (bf16[512,384]{1,0:T(8,128)(2,1)S(1)}, bf16[512,384]{1,0:T(8,128)(2,1)}, u32[]{:S(2)}) copy-start(bf16[512,384]{1,0:T(8,128)(2,1)} %attn_outputs.1) | copy-start | bytes 1179652
  59.4 52.9 %copy-start.7 = (f32[2,4,384]{2,1,0:T(4,128)S(1)}, f32[2,4,384]{2,1,0:T(4,128)}, u32[]{:S(2)}) copy-start(f32[2,4,384]{2,1,0:T(4,128)} %first.1) | copy-start | bytes 36868
  59.4 52.9 %copy-start.8 = (f32[2,4,384]{2,1,0:T(4,128)S(1)}, f32[2,4,384]{2,1,0:T(4,128)}, u32[]{:S(2)}) copy-start(f32[2,4,384]{2,1,0:T(4,128)} %second.1) | copy-start | bytes 36868
  130.4 41.2 %all-to-all-start.4 = ((bf16[8,13,4,768]{3,2,1,0:T(4,128)(2,1)}), bf16[8,13,4,768]{3,2,1,0:T(4,128)(2,1)S(1)}, u32[]{:S(2)}, u32[]{:S(2)}) async-start(bf16[8,13,4,768]{3,2,1,0:T(4,128)(2,1)} %shard_map.151), calls=%async_computation.4 | async-start | bytes 1277952 | tf_op jit(solution)/shard_map/all_to_all | solution.py:375
  133.9 14.6 %collective-permute-start.2 = (bf16[8,12,24,128]{3,2,1,0:T(8,128)(2,1)S(1)}, bf16[8,12,24,128]{3,2,1,0:T(8,128)(2,1)S(1)}, u32[]{:S(2)}, u32[]{:S(2)}) collective-permute-start(bf16[8,12,24,128]{3,2,1,0:T(8,128)(2,1)S(1)} %all_to_all.31.packed), channel_id=1, source_target_pairs={{6,0},{7,1},{0,2},{1,3},{2,4},{3,5},{4,6},{5,7},{14,8},{15,9},{8,1... | collective-permute-start | bytes 1769480 | tf_op jit(solution)/shard_map/ppermute | solution.py:350
  137.0 25.4 %collective-permute-start.1 = (bf16[8,12,24,128]{3,2,1,0:T(8,128)(2,1)S(1)}, bf16[8,12,24,128]{3,2,1,0:T(8,128)(2,1)S(1)}, u32[]{:S(2)}, u32[]{:S(2)}) collective-permute-start(bf16[8,12,24,128]{3,2,1,0:T(8,128)(2,1)S(1)} %all_to_all.31.packed), channel_id=1, source_target_pairs={{4,0},{5,1},{6,2},{7,3},{0,4},{1,5},{2,6},{3,7},{12,8},{13,9},{14,... | collective-permute-start | bytes 1769480 | tf_op jit(solution)/shard_map/ppermute | solution.py:350
  141.3 25.1 %collective-permute-start = (bf16[8,12,24,128]{3,2,1,0:T(8,128)(2,1)S(1)}, bf16[8,12,24,128]{3,2,1,0:T(8,128)(2,1)S(1)}, u32[]{:S(2)}, u32[]{:S(2)}) collective-permute-start(bf16[8,12,24,128]{3,2,1,0:T(8,128)(2,1)S(1)} %all_to_all.31.packed), channel_id=1, source_target_pairs={{2,0},{3,1},{4,2},{5,3},{6,4},{7,5},{0,6},{1,7},{10,8},{11,9},{12,... | collective-permute-start | bytes 1769480 | tf_op jit(solution)/shard_map/ppermute | solution.py:350
  168.1 8.1 %collective-permute-start.3 = (bf16[4,8,12,24,128]{4,3,2,1,0:T(8,128)(2,1)}, bf16[4,8,12,24,128]{4,3,2,1,0:T(8,128)(2,1)}, u32[]{:S(2)}, u32[]{:S(2)}) collective-permute-start(bf16[4,8,12,24,128]{4,3,2,1,0:T(8,128)(2,1)} %pad_maximum_fusion.held), channel_id=1, source_target_pairs={{1,0},{0,1},{3,2},{2,3},{5,4},{4,5},{7,6},{6,7},{9,8},{8,9},{11,10... | collective-permute-start | bytes 7077896 | tf_op jit(solution)/shard_map/ppermute | solution.py:352
  172.2 12.9 %all-to-all-start.5 = ((f32[8,1,128]{2,1,0:T(1,128)}), f32[8,1,128]{2,1,0:T(1,128)S(1)}, u32[]{:S(2)}, u32[]{:S(2)}) async-start(f32[8,1,128]{2,1,0:T(1,128)} %shard_map.152), calls=%async_computation.5 | async-start | bytes 8192 | tf_op jit(solution)/shard_map/all_to_all | solution.py:414
  185.1 2.3 %copy-start = (bf16[6144,384]{1,0:T(8,128)(2,1)S(1)}, bf16[6144,384]{1,0:T(8,128)(2,1)}, u32[]{:S(2)}) copy-start(bf16[6144,384]{1,0:T(8,128)(2,1)} %all-gather.3.cloned.1.call-done) | copy-start | bytes 14155780
  187.5 1.7 copy-start.3
  189.2 1.7 copy-start.4
Sparse Core Ops, SparseCore 0:
  12.3 133.1 all-gather.2

commit v14 on v13

--- a/solution.py
+++ b/solution.py
@@ -129,14 +129,19 @@
     low[...] = jnp.broadcast_to(sent[None], low.shape)
 
 
-def prep_kernel(rank_cols, place, held, other, left, right, own_left, own_right, tile):
+def prep_kernel(rank_cols, place, mine, pair, held, other, left, right, own_left, own_right, tile):
     own = own_left.shape[0]
     span = left.shape[0]
-    chips = held.shape[0]
-    blocks = [[unpacked(by_place(half[s]), 2 * rank_cols).reshape(span, 128) for s in range(chips)] for half in (held, other)]
+    chips = 1 + held.shape[0]
     here = place[1] % 2 == 0
+    same = [mine[...]] + [held[s] for s in range(chips - 1)]
+    cross = [pair[...]] + [other[s] for s in range(chips - 1)]
     by_core = [
-        [jnp.where(here, near, far) for near, far in zip(blocks[core], blocks[1 - core])] for core in range(2)
+        [
+            unpacked(by_place(jnp.where(here, near, far)), 2 * rank_cols).reshape(span, 128)
+            for near, far in zip(*both)
+        ]
+        for both in ((same, cross), (cross, same))
     ]
     for chip in range(chips):
 
@@ -345,18 +350,20 @@
     )(proj, query_cotangent, attn_outputs)
     pieces = lax.all_to_all(partial.reshape(fs, 2 * rows, cols), FS, 0, 0)
 
-    held = [packed]
+    swap = [(t ^ 1, t) for t in range(tp)]
+    pair = lax.ppermute(packed, "tp", swap)
+    held = []
     for step in range(1, tp // 2):
         held.append(lax.ppermute(packed, "tp", [((t + 2 * step) % tp, t) for t in range(tp)]))
     held = jnp.stack(held)
-    other = lax.ppermute(held, "tp", [(t ^ 1, t) for t in range(tp)])
+    other = lax.ppermute(held, "tp", swap)
 
     first_new, second_new, low = pl.pallas_call(
         moment_kernel,
         out_shape=(
             jax.ShapeDtypeStruct(first_moment.shape, f32),
             jax.ShapeDtypeStruct(second_moment.shape, f32),
-            pltpu.HBM((depth, rows, 2 * cols + 128), bf16),
+            jax.ShapeDtypeStruct((depth, rows, 2 * cols + 128), bf16),
         ),
         in_specs=[VMEM] * 3,
         out_specs=(VMEM, VMEM, VMEM),
@@ -387,8 +394,10 @@
         ),
         in_specs=[
             SMEM,
-            pl.BlockSpec((tp // 2, height, per // height, kept, 128), lambda i: (0, 0, i, 0, 0)),
-            pl.BlockSpec((tp // 2, height, per // height, kept, 128), lambda i: (0, 0, i, 0, 0)),
+            pl.BlockSpec((height, per // height, kept, 128), lambda i: (0, i, 0, 0)),
+            pl.BlockSpec((height, per // height, kept, 128), lambda i: (0, i, 0, 0)),
+            pl.BlockSpec((tp // 2 - 1, height, per // height, kept, 128), lambda i: (0, 0, i, 0, 0)),
+            pl.BlockSpec((tp // 2 - 1, height, per // height, kept, 128), lambda i: (0, 0, i, 0, 0)),
         ],
         out_specs=(
             pl.BlockSpec((span, ranks), lambda i: (i, 0)),
@@ -399,7 +408,7 @@
         scratch_shapes=[pltpu.VMEM((2, span, ranks), bf16)],
         compiler_params=SMALL,
         cost_estimate=cost(1 << 30, 30 << 20),
-    )(place, far(held), far(other))
+    )(place, far(packed), far(pair), far(held), far(other))
 
     low, masters = lax.optimization_barrier((low, masters))
     parts = width // span

time: 204 us -> 204 us (level)
  starting transfers between devices: 20.4 us -> 25.5 us
  waiting for transfers between devices: 23.1 us -> 18.1 us
    ppermute x1 -> x2, starting transfers between devices: 3.45 us -> 9.12 us  [the longest x1 5.55 us: body(): pair = lax.ppermute(packed, 'tp', swap)]
    ppermute x3, waiting for transfers between devices: 23.1 us -> 18 us  [body(): lax.ppermute(packed, 'tp', [((t + 2 * step) % tp, t) for t in range(tp)])]
    unnamed x18 -> x24, local copies, waits for them, and re-layouts: 5.69 us -> 5.71 us
  transfers between devices with their start and end apart: 7 -> 8, of which waited for: 3 -> 3; matrix products, arithmetic and copies ran while one was open for 1% -> 1% of each run, Pallas kernels for 7% -> 7%
where the time goes in v14:
time: 204 us; the launch traced here: 203 us
  blocking collectives  116 us (57%)
  starting transfers between devices  25.5 us (12%)
  Pallas kernels  21.4 us (10%)
  waiting for transfers between devices  18.1 us (9%)
  between operations  14.2 us (7%)
  local copies, waits for them, and re-layouts  5.71 us (3%)
    all_to_all x1, blocking collectives, body(): pieces = lax.all_to_all(partial.reshape(fs, 2 * rows, cols), FS, 0, 0)  33.7 us
    all_to_all x1, blocking collectives, body(): packed = lax.all_to_all(packed, 'z', 0, 0)  25.5 us
    all_to_all x1, blocking collectives, body(): packed = lax.all_to_all(packed, 'y', 0, 0)  23 us
    ppermute x3, waiting for transfers between devices, body(): lax.ppermute(packed, 'tp', [((t + 2 * step) % tp, t) for t in range(tp)])  18 us
    all_gather x1, blocking collectives, body(): proj = lax.all_gather(proj, 'tp', axis=0, tiled=True)  17.8 us
    all_to_all x1, blocking collectives, body(): low = lax.all_to_all(low, 'z', 0, 0)  16.5 us
    ppermute x3, starting transfers between devices, body(): lax.ppermute(packed, 'tp', [((t + 2 * step) % tp, t) for t in range(tp)])  8.77 us
    pallas_call x1, Pallas kernels, body(): pl.pallas_call(functools.partial(prep_kernel, rank_cols), grid=(width //...  8.77 us
  transfers between devices with their start and end apart: 8, of which 3 were waited for; matrix products, arithmetic and copies ran while one was open for 1% of the time, Pallas kernels for 7%

profile of v14, /device:TPU:1, one launch (start us, length us, event | category | flops | bytes accessed | tf_op | source)
XLA Modules:
  0.0 203.0 jit_solution(17855500153798192308)
XLA Ops:
  7.2 0.0 all-gather.3.cloned.1.call-start
  7.2 1.6 shard_map.145
  8.8 0.0 all-gather.3.cloned.1.call-update
  8.9 0.0 copy-start.2
  8.9 0.0 copy-start.3
  8.9 25.5 %all_to_all.30.packed = bf16[12,24,128]{2,1,0:T(8,128)(2,1)S(1)} all-to-all(bf16[12,24,128]{2,1,0:T(8,128)(2,1)S(1)} %shard_map.146), channel_id=1, replica_groups=mesh['z'=12,'y'=8,'tp'=8] {'z'}, dimensions={0} | all-to-all | bytes 147456 | tf_op jit(solution)/shard_map/all_to_all | solution.py:322
  34.4 0.1 shard_map.147
  34.5 23.0 %all_to_all.31.packed.mine = bf16[8,12,24,128]{3,2,1,0:T(8,128)(2,1)S(1)} all-to-all(bf16[8,12,24,128]{3,2,1,0:T(8,128)(2,1)S(1)} %shard_map.147), channel_id=1, replica_groups=mesh['z'=12,'y'=8,'tp'=8] {'y'}, dimensions={0} | all-to-all | bytes 1179648 | tf_op jit(solution)/shard_map/all_to_all | solution.py:331
  57.4 0.0 copy-done.2
  57.4 0.0 copy-done.3
  57.5 0.0 copy-start
  57.5 0.0 copy-start.6
  57.5 0.0 copy-start.7
  57.5 2.0 shard_map.148
  59.4 0.0 copy-start.8
  59.4 0.0 copy-start.9
  59.5 17.8 %all_gather.9.proj = bf16[768,512]{1,0:T(8,128)(2,1)S(1)} all-gather(bf16[96,512]{1,0:T(8,128)(2,1)S(1)} %shard_map.148), channel_id=1, replica_groups=mesh['z'=12,'y'=8,'tp'=8] {'tp'}, dimensions={0}, use_global_device_ids=true | all-gather | bytes 884736 | tf_op jit(solution)/shard_map/all_gather | solution.py:341
  77.3 0.0 copy-done.6
  77.3 0.0 copy-done.7
  77.3 1.4 shard_map.149
  78.7 33.7 %all_to_all.32.pieces = bf16[96,8,384]{2,1,0:T(8,128)(2,1)S(1)} all-to-all(bf16[96,8,384]{2,1,0:T(8,128)(2,1)} %bitcast.10), channel_id=1, replica_groups=mesh['z'=12,'y'=8,'tp'=8] {'z','y'}, dimensions={0} | all-to-all | bytes 1179648 | tf_op jit(solution)/shard_map/all_to_all | solution.py:351
  112.3 0.0 copy-done.8
  112.3 0.0 copy-done.9
  112.3 0.7 shard_map.150
  113.1 16.5 %all_to_all.33.low = bf16[12,4,896]{2,1,0:T(4,128)(2,1)S(1)} all-to-all(bf16[12,4,896]{2,1,0:T(4,128)(2,1)S(1)} %get-tuple-element.23), channel_id=1, replica_groups=mesh['z'=12,'y'=8,'tp'=8] {'z'}, dimensions={0} | all-to-all | bytes 172032 | tf_op jit(solution)/shard_map/all_to_all | solution.py:373
  129.5 0.9 shard_map.151
  130.5 3.5 %all-to-all-start.4 = ((bf16[8,13,4,768]{3,2,1,0:T(4,128)(2,1)}), bf16[8,13,4,768]{3,2,1,0:T(4,128)(2,1)S(1)}, u32[]{:S(2)}, u32[]{:S(2)}) async-start(bf16[8,13,4,768]{3,2,1,0:T(4,128)(2,1)} %shard_map.151), calls=%async_computation.4 | async-start | bytes 1277952 | tf_op jit(solution)/shard_map/all_to_all | solution.py:382
  134.0 2.5 %collective-permute-start.3 = (bf16[8,12,24,128]{3,2,1,0:T(8,128)(2,1)S(1)}, bf16[8,12,24,128]{3,2,1,0:T(8,128)(2,1)S(1)}, u32[]{:S(2)}, u32[]{:S(2)}) collective-permute-start(bf16[8,12,24,128]{3,2,1,0:T(8,128)(2,1)S(1)} %all_to_all.31.packed.mine), channel_id=1, source_target_pairs={{6,0},{7,1},{0,2},{1,3},{2,4},{3,5},{4,6},{5,7},{14,8},{15,9},{8,1... | collective-permute-start | bytes 1769480 | tf_op jit(solution)/shard_map/ppermute | solution.py:357
  136.6 4.2 %collective-permute-start.2 = (bf16[8,12,24,128]{3,2,1,0:T(8,128)(2,1)S(1)}, bf16[8,12,24,128]{3,2,1,0:T(8,128)(2,1)}, u32[]{:S(2)}, u32[]{:S(2)}) collective-permute-start(bf16[8,12,24,128]{3,2,1,0:T(8,128)(2,1)S(1)} %all_to_all.31.packed.mine), channel_id=1, source_target_pairs={{4,0},{5,1},{6,2},{7,3},{0,4},{1,5},{2,6},{3,7},{12,8},{13,9},{14,... | collective-permute-start | bytes 1769480 | tf_op jit(solution)/shard_map/ppermute | solution.py:357
  140.8 2.0 %collective-permute-start.1 = (bf16[8,12,24,128]{3,2,1,0:T(8,128)(2,1)S(1)}, bf16[8,12,24,128]{3,2,1,0:T(8,128)(2,1)}, u32[]{:S(2)}, u32[]{:S(2)}) collective-permute-start(bf16[8,12,24,128]{3,2,1,0:T(8,128)(2,1)S(1)} %all_to_all.31.packed.mine), channel_id=1, source_target_pairs={{2,0},{3,1},{4,2},{5,3},{6,4},{7,5},{0,6},{1,7},{10,8},{11,9},{12,... | collective-permute-start | bytes 1769480 | tf_op jit(solution)/shard_map/ppermute | solution.py:357
  142.8 0.1 pad_add_fusion.place
  142.9 0.0 copy-done
  142.9 5.5 %collective-permute-start = (bf16[8,12,24,128]{3,2,1,0:T(8,128)(2,1)S(1)}, bf16[8,12,24,128]{3,2,1,0:T(8,128)(2,1)}, u32[]{:S(2)}, u32[]{:S(2)}) collective-permute-start(bf16[8,12,24,128]{3,2,1,0:T(8,128)(2,1)S(1)} %all_to_all.31.packed.mine), channel_id=1, source_target_pairs={{1,0},{0,1},{3,2},{2,3},{5,4},{4,5},{7,6},{6,7},{9,8},{8,9},{11,10... | collective-permute-start | bytes 1769480 | tf_op jit(solution)/shard_map/ppermute | solution.py:354
  148.5 0.5 collective-permute-done.3
  149.0 0.0 copy-start.11
  149.0 12.9 %collective-permute-done.2 = bf16[8,12,24,128]{3,2,1,0:T(8,128)(2,1)} collective-permute-done((bf16[8,12,24,128]{3,2,1,0:T(8,128)(2,1)S(1)}, bf16[8,12,24,128]{3,2,1,0:T(8,128)(2,1)}, u32[]{:S(2)}, u32[]{:S(2)}) %collective-permute-start.2) | collective-permute-done | bytes 589856 | tf_op jit(solution)/shard_map/ppermute | solution.py:357
  161.9 4.6 %collective-permute-done.1 = bf16[8,12,24,128]{3,2,1,0:T(8,128)(2,1)} collective-permute-done((bf16[8,12,24,128]{3,2,1,0:T(8,128)(2,1)S(1)}, bf16[8,12,24,128]{3,2,1,0:T(8,128)(2,1)}, u32[]{:S(2)}, u32[]{:S(2)}) %collective-permute-start.1) | collective-permute-done | bytes 589856 | tf_op jit(solution)/shard_map/ppermute | solution.py:357
  166.5 0.0 copy-done.11
  166.5 1.6 pad_maximum_fusion.held
  168.1 0.0 copy-start.10
  168.1 3.6 %collective-permute-start.4 = (bf16[3,8,12,24,128]{4,3,2,1,0:T(8,128)(2,1)S(1)}, bf16[3,8,12,24,128]{4,3,2,1,0:T(8,128)(2,1)}, u32[]{:S(2)}, u32[]{:S(2)}) collective-permute-start(bf16[3,8,12,24,128]{4,3,2,1,0:T(8,128)(2,1)S(1)} %pad_maximum_fusion.held), channel_id=1, source_target_pairs={{1,0},{0,1},{3,2},{2,3},{5,4},{4,5},{7,6},{6,7},{9,8},{8,9},{11,10... | collective-permute-start | bytes 5308424 | tf_op jit(solution)/shard_map/ppermute | solution.py:359
  171.7 0.0 all-to-all-done.4.low
  171.7 0.0 all-gather.3.cloned.1.call-done
  171.7 0.6 shard_map.152
  172.3 0.0 copy-done.10
  172.3 4.0 %all-to-all-start.5 = ((f32[8,1,128]{2,1,0:T(1,128)}), f32[8,1,128]{2,1,0:T(1,128)S(1)}, u32[]{:S(2)}, u32[]{:S(2)}) async-start(f32[8,1,128]{2,1,0:T(1,128)} %shard_map.152), calls=%async_computation.5 | async-start | bytes 8192 | tf_op jit(solution)/shard_map/all_to_all | solution.py:423
  176.4 0.0 collective-permute-done.pair
  176.4 0.0 collective-permute-done.4.other
  176.4 8.8 %shard_map.153 = (bf16[3072,384]{1,0:T(8,128)(2,1)}, bf16[384,3072]{1,0:T(8,128)(2,1)}, bf16[32,384]{1,0:T(8,128)(2,1)}, bf16[32,384]{1,0:T(8,128)(2,1)}) custom-call(s32[2]{0:T(128)S(1)} %pad_add_fusion.place, bf16[8,12,24,128]{3,2,1,0:T(8,128)(2,1)} %copy-done, bf16[8,12,24,128]{3,2,1,0:T(8,128)(2,1)} %collective-permute-done.pair, ...), custom_call_target="tpu_custom_call" | custom-call | flops 1073741824 | bytes 31457280 | tf_op jit(solution)/shard_map/pallas_call | solution.py:386
  185.1 0.0 all-to-all-done.5.squares
  185.2 0.0 copy-start.1
  185.2 2.3 %copy-done.1 = bf16[6144,384]{1,0:T(8,128)(2,1)S(1)} copy-done((bf16[6144,384]{1,0:T(8,128)(2,1)S(1)}, bf16[6144,384]{1,0:T(8,128)(2,1)}, u32[]{:S(2)}) %copy-start.1) | copy-done | bytes 4718616
  187.5 0.0 copy-start.4
  187.5 1.7 copy-done.4
  189.2 0.0 copy-start.5
  189.2 1.7 copy-done.5
  190.8 5.3 %shard_map.154 = (bf16[3072,384]{1,0:T(8,128)(2,1)}, bf16[384,3072]{1,0:T(8,128)(2,1)}, f32[32,384]{1,0:T(8,128)}, f32[32,384]{1,0:T(8,128)}) custom-call(f32[8,1,128]{2,1,0:T(1,128)S(1)} %all-to-all-done.5.squares, bf16[8,13,4,768]{3,2,1,0:T(4,128)(2,1)S(1)} %all-to-all-done.4.low, bf16[3072,384]{1,0:T(8,128)(2,1)S(1)} %copy-done.4, ...), custom_call_target="tpu_custom_call" | custom-call | flops 1811939328 | bytes 20971520 | tf_op jit(solution)/shard_map/pallas_call | solution.py:425
  (1 shorter events, 0.0 us)
Async XLA Ops:
  7.2 164.6 %all-gather.3.cloned.1.call-start = ((), (), s32[]{:S(2)}) async-start(), calls=%async_computation.6 | async-start | bytes 4767744 | tf_op jit(solution)/shard_map/all_gather | solution.py:321
  8.9 48.6 %copy-start.2 = (bf16[512,3072]{1,0:T(8,128)(2,1)S(1)}, bf16[512,3072]{1,0:T(8,128)(2,1)}, u32[]{:S(2)}) copy-start(bf16[512,3072]{1,0:T(8,128)(2,1)} %saved_inputs.1) | copy-start | bytes 9437188
  8.9 48.6 %copy-start.3 = (bf16[512,3072]{1,0:T(8,128)(2,1)S(1)}, bf16[512,3072]{1,0:T(8,128)(2,1)}, u32[]{:S(2)}) copy-start(bf16[512,3072]{1,0:T(8,128)(2,1)} %out_cotangent.1) | copy-start | bytes 9437188
  57.5 85.5 %copy-start = (bf16[8,12,24,128]{3,2,1,0:T(8,128)(2,1)}, bf16[8,12,24,128]{3,2,1,0:T(8,128)(2,1)S(1)}, u32[]{:S(2)}) copy-start(bf16[8,12,24,128]{3,2,1,0:T(8,128)(2,1)S(1)} %all_to_all.31.packed.mine) | copy-start | bytes 1769476
  57.5 19.8 %copy-start.6 = (bf16[512,384]{1,0:T(8,128)(2,1)S(1)}, bf16[512,384]{1,0:T(8,128)(2,1)}, u32[]{:S(2)}) copy-start(bf16[512,384]{1,0:T(8,128)(2,1)} %query_cotangent.1) | copy-start | bytes 1179652
  57.5 19.8 %copy-start.7 = (bf16[512,384]{1,0:T(8,128)(2,1)S(1)}, bf16[512,384]{1,0:T(8,128)(2,1)}, u32[]{:S(2)}) copy-start(bf16[512,384]{1,0:T(8,128)(2,1)} %attn_outputs.1) | copy-start | bytes 1179652
  59.4 52.9 %copy-start.8 = (f32[2,4,384]{2,1,0:T(4,128)S(1)}, f32[2,4,384]{2,1,0:T(4,128)}, u32[]{:S(2)}) copy-start(f32[2,4,384]{2,1,0:T(4,128)} %first.1) | copy-start | bytes 36868
  59.4 52.9 %copy-start.9 = (f32[2,4,384]{2,1,0:T(4,128)S(1)}, f32[2,4,384]{2,1,0:T(4,128)}, u32[]{:S(2)}) copy-start(f32[2,4,384]{2,1,0:T(4,128)} %second.1) | copy-start | bytes 36868
  130.5 41.2 %all-to-all-start.4 = ((bf16[8,13,4,768]{3,2,1,0:T(4,128)(2,1)}), bf16[8,13,4,768]{3,2,1,0:T(4,128)(2,1)S(1)}, u32[]{:S(2)}, u32[]{:S(2)}) async-start(bf16[8,13,4,768]{3,2,1,0:T(4,128)(2,1)} %shard_map.151), calls=%async_computation.4 | async-start | bytes 1277952 | tf_op jit(solution)/shard_map/all_to_all | solution.py:382
  134.0 15.0 %collective-permute-start.3 = (bf16[8,12,24,128]{3,2,1,0:T(8,128)(2,1)S(1)}, bf16[8,12,24,128]{3,2,1,0:T(8,128)(2,1)S(1)}, u32[]{:S(2)}, u32[]{:S(2)}) collective-permute-start(bf16[8,12,24,128]{3,2,1,0:T(8,128)(2,1)S(1)} %all_to_all.31.packed.mine), channel_id=1, source_target_pairs={{6,0},{7,1},{0,2},{1,3},{2,4},{3,5},{4,6},{5,7},{14,8},{15,9},{8,1... | collective-permute-start | bytes 1769480 | tf_op jit(solution)/shard_map/ppermute | solution.py:357
  136.6 25.3 %collective-permute-start.2 = (bf16[8,12,24,128]{3,2,1,0:T(8,128)(2,1)S(1)}, bf16[8,12,24,128]{3,2,1,0:T(8,128)(2,1)}, u32[]{:S(2)}, u32[]{:S(2)}) collective-permute-start(bf16[8,12,24,128]{3,2,1,0:T(8,128)(2,1)S(1)} %all_to_all.31.packed.mine), channel_id=1, source_target_pairs={{4,0},{5,1},{6,2},{7,3},{0,4},{1,5},{2,6},{3,7},{12,8},{13,9},{14,... | collective-permute-start | bytes 1769480 | tf_op jit(solution)/shard_map/ppermute | solution.py:357
  140.8 25.7 %collective-permute-start.1 = (bf16[8,12,24,128]{3,2,1,0:T(8,128)(2,1)S(1)}, bf16[8,12,24,128]{3,2,1,0:T(8,128)(2,1)}, u32[]{:S(2)}, u32[]{:S(2)}) collective-permute-start(bf16[8,12,24,128]{3,2,1,0:T(8,128)(2,1)S(1)} %all_to_all.31.packed.mine), channel_id=1, source_target_pairs={{2,0},{3,1},{4,2},{5,3},{6,4},{7,5},{0,6},{1,7},{10,8},{11,9},{12,... | collective-permute-start | bytes 1769480 | tf_op jit(solution)/shard_map/ppermute | solution.py:357
  142.9 33.5 %collective-permute-start = (bf16[8,12,24,128]{3,2,1,0:T(8,128)(2,1)S(1)}, bf16[8,12,24,128]{3,2,1,0:T(8,128)(2,1)}, u32[]{:S(2)}, u32[]{:S(2)}) collective-permute-start(bf16[8,12,24,128]{3,2,1,0:T(8,128)(2,1)S(1)} %all_to_all.31.packed.mine), channel_id=1, source_target_pairs={{1,0},{0,1},{3,2},{2,3},{5,4},{4,5},{7,6},{6,7},{9,8},{8,9},{11,10... | collective-permute-start | bytes 1769480 | tf_op jit(solution)/shard_map/ppermute | solution.py:354
  149.0 17.5 %copy-start.11 = (bf16[8,12,24,128]{3,2,1,0:T(8,128)(2,1)}, bf16[8,12,24,128]{3,2,1,0:T(8,128)(2,1)S(1)}, u32[]{:S(2)}) copy-start(bf16[8,12,24,128]{3,2,1,0:T(8,128)(2,1)S(1)} %collective-permute-done.3) | copy-start | bytes 1769476
  168.1 4.2 %copy-start.10 = (bf16[3,8,12,24,128]{4,3,2,1,0:T(8,128)(2,1)}, bf16[3,8,12,24,128]{4,3,2,1,0:T(8,128)(2,1)S(1)}, u32[]{:S(2)}) copy-start(bf16[3,8,12,24,128]{4,3,2,1,0:T(8,128)(2,1)S(1)} %pad_maximum_fusion.held) | copy-start | bytes 5308420
  168.1 8.2 %collective-permute-start.4 = (bf16[3,8,12,24,128]{4,3,2,1,0:T(8,128)(2,1)S(1)}, bf16[3,8,12,24,128]{4,3,2,1,0:T(8,128)(2,1)}, u32[]{:S(2)}, u32[]{:S(2)}) collective-permute-start(bf16[3,8,12,24,128]{4,3,2,1,0:T(8,128)(2,1)S(1)} %pad_maximum_fusion.held), channel_id=1, source_target_pairs={{1,0},{0,1},{3,2},{2,3},{5,4},{4,5},{7,6},{6,7},{9,8},{8,9},{11,10... | collective-permute-start | bytes 5308424 | tf_op jit(solution)/shard_map/ppermute | solution.py:359
  172.3 12.8 %all-to-all-start.5 = ((f32[8,1,128]{2,1,0:T(1,128)}), f32[8,1,128]{2,1,0:T(1,128)S(1)}, u32[]{:S(2)}, u32[]{:S(2)}) async-start(f32[8,1,128]{2,1,0:T(1,128)} %shard_map.152), calls=%async_computation.5 | async-start | bytes 8192 | tf_op jit(solution)/shard_map/all_to_all | solution.py:423
  185.2 2.3 %copy-start.1 = (bf16[6144,384]{1,0:T(8,128)(2,1)S(1)}, bf16[6144,384]{1,0:T(8,128)(2,1)}, u32[]{:S(2)}) copy-start(bf16[6144,384]{1,0:T(8,128)(2,1)} %all-gather.3.cloned.1.call-done) | copy-start | bytes 14155780
  187.5 1.7 copy-start.4
  189.2 1.7 copy-start.5
Sparse Core Ops, SparseCore 0:
  12.3 133.2 all-gather.2

commit v15 on v13

--- a/solution.py
+++ b/solution.py
@@ -26,16 +26,16 @@
 LONG = cost(1 << 35, 1 << 26)
 
 
-def coded(value):
-    size = value * REACH
+def coded(value, reach=REACH):
+    size = value * reach
     size = size * size
     size = size * size
     return jnp.where(value < 0.0, -size, size).astype(bf16)
 
 
-def decoded(code):
+def decoded(code, reach=REACH):
     wide = code.astype(f32)
-    size = lax.rsqrt(lax.rsqrt(jnp.abs(wide))) * (1.0 / REACH)
+    size = lax.rsqrt(lax.rsqrt(jnp.abs(wide))) * (1.0 / reach)
     return jnp.where(wide < 0.0, -size, size)
 
 
@@ -97,7 +97,15 @@
         parts.append(jnp.dot(ranks, other[...], preferred_element_type=f32).reshape(-1, 8, cols))
     first, second = parts
     both = jnp.concatenate([first[:, :4], second[:, :4], first[:, 4:], second[:, 4:]], axis=1)
-    out[...] = both.astype(bf16)
+    height, depth = out.shape[:2]
+    both = both.astype(bf16).reshape(depth, height // 2, 16, cols)
+    for y in range(0, height, 2):
+        out[y] = both[:, y // 2, :8]
+        out[y + 1] = both[:, y // 2, 8:]
+
+
+def fold_kernel(pieces, out):
+    out[...] = coded(jnp.sum(pieces[...].astype(f32), axis=0), 1.0)
 
 
 def in_three(total):
@@ -110,7 +118,7 @@
 
 def moment_kernel(pieces, first, second, first_new, second_new, low):
     rows = first.shape[1]
-    grads = jnp.sum(pieces[...].astype(f32), axis=0)
+    grads = jnp.sum(decoded(pieces[...], 1.0), axis=0)
     new_first = 0.9 * jnp.concatenate([first[0], first[1]], axis=0) + 0.1 * grads
     new_second = 0.99 * jnp.concatenate([second[0], second[1]], axis=0) + 0.01 * grads * grads
     direction = new_first / (jnp.sqrt(new_second) + 1e-08)
@@ -337,13 +345,22 @@
 
     partial = pl.pallas_call(
         functools.partial(grad_kernel, rank_cols),
-        out_shape=pltpu.HBM((fs // 2, 4 * rows, cols), bf16),
+        out_shape=pltpu.HBM((height, depth, 2 * rows, cols), bf16),
         in_specs=[VMEM] * 3,
         out_specs=VMEM,
         compiler_params=SMALL,
         cost_estimate=cost(4 * ranks * tokens * cols, 2 << 20),
     )(proj, query_cotangent, attn_outputs)
-    pieces = lax.all_to_all(partial.reshape(fs, 2 * rows, cols), FS, 0, 0)
+    pieces = lax.all_to_all(partial, "y", 0, 0)
+    pieces = pl.pallas_call(
+        fold_kernel,
+        out_shape=jax.ShapeDtypeStruct((depth, 2 * rows, cols), bf16),
+        in_specs=[VMEM],
+        out_specs=VMEM,
+        compiler_params=SMALL,
+        cost_estimate=cost(1 << 20, 1 << 20),
+    )(pieces)
+    pieces = lax.all_to_all(pieces, "z", 0, 0)
 
     held = [packed]
     for step in range(1, tp // 2):

time: 204 us -> 204 us (level)
    all_to_all x1, blocking collectives: 16.2 us -> 13.6 us  [body(): low = lax.all_to_all(low, 'z', 0, 0)]
    all_to_all x1 -> x2, blocking collectives: 33.7 us -> 35.8 us  [the longest x1 22.8 us: body(): pieces = lax.all_to_all(partial, 'y', 0, 0)]
where the time goes in v15:
time: 204 us; the launch traced here: 203 us
  blocking collectives  116 us (57%)
  waiting for transfers between devices  22.7 us (11%)
  Pallas kernels  21.8 us (11%)
  starting transfers between devices  20.8 us (10%)
  between operations  14.2 us (7%)
  local copies, waits for them, and re-layouts  5.69 us (3%)
    all_to_all x1, blocking collectives, body(): packed = lax.all_to_all(packed, 'z', 0, 0)  25.5 us
    all_to_all x1, blocking collectives, body(): packed = lax.all_to_all(packed, 'y', 0, 0)  23 us
    all_to_all x1, blocking collectives, body(): pieces = lax.all_to_all(partial, 'y', 0, 0)  22.8 us
    ppermute x3, waiting for transfers between devices, body(): lax.ppermute(packed, 'tp', [((t + 2 * step) % tp, t) for t in range(tp)])  22.7 us
    all_gather x1, blocking collectives, body(): proj = lax.all_gather(proj, 'tp', axis=0, tiled=True)  17.8 us
    all_to_all x1, blocking collectives, body(): low = lax.all_to_all(low, 'z', 0, 0)  13.6 us
    all_to_all x1, blocking collectives, body(): pieces = lax.all_to_all(pieces, 'z', 0, 0)  12.9 us
    ppermute x3, starting transfers between devices, body(): lax.ppermute(packed, 'tp', [((t + 2 * step) % tp, t) for t in range(tp)])  9.67 us
  transfers between devices with their start and end apart: 7, of which 3 were waited for; matrix products, arithmetic and copies ran while one was open for 1% of the time, Pallas kernels for 7%

profile of v15, /device:TPU:1, one launch (start us, length us, event | category | flops | bytes accessed | tf_op | source)
XLA Modules:
  0.0 202.7 jit_solution(16159815069402328474)
XLA Ops:
  7.2 0.0 all-gather.3.cloned.1.call-start
  7.2 1.6 shard_map.145
  8.8 0.0 all-gather.3.cloned.1.call-update
  8.9 0.0 copy-start.1
  8.9 0.0 copy-start.2
  8.9 25.5 %all_to_all.35.packed = bf16[12,24,128]{2,1,0:T(8,128)(2,1)S(1)} all-to-all(bf16[12,24,128]{2,1,0:T(8,128)(2,1)S(1)} %shard_map.146), channel_id=1, replica_groups=mesh['z'=12,'y'=8,'tp'=8] {'z'}, dimensions={0} | all-to-all | bytes 147456 | tf_op jit(solution)/shard_map/all_to_all | solution.py:325
  34.4 0.1 shard_map.147
  34.5 23.0 %all_to_all.36.packed = bf16[8,12,24,128]{3,2,1,0:T(8,128)(2,1)S(1)} all-to-all(bf16[8,12,24,128]{3,2,1,0:T(8,128)(2,1)S(1)} %shard_map.147), channel_id=1, replica_groups=mesh['z'=12,'y'=8,'tp'=8] {'y'}, dimensions={0} | all-to-all | bytes 1179648 | tf_op jit(solution)/shard_map/all_to_all | solution.py:334
  57.4 0.0 copy-done.1
  57.4 0.0 copy-done.2
  57.5 0.0 copy-start.5
  57.5 0.0 copy-start.6
  57.5 2.0 shard_map.148
  59.4 0.0 copy-start.7
  59.4 0.0 copy-start.8
  59.4 17.8 %all_gather.9.proj = bf16[768,512]{1,0:T(8,128)(2,1)S(1)} all-gather(bf16[96,512]{1,0:T(8,128)(2,1)S(1)} %shard_map.148), channel_id=1, replica_groups=mesh['z'=12,'y'=8,'tp'=8] {'tp'}, dimensions={0}, use_global_device_ids=true | all-gather | bytes 884736 | tf_op jit(solution)/shard_map/all_gather | solution.py:344
  77.3 0.0 copy-done.5
  77.3 0.0 copy-done.6
  77.3 1.4 shard_map.149
  78.7 22.8 %all_to_all.37.pieces = bf16[8,12,8,384]{3,2,1,0:T(8,128)(2,1)S(1)} all-to-all(bf16[8,12,8,384]{3,2,1,0:T(8,128)(2,1)} %shard_map.149), channel_id=1, replica_groups=mesh['z'=12,'y'=8,'tp'=8] {'y'}, dimensions={0} | all-to-all | bytes 1179648 | tf_op jit(solution)/shard_map/all_to_all | solution.py:354
  101.5 0.1 shard_map.150
  101.6 12.9 %all_to_all.38.pieces = bf16[12,8,384]{2,1,0:T(8,128)(2,1)S(1)} all-to-all(bf16[12,8,384]{2,1,0:T(8,128)(2,1)S(1)} %shard_map.150), channel_id=1, replica_groups=mesh['z'=12,'y'=8,'tp'=8] {'z'}, dimensions={0} | all-to-all | bytes 147456 | tf_op jit(solution)/shard_map/all_to_all | solution.py:363
  114.5 0.0 copy-done.7
  114.5 0.0 copy-done.8
  114.5 0.8 shard_map.151
  115.4 13.6 %all_to_all.39.low = bf16[12,4,896]{2,1,0:T(4,128)(2,1)S(1)} all-to-all(bf16[12,4,896]{2,1,0:T(4,128)(2,1)} %get-tuple-element.23), channel_id=1, replica_groups=mesh['z'=12,'y'=8,'tp'=8] {'z'}, dimensions={0} | all-to-all | bytes 172032 | tf_op jit(solution)/shard_map/all_to_all | solution.py:383
  129.0 0.9 shard_map.152
  130.0 3.5 %all-to-all-start.5 = ((bf16[8,13,4,768]{3,2,1,0:T(4,128)(2,1)}), bf16[8,13,4,768]{3,2,1,0:T(4,128)(2,1)S(1)}, u32[]{:S(2)}, u32[]{:S(2)}) async-start(bf16[8,13,4,768]{3,2,1,0:T(4,128)(2,1)} %shard_map.152), calls=%async_computation.5 | async-start | bytes 1277952 | tf_op jit(solution)/shard_map/all_to_all | solution.py:392
  133.5 3.4 %collective-permute-start.2 = (bf16[8,12,24,128]{3,2,1,0:T(8,128)(2,1)S(1)}, bf16[8,12,24,128]{3,2,1,0:T(8,128)(2,1)S(1)}, u32[]{:S(2)}, u32[]{:S(2)}) collective-permute-start(bf16[8,12,24,128]{3,2,1,0:T(8,128)(2,1)S(1)} %all_to_all.36.packed), channel_id=1, source_target_pairs={{6,0},{7,1},{0,2},{1,3},{2,4},{3,5},{4,6},{5,7},{14,8},{15,9},{8,1... | collective-permute-start | bytes 1769480 | tf_op jit(solution)/shard_map/ppermute | solution.py:367
  137.0 4.3 %collective-permute-start.1 = (bf16[8,12,24,128]{3,2,1,0:T(8,128)(2,1)S(1)}, bf16[8,12,24,128]{3,2,1,0:T(8,128)(2,1)S(1)}, u32[]{:S(2)}, u32[]{:S(2)}) collective-permute-start(bf16[8,12,24,128]{3,2,1,0:T(8,128)(2,1)S(1)} %all_to_all.36.packed), channel_id=1, source_target_pairs={{4,0},{5,1},{6,2},{7,3},{0,4},{1,5},{2,6},{3,7},{12,8},{13,9},{14,... | collective-permute-start | bytes 1769480 | tf_op jit(solution)/shard_map/ppermute | solution.py:367
  141.3 1.9 collective-permute-start
  143.2 0.1 pad_add_fusion.place
  143.3 3.6 %collective-permute-done.2 = bf16[8,12,24,128]{3,2,1,0:T(8,128)(2,1)S(1)} collective-permute-done((bf16[8,12,24,128]{3,2,1,0:T(8,128)(2,1)S(1)}, bf16[8,12,24,128]{3,2,1,0:T(8,128)(2,1)S(1)}, u32[]{:S(2)}, u32[]{:S(2)}) %collective-permute-start.2) | collective-permute-done | bytes 589856 | tf_op jit(solution)/shard_map/ppermute | solution.py:367
  146.9 14.4 %collective-permute-done.1 = bf16[8,12,24,128]{3,2,1,0:T(8,128)(2,1)S(1)} collective-permute-done((bf16[8,12,24,128]{3,2,1,0:T(8,128)(2,1)S(1)}, bf16[8,12,24,128]{3,2,1,0:T(8,128)(2,1)S(1)}, u32[]{:S(2)}, u32[]{:S(2)}) %collective-permute-start.1) | collective-permute-done | bytes 589856 | tf_op jit(solution)/shard_map/ppermute | solution.py:367
  161.3 4.6 %collective-permute-done = bf16[8,12,24,128]{3,2,1,0:T(8,128)(2,1)S(1)} collective-permute-done((bf16[8,12,24,128]{3,2,1,0:T(8,128)(2,1)S(1)}, bf16[8,12,24,128]{3,2,1,0:T(8,128)(2,1)S(1)}, u32[]{:S(2)}, u32[]{:S(2)}) %collective-permute-start) | collective-permute-done | bytes 589856 | tf_op jit(solution)/shard_map/ppermute | solution.py:367
  166.0 1.7 pad_maximum_fusion.held
  167.7 3.6 %collective-permute-start.3 = (bf16[4,8,12,24,128]{4,3,2,1,0:T(8,128)(2,1)}, bf16[4,8,12,24,128]{4,3,2,1,0:T(8,128)(2,1)}, u32[]{:S(2)}, u32[]{:S(2)}) collective-permute-start(bf16[4,8,12,24,128]{4,3,2,1,0:T(8,128)(2,1)} %pad_maximum_fusion.held), channel_id=1, source_target_pairs={{1,0},{0,1},{3,2},{2,3},{5,4},{4,5},{7,6},{6,7},{9,8},{8,9},{11,10... | collective-permute-start | bytes 7077896 | tf_op jit(solution)/shard_map/ppermute | solution.py:369
  171.2 0.0 all-to-all-done.5.low
  171.3 0.0 all-gather.3.cloned.1.call-done
  171.3 0.6 shard_map.153
  171.9 4.0 %all-to-all-start.6 = ((f32[8,1,128]{2,1,0:T(1,128)}), f32[8,1,128]{2,1,0:T(1,128)S(1)}, u32[]{:S(2)}, u32[]{:S(2)}) async-start(f32[8,1,128]{2,1,0:T(1,128)} %shard_map.153), calls=%async_computation.6 | async-start | bytes 8192 | tf_op jit(solution)/shard_map/all_to_all | solution.py:431
  175.9 0.0 collective-permute-done.3.other
  175.9 8.9 %shard_map.154 = (bf16[3072,384]{1,0:T(8,128)(2,1)}, bf16[384,3072]{1,0:T(8,128)(2,1)}, bf16[32,384]{1,0:T(8,128)(2,1)}, bf16[32,384]{1,0:T(8,128)(2,1)}) custom-call(s32[2]{0:T(128)S(1)} %pad_add_fusion.place, bf16[4,8,12,24,128]{4,3,2,1,0:T(8,128)(2,1)} %pad_maximum_fusion.held, bf16[4,8,12,24,128]{4,3,2,1,0:T(8,128)(2,1)} %collective-permute-done.3.other), custom_call_target="tpu_custom_call" | custom-call | flops 1073741824 | bytes 31457280 | tf_op jit(solution)/shard_map/pallas_call | solution.py:396
  184.8 0.0 all-to-all-done.6.squares
  184.8 0.0 copy-start
  184.8 2.3 %copy-done = bf16[6144,384]{1,0:T(8,128)(2,1)S(1)} copy-done((bf16[6144,384]{1,0:T(8,128)(2,1)S(1)}, bf16[6144,384]{1,0:T(8,128)(2,1)}, u32[]{:S(2)}) %copy-start) | copy-done | bytes 4718616
  187.2 0.0 copy-start.3
  187.2 1.7 copy-done.3
  188.8 0.0 copy-start.4
  188.8 1.7 copy-done.4
  190.5 5.3 %shard_map.155 = (bf16[3072,384]{1,0:T(8,128)(2,1)}, bf16[384,3072]{1,0:T(8,128)(2,1)}, f32[32,384]{1,0:T(8,128)}, f32[32,384]{1,0:T(8,128)}) custom-call(f32[8,1,128]{2,1,0:T(1,128)S(1)} %all-to-all-done.6.squares, bf16[8,13,4,768]{3,2,1,0:T(4,128)(2,1)S(1)} %all-to-all-done.5.low, bf16[3072,384]{1,0:T(8,128)(2,1)S(1)} %copy-done.3, ...), custom_call_target="tpu_custom_call" | custom-call | flops 1811939328 | bytes 20971520 | tf_op jit(solution)/shard_map/pallas_call | solution.py:433
  (1 shorter events, 0.0 us)
Async XLA Ops:
  7.2 164.1 %all-gather.3.cloned.1.call-start = ((), (), s32[]{:S(2)}) async-start(), calls=%async_computation.7 | async-start | bytes 4767744 | tf_op jit(solution)/shard_map/all_gather | solution.py:324
  8.9 48.6 %copy-start.1 = (bf16[512,3072]{1,0:T(8,128)(2,1)S(1)}, bf16[512,3072]{1,0:T(8,128)(2,1)}, u32[]{:S(2)}) copy-start(bf16[512,3072]{1,0:T(8,128)(2,1)} %saved_inputs.1) | copy-start | bytes 9437188
  8.9 48.6 %copy-start.2 = (bf16[512,3072]{1,0:T(8,128)(2,1)S(1)}, bf16[512,3072]{1,0:T(8,128)(2,1)}, u32[]{:S(2)}) copy-start(bf16[512,3072]{1,0:T(8,128)(2,1)} %out_cotangent.1) | copy-start | bytes 9437188
  57.5 19.8 %copy-start.5 = (bf16[512,384]{1,0:T(8,128)(2,1)S(1)}, bf16[512,384]{1,0:T(8,128)(2,1)}, u32[]{:S(2)}) copy-start(bf16[512,384]{1,0:T(8,128)(2,1)} %query_cotangent.1) | copy-start | bytes 1179652
  57.5 19.8 %copy-start.6 = (bf16[512,384]{1,0:T(8,128)(2,1)S(1)}, bf16[512,384]{1,0:T(8,128)(2,1)}, u32[]{:S(2)}) copy-start(bf16[512,384]{1,0:T(8,128)(2,1)} %attn_outputs.1) | copy-start | bytes 1179652
  59.4 55.1 %copy-start.7 = (f32[2,4,384]{2,1,0:T(4,128)S(1)}, f32[2,4,384]{2,1,0:T(4,128)}, u32[]{:S(2)}) copy-start(f32[2,4,384]{2,1,0:T(4,128)} %first.1) | copy-start | bytes 36868
  59.4 55.1 %copy-start.8 = (f32[2,4,384]{2,1,0:T(4,128)S(1)}, f32[2,4,384]{2,1,0:T(4,128)}, u32[]{:S(2)}) copy-start(f32[2,4,384]{2,1,0:T(4,128)} %second.1) | copy-start | bytes 36868
  130.0 41.3 %all-to-all-start.5 = ((bf16[8,13,4,768]{3,2,1,0:T(4,128)(2,1)}), bf16[8,13,4,768]{3,2,1,0:T(4,128)(2,1)S(1)}, u32[]{:S(2)}, u32[]{:S(2)}) async-start(bf16[8,13,4,768]{3,2,1,0:T(4,128)(2,1)} %shard_map.152), calls=%async_computation.5 | async-start | bytes 1277952 | tf_op jit(solution)/shard_map/all_to_all | solution.py:392
  133.5 13.4 %collective-permute-start.2 = (bf16[8,12,24,128]{3,2,1,0:T(8,128)(2,1)S(1)}, bf16[8,12,24,128]{3,2,1,0:T(8,128)(2,1)S(1)}, u32[]{:S(2)}, u32[]{:S(2)}) collective-permute-start(bf16[8,12,24,128]{3,2,1,0:T(8,128)(2,1)S(1)} %all_to_all.36.packed), channel_id=1, source_target_pairs={{6,0},{7,1},{0,2},{1,3},{2,4},{3,5},{4,6},{5,7},{14,8},{15,9},{8,1... | collective-permute-start | bytes 1769480 | tf_op jit(solution)/shard_map/ppermute | solution.py:367
  137.0 24.4 %collective-permute-start.1 = (bf16[8,12,24,128]{3,2,1,0:T(8,128)(2,1)S(1)}, bf16[8,12,24,128]{3,2,1,0:T(8,128)(2,1)S(1)}, u32[]{:S(2)}, u32[]{:S(2)}) collective-permute-start(bf16[8,12,24,128]{3,2,1,0:T(8,128)(2,1)S(1)} %all_to_all.36.packed), channel_id=1, source_target_pairs={{4,0},{5,1},{6,2},{7,3},{0,4},{1,5},{2,6},{3,7},{12,8},{13,9},{14,... | collective-permute-start | bytes 1769480 | tf_op jit(solution)/shard_map/ppermute | solution.py:367
  141.3 24.7 %collective-permute-start = (bf16[8,12,24,128]{3,2,1,0:T(8,128)(2,1)S(1)}, bf16[8,12,24,128]{3,2,1,0:T(8,128)(2,1)S(1)}, u32[]{:S(2)}, u32[]{:S(2)}) collective-permute-start(bf16[8,12,24,128]{3,2,1,0:T(8,128)(2,1)S(1)} %all_to_all.36.packed), channel_id=1, source_target_pairs={{2,0},{3,1},{4,2},{5,3},{6,4},{7,5},{0,6},{1,7},{10,8},{11,9},{12,... | collective-permute-start | bytes 1769480 | tf_op jit(solution)/shard_map/ppermute | solution.py:367
  167.7 8.2 %collective-permute-start.3 = (bf16[4,8,12,24,128]{4,3,2,1,0:T(8,128)(2,1)}, bf16[4,8,12,24,128]{4,3,2,1,0:T(8,128)(2,1)}, u32[]{:S(2)}, u32[]{:S(2)}) collective-permute-start(bf16[4,8,12,24,128]{4,3,2,1,0:T(8,128)(2,1)} %pad_maximum_fusion.held), channel_id=1, source_target_pairs={{1,0},{0,1},{3,2},{2,3},{5,4},{4,5},{7,6},{6,7},{9,8},{8,9},{11,10... | collective-permute-start | bytes 7077896 | tf_op jit(solution)/shard_map/ppermute | solution.py:369
  171.9 12.9 %all-to-all-start.6 = ((f32[8,1,128]{2,1,0:T(1,128)}), f32[8,1,128]{2,1,0:T(1,128)S(1)}, u32[]{:S(2)}, u32[]{:S(2)}) async-start(f32[8,1,128]{2,1,0:T(1,128)} %shard_map.153), calls=%async_computation.6 | async-start | bytes 8192 | tf_op jit(solution)/shard_map/all_to_all | solution.py:431
  184.8 2.3 %copy-start = (bf16[6144,384]{1,0:T(8,128)(2,1)S(1)}, bf16[6144,384]{1,0:T(8,128)(2,1)}, u32[]{:S(2)}) copy-start(bf16[6144,384]{1,0:T(8,128)(2,1)} %all-gather.3.cloned.1.call-done) | copy-start | bytes 14155780
  187.2 1.7 copy-start.3
  188.8 1.7 copy-start.4
Sparse Core Ops, SparseCore 0:
  12.3 131.6 all-gather.2

commit v16 on v13

--- a/solution.py
+++ b/solution.py
@@ -16,6 +16,7 @@
 ANY = pl.BlockSpec(memory_space=pl.ANY)
 SMEM = pl.BlockSpec(memory_space=pltpu.SMEM)
 REACH = 2.0**34
+GRAD_REACH = 2.0**10
 SMALL = pltpu.CompilerParams(vmem_limit_bytes=16 << 20)
 
 
@@ -26,23 +27,23 @@
 LONG = cost(1 << 35, 1 << 26)
 
 
-def coded(value):
-    size = value * REACH
+def coded(value, reach):
+    size = value * reach
     size = size * size
     size = size * size
     return jnp.where(value < 0.0, -size, size).astype(bf16)
 
 
-def decoded(code):
+def decoded(code, reach):
     wide = code.astype(f32)
-    size = lax.rsqrt(lax.rsqrt(jnp.abs(wide))) * (1.0 / REACH)
+    size = lax.rsqrt(lax.rsqrt(jnp.abs(wide))) * (1.0 / reach)
     return jnp.where(wide < 0.0, -size, size)
 
 
 def send_kernel(left, right, query_master, out_master, out, masters):
     own = query_master.shape[0]
-    masters[:own] = coded(query_master[...])
-    masters[own:] = coded(out_master[...])
+    masters[:own] = coded(query_master[...], REACH)
+    masters[own:] = coded(out_master[...], REACH)
     both = jnp.concatenate([left[...].astype(f32), right[...].astype(f32)], axis=1)
     used = both.shape[1]
     free = 128 - used
@@ -97,7 +98,7 @@
         parts.append(jnp.dot(ranks, other[...], preferred_element_type=f32).reshape(-1, 8, cols))
     first, second = parts
     both = jnp.concatenate([first[:, :4], second[:, :4], first[:, 4:], second[:, 4:]], axis=1)
-    out[...] = both.astype(bf16)
+    out[...] = coded(both, GRAD_REACH)
 
 
 def in_three(total):
@@ -110,7 +111,7 @@
 
 def moment_kernel(pieces, first, second, first_new, second_new, low):
     rows = first.shape[1]
-    grads = jnp.sum(pieces[...].astype(f32), axis=0)
+    grads = jnp.sum(decoded(pieces[...], GRAD_REACH), axis=0)
     new_first = 0.9 * jnp.concatenate([first[0], first[1]], axis=0) + 0.1 * grads
     new_second = 0.99 * jnp.concatenate([second[0], second[1]], axis=0) + 0.01 * grads * grads
     direction = new_first / (jnp.sqrt(new_second) + 1e-08)
@@ -243,12 +244,12 @@
         at = pl.ds(i * span, span)
         codes = masters[i * per : (i + 1) * per]
         moved = jnp.dot(left[at], first[...], preferred_element_type=f32)
-        kept = decoded(codes[:, :own].reshape(span, cols))
+        kept = decoded(codes[:, :own].reshape(span, cols), REACH)
         near_query[at] = (kept - scales[0] * moved).astype(bf16)
         sent.append(pltpu.make_async_copy(near_query.at[at], query_copy.at[at], left_for.at[i, 0]))
         sent[-1].start()
         moved = jnp.dot(second_turned, right[:, at], preferred_element_type=f32)
-        kept = decoded(codes[:, own:].reshape(span, cols).T)
+        kept = decoded(codes[:, own:].reshape(span, cols).T, REACH)
         near_out[:, at] = (kept - scales[1] * moved).astype(bf16)
         sent.append(pltpu.make_async_copy(near_out.at[:, at], out_copy.at[:, at], left_for.at[i, 1]))
         sent[-1].start()

time: 204 us -> 205 us (level)
  transfers between devices with their start and end apart: 7 -> 7, of which waited for: 3 -> 3; matrix products, arithmetic and copies ran while one was open for 1% -> 1% of each run, Pallas kernels for 7% -> 8%
where the time goes in v16:
time: 205 us; the launch traced here: 204 us
  blocking collectives  117 us (57%)
  waiting for transfers between devices  23.7 us (12%)
  Pallas kernels  22.4 us (11%)
  starting transfers between devices  19.8 us (10%)
  between operations  14.2 us (7%)
  local copies, waits for them, and re-layouts  5.69 us (3%)
    all_to_all x1, blocking collectives, body(): pieces = lax.all_to_all(partial.reshape(fs, 2 * rows, cols), FS, 0, 0)  33.7 us
    all_to_all x1, blocking collectives, body(): packed = lax.all_to_all(packed, 'z', 0, 0)  25.5 us
    ppermute x3, waiting for transfers between devices, body(): lax.ppermute(packed, 'tp', [((t + 2 * step) % tp, t) for t in range(tp)])  23.6 us
    all_to_all x1, blocking collectives, body(): packed = lax.all_to_all(packed, 'y', 0, 0)  23 us
    all_gather x1, blocking collectives, body(): proj = lax.all_gather(proj, 'tp', axis=0, tiled=True)  17.8 us
    all_to_all x1, blocking collectives, body(): low = lax.all_to_all(low, 'z', 0, 0)  16.6 us
    pallas_call x1, Pallas kernels, body(): pl.pallas_call(functools.partial(prep_kernel, rank_cols), grid=(width //...  8.91 us
    ppermute x3, starting transfers between devices, body(): lax.ppermute(packed, 'tp', [((t + 2 * step) % tp, t) for t in range(tp)])  8.72 us
  transfers between devices with their start and end apart: 7, of which 3 were waited for; matrix products, arithmetic and copies ran while one was open for 1% of the time, Pallas kernels for 8%

profile of v16, /device:TPU:1, one launch (start us, length us, event | category | flops | bytes accessed | tf_op | source)
XLA Modules:
  0.0 204.1 jit_solution(4568967385336131730)
XLA Ops:
  7.2 0.0 all-gather.3.cloned.1.call-start
  7.2 1.6 shard_map.145
  8.8 0.0 all-gather.3.cloned.1.call-update
  8.9 0.0 copy-start.1
  8.9 0.0 copy-start.2
  8.9 25.5 %all_to_all.30.packed = bf16[12,24,128]{2,1,0:T(8,128)(2,1)S(1)} all-to-all(bf16[12,24,128]{2,1,0:T(8,128)(2,1)S(1)} %shard_map.146), channel_id=1, replica_groups=mesh['z'=12,'y'=8,'tp'=8] {'z'}, dimensions={0} | all-to-all | bytes 147456 | tf_op jit(solution)/shard_map/all_to_all | solution.py:318
  34.4 0.1 shard_map.147
  34.5 23.0 %all_to_all.31.packed = bf16[8,12,24,128]{3,2,1,0:T(8,128)(2,1)S(1)} all-to-all(bf16[8,12,24,128]{3,2,1,0:T(8,128)(2,1)S(1)} %shard_map.147), channel_id=1, replica_groups=mesh['z'=12,'y'=8,'tp'=8] {'y'}, dimensions={0} | all-to-all | bytes 1179648 | tf_op jit(solution)/shard_map/all_to_all | solution.py:327
  57.4 0.0 copy-done.1
  57.4 0.0 copy-done.2
  57.5 0.0 copy-start.5
  57.5 0.0 copy-start.6
  57.5 2.0 shard_map.148
  59.4 0.0 copy-start.7
  59.4 0.0 copy-start.8
  59.4 17.8 %all_gather.9.proj = bf16[768,512]{1,0:T(8,128)(2,1)S(1)} all-gather(bf16[96,512]{1,0:T(8,128)(2,1)S(1)} %shard_map.148), channel_id=1, replica_groups=mesh['z'=12,'y'=8,'tp'=8] {'tp'}, dimensions={0}, use_global_device_ids=true | all-gather | bytes 884736 | tf_op jit(solution)/shard_map/all_gather | solution.py:337
  77.3 0.0 copy-done.5
  77.3 0.0 copy-done.6
  77.3 1.6 shard_map.149
  78.9 33.7 %all_to_all.32.pieces = bf16[96,8,384]{2,1,0:T(8,128)(2,1)S(1)} all-to-all(bf16[96,8,384]{2,1,0:T(8,128)(2,1)} %bitcast.12), channel_id=1, replica_groups=mesh['z'=12,'y'=8,'tp'=8] {'z','y'}, dimensions={0} | all-to-all | bytes 1179648 | tf_op jit(solution)/shard_map/all_to_all | solution.py:347
  112.5 0.0 copy-done.7
  112.5 0.0 copy-done.8
  112.6 1.4 shard_map.150
  113.9 16.6 %all_to_all.33.low = bf16[12,4,896]{2,1,0:T(4,128)(2,1)S(1)} all-to-all(bf16[12,4,896]{2,1,0:T(4,128)(2,1)} %get-tuple-element.23), channel_id=1, replica_groups=mesh['z'=12,'y'=8,'tp'=8] {'z'}, dimensions={0} | all-to-all | bytes 172032 | tf_op jit(solution)/shard_map/all_to_all | solution.py:367
  130.6 0.9 shard_map.151
  131.5 3.5 %all-to-all-start.4 = ((bf16[8,13,4,768]{3,2,1,0:T(4,128)(2,1)}), bf16[8,13,4,768]{3,2,1,0:T(4,128)(2,1)S(1)}, u32[]{:S(2)}, u32[]{:S(2)}) async-start(bf16[8,13,4,768]{3,2,1,0:T(4,128)(2,1)} %shard_map.151), calls=%async_computation.4 | async-start | bytes 1277952 | tf_op jit(solution)/shard_map/all_to_all | solution.py:376
  135.1 2.5 %collective-permute-start.2 = (bf16[8,12,24,128]{3,2,1,0:T(8,128)(2,1)S(1)}, bf16[8,12,24,128]{3,2,1,0:T(8,128)(2,1)S(1)}, u32[]{:S(2)}, u32[]{:S(2)}) collective-permute-start(bf16[8,12,24,128]{3,2,1,0:T(8,128)(2,1)S(1)} %all_to_all.31.packed), channel_id=1, source_target_pairs={{6,0},{7,1},{0,2},{1,3},{2,4},{3,5},{4,6},{5,7},{14,8},{15,9},{8,1... | collective-permute-start | bytes 1769480 | tf_op jit(solution)/shard_map/ppermute | solution.py:351
  137.6 4.3 %collective-permute-start.1 = (bf16[8,12,24,128]{3,2,1,0:T(8,128)(2,1)S(1)}, bf16[8,12,24,128]{3,2,1,0:T(8,128)(2,1)S(1)}, u32[]{:S(2)}, u32[]{:S(2)}) collective-permute-start(bf16[8,12,24,128]{3,2,1,0:T(8,128)(2,1)S(1)} %all_to_all.31.packed), channel_id=1, source_target_pairs={{4,0},{5,1},{6,2},{7,3},{0,4},{1,5},{2,6},{3,7},{12,8},{13,9},{14,... | collective-permute-start | bytes 1769480 | tf_op jit(solution)/shard_map/ppermute | solution.py:351
  141.8 1.9 collective-permute-start
  143.8 0.1 pad_add_fusion.place
  143.9 6.6 %collective-permute-done.2 = bf16[8,12,24,128]{3,2,1,0:T(8,128)(2,1)S(1)} collective-permute-done((bf16[8,12,24,128]{3,2,1,0:T(8,128)(2,1)S(1)}, bf16[8,12,24,128]{3,2,1,0:T(8,128)(2,1)S(1)}, u32[]{:S(2)}, u32[]{:S(2)}) %collective-permute-start.2) | collective-permute-done | bytes 589856 | tf_op jit(solution)/shard_map/ppermute | solution.py:351
  150.4 12.1 %collective-permute-done.1 = bf16[8,12,24,128]{3,2,1,0:T(8,128)(2,1)S(1)} collective-permute-done((bf16[8,12,24,128]{3,2,1,0:T(8,128)(2,1)S(1)}, bf16[8,12,24,128]{3,2,1,0:T(8,128)(2,1)S(1)}, u32[]{:S(2)}, u32[]{:S(2)}) %collective-permute-start.1) | collective-permute-done | bytes 589856 | tf_op jit(solution)/shard_map/ppermute | solution.py:351
  162.6 5.0 %collective-permute-done = bf16[8,12,24,128]{3,2,1,0:T(8,128)(2,1)S(1)} collective-permute-done((bf16[8,12,24,128]{3,2,1,0:T(8,128)(2,1)S(1)}, bf16[8,12,24,128]{3,2,1,0:T(8,128)(2,1)S(1)}, u32[]{:S(2)}, u32[]{:S(2)}) %collective-permute-start) | collective-permute-done | bytes 589856 | tf_op jit(solution)/shard_map/ppermute | solution.py:351
  167.5 1.7 pad_maximum_fusion.held
  169.2 3.5 %collective-permute-start.3 = (bf16[4,8,12,24,128]{4,3,2,1,0:T(8,128)(2,1)}, bf16[4,8,12,24,128]{4,3,2,1,0:T(8,128)(2,1)}, u32[]{:S(2)}, u32[]{:S(2)}) collective-permute-start(bf16[4,8,12,24,128]{4,3,2,1,0:T(8,128)(2,1)} %pad_maximum_fusion.held), channel_id=1, source_target_pairs={{1,0},{0,1},{3,2},{2,3},{5,4},{4,5},{7,6},{6,7},{9,8},{8,9},{11,10... | collective-permute-start | bytes 7077896 | tf_op jit(solution)/shard_map/ppermute | solution.py:353
  172.7 0.0 all-to-all-done.4.low
  172.7 0.0 all-gather.3.cloned.1.call-done
  172.7 0.6 shard_map.152
  173.3 4.0 %all-to-all-start.5 = ((f32[8,1,128]{2,1,0:T(1,128)}), f32[8,1,128]{2,1,0:T(1,128)S(1)}, u32[]{:S(2)}, u32[]{:S(2)}) async-start(f32[8,1,128]{2,1,0:T(1,128)} %shard_map.152), calls=%async_computation.5 | async-start | bytes 8192 | tf_op jit(solution)/shard_map/all_to_all | solution.py:415
  177.4 0.0 collective-permute-done.3.other
  177.4 8.9 %shard_map.153 = (bf16[3072,384]{1,0:T(8,128)(2,1)}, bf16[384,3072]{1,0:T(8,128)(2,1)}, bf16[32,384]{1,0:T(8,128)(2,1)}, bf16[32,384]{1,0:T(8,128)(2,1)}) custom-call(s32[2]{0:T(128)S(1)} %pad_add_fusion.place, bf16[4,8,12,24,128]{4,3,2,1,0:T(8,128)(2,1)} %pad_maximum_fusion.held, bf16[4,8,12,24,128]{4,3,2,1,0:T(8,128)(2,1)} %collective-permute-done.3.other), custom_call_target="tpu_custom_call" | custom-call | flops 1073741824 | bytes 31457280 | tf_op jit(solution)/shard_map/pallas_call | solution.py:380
  186.3 0.0 all-to-all-done.5.squares
  186.3 0.0 copy-start
  186.3 2.3 %copy-done = bf16[6144,384]{1,0:T(8,128)(2,1)S(1)} copy-done((bf16[6144,384]{1,0:T(8,128)(2,1)S(1)}, bf16[6144,384]{1,0:T(8,128)(2,1)}, u32[]{:S(2)}) %copy-start) | copy-done | bytes 4718616
  188.6 0.0 copy-start.3
  188.6 1.7 copy-done.3
  190.3 0.0 copy-start.4
  190.3 1.7 copy-done.4
  191.9 5.3 %shard_map.154 = (bf16[3072,384]{1,0:T(8,128)(2,1)}, bf16[384,3072]{1,0:T(8,128)(2,1)}, f32[32,384]{1,0:T(8,128)}, f32[32,384]{1,0:T(8,128)}) custom-call(f32[8,1,128]{2,1,0:T(1,128)S(1)} %all-to-all-done.5.squares, bf16[8,13,4,768]{3,2,1,0:T(4,128)(2,1)S(1)} %all-to-all-done.4.low, bf16[3072,384]{1,0:T(8,128)(2,1)S(1)} %copy-done.3, ...), custom_call_target="tpu_custom_call" | custom-call | flops 1811939328 | bytes 20971520 | tf_op jit(solution)/shard_map/pallas_call | solution.py:417
  (1 shorter events, 0.0 us)
Async XLA Ops:
  7.2 165.6 %all-gather.3.cloned.1.call-start = ((), (), s32[]{:S(2)}) async-start(), calls=%async_computation.6 | async-start | bytes 4767744 | tf_op jit(solution)/shard_map/all_gather | solution.py:317
  8.9 48.6 %copy-start.1 = (bf16[512,3072]{1,0:T(8,128)(2,1)S(1)}, bf16[512,3072]{1,0:T(8,128)(2,1)}, u32[]{:S(2)}) copy-start(bf16[512,3072]{1,0:T(8,128)(2,1)} %saved_inputs.1) | copy-start | bytes 9437188
  8.9 48.6 %copy-start.2 = (bf16[512,3072]{1,0:T(8,128)(2,1)S(1)}, bf16[512,3072]{1,0:T(8,128)(2,1)}, u32[]{:S(2)}) copy-start(bf16[512,3072]{1,0:T(8,128)(2,1)} %out_cotangent.1) | copy-start | bytes 9437188
  57.5 19.8 %copy-start.5 = (bf16[512,384]{1,0:T(8,128)(2,1)S(1)}, bf16[512,384]{1,0:T(8,128)(2,1)}, u32[]{:S(2)}) copy-start(bf16[512,384]{1,0:T(8,128)(2,1)} %query_cotangent.1) | copy-start | bytes 1179652
  57.5 19.8 %copy-start.6 = (bf16[512,384]{1,0:T(8,128)(2,1)S(1)}, bf16[512,384]{1,0:T(8,128)(2,1)}, u32[]{:S(2)}) copy-start(bf16[512,384]{1,0:T(8,128)(2,1)} %attn_outputs.1) | copy-start | bytes 1179652
  59.4 53.1 %copy-start.7 = (f32[2,4,384]{2,1,0:T(4,128)S(1)}, f32[2,4,384]{2,1,0:T(4,128)}, u32[]{:S(2)}) copy-start(f32[2,4,384]{2,1,0:T(4,128)} %first.1) | copy-start | bytes 36868
  59.4 53.1 %copy-start.8 = (f32[2,4,384]{2,1,0:T(4,128)S(1)}, f32[2,4,384]{2,1,0:T(4,128)}, u32[]{:S(2)}) copy-start(f32[2,4,384]{2,1,0:T(4,128)} %second.1) | copy-start | bytes 36868
  131.5 41.2 %all-to-all-start.4 = ((bf16[8,13,4,768]{3,2,1,0:T(4,128)(2,1)}), bf16[8,13,4,768]{3,2,1,0:T(4,128)(2,1)S(1)}, u32[]{:S(2)}, u32[]{:S(2)}) async-start(bf16[8,13,4,768]{3,2,1,0:T(4,128)(2,1)} %shard_map.151), calls=%async_computation.4 | async-start | bytes 1277952 | tf_op jit(solution)/shard_map/all_to_all | solution.py:376
  135.1 15.4 %collective-permute-start.2 = (bf16[8,12,24,128]{3,2,1,0:T(8,128)(2,1)S(1)}, bf16[8,12,24,128]{3,2,1,0:T(8,128)(2,1)S(1)}, u32[]{:S(2)}, u32[]{:S(2)}) collective-permute-start(bf16[8,12,24,128]{3,2,1,0:T(8,128)(2,1)S(1)} %all_to_all.31.packed), channel_id=1, source_target_pairs={{6,0},{7,1},{0,2},{1,3},{2,4},{3,5},{4,6},{5,7},{14,8},{15,9},{8,1... | collective-permute-start | bytes 1769480 | tf_op jit(solution)/shard_map/ppermute | solution.py:351
  137.6 25.0 %collective-permute-start.1 = (bf16[8,12,24,128]{3,2,1,0:T(8,128)(2,1)S(1)}, bf16[8,12,24,128]{3,2,1,0:T(8,128)(2,1)S(1)}, u32[]{:S(2)}, u32[]{:S(2)}) collective-permute-start(bf16[8,12,24,128]{3,2,1,0:T(8,128)(2,1)S(1)} %all_to_all.31.packed), channel_id=1, source_target_pairs={{4,0},{5,1},{6,2},{7,3},{0,4},{1,5},{2,6},{3,7},{12,8},{13,9},{14,... | collective-permute-start | bytes 1769480 | tf_op jit(solution)/shard_map/ppermute | solution.py:351
  141.8 25.7 %collective-permute-start = (bf16[8,12,24,128]{3,2,1,0:T(8,128)(2,1)S(1)}, bf16[8,12,24,128]{3,2,1,0:T(8,128)(2,1)S(1)}, u32[]{:S(2)}, u32[]{:S(2)}) collective-permute-start(bf16[8,12,24,128]{3,2,1,0:T(8,128)(2,1)S(1)} %all_to_all.31.packed), channel_id=1, source_target_pairs={{2,0},{3,1},{4,2},{5,3},{6,4},{7,5},{0,6},{1,7},{10,8},{11,9},{12,... | collective-permute-start | bytes 1769480 | tf_op jit(solution)/shard_map/ppermute | solution.py:351
  169.2 8.1 %collective-permute-start.3 = (bf16[4,8,12,24,128]{4,3,2,1,0:T(8,128)(2,1)}, bf16[4,8,12,24,128]{4,3,2,1,0:T(8,128)(2,1)}, u32[]{:S(2)}, u32[]{:S(2)}) collective-permute-start(bf16[4,8,12,24,128]{4,3,2,1,0:T(8,128)(2,1)} %pad_maximum_fusion.held), channel_id=1, source_target_pairs={{1,0},{0,1},{3,2},{2,3},{5,4},{4,5},{7,6},{6,7},{9,8},{8,9},{11,10... | collective-permute-start | bytes 7077896 | tf_op jit(solution)/shard_map/ppermute | solution.py:353
  173.3 12.9 %all-to-all-start.5 = ((f32[8,1,128]{2,1,0:T(1,128)}), f32[8,1,128]{2,1,0:T(1,128)S(1)}, u32[]{:S(2)}, u32[]{:S(2)}) async-start(f32[8,1,128]{2,1,0:T(1,128)} %shard_map.152), calls=%async_computation.5 | async-start | bytes 8192 | tf_op jit(solution)/shard_map/all_to_all | solution.py:415
  186.3 2.3 %copy-start = (bf16[6144,384]{1,0:T(8,128)(2,1)S(1)}, bf16[6144,384]{1,0:T(8,128)(2,1)}, u32[]{:S(2)}) copy-start(bf16[6144,384]{1,0:T(8,128)(2,1)} %all-gather.3.cloned.1.call-done) | copy-start | bytes 14155780
  188.6 1.7 copy-start.3
  190.3 1.7 copy-start.4
Sparse Core Ops, SparseCore 0:
  12.3 135.1 all-gather.2

commit v17 on v16

--- a/solution.py
+++ b/solution.py
@@ -158,6 +158,28 @@
         own_right[...] = tile[1, rows]
 
 
+def decode_kernel(span, masters, out_all, near, near_out, arrived, left_for):
+    own = near.shape[1]
+    cols = near.shape[2]
+    per = span // own
+    parts = masters.shape[0] // per
+    copies = []
+    for i in range(parts):
+        held = pl.ds(i * per, per)
+        copies.append(pltpu.make_async_copy(masters.at[held, pl.ds(own, own)], near.at[held], arrived.at[i]))
+        copies[-1].start()
+    sent = []
+    for i in range(parts):
+        at = pl.ds(i * span, span)
+        copies[i].wait()
+        codes = near[i * per : (i + 1) * per].reshape(span, cols)
+        near_out[:, at] = decoded(codes.T, REACH)
+        sent.append(pltpu.make_async_copy(near_out.at[:, at], out_all.at[:, at], left_for.at[i]))
+        sent[-1].start()
+    for copy in sent:
+        copy.wait()
+
+
 def spread_kernel(low, out):
     depth, _, lanes = low.shape
     lanes = lanes - 128
@@ -188,6 +210,7 @@
     left,
     right,
     masters,
+    out_all,
     own_left,
     own_right,
     query_master,
@@ -249,8 +272,7 @@
         sent.append(pltpu.make_async_copy(near_query.at[at], query_copy.at[at], left_for.at[i, 0]))
         sent[-1].start()
         moved = jnp.dot(second_turned, right[:, at], preferred_element_type=f32)
-        kept = decoded(codes[:, own:].reshape(span, cols).T, REACH)
-        near_out[:, at] = (kept - scales[1] * moved).astype(bf16)
+        near_out[:, at] = (out_all[:, at] - scales[1] * moved).astype(bf16)
         sent.append(pltpu.make_async_copy(near_out.at[:, at], out_copy.at[:, at], left_for.at[i, 1]))
         sent[-1].start()
     for copy in own_copies:
@@ -402,8 +424,21 @@
         cost_estimate=cost(1 << 30, 30 << 20),
     )(place, far(held), far(other))
 
-    low, masters = lax.optimization_barrier((low, masters))
     parts = width // span
+    out_all = pl.pallas_call(
+        functools.partial(decode_kernel, span),
+        out_shape=pltpu.HBM((cols, width), f32),
+        in_specs=[ANY],
+        out_specs=ANY,
+        scratch_shapes=[
+            pltpu.VMEM((fs, own, cols), bf16),
+            pltpu.VMEM((cols, width), f32),
+            pltpu.SemaphoreType.DMA((parts,)),
+            pltpu.SemaphoreType.DMA((parts,)),
+        ],
+        compiler_params=SMALL,
+        cost_estimate=cost(1 << 28, 8 << 20),
+    )(far(masters))
     squares = pl.pallas_call(
         sums_kernel,
         out_shape=jax.ShapeDtypeStruct((tp, 1, 128), f32),
@@ -422,7 +457,7 @@
             pltpu.HBM((own, cols), f32),
             pltpu.HBM((own, cols), f32),
         ),
-        in_specs=[VMEM] * 5 + [ANY] * 4,
+        in_specs=[VMEM] * 6 + [ANY] * 4,
         out_specs=(ANY,) * 4,
         scratch_shapes=[
             pltpu.VMEM((width, cols), bf16),
@@ -438,17 +473,7 @@
         ],
         compiler_params=SMALL,
         cost_estimate=cost(4 * width * ranks * cols, 20 << 20),
-    )(
-        squares,
-        low,
-        left,
-        right,
-        masters,
-        far(own_left),
-        far(own_right),
-        far(query_master),
-        far(out_master.T),
-    )
+    )(squares, low, left, right, masters, out_all, far(own_left), far(own_right), far(query_master), far(out_master.T))
     return (query_new, out_new.T, query_copy, out_copy, first_new, second_new)
 
 

time: 205 us -> 212 us (1.034)
  blocking collectives: 117 us -> 94.5 us
  waiting for transfers between devices: 23.7 us -> 37.8 us
  starting transfers between devices: 19.8 us -> 30.3 us
  Pallas kernels: 22.4 us -> 26.3 us
    all_to_all x1 -> x0, blocking collectives: 33.7 us -> none  [body(): pieces = lax.all_to_all(partial.reshape(fs, 2 * rows, cols), FS, 0, 0)]
    all_to_all x0 -> x1, waiting for transfers between devices: none -> 28.5 us  [body(): pieces = lax.all_to_all(partial.reshape(fs, 2 * rows, cols), FS, 0, 0)]
    ppermute x3, waiting for transfers between devices: 23.6 us -> 0.01 us  [body(): lax.ppermute(packed, 'tp', [((t + 2 * step) % tp, t) for t in range(tp)])]
    all_gather x1, blocking collectives: 17.8 us -> 30.2 us  [body(): proj = lax.all_gather(proj, 'tp', axis=0, tiled=True)]
    all_to_all x1, waiting for transfers between devices: 0.01 us -> 8.68 us  [body(): low = lax.all_to_all(low, 'y', 0, 0)]
    all_to_all x0 -> x1, starting transfers between devices: none -> 6.47 us  [body(): pieces = lax.all_to_all(partial.reshape(fs, 2 * rows, cols), FS, 0, 0)]
    pallas_call x0 -> x1, Pallas kernels: none -> 3.93 us  [body(): pl.pallas_call(functools.partial(decode_kernel, span), out_shape=pltpu.HB...]
    all_to_all x1, starting transfers between devices: 4.02 us -> 6.85 us  [body(): squares = lax.all_to_all(squares, 'tp', 0, 0)]
  transfers between devices with their start and end apart: 7 -> 8, of which waited for: 3 -> 3; matrix products, arithmetic and copies ran while one was open for 1% -> 1% of each run, Pallas kernels for 8% -> 9%
where the time goes in v17:
time: 212 us; the launch traced here: 211 us
  blocking collectives  94.5 us (45%)
  waiting for transfers between devices  37.8 us (18%)
  starting transfers between devices  30.3 us (14%)
  Pallas kernels  26.3 us (12%)
  between operations  14.2 us (7%)
  local copies, waits for them, and re-layouts  6.37 us (3%)
    all_gather x1, blocking collectives, body(): proj = lax.all_gather(proj, 'tp', axis=0, tiled=True)  30.2 us
    all_to_all x1, waiting for transfers between devices, body(): pieces = lax.all_to_all(partial.reshape(fs, 2 * rows, cols), FS, 0, 0)  28.5 us
    all_to_all x1, blocking collectives, body(): packed = lax.all_to_all(packed, 'z', 0, 0)  25.5 us
    all_to_all x1, blocking collectives, body(): packed = lax.all_to_all(packed, 'y', 0, 0)  23 us
    all_to_all x1, blocking collectives, body(): low = lax.all_to_all(low, 'z', 0, 0)  15.9 us
    ppermute x3, starting transfers between devices, body(): lax.ppermute(packed, 'tp', [((t + 2 * step) % tp, t) for t in range(tp)])  10.7 us
    pallas_call x1, Pallas kernels, body(): pl.pallas_call(functools.partial(prep_kernel, rank_cols), grid=(width //...  8.94 us
    all_to_all x1, waiting for transfers between devices, body(): low = lax.all_to_all(low, 'y', 0, 0)  8.68 us
  transfers between devices with their start and end apart: 8, of which 3 were waited for; matrix products, arithmetic and copies ran while one was open for 1% of the time, Pallas kernels for 9%

profile of v17, /device:TPU:1, one launch (start us, length us, event | category | flops | bytes accessed | tf_op | source)
XLA Modules:
  0.0 211.2 jit_solution(7078352074998643582)
XLA Ops:
  7.2 0.0 all-gather.3.cloned.1.call-start
  7.2 1.6 shard_map.145
  8.8 0.0 all-gather.3.cloned.1.call-update
  8.9 0.0 copy-start.2
  8.9 0.0 copy-start.3
  8.9 25.5 %all_to_all.30.packed = bf16[12,24,128]{2,1,0:T(8,128)(2,1)S(1)} all-to-all(bf16[12,24,128]{2,1,0:T(8,128)(2,1)S(1)} %shard_map.146), channel_id=1, replica_groups=mesh['z'=12,'y'=8,'tp'=8] {'z'}, dimensions={0} | all-to-all | bytes 147456 | tf_op jit(solution)/shard_map/all_to_all | solution.py:340
  34.4 0.1 shard_map.147
  34.5 23.0 %all_to_all.31.packed = bf16[8,12,24,128]{3,2,1,0:T(8,128)(2,1)S(1)} all-to-all(bf16[8,12,24,128]{3,2,1,0:T(8,128)(2,1)S(1)} %shard_map.147), channel_id=1, replica_groups=mesh['z'=12,'y'=8,'tp'=8] {'y'}, dimensions={0} | all-to-all | bytes 1179648 | tf_op jit(solution)/shard_map/all_to_all | solution.py:349
  57.4 0.0 copy-start.6
  57.4 0.0 copy-start.7
  57.5 3.3 %collective-permute-start.2 = (bf16[8,12,24,128]{3,2,1,0:T(8,128)(2,1)S(1)}, bf16[8,12,24,128]{3,2,1,0:T(8,128)(2,1)S(1)}, u32[]{:S(2)}, u32[]{:S(2)}) collective-permute-start(bf16[8,12,24,128]{3,2,1,0:T(8,128)(2,1)S(1)} %all_to_all.31.packed), channel_id=1, source_target_pairs={{6,0},{7,1},{0,2},{1,3},{2,4},{3,5},{4,6},{5,7},{14,8},{15,9},{8,1... | collective-permute-start | bytes 1769480 | tf_op jit(solution)/shard_map/ppermute | solution.py:373
  60.8 4.4 %collective-permute-start.1 = (bf16[8,12,24,128]{3,2,1,0:T(8,128)(2,1)S(1)}, bf16[8,12,24,128]{3,2,1,0:T(8,128)(2,1)S(1)}, u32[]{:S(2)}, u32[]{:S(2)}) collective-permute-start(bf16[8,12,24,128]{3,2,1,0:T(8,128)(2,1)S(1)} %all_to_all.31.packed), channel_id=1, source_target_pairs={{4,0},{5,1},{6,2},{7,3},{0,4},{1,5},{2,6},{3,7},{12,8},{13,9},{14,... | collective-permute-start | bytes 1769480 | tf_op jit(solution)/shard_map/ppermute | solution.py:373
  65.1 3.1 %collective-permute-start = (bf16[8,12,24,128]{3,2,1,0:T(8,128)(2,1)S(1)}, bf16[8,12,24,128]{3,2,1,0:T(8,128)(2,1)S(1)}, u32[]{:S(2)}, u32[]{:S(2)}) collective-permute-start(bf16[8,12,24,128]{3,2,1,0:T(8,128)(2,1)S(1)} %all_to_all.31.packed), channel_id=1, source_target_pairs={{2,0},{3,1},{4,2},{5,3},{6,4},{7,5},{0,6},{1,7},{10,8},{11,9},{12,... | collective-permute-start | bytes 1769480 | tf_op jit(solution)/shard_map/ppermute | solution.py:373
  68.2 0.0 copy-done.2
  68.2 0.0 copy-done.3
  68.2 2.0 shard_map.148
  70.2 30.2 %all_gather.9.proj = bf16[768,512]{1,0:T(8,128)(2,1)S(1)} all-gather(bf16[96,512]{1,0:T(8,128)(2,1)S(1)} %shard_map.148), channel_id=1, replica_groups=mesh['z'=12,'y'=8,'tp'=8] {'tp'}, dimensions={0}, use_global_device_ids=true | all-gather | bytes 884736 | tf_op jit(solution)/shard_map/all_gather | solution.py:359
  100.3 0.0 copy-done.6
  100.3 0.0 copy-done.7
  100.4 1.6 shard_map.149
  102.0 6.5 %all-to-all-start.2 = ((bf16[96,8,384]{2,1,0:T(8,128)(2,1)}), bf16[96,8,384]{2,1,0:T(8,128)(2,1)S(1)}, u32[]{:S(2)}, u32[]{:S(2)}) async-start(bf16[96,8,384]{2,1,0:T(8,128)(2,1)} %bitcast.13), calls=%async_computation.2 | async-start | bytes 1179648 | tf_op jit(solution)/shard_map/all_to_all | solution.py:369
  108.4 0.0 collective-permute-done.2
  108.5 0.0 collective-permute-done.1
  108.5 0.0 collective-permute-done
  108.5 0.0 copy-start.8
  108.5 0.0 copy-start.9
  108.5 1.7 pad_maximum_fusion.held
  110.2 2.3 %collective-permute-start.3 = (bf16[4,8,12,24,128]{4,3,2,1,0:T(8,128)(2,1)}, bf16[4,8,12,24,128]{4,3,2,1,0:T(8,128)(2,1)}, u32[]{:S(2)}, u32[]{:S(2)}) collective-permute-start(bf16[4,8,12,24,128]{4,3,2,1,0:T(8,128)(2,1)} %pad_maximum_fusion.held), channel_id=1, source_target_pairs={{1,0},{0,1},{3,2},{2,3},{5,4},{4,5},{7,6},{6,7},{9,8},{8,9},{11,10... | collective-permute-start | bytes 7077896 | tf_op jit(solution)/shard_map/ppermute | solution.py:375
  112.6 28.5 %all-to-all-done.2.pieces = bf16[96,8,384]{2,1,0:T(8,128)(2,1)S(1)} async-done(((bf16[96,8,384]{2,1,0:T(8,128)(2,1)}), bf16[96,8,384]{2,1,0:T(8,128)(2,1)S(1)}, u32[]{:S(2)}, u32[]{:S(2)}) %all-to-all-start.2) | async-done | bytes 589856 | tf_op jit(solution)/shard_map/all_to_all | solution.py:369
  141.0 0.0 copy-done.8
  141.1 0.0 copy-done.9
  141.1 1.4 shard_map.150
  142.4 15.9 %all_to_all.32.low = bf16[12,4,896]{2,1,0:T(4,128)(2,1)S(1)} all-to-all(bf16[12,4,896]{2,1,0:T(4,128)(2,1)} %get-tuple-element.21), channel_id=1, replica_groups=mesh['z'=12,'y'=8,'tp'=8] {'z'}, dimensions={0} | all-to-all | bytes 172032 | tf_op jit(solution)/shard_map/all_to_all | solution.py:389
  158.4 0.9 shard_map.151
  159.3 3.8 %all-to-all-start.4 = ((bf16[8,13,4,768]{3,2,1,0:T(4,128)(2,1)}), bf16[8,13,4,768]{3,2,1,0:T(4,128)(2,1)S(1)}, u32[]{:S(2)}, u32[]{:S(2)}) async-start(bf16[8,13,4,768]{3,2,1,0:T(4,128)(2,1)} %shard_map.151), calls=%async_computation.4 | async-start | bytes 1277952 | tf_op jit(solution)/shard_map/all_to_all | solution.py:398
  163.1 0.1 pad_add_fusion.place
  163.2 0.0 collective-permute-done.3.other
  163.2 8.9 %shard_map.153 = (bf16[3072,384]{1,0:T(8,128)(2,1)}, bf16[384,3072]{1,0:T(8,128)(2,1)}, bf16[32,384]{1,0:T(8,128)(2,1)}, bf16[32,384]{1,0:T(8,128)(2,1)}) custom-call(s32[2]{0:T(128)S(1)} %pad_add_fusion.place, bf16[4,8,12,24,128]{4,3,2,1,0:T(8,128)(2,1)} %pad_maximum_fusion.held, bf16[4,8,12,24,128]{4,3,2,1,0:T(8,128)(2,1)} %collective-permute-done.3.other), custom_call_target="tpu_custom_call" | custom-call | flops 1073741824 | bytes 31457280 | tf_op jit(solution)/shard_map/pallas_call | solution.py:402
  172.1 8.7 %all-to-all-done.4.low = bf16[8,13,4,768]{3,2,1,0:T(4,128)(2,1)S(1)} async-done(((bf16[8,13,4,768]{3,2,1,0:T(4,128)(2,1)}), bf16[8,13,4,768]{3,2,1,0:T(4,128)(2,1)S(1)}, u32[]{:S(2)}, u32[]{:S(2)}) %all-to-all-start.4) | async-done | bytes 639008 | tf_op jit(solution)/shard_map/all_to_all | solution.py:398
  180.8 0.6 shard_map.152
  181.4 6.8 %all-to-all-start.5 = ((f32[8,1,128]{2,1,0:T(1,128)}), f32[8,1,128]{2,1,0:T(1,128)S(1)}, u32[]{:S(2)}, u32[]{:S(2)}) async-start(f32[8,1,128]{2,1,0:T(1,128)} %shard_map.152), calls=%async_computation.5 | async-start | bytes 8192 | tf_op jit(solution)/shard_map/all_to_all | solution.py:450
  188.3 0.0 all-gather.3.cloned.1.call-done
  188.3 0.0 copy-start.4
  188.3 3.9 %shard_map.154.out_all = f32[384,3072]{1,0:T(8,128)} custom-call(bf16[96,64,384]{2,1,0:T(8,128)(2,1)} %bitcast.10), custom_call_target="tpu_custom_call" | custom-call | flops 268435456 | bytes 8388608 | tf_op jit(solution)/shard_map/pallas_call | solution.py:428
  192.2 0.6 all-to-all-done.5.squares
  192.8 0.0 copy-done.4
  192.8 0.0 copy-start
  192.8 2.3 %copy-done = bf16[6144,384]{1,0:T(8,128)(2,1)S(1)} copy-done((bf16[6144,384]{1,0:T(8,128)(2,1)S(1)}, bf16[6144,384]{1,0:T(8,128)(2,1)}, u32[]{:S(2)}) %copy-start) | copy-done | bytes 4718616
  195.1 0.0 copy-start.1
  195.1 2.3 %copy-done.1 = f32[384,3072]{1,0:T(8,128)S(1)} copy-done((f32[384,3072]{1,0:T(8,128)S(1)}, f32[384,3072]{1,0:T(8,128)}, u32[]{:S(2)}) %copy-start.1) | copy-done | bytes 4718616
  197.5 0.0 copy-start.5
  197.5 1.7 copy-done.5
  199.1 5.2 %shard_map.155 = (bf16[3072,384]{1,0:T(8,128)(2,1)}, bf16[384,3072]{1,0:T(8,128)(2,1)}, f32[32,384]{1,0:T(8,128)}, f32[32,384]{1,0:T(8,128)}) custom-call(f32[8,1,128]{2,1,0:T(1,128)S(1)} %all-to-all-done.5.squares, bf16[8,13,4,768]{3,2,1,0:T(4,128)(2,1)S(1)} %all-to-all-done.4.low, bf16[3072,384]{1,0:T(8,128)(2,1)S(1)} %copy-done.4, ...), custom_call_target="tpu_custom_call" | custom-call | flops 1811939328 | bytes 20971520 | tf_op jit(solution)/shard_map/pallas_call | solution.py:452
  (1 shorter events, 0.0 us)
Async XLA Ops:
  7.2 181.1 %all-gather.3.cloned.1.call-start = ((), (), s32[]{:S(2)}) async-start(), calls=%async_computation.6 | async-start | bytes 4767744 | tf_op jit(solution)/shard_map/all_gather | solution.py:339
  8.9 59.4 %copy-start.2 = (bf16[512,3072]{1,0:T(8,128)(2,1)S(1)}, bf16[512,3072]{1,0:T(8,128)(2,1)}, u32[]{:S(2)}) copy-start(bf16[512,3072]{1,0:T(8,128)(2,1)} %saved_inputs.1) | copy-start | bytes 9437188
  8.9 59.4 %copy-start.3 = (bf16[512,3072]{1,0:T(8,128)(2,1)S(1)}, bf16[512,3072]{1,0:T(8,128)(2,1)}, u32[]{:S(2)}) copy-start(bf16[512,3072]{1,0:T(8,128)(2,1)} %out_cotangent.1) | copy-start | bytes 9437188
  57.4 42.9 %copy-start.6 = (bf16[512,384]{1,0:T(8,128)(2,1)S(1)}, bf16[512,384]{1,0:T(8,128)(2,1)}, u32[]{:S(2)}) copy-start(bf16[512,384]{1,0:T(8,128)(2,1)} %query_cotangent.1) | copy-start | bytes 1179652
  57.4 42.9 %copy-start.7 = (bf16[512,384]{1,0:T(8,128)(2,1)S(1)}, bf16[512,384]{1,0:T(8,128)(2,1)}, u32[]{:S(2)}) copy-start(bf16[512,384]{1,0:T(8,128)(2,1)} %attn_outputs.1) | copy-start | bytes 1179652
  57.5 51.0 %collective-permute-start.2 = (bf16[8,12,24,128]{3,2,1,0:T(8,128)(2,1)S(1)}, bf16[8,12,24,128]{3,2,1,0:T(8,128)(2,1)S(1)}, u32[]{:S(2)}, u32[]{:S(2)}) collective-permute-start(bf16[8,12,24,128]{3,2,1,0:T(8,128)(2,1)S(1)} %all_to_all.31.packed), channel_id=1, source_target_pairs={{6,0},{7,1},{0,2},{1,3},{2,4},{3,5},{4,6},{5,7},{14,8},{15,9},{8,1... | collective-permute-start | bytes 1769480 | tf_op jit(solution)/shard_map/ppermute | solution.py:373
  60.8 47.7 %collective-permute-start.1 = (bf16[8,12,24,128]{3,2,1,0:T(8,128)(2,1)S(1)}, bf16[8,12,24,128]{3,2,1,0:T(8,128)(2,1)S(1)}, u32[]{:S(2)}, u32[]{:S(2)}) collective-permute-start(bf16[8,12,24,128]{3,2,1,0:T(8,128)(2,1)S(1)} %all_to_all.31.packed), channel_id=1, source_target_pairs={{4,0},{5,1},{6,2},{7,3},{0,4},{1,5},{2,6},{3,7},{12,8},{13,9},{14,... | collective-permute-start | bytes 1769480 | tf_op jit(solution)/shard_map/ppermute | solution.py:373
  65.1 43.3 %collective-permute-start = (bf16[8,12,24,128]{3,2,1,0:T(8,128)(2,1)S(1)}, bf16[8,12,24,128]{3,2,1,0:T(8,128)(2,1)S(1)}, u32[]{:S(2)}, u32[]{:S(2)}) collective-permute-start(bf16[8,12,24,128]{3,2,1,0:T(8,128)(2,1)S(1)} %all_to_all.31.packed), channel_id=1, source_target_pairs={{2,0},{3,1},{4,2},{5,3},{6,4},{7,5},{0,6},{1,7},{10,8},{11,9},{12,... | collective-permute-start | bytes 1769480 | tf_op jit(solution)/shard_map/ppermute | solution.py:373
  102.0 39.1 %all-to-all-start.2 = ((bf16[96,8,384]{2,1,0:T(8,128)(2,1)}), bf16[96,8,384]{2,1,0:T(8,128)(2,1)S(1)}, u32[]{:S(2)}, u32[]{:S(2)}) async-start(bf16[96,8,384]{2,1,0:T(8,128)(2,1)} %bitcast.13), calls=%async_computation.2 | async-start | bytes 1179648 | tf_op jit(solution)/shard_map/all_to_all | solution.py:369
  108.5 32.6 %copy-start.8 = (f32[2,4,384]{2,1,0:T(4,128)S(1)}, f32[2,4,384]{2,1,0:T(4,128)}, u32[]{:S(2)}) copy-start(f32[2,4,384]{2,1,0:T(4,128)} %first.1) | copy-start | bytes 36868
  108.5 32.6 %copy-start.9 = (f32[2,4,384]{2,1,0:T(4,128)S(1)}, f32[2,4,384]{2,1,0:T(4,128)}, u32[]{:S(2)}) copy-start(f32[2,4,384]{2,1,0:T(4,128)} %second.1) | copy-start | bytes 36868
  110.2 53.0 %collective-permute-start.3 = (bf16[4,8,12,24,128]{4,3,2,1,0:T(8,128)(2,1)}, bf16[4,8,12,24,128]{4,3,2,1,0:T(8,128)(2,1)}, u32[]{:S(2)}, u32[]{:S(2)}) collective-permute-start(bf16[4,8,12,24,128]{4,3,2,1,0:T(8,128)(2,1)} %pad_maximum_fusion.held), channel_id=1, source_target_pairs={{1,0},{0,1},{3,2},{2,3},{5,4},{4,5},{7,6},{6,7},{9,8},{8,9},{11,10... | collective-permute-start | bytes 7077896 | tf_op jit(solution)/shard_map/ppermute | solution.py:375
  159.3 21.5 %all-to-all-start.4 = ((bf16[8,13,4,768]{3,2,1,0:T(4,128)(2,1)}), bf16[8,13,4,768]{3,2,1,0:T(4,128)(2,1)S(1)}, u32[]{:S(2)}, u32[]{:S(2)}) async-start(bf16[8,13,4,768]{3,2,1,0:T(4,128)(2,1)} %shard_map.151), calls=%async_computation.4 | async-start | bytes 1277952 | tf_op jit(solution)/shard_map/all_to_all | solution.py:398
  181.4 11.4 %all-to-all-start.5 = ((f32[8,1,128]{2,1,0:T(1,128)}), f32[8,1,128]{2,1,0:T(1,128)S(1)}, u32[]{:S(2)}, u32[]{:S(2)}) async-start(f32[8,1,128]{2,1,0:T(1,128)} %shard_map.152), calls=%async_computation.5 | async-start | bytes 8192 | tf_op jit(solution)/shard_map/all_to_all | solution.py:450
  188.3 4.5 %copy-start.4 = (bf16[3072,384]{1,0:T(8,128)(2,1)S(1)}, bf16[3072,384]{1,0:T(8,128)(2,1)}, u32[]{:S(2)}) copy-start(bf16[3072,384]{1,0:T(8,128)(2,1)} %get-tuple-element.22.left) | copy-start | bytes 7077892
  192.8 2.3 %copy-start = (bf16[6144,384]{1,0:T(8,128)(2,1)S(1)}, bf16[6144,384]{1,0:T(8,128)(2,1)}, u32[]{:S(2)}) copy-start(bf16[6144,384]{1,0:T(8,128)(2,1)} %all-gather.3.cloned.1.call-done) | copy-start | bytes 14155780
  195.1 2.3 %copy-start.1 = (f32[384,3072]{1,0:T(8,128)S(1)}, f32[384,3072]{1,0:T(8,128)}, u32[]{:S(2)}) copy-start(f32[384,3072]{1,0:T(8,128)} %shard_map.154.out_all) | copy-start | bytes 14155780
  197.5 1.7 copy-start.5
Sparse Core Ops, SparseCore 0:
  12.3 144.3 all-gather.2

commit v18 on v16

--- a/solution.py
+++ b/solution.py
@@ -95,10 +95,11 @@
     for k, other in enumerate((query_cotangent, attn_outputs)):
         starts = range(k * rank_cols, proj.shape[0], 2 * rank_cols)
         ranks = jnp.concatenate([proj[at : at + rank_cols] for at in starts], axis=0)
-        parts.append(jnp.dot(ranks, other[...], preferred_element_type=f32).reshape(-1, 8, cols))
+        share = jnp.dot(ranks, other[...], preferred_element_type=f32)
+        parts.append(coded(share, GRAD_REACH).astype(f32).reshape(-1, 8, cols))
     first, second = parts
     both = jnp.concatenate([first[:, :4], second[:, :4], first[:, 4:], second[:, 4:]], axis=1)
-    out[...] = coded(both, GRAD_REACH)
+    out[...] = both.astype(bf16)
 
 
 def in_three(total):
@@ -111,7 +112,9 @@
 
 def moment_kernel(pieces, first, second, first_new, second_new, low):
     rows = first.shape[1]
-    grads = jnp.sum(decoded(pieces[...], GRAD_REACH), axis=0)
+    grads = 0.0
+    for i in range(pieces.shape[0]):
+        grads = grads + decoded(pieces[i], GRAD_REACH)
     new_first = 0.9 * jnp.concatenate([first[0], first[1]], axis=0) + 0.1 * grads
     new_second = 0.99 * jnp.concatenate([second[0], second[1]], axis=0) + 0.01 * grads * grads
     direction = new_first / (jnp.sqrt(new_second) + 1e-08)

time: 205 us -> 204 us (level)
  transfers between devices with their start and end apart: 7 -> 7, of which waited for: 3 -> 3; matrix products, arithmetic and copies ran while one was open for 1% -> 1% of each run, Pallas kernels for 8% -> 7%
where the time goes in v18:
time: 204 us; the launch traced here: 203 us
  blocking collectives  116 us (57%)
  waiting for transfers between devices  23.4 us (11%)
  Pallas kernels  22.1 us (11%)
  starting transfers between devices  20 us (10%)
  between operations  14.2 us (7%)
  local copies, waits for them, and re-layouts  5.69 us (3%)
    all_to_all x1, blocking collectives, body(): pieces = lax.all_to_all(partial.reshape(fs, 2 * rows, cols), FS, 0, 0)  33.7 us
    all_to_all x1, blocking collectives, body(): packed = lax.all_to_all(packed, 'z', 0, 0)  25.5 us
    ppermute x3, waiting for transfers between devices, body(): lax.ppermute(packed, 'tp', [((t + 2 * step) % tp, t) for t in range(tp)])  23.4 us
    all_to_all x1, blocking collectives, body(): packed = lax.all_to_all(packed, 'y', 0, 0)  23 us
    all_gather x1, blocking collectives, body(): proj = lax.all_gather(proj, 'tp', axis=0, tiled=True)  17.8 us
    all_to_all x1, blocking collectives, body(): low = lax.all_to_all(low, 'z', 0, 0)  16.2 us
    ppermute x3, starting transfers between devices, body(): lax.ppermute(packed, 'tp', [((t + 2 * step) % tp, t) for t in range(tp)])  8.99 us
    pallas_call x1, Pallas kernels, body(): pl.pallas_call(functools.partial(prep_kernel, rank_cols), grid=(width //...  8.91 us
  transfers between devices with their start and end apart: 7, of which 3 were waited for; matrix products, arithmetic and copies ran while one was open for 1% of the time, Pallas kernels for 7%

profile of v18, /device:TPU:1, one launch (start us, length us, event | category | flops | bytes accessed | tf_op | source)
XLA Modules:
  0.0 203.4 jit_solution(14717352885161855350)
XLA Ops:
  7.2 0.0 all-gather.3.cloned.1.call-start
  7.2 1.6 shard_map.145
  8.8 0.0 all-gather.3.cloned.1.call-update
  8.9 0.0 copy-start.1
  8.9 0.0 copy-start.2
  8.9 25.5 %all_to_all.30.packed = bf16[12,24,128]{2,1,0:T(8,128)(2,1)S(1)} all-to-all(bf16[12,24,128]{2,1,0:T(8,128)(2,1)S(1)} %shard_map.146), channel_id=1, replica_groups=mesh['z'=12,'y'=8,'tp'=8] {'z'}, dimensions={0} | all-to-all | bytes 147456 | tf_op jit(solution)/shard_map/all_to_all | solution.py:321
  34.4 0.1 shard_map.147
  34.5 23.0 %all_to_all.31.packed = bf16[8,12,24,128]{3,2,1,0:T(8,128)(2,1)S(1)} all-to-all(bf16[8,12,24,128]{3,2,1,0:T(8,128)(2,1)S(1)} %shard_map.147), channel_id=1, replica_groups=mesh['z'=12,'y'=8,'tp'=8] {'y'}, dimensions={0} | all-to-all | bytes 1179648 | tf_op jit(solution)/shard_map/all_to_all | solution.py:330
  57.4 0.0 copy-done.1
  57.4 0.0 copy-done.2
  57.5 0.0 copy-start.5
  57.5 0.0 copy-start.6
  57.5 2.0 shard_map.148
  59.4 0.0 copy-start.7
  59.4 0.0 copy-start.8
  59.4 17.8 %all_gather.9.proj = bf16[768,512]{1,0:T(8,128)(2,1)S(1)} all-gather(bf16[96,512]{1,0:T(8,128)(2,1)S(1)} %shard_map.148), channel_id=1, replica_groups=mesh['z'=12,'y'=8,'tp'=8] {'tp'}, dimensions={0}, use_global_device_ids=true | all-gather | bytes 884736 | tf_op jit(solution)/shard_map/all_gather | solution.py:340
  77.3 0.0 copy-done.5
  77.3 0.0 copy-done.6
  77.3 1.5 shard_map.149
  78.8 33.7 %all_to_all.32.pieces = bf16[96,8,384]{2,1,0:T(8,128)(2,1)S(1)} all-to-all(bf16[96,8,384]{2,1,0:T(8,128)(2,1)} %bitcast.12), channel_id=1, replica_groups=mesh['z'=12,'y'=8,'tp'=8] {'z','y'}, dimensions={0} | all-to-all | bytes 1179648 | tf_op jit(solution)/shard_map/all_to_all | solution.py:350
  112.4 0.0 copy-done.7
  112.4 0.0 copy-done.8
  112.4 1.1 shard_map.150
  113.6 16.2 %all_to_all.33.low = bf16[12,4,896]{2,1,0:T(4,128)(2,1)S(1)} all-to-all(bf16[12,4,896]{2,1,0:T(4,128)(2,1)} %get-tuple-element.23), channel_id=1, replica_groups=mesh['z'=12,'y'=8,'tp'=8] {'z'}, dimensions={0} | all-to-all | bytes 172032 | tf_op jit(solution)/shard_map/all_to_all | solution.py:370
  129.8 0.9 shard_map.151
  130.7 3.5 %all-to-all-start.4 = ((bf16[8,13,4,768]{3,2,1,0:T(4,128)(2,1)}), bf16[8,13,4,768]{3,2,1,0:T(4,128)(2,1)S(1)}, u32[]{:S(2)}, u32[]{:S(2)}) async-start(bf16[8,13,4,768]{3,2,1,0:T(4,128)(2,1)} %shard_map.151), calls=%async_computation.4 | async-start | bytes 1277952 | tf_op jit(solution)/shard_map/all_to_all | solution.py:379
  134.3 2.8 %collective-permute-start.2 = (bf16[8,12,24,128]{3,2,1,0:T(8,128)(2,1)S(1)}, bf16[8,12,24,128]{3,2,1,0:T(8,128)(2,1)S(1)}, u32[]{:S(2)}, u32[]{:S(2)}) collective-permute-start(bf16[8,12,24,128]{3,2,1,0:T(8,128)(2,1)S(1)} %all_to_all.31.packed), channel_id=1, source_target_pairs={{6,0},{7,1},{0,2},{1,3},{2,4},{3,5},{4,6},{5,7},{14,8},{15,9},{8,1... | collective-permute-start | bytes 1769480 | tf_op jit(solution)/shard_map/ppermute | solution.py:354
  137.1 4.3 %collective-permute-start.1 = (bf16[8,12,24,128]{3,2,1,0:T(8,128)(2,1)S(1)}, bf16[8,12,24,128]{3,2,1,0:T(8,128)(2,1)S(1)}, u32[]{:S(2)}, u32[]{:S(2)}) collective-permute-start(bf16[8,12,24,128]{3,2,1,0:T(8,128)(2,1)S(1)} %all_to_all.31.packed), channel_id=1, source_target_pairs={{4,0},{5,1},{6,2},{7,3},{0,4},{1,5},{2,6},{3,7},{12,8},{13,9},{14,... | collective-permute-start | bytes 1769480 | tf_op jit(solution)/shard_map/ppermute | solution.py:354
  141.4 1.9 collective-permute-start
  143.3 0.1 pad_add_fusion.place
  143.4 5.6 %collective-permute-done.2 = bf16[8,12,24,128]{3,2,1,0:T(8,128)(2,1)S(1)} collective-permute-done((bf16[8,12,24,128]{3,2,1,0:T(8,128)(2,1)S(1)}, bf16[8,12,24,128]{3,2,1,0:T(8,128)(2,1)S(1)}, u32[]{:S(2)}, u32[]{:S(2)}) %collective-permute-start.2) | collective-permute-done | bytes 589856 | tf_op jit(solution)/shard_map/ppermute | solution.py:354
  149.0 13.2 %collective-permute-done.1 = bf16[8,12,24,128]{3,2,1,0:T(8,128)(2,1)S(1)} collective-permute-done((bf16[8,12,24,128]{3,2,1,0:T(8,128)(2,1)S(1)}, bf16[8,12,24,128]{3,2,1,0:T(8,128)(2,1)S(1)}, u32[]{:S(2)}, u32[]{:S(2)}) %collective-permute-start.1) | collective-permute-done | bytes 589856 | tf_op jit(solution)/shard_map/ppermute | solution.py:354
  162.2 4.6 %collective-permute-done = bf16[8,12,24,128]{3,2,1,0:T(8,128)(2,1)S(1)} collective-permute-done((bf16[8,12,24,128]{3,2,1,0:T(8,128)(2,1)S(1)}, bf16[8,12,24,128]{3,2,1,0:T(8,128)(2,1)S(1)}, u32[]{:S(2)}, u32[]{:S(2)}) %collective-permute-start) | collective-permute-done | bytes 589856 | tf_op jit(solution)/shard_map/ppermute | solution.py:354
  166.8 1.7 pad_maximum_fusion.held
  168.5 3.5 %collective-permute-start.3 = (bf16[4,8,12,24,128]{4,3,2,1,0:T(8,128)(2,1)}, bf16[4,8,12,24,128]{4,3,2,1,0:T(8,128)(2,1)}, u32[]{:S(2)}, u32[]{:S(2)}) collective-permute-start(bf16[4,8,12,24,128]{4,3,2,1,0:T(8,128)(2,1)} %pad_maximum_fusion.held), channel_id=1, source_target_pairs={{1,0},{0,1},{3,2},{2,3},{5,4},{4,5},{7,6},{6,7},{9,8},{8,9},{11,10... | collective-permute-start | bytes 7077896 | tf_op jit(solution)/shard_map/ppermute | solution.py:356
  171.9 0.0 all-to-all-done.4.low
  171.9 0.0 all-gather.3.cloned.1.call-done
  172.0 0.6 shard_map.152
  172.6 4.0 %all-to-all-start.5 = ((f32[8,1,128]{2,1,0:T(1,128)}), f32[8,1,128]{2,1,0:T(1,128)S(1)}, u32[]{:S(2)}, u32[]{:S(2)}) async-start(f32[8,1,128]{2,1,0:T(1,128)} %shard_map.152), calls=%async_computation.5 | async-start | bytes 8192 | tf_op jit(solution)/shard_map/all_to_all | solution.py:418
  176.6 0.0 collective-permute-done.3.other
  176.6 8.9 %shard_map.153 = (bf16[3072,384]{1,0:T(8,128)(2,1)}, bf16[384,3072]{1,0:T(8,128)(2,1)}, bf16[32,384]{1,0:T(8,128)(2,1)}, bf16[32,384]{1,0:T(8,128)(2,1)}) custom-call(s32[2]{0:T(128)S(1)} %pad_add_fusion.place, bf16[4,8,12,24,128]{4,3,2,1,0:T(8,128)(2,1)} %pad_maximum_fusion.held, bf16[4,8,12,24,128]{4,3,2,1,0:T(8,128)(2,1)} %collective-permute-done.3.other), custom_call_target="tpu_custom_call" | custom-call | flops 1073741824 | bytes 31457280 | tf_op jit(solution)/shard_map/pallas_call | solution.py:383
  185.5 0.0 all-to-all-done.5.squares
  185.5 0.0 copy-start
  185.5 2.3 %copy-done = bf16[6144,384]{1,0:T(8,128)(2,1)S(1)} copy-done((bf16[6144,384]{1,0:T(8,128)(2,1)S(1)}, bf16[6144,384]{1,0:T(8,128)(2,1)}, u32[]{:S(2)}) %copy-start) | copy-done | bytes 4718616
  187.8 0.0 copy-start.3
  187.8 1.7 copy-done.3
  189.5 0.0 copy-start.4
  189.5 1.7 copy-done.4
  191.2 5.3 %shard_map.154 = (bf16[3072,384]{1,0:T(8,128)(2,1)}, bf16[384,3072]{1,0:T(8,128)(2,1)}, f32[32,384]{1,0:T(8,128)}, f32[32,384]{1,0:T(8,128)}) custom-call(f32[8,1,128]{2,1,0:T(1,128)S(1)} %all-to-all-done.5.squares, bf16[8,13,4,768]{3,2,1,0:T(4,128)(2,1)S(1)} %all-to-all-done.4.low, bf16[3072,384]{1,0:T(8,128)(2,1)S(1)} %copy-done.3, ...), custom_call_target="tpu_custom_call" | custom-call | flops 1811939328 | bytes 20971520 | tf_op jit(solution)/shard_map/pallas_call | solution.py:420
  (1 shorter events, 0.0 us)
Async XLA Ops:
  7.2 164.8 %all-gather.3.cloned.1.call-start = ((), (), s32[]{:S(2)}) async-start(), calls=%async_computation.6 | async-start | bytes 4767744 | tf_op jit(solution)/shard_map/all_gather | solution.py:320
  8.9 48.6 %copy-start.1 = (bf16[512,3072]{1,0:T(8,128)(2,1)S(1)}, bf16[512,3072]{1,0:T(8,128)(2,1)}, u32[]{:S(2)}) copy-start(bf16[512,3072]{1,0:T(8,128)(2,1)} %saved_inputs.1) | copy-start | bytes 9437188
  8.9 48.6 %copy-start.2 = (bf16[512,3072]{1,0:T(8,128)(2,1)S(1)}, bf16[512,3072]{1,0:T(8,128)(2,1)}, u32[]{:S(2)}) copy-start(bf16[512,3072]{1,0:T(8,128)(2,1)} %out_cotangent.1) | copy-start | bytes 9437188
  57.5 19.8 %copy-start.5 = (bf16[512,384]{1,0:T(8,128)(2,1)S(1)}, bf16[512,384]{1,0:T(8,128)(2,1)}, u32[]{:S(2)}) copy-start(bf16[512,384]{1,0:T(8,128)(2,1)} %query_cotangent.1) | copy-start | bytes 1179652
  57.5 19.8 %copy-start.6 = (bf16[512,384]{1,0:T(8,128)(2,1)S(1)}, bf16[512,384]{1,0:T(8,128)(2,1)}, u32[]{:S(2)}) copy-start(bf16[512,384]{1,0:T(8,128)(2,1)} %attn_outputs.1) | copy-start | bytes 1179652
  59.4 53.0 %copy-start.7 = (f32[2,4,384]{2,1,0:T(4,128)S(1)}, f32[2,4,384]{2,1,0:T(4,128)}, u32[]{:S(2)}) copy-start(f32[2,4,384]{2,1,0:T(4,128)} %first.1) | copy-start | bytes 36868
  59.4 53.0 %copy-start.8 = (f32[2,4,384]{2,1,0:T(4,128)S(1)}, f32[2,4,384]{2,1,0:T(4,128)}, u32[]{:S(2)}) copy-start(f32[2,4,384]{2,1,0:T(4,128)} %second.1) | copy-start | bytes 36868
  130.7 41.2 %all-to-all-start.4 = ((bf16[8,13,4,768]{3,2,1,0:T(4,128)(2,1)}), bf16[8,13,4,768]{3,2,1,0:T(4,128)(2,1)S(1)}, u32[]{:S(2)}, u32[]{:S(2)}) async-start(bf16[8,13,4,768]{3,2,1,0:T(4,128)(2,1)} %shard_map.151), calls=%async_computation.4 | async-start | bytes 1277952 | tf_op jit(solution)/shard_map/all_to_all | solution.py:379
  134.3 14.7 %collective-permute-start.2 = (bf16[8,12,24,128]{3,2,1,0:T(8,128)(2,1)S(1)}, bf16[8,12,24,128]{3,2,1,0:T(8,128)(2,1)S(1)}, u32[]{:S(2)}, u32[]{:S(2)}) collective-permute-start(bf16[8,12,24,128]{3,2,1,0:T(8,128)(2,1)S(1)} %all_to_all.31.packed), channel_id=1, source_target_pairs={{6,0},{7,1},{0,2},{1,3},{2,4},{3,5},{4,6},{5,7},{14,8},{15,9},{8,1... | collective-permute-start | bytes 1769480 | tf_op jit(solution)/shard_map/ppermute | solution.py:354
  137.1 25.1 %collective-permute-start.1 = (bf16[8,12,24,128]{3,2,1,0:T(8,128)(2,1)S(1)}, bf16[8,12,24,128]{3,2,1,0:T(8,128)(2,1)S(1)}, u32[]{:S(2)}, u32[]{:S(2)}) collective-permute-start(bf16[8,12,24,128]{3,2,1,0:T(8,128)(2,1)S(1)} %all_to_all.31.packed), channel_id=1, source_target_pairs={{4,0},{5,1},{6,2},{7,3},{0,4},{1,5},{2,6},{3,7},{12,8},{13,9},{14,... | collective-permute-start | bytes 1769480 | tf_op jit(solution)/shard_map/ppermute | solution.py:354
  141.4 25.4 %collective-permute-start = (bf16[8,12,24,128]{3,2,1,0:T(8,128)(2,1)S(1)}, bf16[8,12,24,128]{3,2,1,0:T(8,128)(2,1)S(1)}, u32[]{:S(2)}, u32[]{:S(2)}) collective-permute-start(bf16[8,12,24,128]{3,2,1,0:T(8,128)(2,1)S(1)} %all_to_all.31.packed), channel_id=1, source_target_pairs={{2,0},{3,1},{4,2},{5,3},{6,4},{7,5},{0,6},{1,7},{10,8},{11,9},{12,... | collective-permute-start | bytes 1769480 | tf_op jit(solution)/shard_map/ppermute | solution.py:354
  168.5 8.1 %collective-permute-start.3 = (bf16[4,8,12,24,128]{4,3,2,1,0:T(8,128)(2,1)}, bf16[4,8,12,24,128]{4,3,2,1,0:T(8,128)(2,1)}, u32[]{:S(2)}, u32[]{:S(2)}) collective-permute-start(bf16[4,8,12,24,128]{4,3,2,1,0:T(8,128)(2,1)} %pad_maximum_fusion.held), channel_id=1, source_target_pairs={{1,0},{0,1},{3,2},{2,3},{5,4},{4,5},{7,6},{6,7},{9,8},{8,9},{11,10... | collective-permute-start | bytes 7077896 | tf_op jit(solution)/shard_map/ppermute | solution.py:356
  172.6 12.9 %all-to-all-start.5 = ((f32[8,1,128]{2,1,0:T(1,128)}), f32[8,1,128]{2,1,0:T(1,128)S(1)}, u32[]{:S(2)}, u32[]{:S(2)}) async-start(f32[8,1,128]{2,1,0:T(1,128)} %shard_map.152), calls=%async_computation.5 | async-start | bytes 8192 | tf_op jit(solution)/shard_map/all_to_all | solution.py:418
  185.5 2.3 %copy-start = (bf16[6144,384]{1,0:T(8,128)(2,1)S(1)}, bf16[6144,384]{1,0:T(8,128)(2,1)}, u32[]{:S(2)}) copy-start(bf16[6144,384]{1,0:T(8,128)(2,1)} %all-gather.3.cloned.1.call-done) | copy-start | bytes 14155780
  187.8 1.7 copy-start.3
  189.5 1.7 copy-start.4
Sparse Core Ops, SparseCore 0:
  12.3 134.8 all-gather.2

commit v19 on v18

--- a/solution.py
+++ b/solution.py
@@ -15,6 +15,7 @@
 VMEM = pl.BlockSpec(memory_space=pltpu.VMEM)
 ANY = pl.BlockSpec(memory_space=pl.ANY)
 SMEM = pl.BlockSpec(memory_space=pltpu.SMEM)
+ORDER = tuple(7 * a % 12 * 8 + 3 * b % 8 for a in range(12) for b in range(8))
 REACH = 2.0**34
 GRAD_REACH = 2.0**10
 SMALL = pltpu.CompilerParams(vmem_limit_bytes=16 << 20)
@@ -99,7 +100,9 @@
         parts.append(coded(share, GRAD_REACH).astype(f32).reshape(-1, 8, cols))
     first, second = parts
     both = jnp.concatenate([first[:, :4], second[:, :4], first[:, 4:], second[:, 4:]], axis=1)
-    out[...] = both.astype(bf16)
+    both = both.astype(bf16)
+    for j, f in enumerate(ORDER):
+        out[j] = both[f // 2, f % 2 * 8 : f % 2 * 8 + 8]
 
 
 def in_three(total):
@@ -341,13 +344,13 @@
 
     partial = pl.pallas_call(
         functools.partial(grad_kernel, rank_cols),
-        out_shape=pltpu.HBM((fs // 2, 4 * rows, cols), bf16),
+        out_shape=pltpu.HBM((fs, 2 * rows, cols), bf16),
         in_specs=[VMEM] * 3,
         out_specs=VMEM,
         compiler_params=SMALL,
         cost_estimate=cost(4 * ranks * tokens * cols, 2 << 20),
     )(proj, query_cotangent, attn_outputs)
-    pieces = lax.all_to_all(partial.reshape(fs, 2 * rows, cols), FS, 0, 0)
+    pieces = lax.all_to_all(partial, FS, 0, 0, axis_index_groups=[list(ORDER)])
 
     held = [packed]
     for step in range(1, tp // 2):

time: 204 us -> 204 us (level)
    all_to_all x1, blocking collectives: 33.7 us -> 31 us  [body(): pieces = lax.all_to_all(partial, FS, 0, 0, axis_index_groups=[list(ORDER)])]
    all_to_all x1, starting transfers between devices: 3.54 us -> 5.7 us  [body(): low = lax.all_to_all(low, 'y', 0, 0)]
where the time goes in v19:
time: 204 us; the launch traced here: 203 us
  blocking collectives  114 us (56%)
  waiting for transfers between devices  23.7 us (12%)
  Pallas kernels  22.1 us (11%)
  starting transfers between devices  21.9 us (11%)
  between operations  14.2 us (7%)
  local copies, waits for them, and re-layouts  5.69 us (3%)
    all_to_all x1, blocking collectives, body(): pieces = lax.all_to_all(partial, FS, 0, 0, axis_index_groups=[list(ORDER)])  31 us
    all_to_all x1, blocking collectives, body(): packed = lax.all_to_all(packed, 'z', 0, 0)  25.5 us
    ppermute x3, waiting for transfers between devices, body(): lax.ppermute(packed, 'tp', [((t + 2 * step) % tp, t) for t in range(tp)])  23.7 us
    all_to_all x1, blocking collectives, body(): packed = lax.all_to_all(packed, 'y', 0, 0)  23 us
    all_gather x1, blocking collectives, body(): proj = lax.all_gather(proj, 'tp', axis=0, tiled=True)  17.8 us
    all_to_all x1, blocking collectives, body(): low = lax.all_to_all(low, 'z', 0, 0)  16.6 us
    pallas_call x1, Pallas kernels, body(): pl.pallas_call(functools.partial(prep_kernel, rank_cols), grid=(width //...  8.91 us
    ppermute x3, starting transfers between devices, body(): lax.ppermute(packed, 'tp', [((t + 2 * step) % tp, t) for t in range(tp)])  8.67 us
  transfers between devices with their start and end apart: 7, of which 3 were waited for; matrix products, arithmetic and copies ran while one was open for 1% of the time, Pallas kernels for 7%

profile of v19, /device:TPU:1, one launch (start us, length us, event | category | flops | bytes accessed | tf_op | source)
XLA Modules:
  0.0 203.2 jit_solution(6588540155681078694)
XLA Ops:
  7.2 0.0 all-gather.3.cloned.1.call-start
  7.2 1.6 shard_map.145
  8.8 0.0 all-gather.3.cloned.1.call-update
  8.9 0.0 copy-start.1
  8.9 0.0 copy-start.2
  8.9 25.5 %all_to_all.30.packed = bf16[12,24,128]{2,1,0:T(8,128)(2,1)S(1)} all-to-all(bf16[12,24,128]{2,1,0:T(8,128)(2,1)S(1)} %shard_map.146), channel_id=1, replica_groups=mesh['z'=12,'y'=8,'tp'=8] {'z'}, dimensions={0} | all-to-all | bytes 147456 | tf_op jit(solution)/shard_map/all_to_all | solution.py:324
  34.4 0.1 shard_map.147
  34.5 23.0 %all_to_all.31.packed = bf16[8,12,24,128]{3,2,1,0:T(8,128)(2,1)S(1)} all-to-all(bf16[8,12,24,128]{3,2,1,0:T(8,128)(2,1)S(1)} %shard_map.147), channel_id=1, replica_groups=mesh['z'=12,'y'=8,'tp'=8] {'y'}, dimensions={0} | all-to-all | bytes 1179648 | tf_op jit(solution)/shard_map/all_to_all | solution.py:333
  57.4 0.0 copy-done.1
  57.4 0.0 copy-done.2
  57.5 0.0 copy-start.5
  57.5 0.0 copy-start.6
  57.5 2.0 shard_map.148
  59.4 0.0 copy-start.7
  59.4 0.0 copy-start.8
  59.4 17.8 %all_gather.9.proj = bf16[768,512]{1,0:T(8,128)(2,1)S(1)} all-gather(bf16[96,512]{1,0:T(8,128)(2,1)S(1)} %shard_map.148), channel_id=1, replica_groups=mesh['z'=12,'y'=8,'tp'=8] {'tp'}, dimensions={0}, use_global_device_ids=true | all-gather | bytes 884736 | tf_op jit(solution)/shard_map/all_gather | solution.py:343
  77.3 0.0 copy-done.5
  77.3 0.0 copy-done.6
  77.3 1.5 shard_map.149
  78.8 31.0 %all_to_all.32.pieces = bf16[96,8,384]{2,1,0:T(8,128)(2,1)S(1)} all-to-all(bf16[96,8,384]{2,1,0:T(8,128)(2,1)} %shard_map.149), channel_id=1, replica_groups={{0,24,48,8,32,56,16,40,448,472,496,456,480,504,464,488,128,152,176,136,..., dimensions={0} | all-to-all | bytes 1179648 | tf_op jit(solution)/shard_map/all_to_all | solution.py:353
  109.8 0.0 copy-done.7
  109.8 0.0 copy-done.8
  109.8 1.1 shard_map.150
  110.9 16.6 %all_to_all.33.low = bf16[12,4,896]{2,1,0:T(4,128)(2,1)S(1)} all-to-all(bf16[12,4,896]{2,1,0:T(4,128)(2,1)} %get-tuple-element.23), channel_id=1, replica_groups=mesh['z'=12,'y'=8,'tp'=8] {'z'}, dimensions={0} | all-to-all | bytes 172032 | tf_op jit(solution)/shard_map/all_to_all | solution.py:373
  127.5 0.9 shard_map.151
  128.4 5.7 %all-to-all-start.4 = ((bf16[8,13,4,768]{3,2,1,0:T(4,128)(2,1)}), bf16[8,13,4,768]{3,2,1,0:T(4,128)(2,1)S(1)}, u32[]{:S(2)}, u32[]{:S(2)}) async-start(bf16[8,13,4,768]{3,2,1,0:T(4,128)(2,1)} %shard_map.151), calls=%async_computation.4 | async-start | bytes 1277952 | tf_op jit(solution)/shard_map/all_to_all | solution.py:382
  134.1 2.4 %collective-permute-start.2 = (bf16[8,12,24,128]{3,2,1,0:T(8,128)(2,1)S(1)}, bf16[8,12,24,128]{3,2,1,0:T(8,128)(2,1)S(1)}, u32[]{:S(2)}, u32[]{:S(2)}) collective-permute-start(bf16[8,12,24,128]{3,2,1,0:T(8,128)(2,1)S(1)} %all_to_all.31.packed), channel_id=1, source_target_pairs={{6,0},{7,1},{0,2},{1,3},{2,4},{3,5},{4,6},{5,7},{14,8},{15,9},{8,1... | collective-permute-start | bytes 1769480 | tf_op jit(solution)/shard_map/ppermute | solution.py:357
  136.6 4.3 %collective-permute-start.1 = (bf16[8,12,24,128]{3,2,1,0:T(8,128)(2,1)S(1)}, bf16[8,12,24,128]{3,2,1,0:T(8,128)(2,1)S(1)}, u32[]{:S(2)}, u32[]{:S(2)}) collective-permute-start(bf16[8,12,24,128]{3,2,1,0:T(8,128)(2,1)S(1)} %all_to_all.31.packed), channel_id=1, source_target_pairs={{4,0},{5,1},{6,2},{7,3},{0,4},{1,5},{2,6},{3,7},{12,8},{13,9},{14,... | collective-permute-start | bytes 1769480 | tf_op jit(solution)/shard_map/ppermute | solution.py:357
  140.9 1.9 collective-permute-start
  142.8 0.1 pad_add_fusion.place
  142.9 5.6 %collective-permute-done.2 = bf16[8,12,24,128]{3,2,1,0:T(8,128)(2,1)S(1)} collective-permute-done((bf16[8,12,24,128]{3,2,1,0:T(8,128)(2,1)S(1)}, bf16[8,12,24,128]{3,2,1,0:T(8,128)(2,1)S(1)}, u32[]{:S(2)}, u32[]{:S(2)}) %collective-permute-start.2) | collective-permute-done | bytes 589856 | tf_op jit(solution)/shard_map/ppermute | solution.py:357
  148.5 12.1 %collective-permute-done.1 = bf16[8,12,24,128]{3,2,1,0:T(8,128)(2,1)S(1)} collective-permute-done((bf16[8,12,24,128]{3,2,1,0:T(8,128)(2,1)S(1)}, bf16[8,12,24,128]{3,2,1,0:T(8,128)(2,1)S(1)}, u32[]{:S(2)}, u32[]{:S(2)}) %collective-permute-start.1) | collective-permute-done | bytes 589856 | tf_op jit(solution)/shard_map/ppermute | solution.py:357
  160.6 6.0 %collective-permute-done = bf16[8,12,24,128]{3,2,1,0:T(8,128)(2,1)S(1)} collective-permute-done((bf16[8,12,24,128]{3,2,1,0:T(8,128)(2,1)S(1)}, bf16[8,12,24,128]{3,2,1,0:T(8,128)(2,1)S(1)}, u32[]{:S(2)}, u32[]{:S(2)}) %collective-permute-start) | collective-permute-done | bytes 589856 | tf_op jit(solution)/shard_map/ppermute | solution.py:357
  166.6 1.7 pad_maximum_fusion.held
  168.3 3.5 %collective-permute-start.3 = (bf16[4,8,12,24,128]{4,3,2,1,0:T(8,128)(2,1)}, bf16[4,8,12,24,128]{4,3,2,1,0:T(8,128)(2,1)}, u32[]{:S(2)}, u32[]{:S(2)}) collective-permute-start(bf16[4,8,12,24,128]{4,3,2,1,0:T(8,128)(2,1)} %pad_maximum_fusion.held), channel_id=1, source_target_pairs={{1,0},{0,1},{3,2},{2,3},{5,4},{4,5},{7,6},{6,7},{9,8},{8,9},{11,10... | collective-permute-start | bytes 7077896 | tf_op jit(solution)/shard_map/ppermute | solution.py:359
  171.8 0.0 all-to-all-done.4.low
  171.8 0.0 all-gather.3.cloned.1.call-done
  171.8 0.6 shard_map.152
  172.4 4.0 %all-to-all-start.5 = ((f32[8,1,128]{2,1,0:T(1,128)}), f32[8,1,128]{2,1,0:T(1,128)S(1)}, u32[]{:S(2)}, u32[]{:S(2)}) async-start(f32[8,1,128]{2,1,0:T(1,128)} %shard_map.152), calls=%async_computation.5 | async-start | bytes 8192 | tf_op jit(solution)/shard_map/all_to_all | solution.py:421
  176.4 0.0 collective-permute-done.3.other
  176.4 8.9 %shard_map.153 = (bf16[3072,384]{1,0:T(8,128)(2,1)}, bf16[384,3072]{1,0:T(8,128)(2,1)}, bf16[32,384]{1,0:T(8,128)(2,1)}, bf16[32,384]{1,0:T(8,128)(2,1)}) custom-call(s32[2]{0:T(128)S(1)} %pad_add_fusion.place, bf16[4,8,12,24,128]{4,3,2,1,0:T(8,128)(2,1)} %pad_maximum_fusion.held, bf16[4,8,12,24,128]{4,3,2,1,0:T(8,128)(2,1)} %collective-permute-done.3.other), custom_call_target="tpu_custom_call" | custom-call | flops 1073741824 | bytes 31457280 | tf_op jit(solution)/shard_map/pallas_call | solution.py:386
  185.3 0.0 all-to-all-done.5.squares
  185.3 0.0 copy-start
  185.3 2.3 %copy-done = bf16[6144,384]{1,0:T(8,128)(2,1)S(1)} copy-done((bf16[6144,384]{1,0:T(8,128)(2,1)S(1)}, bf16[6144,384]{1,0:T(8,128)(2,1)}, u32[]{:S(2)}) %copy-start) | copy-done | bytes 4718616
  187.7 0.0 copy-start.3
  187.7 1.7 copy-done.3
  189.3 0.0 copy-start.4
  189.3 1.7 copy-done.4
  191.0 5.3 %shard_map.154 = (bf16[3072,384]{1,0:T(8,128)(2,1)}, bf16[384,3072]{1,0:T(8,128)(2,1)}, f32[32,384]{1,0:T(8,128)}, f32[32,384]{1,0:T(8,128)}) custom-call(f32[8,1,128]{2,1,0:T(1,128)S(1)} %all-to-all-done.5.squares, bf16[8,13,4,768]{3,2,1,0:T(4,128)(2,1)S(1)} %all-to-all-done.4.low, bf16[3072,384]{1,0:T(8,128)(2,1)S(1)} %copy-done.3, ...), custom_call_target="tpu_custom_call" | custom-call | flops 1811939328 | bytes 20971520 | tf_op jit(solution)/shard_map/pallas_call | solution.py:423
  (1 shorter events, 0.0 us)
Async XLA Ops:
  7.2 164.6 %all-gather.3.cloned.1.call-start = ((), (), s32[]{:S(2)}) async-start(), calls=%async_computation.6 | async-start | bytes 4767744 | tf_op jit(solution)/shard_map/all_gather | solution.py:323
  8.9 48.6 %copy-start.1 = (bf16[512,3072]{1,0:T(8,128)(2,1)S(1)}, bf16[512,3072]{1,0:T(8,128)(2,1)}, u32[]{:S(2)}) copy-start(bf16[512,3072]{1,0:T(8,128)(2,1)} %saved_inputs.1) | copy-start | bytes 9437188
  8.9 48.6 %copy-start.2 = (bf16[512,3072]{1,0:T(8,128)(2,1)S(1)}, bf16[512,3072]{1,0:T(8,128)(2,1)}, u32[]{:S(2)}) copy-start(bf16[512,3072]{1,0:T(8,128)(2,1)} %out_cotangent.1) | copy-start | bytes 9437188
  57.5 19.8 %copy-start.5 = (bf16[512,384]{1,0:T(8,128)(2,1)S(1)}, bf16[512,384]{1,0:T(8,128)(2,1)}, u32[]{:S(2)}) copy-start(bf16[512,384]{1,0:T(8,128)(2,1)} %query_cotangent.1) | copy-start | bytes 1179652
  57.5 19.8 %copy-start.6 = (bf16[512,384]{1,0:T(8,128)(2,1)S(1)}, bf16[512,384]{1,0:T(8,128)(2,1)}, u32[]{:S(2)}) copy-start(bf16[512,384]{1,0:T(8,128)(2,1)} %attn_outputs.1) | copy-start | bytes 1179652
  59.4 50.3 %copy-start.7 = (f32[2,4,384]{2,1,0:T(4,128)S(1)}, f32[2,4,384]{2,1,0:T(4,128)}, u32[]{:S(2)}) copy-start(f32[2,4,384]{2,1,0:T(4,128)} %first.1) | copy-start | bytes 36868
  59.4 50.3 %copy-start.8 = (f32[2,4,384]{2,1,0:T(4,128)S(1)}, f32[2,4,384]{2,1,0:T(4,128)}, u32[]{:S(2)}) copy-start(f32[2,4,384]{2,1,0:T(4,128)} %second.1) | copy-start | bytes 36868
  128.4 43.3 %all-to-all-start.4 = ((bf16[8,13,4,768]{3,2,1,0:T(4,128)(2,1)}), bf16[8,13,4,768]{3,2,1,0:T(4,128)(2,1)S(1)}, u32[]{:S(2)}, u32[]{:S(2)}) async-start(bf16[8,13,4,768]{3,2,1,0:T(4,128)(2,1)} %shard_map.151), calls=%async_computation.4 | async-start | bytes 1277952 | tf_op jit(solution)/shard_map/all_to_all | solution.py:382
  134.1 14.4 %collective-permute-start.2 = (bf16[8,12,24,128]{3,2,1,0:T(8,128)(2,1)S(1)}, bf16[8,12,24,128]{3,2,1,0:T(8,128)(2,1)S(1)}, u32[]{:S(2)}, u32[]{:S(2)}) collective-permute-start(bf16[8,12,24,128]{3,2,1,0:T(8,128)(2,1)S(1)} %all_to_all.31.packed), channel_id=1, source_target_pairs={{6,0},{7,1},{0,2},{1,3},{2,4},{3,5},{4,6},{5,7},{14,8},{15,9},{8,1... | collective-permute-start | bytes 1769480 | tf_op jit(solution)/shard_map/ppermute | solution.py:357
  136.6 24.0 %collective-permute-start.1 = (bf16[8,12,24,128]{3,2,1,0:T(8,128)(2,1)S(1)}, bf16[8,12,24,128]{3,2,1,0:T(8,128)(2,1)S(1)}, u32[]{:S(2)}, u32[]{:S(2)}) collective-permute-start(bf16[8,12,24,128]{3,2,1,0:T(8,128)(2,1)S(1)} %all_to_all.31.packed), channel_id=1, source_target_pairs={{4,0},{5,1},{6,2},{7,3},{0,4},{1,5},{2,6},{3,7},{12,8},{13,9},{14,... | collective-permute-start | bytes 1769480 | tf_op jit(solution)/shard_map/ppermute | solution.py:357
  140.9 25.7 %collective-permute-start = (bf16[8,12,24,128]{3,2,1,0:T(8,128)(2,1)S(1)}, bf16[8,12,24,128]{3,2,1,0:T(8,128)(2,1)S(1)}, u32[]{:S(2)}, u32[]{:S(2)}) collective-permute-start(bf16[8,12,24,128]{3,2,1,0:T(8,128)(2,1)S(1)} %all_to_all.31.packed), channel_id=1, source_target_pairs={{2,0},{3,1},{4,2},{5,3},{6,4},{7,5},{0,6},{1,7},{10,8},{11,9},{12,... | collective-permute-start | bytes 1769480 | tf_op jit(solution)/shard_map/ppermute | solution.py:357
  168.3 8.1 %collective-permute-start.3 = (bf16[4,8,12,24,128]{4,3,2,1,0:T(8,128)(2,1)}, bf16[4,8,12,24,128]{4,3,2,1,0:T(8,128)(2,1)}, u32[]{:S(2)}, u32[]{:S(2)}) collective-permute-start(bf16[4,8,12,24,128]{4,3,2,1,0:T(8,128)(2,1)} %pad_maximum_fusion.held), channel_id=1, source_target_pairs={{1,0},{0,1},{3,2},{2,3},{5,4},{4,5},{7,6},{6,7},{9,8},{8,9},{11,10... | collective-permute-start | bytes 7077896 | tf_op jit(solution)/shard_map/ppermute | solution.py:359
  172.4 12.9 %all-to-all-start.5 = ((f32[8,1,128]{2,1,0:T(1,128)}), f32[8,1,128]{2,1,0:T(1,128)S(1)}, u32[]{:S(2)}, u32[]{:S(2)}) async-start(f32[8,1,128]{2,1,0:T(1,128)} %shard_map.152), calls=%async_computation.5 | async-start | bytes 8192 | tf_op jit(solution)/shard_map/all_to_all | solution.py:421
  185.3 2.3 %copy-start = (bf16[6144,384]{1,0:T(8,128)(2,1)S(1)}, bf16[6144,384]{1,0:T(8,128)(2,1)}, u32[]{:S(2)}) copy-start(bf16[6144,384]{1,0:T(8,128)(2,1)} %all-gather.3.cloned.1.call-done) | copy-start | bytes 14155780
  187.7 1.7 copy-start.3
  189.3 1.7 copy-start.4
Sparse Core Ops, SparseCore 0:
  12.3 132.6 all-gather.2

commit v20 on v19

--- a/solution.py
+++ b/solution.py
@@ -16,6 +16,8 @@
 ANY = pl.BlockSpec(memory_space=pl.ANY)
 SMEM = pl.BlockSpec(memory_space=pltpu.SMEM)
 ORDER = tuple(7 * a % 12 * 8 + 3 * b % 8 for a in range(12) for b in range(8))
+Y_ORDER = tuple(3 * b % 8 for b in range(8))
+Y_PLACE = tuple(Y_ORDER.index(y) for y in range(8))
 REACH = 2.0**34
 GRAD_REACH = 2.0**10
 SMALL = pltpu.CompilerParams(vmem_limit_bytes=16 << 20)
@@ -60,8 +62,7 @@
 
 
 def by_place(packed):
-    height, depth = packed.shape[:2]
-    return jnp.concatenate([packed[y, z][None] for z in range(depth) for y in range(height)], axis=0)
+    return jnp.concatenate([packed[y, z][None] for z in range(packed.shape[1]) for y in Y_PLACE], axis=0)
 
 
 def hold_kernel(masters, packed, out):
@@ -232,7 +233,7 @@
     rows = low.shape[2]
     group = 16 // rows
     for g in range(0, first.shape[0] // rows, group):
-        part = [low[f % height, f // height].astype(f32) for f in range(g, g + group)]
+        part = [low[Y_PLACE[f % height], f // height].astype(f32) for f in range(g, g + group)]
         part = jnp.concatenate(part, axis=0).astype(bf16)
         first[g * rows : (g + group) * rows] = part[:, :cols]
         second[g * rows : (g + group) * rows] = part[:, cols:]
@@ -330,7 +331,7 @@
         compiler_params=SMALL,
         cost_estimate=cost(1 << 16, 1 << 20),
     )(packed)
-    packed = lax.all_to_all(packed, "y", 0, 0)
+    packed = lax.all_to_all(packed, "y", 0, 0, axis_index_groups=[list(Y_ORDER)])
     proj = pl.pallas_call(
         functools.partial(proj_kernel, used),
         out_shape=jax.ShapeDtypeStruct((used, tokens), bf16),
@@ -379,7 +380,7 @@
         compiler_params=SMALL,
         cost_estimate=cost(1 << 16, 1 << 20),
     )(low)
-    low = lax.all_to_all(low, "y", 0, 0)
+    low = lax.all_to_all(low, "y", 0, 0, axis_index_groups=[list(Y_ORDER)])
 
     span = width // 4
     per = span // own

time: 204 us -> 204 us (level)
  no operation moved by 1% of the time
where the time goes in v20:
time: 204 us; the launch traced here: 203 us
  blocking collectives  114 us (56%)
  waiting for transfers between devices  23.7 us (12%)
  Pallas kernels  22.1 us (11%)
  starting transfers between devices  21.8 us (11%)
  between operations  14.2 us (7%)
  local copies, waits for them, and re-layouts  5.69 us (3%)
    all_to_all x1, blocking collectives, body(): pieces = lax.all_to_all(partial, FS, 0, 0, axis_index_groups=[list(ORDER)])  31 us
    all_to_all x1, blocking collectives, body(): packed = lax.all_to_all(packed, 'z', 0, 0)  25.5 us
    ppermute x3, waiting for transfers between devices, body(): lax.ppermute(packed, 'tp', [((t + 2 * step) % tp, t) for t in range(tp)])  23.7 us
    all_to_all x1, blocking collectives, body(): lax.all_to_all(packed, 'y', 0, 0, axis_index_groups=[list(Y_ORDER)])  23 us
    all_gather x1, blocking collectives, body(): proj = lax.all_gather(proj, 'tp', axis=0, tiled=True)  17.6 us
    all_to_all x1, blocking collectives, body(): low = lax.all_to_all(low, 'z', 0, 0)  16.6 us
    pallas_call x1, Pallas kernels, body(): pl.pallas_call(functools.partial(prep_kernel, rank_cols), grid=(width //...  8.91 us
    ppermute x3, starting transfers between devices, body(): lax.ppermute(packed, 'tp', [((t + 2 * step) % tp, t) for t in range(tp)])  8.68 us
  transfers between devices with their start and end apart: 7, of which 3 were waited for; matrix products, arithmetic and copies ran while one was open for 1% of the time, Pallas kernels for 7%

profile of v20, /device:TPU:1, one launch (start us, length us, event | category | flops | bytes accessed | tf_op | source)
XLA Modules:
  0.0 203.0 jit_solution(1040393860038956454)
XLA Ops:
  7.2 0.0 all-gather.3.cloned.1.call-start
  7.2 1.6 shard_map.145
  8.8 0.0 all-gather.3.cloned.1.call-update
  8.9 0.0 copy-start.1
  8.9 0.0 copy-start.2
  8.9 25.5 %all_to_all.30.packed = bf16[12,24,128]{2,1,0:T(8,128)(2,1)S(1)} all-to-all(bf16[12,24,128]{2,1,0:T(8,128)(2,1)S(1)} %shard_map.146), channel_id=1, replica_groups=mesh['z'=12,'y'=8,'tp'=8] {'z'}, dimensions={0} | all-to-all | bytes 147456 | tf_op jit(solution)/shard_map/all_to_all | solution.py:325
  34.4 0.1 shard_map.147
  34.5 23.0 %all_to_all.31.packed = bf16[8,12,24,128]{3,2,1,0:T(8,128)(2,1)S(1)} all-to-all(bf16[8,12,24,128]{3,2,1,0:T(8,128)(2,1)S(1)} %shard_map.147), channel_id=1, replica_groups={{0,24,48,8,32,56,16,40},{1,25,49,9,33,57,17,41},{2,26,50,10,34,58,18,42..., dimensions={0} | all-to-all | bytes 1179648 | tf_op jit(solution)/shard_map/all_to_all | solution.py:334
  57.4 0.0 copy-done.1
  57.4 0.0 copy-done.2
  57.4 0.0 copy-start.5
  57.4 0.0 copy-start.6
  57.5 2.0 shard_map.148
  59.4 0.0 copy-start.7
  59.4 0.0 copy-start.8
  59.4 17.6 %all_gather.9.proj = bf16[768,512]{1,0:T(8,128)(2,1)S(1)} all-gather(bf16[96,512]{1,0:T(8,128)(2,1)S(1)} %shard_map.148), channel_id=1, replica_groups=mesh['z'=12,'y'=8,'tp'=8] {'tp'}, dimensions={0}, use_global_device_ids=true | all-gather | bytes 884736 | tf_op jit(solution)/shard_map/all_gather | solution.py:344
  77.1 0.0 copy-done.5
  77.1 0.0 copy-done.6
  77.1 1.5 shard_map.149
  78.6 31.0 %all_to_all.32.pieces = bf16[96,8,384]{2,1,0:T(8,128)(2,1)S(1)} all-to-all(bf16[96,8,384]{2,1,0:T(8,128)(2,1)} %shard_map.149), channel_id=1, replica_groups={{0,24,48,8,32,56,16,40,448,472,496,456,480,504,464,488,128,152,176,136,..., dimensions={0} | all-to-all | bytes 1179648 | tf_op jit(solution)/shard_map/all_to_all | solution.py:354
  109.6 0.0 copy-done.7
  109.6 0.0 copy-done.8
  109.6 1.1 shard_map.150
  110.7 16.6 %all_to_all.33.low = bf16[12,4,896]{2,1,0:T(4,128)(2,1)S(1)} all-to-all(bf16[12,4,896]{2,1,0:T(4,128)(2,1)} %get-tuple-element.23), channel_id=1, replica_groups=mesh['z'=12,'y'=8,'tp'=8] {'z'}, dimensions={0} | all-to-all | bytes 172032 | tf_op jit(solution)/shard_map/all_to_all | solution.py:374
  127.3 0.9 shard_map.151
  128.3 5.6 %all-to-all-start.4 = ((bf16[8,13,4,768]{3,2,1,0:T(4,128)(2,1)}), bf16[8,13,4,768]{3,2,1,0:T(4,128)(2,1)S(1)}, u32[]{:S(2)}, u32[]{:S(2)}) async-start(bf16[8,13,4,768]{3,2,1,0:T(4,128)(2,1)} %shard_map.151), calls=%async_computation.4 | async-start | bytes 1277952 | tf_op jit(solution)/shard_map/all_to_all | solution.py:383
  133.9 2.5 %collective-permute-start.2 = (bf16[8,12,24,128]{3,2,1,0:T(8,128)(2,1)S(1)}, bf16[8,12,24,128]{3,2,1,0:T(8,128)(2,1)S(1)}, u32[]{:S(2)}, u32[]{:S(2)}) collective-permute-start(bf16[8,12,24,128]{3,2,1,0:T(8,128)(2,1)S(1)} %all_to_all.31.packed), channel_id=1, source_target_pairs={{6,0},{7,1},{0,2},{1,3},{2,4},{3,5},{4,6},{5,7},{14,8},{15,9},{8,1... | collective-permute-start | bytes 1769480 | tf_op jit(solution)/shard_map/ppermute | solution.py:358
  136.4 4.3 %collective-permute-start.1 = (bf16[8,12,24,128]{3,2,1,0:T(8,128)(2,1)S(1)}, bf16[8,12,24,128]{3,2,1,0:T(8,128)(2,1)S(1)}, u32[]{:S(2)}, u32[]{:S(2)}) collective-permute-start(bf16[8,12,24,128]{3,2,1,0:T(8,128)(2,1)S(1)} %all_to_all.31.packed), channel_id=1, source_target_pairs={{4,0},{5,1},{6,2},{7,3},{0,4},{1,5},{2,6},{3,7},{12,8},{13,9},{14,... | collective-permute-start | bytes 1769480 | tf_op jit(solution)/shard_map/ppermute | solution.py:358
  140.7 1.9 collective-permute-start
  142.6 0.1 pad_add_fusion.place
  142.7 5.5 %collective-permute-done.2 = bf16[8,12,24,128]{3,2,1,0:T(8,128)(2,1)S(1)} collective-permute-done((bf16[8,12,24,128]{3,2,1,0:T(8,128)(2,1)S(1)}, bf16[8,12,24,128]{3,2,1,0:T(8,128)(2,1)S(1)}, u32[]{:S(2)}, u32[]{:S(2)}) %collective-permute-start.2) | collective-permute-done | bytes 589856 | tf_op jit(solution)/shard_map/ppermute | solution.py:358
  148.2 12.2 %collective-permute-done.1 = bf16[8,12,24,128]{3,2,1,0:T(8,128)(2,1)S(1)} collective-permute-done((bf16[8,12,24,128]{3,2,1,0:T(8,128)(2,1)S(1)}, bf16[8,12,24,128]{3,2,1,0:T(8,128)(2,1)S(1)}, u32[]{:S(2)}, u32[]{:S(2)}) %collective-permute-start.1) | collective-permute-done | bytes 589856 | tf_op jit(solution)/shard_map/ppermute | solution.py:358
  160.4 5.9 %collective-permute-done = bf16[8,12,24,128]{3,2,1,0:T(8,128)(2,1)S(1)} collective-permute-done((bf16[8,12,24,128]{3,2,1,0:T(8,128)(2,1)S(1)}, bf16[8,12,24,128]{3,2,1,0:T(8,128)(2,1)S(1)}, u32[]{:S(2)}, u32[]{:S(2)}) %collective-permute-start) | collective-permute-done | bytes 589856 | tf_op jit(solution)/shard_map/ppermute | solution.py:358
  166.4 1.7 pad_maximum_fusion.held
  168.1 3.5 %collective-permute-start.3 = (bf16[4,8,12,24,128]{4,3,2,1,0:T(8,128)(2,1)}, bf16[4,8,12,24,128]{4,3,2,1,0:T(8,128)(2,1)}, u32[]{:S(2)}, u32[]{:S(2)}) collective-permute-start(bf16[4,8,12,24,128]{4,3,2,1,0:T(8,128)(2,1)} %pad_maximum_fusion.held), channel_id=1, source_target_pairs={{1,0},{0,1},{3,2},{2,3},{5,4},{4,5},{7,6},{6,7},{9,8},{8,9},{11,10... | collective-permute-start | bytes 7077896 | tf_op jit(solution)/shard_map/ppermute | solution.py:360
  171.5 0.0 all-to-all-done.4.low
  171.5 0.0 all-gather.3.cloned.1.call-done
  171.6 0.6 shard_map.152
  172.2 4.0 %all-to-all-start.5 = ((f32[8,1,128]{2,1,0:T(1,128)}), f32[8,1,128]{2,1,0:T(1,128)S(1)}, u32[]{:S(2)}, u32[]{:S(2)}) async-start(f32[8,1,128]{2,1,0:T(1,128)} %shard_map.152), calls=%async_computation.5 | async-start | bytes 8192 | tf_op jit(solution)/shard_map/all_to_all | solution.py:422
  176.2 0.0 collective-permute-done.3.other
  176.2 8.9 %shard_map.153 = (bf16[3072,384]{1,0:T(8,128)(2,1)}, bf16[384,3072]{1,0:T(8,128)(2,1)}, bf16[32,384]{1,0:T(8,128)(2,1)}, bf16[32,384]{1,0:T(8,128)(2,1)}) custom-call(s32[2]{0:T(128)S(1)} %pad_add_fusion.place, bf16[4,8,12,24,128]{4,3,2,1,0:T(8,128)(2,1)} %pad_maximum_fusion.held, bf16[4,8,12,24,128]{4,3,2,1,0:T(8,128)(2,1)} %collective-permute-done.3.other), custom_call_target="tpu_custom_call" | custom-call | flops 1073741824 | bytes 31457280 | tf_op jit(solution)/shard_map/pallas_call | solution.py:387
  185.1 0.0 all-to-all-done.5.squares
  185.1 0.0 copy-start
  185.1 2.3 %copy-done = bf16[6144,384]{1,0:T(8,128)(2,1)S(1)} copy-done((bf16[6144,384]{1,0:T(8,128)(2,1)S(1)}, bf16[6144,384]{1,0:T(8,128)(2,1)}, u32[]{:S(2)}) %copy-start) | copy-done | bytes 4718616
  187.4 0.0 copy-start.3
  187.4 1.7 copy-done.3
  189.1 0.0 copy-start.4
  189.1 1.7 copy-done.4
  190.8 5.3 %shard_map.154 = (bf16[3072,384]{1,0:T(8,128)(2,1)}, bf16[384,3072]{1,0:T(8,128)(2,1)}, f32[32,384]{1,0:T(8,128)}, f32[32,384]{1,0:T(8,128)}) custom-call(f32[8,1,128]{2,1,0:T(1,128)S(1)} %all-to-all-done.5.squares, bf16[8,13,4,768]{3,2,1,0:T(4,128)(2,1)S(1)} %all-to-all-done.4.low, bf16[3072,384]{1,0:T(8,128)(2,1)S(1)} %copy-done.3, ...), custom_call_target="tpu_custom_call" | custom-call | flops 1811939328 | bytes 20971520 | tf_op jit(solution)/shard_map/pallas_call | solution.py:424
  (1 shorter events, 0.0 us)
Async XLA Ops:
  7.2 164.4 %all-gather.3.cloned.1.call-start = ((), (), s32[]{:S(2)}) async-start(), calls=%async_computation.6 | async-start | bytes 4767744 | tf_op jit(solution)/shard_map/all_gather | solution.py:324
  8.9 48.6 %copy-start.1 = (bf16[512,3072]{1,0:T(8,128)(2,1)S(1)}, bf16[512,3072]{1,0:T(8,128)(2,1)}, u32[]{:S(2)}) copy-start(bf16[512,3072]{1,0:T(8,128)(2,1)} %saved_inputs.1) | copy-start | bytes 9437188
  8.9 48.6 %copy-start.2 = (bf16[512,3072]{1,0:T(8,128)(2,1)S(1)}, bf16[512,3072]{1,0:T(8,128)(2,1)}, u32[]{:S(2)}) copy-start(bf16[512,3072]{1,0:T(8,128)(2,1)} %out_cotangent.1) | copy-start | bytes 9437188
  57.4 19.6 %copy-start.5 = (bf16[512,384]{1,0:T(8,128)(2,1)S(1)}, bf16[512,384]{1,0:T(8,128)(2,1)}, u32[]{:S(2)}) copy-start(bf16[512,384]{1,0:T(8,128)(2,1)} %query_cotangent.1) | copy-start | bytes 1179652
  57.4 19.6 %copy-start.6 = (bf16[512,384]{1,0:T(8,128)(2,1)S(1)}, bf16[512,384]{1,0:T(8,128)(2,1)}, u32[]{:S(2)}) copy-start(bf16[512,384]{1,0:T(8,128)(2,1)} %attn_outputs.1) | copy-start | bytes 1179652
  59.4 50.2 %copy-start.7 = (f32[2,4,384]{2,1,0:T(4,128)S(1)}, f32[2,4,384]{2,1,0:T(4,128)}, u32[]{:S(2)}) copy-start(f32[2,4,384]{2,1,0:T(4,128)} %first.1) | copy-start | bytes 36868
  59.4 50.2 %copy-start.8 = (f32[2,4,384]{2,1,0:T(4,128)S(1)}, f32[2,4,384]{2,1,0:T(4,128)}, u32[]{:S(2)}) copy-start(f32[2,4,384]{2,1,0:T(4,128)} %second.1) | copy-start | bytes 36868
  128.3 43.3 %all-to-all-start.4 = ((bf16[8,13,4,768]{3,2,1,0:T(4,128)(2,1)}), bf16[8,13,4,768]{3,2,1,0:T(4,128)(2,1)S(1)}, u32[]{:S(2)}, u32[]{:S(2)}) async-start(bf16[8,13,4,768]{3,2,1,0:T(4,128)(2,1)} %shard_map.151), calls=%async_computation.4 | async-start | bytes 1277952 | tf_op jit(solution)/shard_map/all_to_all | solution.py:383
  133.9 14.3 %collective-permute-start.2 = (bf16[8,12,24,128]{3,2,1,0:T(8,128)(2,1)S(1)}, bf16[8,12,24,128]{3,2,1,0:T(8,128)(2,1)S(1)}, u32[]{:S(2)}, u32[]{:S(2)}) collective-permute-start(bf16[8,12,24,128]{3,2,1,0:T(8,128)(2,1)S(1)} %all_to_all.31.packed), channel_id=1, source_target_pairs={{6,0},{7,1},{0,2},{1,3},{2,4},{3,5},{4,6},{5,7},{14,8},{15,9},{8,1... | collective-permute-start | bytes 1769480 | tf_op jit(solution)/shard_map/ppermute | solution.py:358
  136.4 24.1 %collective-permute-start.1 = (bf16[8,12,24,128]{3,2,1,0:T(8,128)(2,1)S(1)}, bf16[8,12,24,128]{3,2,1,0:T(8,128)(2,1)S(1)}, u32[]{:S(2)}, u32[]{:S(2)}) collective-permute-start(bf16[8,12,24,128]{3,2,1,0:T(8,128)(2,1)S(1)} %all_to_all.31.packed), channel_id=1, source_target_pairs={{4,0},{5,1},{6,2},{7,3},{0,4},{1,5},{2,6},{3,7},{12,8},{13,9},{14,... | collective-permute-start | bytes 1769480 | tf_op jit(solution)/shard_map/ppermute | solution.py:358
  140.7 25.7 %collective-permute-start = (bf16[8,12,24,128]{3,2,1,0:T(8,128)(2,1)S(1)}, bf16[8,12,24,128]{3,2,1,0:T(8,128)(2,1)S(1)}, u32[]{:S(2)}, u32[]{:S(2)}) collective-permute-start(bf16[8,12,24,128]{3,2,1,0:T(8,128)(2,1)S(1)} %all_to_all.31.packed), channel_id=1, source_target_pairs={{2,0},{3,1},{4,2},{5,3},{6,4},{7,5},{0,6},{1,7},{10,8},{11,9},{12,... | collective-permute-start | bytes 1769480 | tf_op jit(solution)/shard_map/ppermute | solution.py:358
  168.1 8.1 %collective-permute-start.3 = (bf16[4,8,12,24,128]{4,3,2,1,0:T(8,128)(2,1)}, bf16[4,8,12,24,128]{4,3,2,1,0:T(8,128)(2,1)}, u32[]{:S(2)}, u32[]{:S(2)}) collective-permute-start(bf16[4,8,12,24,128]{4,3,2,1,0:T(8,128)(2,1)} %pad_maximum_fusion.held), channel_id=1, source_target_pairs={{1,0},{0,1},{3,2},{2,3},{5,4},{4,5},{7,6},{6,7},{9,8},{8,9},{11,10... | collective-permute-start | bytes 7077896 | tf_op jit(solution)/shard_map/ppermute | solution.py:360
  172.2 12.9 %all-to-all-start.5 = ((f32[8,1,128]{2,1,0:T(1,128)}), f32[8,1,128]{2,1,0:T(1,128)S(1)}, u32[]{:S(2)}, u32[]{:S(2)}) async-start(f32[8,1,128]{2,1,0:T(1,128)} %shard_map.152), calls=%async_computation.5 | async-start | bytes 8192 | tf_op jit(solution)/shard_map/all_to_all | solution.py:422
  185.1 2.3 %copy-start = (bf16[6144,384]{1,0:T(8,128)(2,1)S(1)}, bf16[6144,384]{1,0:T(8,128)(2,1)}, u32[]{:S(2)}) copy-start(bf16[6144,384]{1,0:T(8,128)(2,1)} %all-gather.3.cloned.1.call-done) | copy-start | bytes 14155780
  187.4 1.7 copy-start.3
  189.1 1.7 copy-start.4
Sparse Core Ops, SparseCore 0:
  12.3 132.6 all-gather.2

commit v21 on v20

--- a/solution.py
+++ b/solution.py
@@ -15,9 +15,11 @@
 VMEM = pl.BlockSpec(memory_space=pltpu.VMEM)
 ANY = pl.BlockSpec(memory_space=pl.ANY)
 SMEM = pl.BlockSpec(memory_space=pltpu.SMEM)
-ORDER = tuple(7 * a % 12 * 8 + 3 * b % 8 for a in range(12) for b in range(8))
+ORDER = tuple(7 * a % 12 * 8 + (3 * b + 5 * a) % 8 for b in range(8) for a in range(12))
 Y_ORDER = tuple(3 * b % 8 for b in range(8))
 Y_PLACE = tuple(Y_ORDER.index(y) for y in range(8))
+Z_ORDER = tuple(7 * a % 12 for a in range(12))
+Z_PLACE = tuple(Z_ORDER.index(z) for z in range(12))
 REACH = 2.0**34
 GRAD_REACH = 2.0**10
 SMALL = pltpu.CompilerParams(vmem_limit_bytes=16 << 20)
@@ -233,7 +235,7 @@
     rows = low.shape[2]
     group = 16 // rows
     for g in range(0, first.shape[0] // rows, group):
-        part = [low[Y_PLACE[f % height], f // height].astype(f32) for f in range(g, g + group)]
+        part = [low[Y_PLACE[f % height], Z_PLACE[f // height]].astype(f32) for f in range(g, g + group)]
         part = jnp.concatenate(part, axis=0).astype(bf16)
         first[g * rows : (g + group) * rows] = part[:, :cols]
         second[g * rows : (g + group) * rows] = part[:, cols:]
@@ -371,7 +373,7 @@
         compiler_params=SMALL,
         cost_estimate=cost(1 << 20, 2 << 20),
     )(pieces, first_moment, second_moment)
-    low = lax.all_to_all(low, "z", 0, 0)
+    low = lax.all_to_all(low, "z", 0, 0, axis_index_groups=[list(Z_ORDER)])
     low = pl.pallas_call(
         spread_kernel,
         out_shape=pltpu.HBM((height, depth + 1, rows, 2 * cols), bf16),

time: 204 us -> 204 us (level)
    all_to_all x1, blocking collectives: 31 us -> 36.6 us  [body(): pieces = lax.all_to_all(partial, FS, 0, 0, axis_index_groups=[list(ORDER)])]
    all_to_all x1, blocking collectives: 16.6 us -> 13.2 us  [body(): low = lax.all_to_all(low, 'z', 0, 0, axis_index_groups=[list(Z_ORDER)])]
    all_to_all x1, starting transfers between devices: 5.64 us -> 3.58 us  [body(): low = lax.all_to_all(low, 'y', 0, 0, axis_index_groups=[list(Y_ORDER)])]
where the time goes in v21:
time: 204 us; the launch traced here: 203 us
  blocking collectives  116 us (57%)
  waiting for transfers between devices  22.8 us (11%)
  Pallas kernels  22.1 us (11%)
  starting transfers between devices  20.7 us (10%)
  between operations  14.2 us (7%)
  local copies, waits for them, and re-layouts  5.69 us (3%)
    all_to_all x1, blocking collectives, body(): pieces = lax.all_to_all(partial, FS, 0, 0, axis_index_groups=[list(ORDER)])  36.6 us
    all_to_all x1, blocking collectives, body(): packed = lax.all_to_all(packed, 'z', 0, 0)  25.5 us
    all_to_all x1, blocking collectives, body(): lax.all_to_all(packed, 'y', 0, 0, axis_index_groups=[list(Y_ORDER)])  23 us
    ppermute x3, waiting for transfers between devices, body(): lax.ppermute(packed, 'tp', [((t + 2 * step) % tp, t) for t in range(tp)])  22.7 us
    all_gather x1, blocking collectives, body(): proj = lax.all_gather(proj, 'tp', axis=0, tiled=True)  17.6 us
    all_to_all x1, blocking collectives, body(): low = lax.all_to_all(low, 'z', 0, 0, axis_index_groups=[list(Z_ORDER)])  13.2 us
    ppermute x3, starting transfers between devices, body(): lax.ppermute(packed, 'tp', [((t + 2 * step) % tp, t) for t in range(tp)])  9.12 us
    pallas_call x1, Pallas kernels, body(): pl.pallas_call(functools.partial(prep_kernel, rank_cols), grid=(width //...  8.91 us
  transfers between devices with their start and end apart: 7, of which 3 were waited for; matrix products, arithmetic and copies ran while one was open for 1% of the time, Pallas kernels for 7%

profile of v21, /device:TPU:1, one launch (start us, length us, event | category | flops | bytes accessed | tf_op | source)
XLA Modules:
  0.0 203.2 jit_solution(7165453614416932428)
XLA Ops:
  7.2 0.0 all-gather.3.cloned.1.call-start
  7.2 1.6 shard_map.145
  8.8 0.0 all-gather.3.cloned.1.call-update
  8.9 0.0 copy-start.1
  8.9 0.0 copy-start.2
  8.9 25.5 %all_to_all.30.packed = bf16[12,24,128]{2,1,0:T(8,128)(2,1)S(1)} all-to-all(bf16[12,24,128]{2,1,0:T(8,128)(2,1)S(1)} %shard_map.146), channel_id=1, replica_groups=mesh['z'=12,'y'=8,'tp'=8] {'z'}, dimensions={0} | all-to-all | bytes 147456 | tf_op jit(solution)/shard_map/all_to_all | solution.py:327
  34.4 0.1 shard_map.147
  34.5 23.0 %all_to_all.31.packed = bf16[8,12,24,128]{3,2,1,0:T(8,128)(2,1)S(1)} all-to-all(bf16[8,12,24,128]{3,2,1,0:T(8,128)(2,1)S(1)} %shard_map.147), channel_id=1, replica_groups={{0,24,48,8,32,56,16,40},{1,25,49,9,33,57,17,41},{2,26,50,10,34,58,18,42..., dimensions={0} | all-to-all | bytes 1179648 | tf_op jit(solution)/shard_map/all_to_all | solution.py:336
  57.4 0.0 copy-done.1
  57.4 0.0 copy-done.2
  57.4 0.0 copy-start.5
  57.4 0.0 copy-start.6
  57.5 2.0 shard_map.148
  59.4 0.0 copy-start.7
  59.4 0.0 copy-start.8
  59.4 17.6 %all_gather.9.proj = bf16[768,512]{1,0:T(8,128)(2,1)S(1)} all-gather(bf16[96,512]{1,0:T(8,128)(2,1)S(1)} %shard_map.148), channel_id=1, replica_groups=mesh['z'=12,'y'=8,'tp'=8] {'tp'}, dimensions={0}, use_global_device_ids=true | all-gather | bytes 884736 | tf_op jit(solution)/shard_map/all_gather | solution.py:346
  77.1 0.0 copy-done.5
  77.1 0.0 copy-done.6
  77.1 1.5 shard_map.149
  78.6 36.6 %all_to_all.32.pieces = bf16[96,8,384]{2,1,0:T(8,128)(2,1)S(1)} all-to-all(bf16[96,8,384]{2,1,0:T(8,128)(2,1)} %shard_map.149), channel_id=1, replica_groups={{0,488,144,632,288,712,432,88,512,232,656,376,24,448,168,592,312,736,39..., dimensions={0} | all-to-all | bytes 1179648 | tf_op jit(solution)/shard_map/all_to_all | solution.py:356
  115.2 0.0 copy-done.7
  115.2 0.0 copy-done.8
  115.2 1.1 shard_map.150
  116.4 13.2 %all_to_all.33.low = bf16[12,4,896]{2,1,0:T(4,128)(2,1)S(1)} all-to-all(bf16[12,4,896]{2,1,0:T(4,128)(2,1)} %get-tuple-element.23), channel_id=1, replica_groups={{0,448,128,576,256,704,384,64,512,192,640,320},{1,449,129,577,257,705,3..., dimensions={0} | all-to-all | bytes 172032 | tf_op jit(solution)/shard_map/all_to_all | solution.py:376
  129.6 0.9 shard_map.151
  130.5 3.6 %all-to-all-start.4 = ((bf16[8,13,4,768]{3,2,1,0:T(4,128)(2,1)}), bf16[8,13,4,768]{3,2,1,0:T(4,128)(2,1)S(1)}, u32[]{:S(2)}, u32[]{:S(2)}) async-start(bf16[8,13,4,768]{3,2,1,0:T(4,128)(2,1)} %shard_map.151), calls=%async_computation.4 | async-start | bytes 1277952 | tf_op jit(solution)/shard_map/all_to_all | solution.py:385
  134.1 2.8 %collective-permute-start.2 = (bf16[8,12,24,128]{3,2,1,0:T(8,128)(2,1)S(1)}, bf16[8,12,24,128]{3,2,1,0:T(8,128)(2,1)S(1)}, u32[]{:S(2)}, u32[]{:S(2)}) collective-permute-start(bf16[8,12,24,128]{3,2,1,0:T(8,128)(2,1)S(1)} %all_to_all.31.packed), channel_id=1, source_target_pairs={{6,0},{7,1},{0,2},{1,3},{2,4},{3,5},{4,6},{5,7},{14,8},{15,9},{8,1... | collective-permute-start | bytes 1769480 | tf_op jit(solution)/shard_map/ppermute | solution.py:360
  136.9 4.4 %collective-permute-start.1 = (bf16[8,12,24,128]{3,2,1,0:T(8,128)(2,1)S(1)}, bf16[8,12,24,128]{3,2,1,0:T(8,128)(2,1)S(1)}, u32[]{:S(2)}, u32[]{:S(2)}) collective-permute-start(bf16[8,12,24,128]{3,2,1,0:T(8,128)(2,1)S(1)} %all_to_all.31.packed), channel_id=1, source_target_pairs={{4,0},{5,1},{6,2},{7,3},{0,4},{1,5},{2,6},{3,7},{12,8},{13,9},{14,... | collective-permute-start | bytes 1769480 | tf_op jit(solution)/shard_map/ppermute | solution.py:360
  141.3 1.9 collective-permute-start
  143.2 0.1 pad_add_fusion.place
  143.3 3.8 %collective-permute-done.2 = bf16[8,12,24,128]{3,2,1,0:T(8,128)(2,1)S(1)} collective-permute-done((bf16[8,12,24,128]{3,2,1,0:T(8,128)(2,1)S(1)}, bf16[8,12,24,128]{3,2,1,0:T(8,128)(2,1)S(1)}, u32[]{:S(2)}, u32[]{:S(2)}) %collective-permute-start.2) | collective-permute-done | bytes 589856 | tf_op jit(solution)/shard_map/ppermute | solution.py:360
  147.1 13.5 %collective-permute-done.1 = bf16[8,12,24,128]{3,2,1,0:T(8,128)(2,1)S(1)} collective-permute-done((bf16[8,12,24,128]{3,2,1,0:T(8,128)(2,1)S(1)}, bf16[8,12,24,128]{3,2,1,0:T(8,128)(2,1)S(1)}, u32[]{:S(2)}, u32[]{:S(2)}) %collective-permute-start.1) | collective-permute-done | bytes 589856 | tf_op jit(solution)/shard_map/ppermute | solution.py:360
  160.6 5.5 %collective-permute-done = bf16[8,12,24,128]{3,2,1,0:T(8,128)(2,1)S(1)} collective-permute-done((bf16[8,12,24,128]{3,2,1,0:T(8,128)(2,1)S(1)}, bf16[8,12,24,128]{3,2,1,0:T(8,128)(2,1)S(1)}, u32[]{:S(2)}, u32[]{:S(2)}) %collective-permute-start) | collective-permute-done | bytes 589856 | tf_op jit(solution)/shard_map/ppermute | solution.py:360
  166.1 1.7 pad_maximum_fusion.held
  167.8 3.9 %collective-permute-start.3 = (bf16[4,8,12,24,128]{4,3,2,1,0:T(8,128)(2,1)}, bf16[4,8,12,24,128]{4,3,2,1,0:T(8,128)(2,1)}, u32[]{:S(2)}, u32[]{:S(2)}) collective-permute-start(bf16[4,8,12,24,128]{4,3,2,1,0:T(8,128)(2,1)} %pad_maximum_fusion.held), channel_id=1, source_target_pairs={{1,0},{0,1},{3,2},{2,3},{5,4},{4,5},{7,6},{6,7},{9,8},{8,9},{11,10... | collective-permute-start | bytes 7077896 | tf_op jit(solution)/shard_map/ppermute | solution.py:362
  171.7 0.0 all-to-all-done.4.low
  171.7 0.0 all-gather.3.cloned.1.call-done
  171.7 0.6 shard_map.152
  172.3 4.0 %all-to-all-start.5 = ((f32[8,1,128]{2,1,0:T(1,128)}), f32[8,1,128]{2,1,0:T(1,128)S(1)}, u32[]{:S(2)}, u32[]{:S(2)}) async-start(f32[8,1,128]{2,1,0:T(1,128)} %shard_map.152), calls=%async_computation.5 | async-start | bytes 8192 | tf_op jit(solution)/shard_map/all_to_all | solution.py:424
  176.4 0.0 collective-permute-done.3.other
  176.4 8.9 %shard_map.153 = (bf16[3072,384]{1,0:T(8,128)(2,1)}, bf16[384,3072]{1,0:T(8,128)(2,1)}, bf16[32,384]{1,0:T(8,128)(2,1)}, bf16[32,384]{1,0:T(8,128)(2,1)}) custom-call(s32[2]{0:T(128)S(1)} %pad_add_fusion.place, bf16[4,8,12,24,128]{4,3,2,1,0:T(8,128)(2,1)} %pad_maximum_fusion.held, bf16[4,8,12,24,128]{4,3,2,1,0:T(8,128)(2,1)} %collective-permute-done.3.other), custom_call_target="tpu_custom_call" | custom-call | flops 1073741824 | bytes 31457280 | tf_op jit(solution)/shard_map/pallas_call | solution.py:389
  185.3 0.0 all-to-all-done.5.squares
  185.3 0.0 copy-start
  185.3 2.3 %copy-done = bf16[6144,384]{1,0:T(8,128)(2,1)S(1)} copy-done((bf16[6144,384]{1,0:T(8,128)(2,1)S(1)}, bf16[6144,384]{1,0:T(8,128)(2,1)}, u32[]{:S(2)}) %copy-start) | copy-done | bytes 4718616
  187.6 0.0 copy-start.3
  187.6 1.7 copy-done.3
  189.3 0.0 copy-start.4
  189.3 1.7 copy-done.4
  191.0 5.3 %shard_map.154 = (bf16[3072,384]{1,0:T(8,128)(2,1)}, bf16[384,3072]{1,0:T(8,128)(2,1)}, f32[32,384]{1,0:T(8,128)}, f32[32,384]{1,0:T(8,128)}) custom-call(f32[8,1,128]{2,1,0:T(1,128)S(1)} %all-to-all-done.5.squares, bf16[8,13,4,768]{3,2,1,0:T(4,128)(2,1)S(1)} %all-to-all-done.4.low, bf16[3072,384]{1,0:T(8,128)(2,1)S(1)} %copy-done.3, ...), custom_call_target="tpu_custom_call" | custom-call | flops 1811939328 | bytes 20971520 | tf_op jit(solution)/shard_map/pallas_call | solution.py:426
  (1 shorter events, 0.0 us)
Async XLA Ops:
  7.2 164.6 %all-gather.3.cloned.1.call-start = ((), (), s32[]{:S(2)}) async-start(), calls=%async_computation.6 | async-start | bytes 4767744 | tf_op jit(solution)/shard_map/all_gather | solution.py:326
  8.9 48.6 %copy-start.1 = (bf16[512,3072]{1,0:T(8,128)(2,1)S(1)}, bf16[512,3072]{1,0:T(8,128)(2,1)}, u32[]{:S(2)}) copy-start(bf16[512,3072]{1,0:T(8,128)(2,1)} %saved_inputs.1) | copy-start | bytes 9437188
  8.9 48.6 %copy-start.2 = (bf16[512,3072]{1,0:T(8,128)(2,1)S(1)}, bf16[512,3072]{1,0:T(8,128)(2,1)}, u32[]{:S(2)}) copy-start(bf16[512,3072]{1,0:T(8,128)(2,1)} %out_cotangent.1) | copy-start | bytes 9437188
  57.4 19.6 %copy-start.5 = (bf16[512,384]{1,0:T(8,128)(2,1)S(1)}, bf16[512,384]{1,0:T(8,128)(2,1)}, u32[]{:S(2)}) copy-start(bf16[512,384]{1,0:T(8,128)(2,1)} %query_cotangent.1) | copy-start | bytes 1179652
  57.4 19.6 %copy-start.6 = (bf16[512,384]{1,0:T(8,128)(2,1)S(1)}, bf16[512,384]{1,0:T(8,128)(2,1)}, u32[]{:S(2)}) copy-start(bf16[512,384]{1,0:T(8,128)(2,1)} %attn_outputs.1) | copy-start | bytes 1179652
  59.4 55.8 %copy-start.7 = (f32[2,4,384]{2,1,0:T(4,128)S(1)}, f32[2,4,384]{2,1,0:T(4,128)}, u32[]{:S(2)}) copy-start(f32[2,4,384]{2,1,0:T(4,128)} %first.1) | copy-start | bytes 36868
  59.4 55.8 %copy-start.8 = (f32[2,4,384]{2,1,0:T(4,128)S(1)}, f32[2,4,384]{2,1,0:T(4,128)}, u32[]{:S(2)}) copy-start(f32[2,4,384]{2,1,0:T(4,128)} %second.1) | copy-start | bytes 36868
  130.5 41.2 %all-to-all-start.4 = ((bf16[8,13,4,768]{3,2,1,0:T(4,128)(2,1)}), bf16[8,13,4,768]{3,2,1,0:T(4,128)(2,1)S(1)}, u32[]{:S(2)}, u32[]{:S(2)}) async-start(bf16[8,13,4,768]{3,2,1,0:T(4,128)(2,1)} %shard_map.151), calls=%async_computation.4 | async-start | bytes 1277952 | tf_op jit(solution)/shard_map/all_to_all | solution.py:385
  134.1 13.0 %collective-permute-start.2 = (bf16[8,12,24,128]{3,2,1,0:T(8,128)(2,1)S(1)}, bf16[8,12,24,128]{3,2,1,0:T(8,128)(2,1)S(1)}, u32[]{:S(2)}, u32[]{:S(2)}) collective-permute-start(bf16[8,12,24,128]{3,2,1,0:T(8,128)(2,1)S(1)} %all_to_all.31.packed), channel_id=1, source_target_pairs={{6,0},{7,1},{0,2},{1,3},{2,4},{3,5},{4,6},{5,7},{14,8},{15,9},{8,1... | collective-permute-start | bytes 1769480 | tf_op jit(solution)/shard_map/ppermute | solution.py:360
  136.9 23.7 %collective-permute-start.1 = (bf16[8,12,24,128]{3,2,1,0:T(8,128)(2,1)S(1)}, bf16[8,12,24,128]{3,2,1,0:T(8,128)(2,1)S(1)}, u32[]{:S(2)}, u32[]{:S(2)}) collective-permute-start(bf16[8,12,24,128]{3,2,1,0:T(8,128)(2,1)S(1)} %all_to_all.31.packed), channel_id=1, source_target_pairs={{4,0},{5,1},{6,2},{7,3},{0,4},{1,5},{2,6},{3,7},{12,8},{13,9},{14,... | collective-permute-start | bytes 1769480 | tf_op jit(solution)/shard_map/ppermute | solution.py:360
  141.3 24.8 %collective-permute-start = (bf16[8,12,24,128]{3,2,1,0:T(8,128)(2,1)S(1)}, bf16[8,12,24,128]{3,2,1,0:T(8,128)(2,1)S(1)}, u32[]{:S(2)}, u32[]{:S(2)}) collective-permute-start(bf16[8,12,24,128]{3,2,1,0:T(8,128)(2,1)S(1)} %all_to_all.31.packed), channel_id=1, source_target_pairs={{2,0},{3,1},{4,2},{5,3},{6,4},{7,5},{0,6},{1,7},{10,8},{11,9},{12,... | collective-permute-start | bytes 1769480 | tf_op jit(solution)/shard_map/ppermute | solution.py:360
  167.8 8.6 %collective-permute-start.3 = (bf16[4,8,12,24,128]{4,3,2,1,0:T(8,128)(2,1)}, bf16[4,8,12,24,128]{4,3,2,1,0:T(8,128)(2,1)}, u32[]{:S(2)}, u32[]{:S(2)}) collective-permute-start(bf16[4,8,12,24,128]{4,3,2,1,0:T(8,128)(2,1)} %pad_maximum_fusion.held), channel_id=1, source_target_pairs={{1,0},{0,1},{3,2},{2,3},{5,4},{4,5},{7,6},{6,7},{9,8},{8,9},{11,10... | collective-permute-start | bytes 7077896 | tf_op jit(solution)/shard_map/ppermute | solution.py:362
  172.3 12.9 %all-to-all-start.5 = ((f32[8,1,128]{2,1,0:T(1,128)}), f32[8,1,128]{2,1,0:T(1,128)S(1)}, u32[]{:S(2)}, u32[]{:S(2)}) async-start(f32[8,1,128]{2,1,0:T(1,128)} %shard_map.152), calls=%async_computation.5 | async-start | bytes 8192 | tf_op jit(solution)/shard_map/all_to_all | solution.py:424
  185.3 2.3 %copy-start = (bf16[6144,384]{1,0:T(8,128)(2,1)S(1)}, bf16[6144,384]{1,0:T(8,128)(2,1)}, u32[]{:S(2)}) copy-start(bf16[6144,384]{1,0:T(8,128)(2,1)} %all-gather.3.cloned.1.call-done) | copy-start | bytes 14155780
  187.6 1.7 copy-start.3
  189.3 1.7 copy-start.4
Sparse Core Ops, SparseCore 0:
  12.3 133.1 all-gather.2
